TPU v7x, 512 devices: a whole 4x4x16 slice. The times are simulated.
512 devices in a mesh: sp: 32 (over z, core), tp: 16 (over y, x).
Axes of the slice: x: 4, y: 4, z: 16, core: 2. Of those that a mesh axis runs over, the one named last changes fastest.
Arguments:
- moe_input: bfloat16 [8192, 2048], P('sp', 'tp'), may hold values from -6 to 6
- out_grad: bfloat16 [8192, 2048], P('sp', 'tp'), may hold values from -12 to 12
- routes: int32 [8192, 2], P('sp'), may hold values from 0 to 31, all different within a row; in each aligned block of 256 rows (0 to 255, 256 to 511, ...) at most 20 rows name the same one
- route_weight: float32 [8192, 2], P('sp'), may hold values from 0.2 to 1.5
- w_gate: bfloat16 [32, 2048, 2048], P('sp', None, 'tp'), may hold values from -0.125 to 0.125
- w_up: bfloat16 [32, 2048, 2048], P('sp', None, 'tp'), may hold values from -0.125 to 0.125
- w_down: bfloat16 [32, 2048, 2048], P('sp', 'tp'), may hold values from -0.125 to 0.125
- w_out: bfloat16 [2048, 2048], P(None, 'tp'), may hold values from -0.125 to 0.125
- queries: bfloat16 [8192, 1024], P('sp', 'tp'), may hold values from -6 to 6
- key_rows: bfloat16 [8192, 1024], P('sp', 'tp'), may hold values from -6 to 6
- value_rows: bfloat16 [8192, 2048], P('sp', 'tp'), may hold values from -6 to 6
- log_decay: float32 [8192, 1024], P('sp', 'tp'), may hold values from -1 to 0
Outputs:
- grad_gate: bfloat16 [32, 2048, 2048], P('sp', None, 'tp')
- grad_up: bfloat16 [32, 2048, 2048], P('sp', None, 'tp')
- grad_down: bfloat16 [32, 2048, 2048], P('sp', 'tp')
- grad_proj: float32 [2048, 2048], P('sp', 'tp')
- grad_queries: bfloat16 [8192, 1024], P('sp', 'tp')
- grad_keys: bfloat16 [8192, 1024], P('sp', 'tp')
- grad_values: bfloat16 [8192, 2048], P('sp', 'tp')
- grad_decay: float32 [8192, 1024], P('sp', 'tp')
Inputs may be any that keep to these rules, and one draw needn't show every extreme that they name: `routes`: A token's experts differ. Within each aligned block of 256 tokens no expert is named more than 20 times, and in some block one expert is named exactly 20 times.
All inputs are finite; a program needn't handle non-finite values.
Results may differ from a plain program's by a relative error of at most 0.025.
Values may be sent and summed in bfloat16 or wider, within the bound.
No kernel may reach another device: no remote copies, remote signals or barrier semaphores. Data moves between devices by JAX's collectives and lax.ppermute only.
A program may use at most 64 MiB of HBM per device.

v0:
```python
import jax
import jax.numpy as jnp
from jax import lax
from jax.sharding import Mesh
from jax.sharding import PartitionSpec as P

KEY_CHANNELS = 32
VAL_DIM = 64
TOP = 2
BLOCK = 64
SP = ("sp_0", "sp_1")


def sent_to_all(shard, axis):
    size = lax.axis_size(axis)
    return lax.all_to_all(
        jnp.broadcast_to(shard[None], (size, *shard.shape)), axis, 0, 0, tiled=True
    )


def collected_together(shard, axis):
    leaves = jax.tree.leaves(shard)
    order = sorted(range(len(leaves)), key=lambda k: -leaves[k].size)
    width = (1, *leaves[order[0]].shape)[-1]
    lines = [
        jnp.pad(leaves[k].reshape(-1), (0, -leaves[k].size % width)).reshape(-1, width)
        for k in order
    ]
    both, at, found = (sent_to_all(jnp.concatenate(lines), axis), 0, {})
    for k, line in zip(order, lines):
        section = both[:, at : at + len(line)].reshape(len(both), -1)
        found[k] = section[:, : leaves[k].size].reshape(-1, *leaves[k].shape)
        at += len(line)
    numbers = iter(range(len(leaves)))
    return jax.tree.map(lambda _: found[next(numbers)], shard)


def folded_in_pairs(pieces, combine):
    while len(jax.tree.leaves(pieces)[0]) > 1:
        pieces = jax.vmap(combine)(
            *(jax.tree.map(lambda part: part[side::2], pieces) for side in (0, 1))
        )
    return jax.tree.map(lambda part: part[0], pieces)


def entering_2(shard, axis, combine, identity):
    size, position = (lax.axis_size(axis), lax.axis_index(axis))
    passed = jnp.arange(size) < position

    def kept(part, zero, own):
        part = jnp.where(
            passed.reshape(-1, *(1 for _ in own.shape)), part, jnp.asarray(zero, own.dtype)
        )
        return part

    pieces = collected_together(shard, axis)
    return folded_in_pairs(jax.tree.map(kept, pieces, identity, shard), combine)


def sent_together(arrays, axis, split_dim, concat_dim, along):
    both = jnp.concatenate(arrays, axis=along)
    whole, at, done = (
        lax.all_to_all(both, axis, split_axis=split_dim, concat_axis=concat_dim, tiled=True),
        0,
        [],
    )
    for a in arrays:
        done.append(lax.slice_in_dim(whole, at, at + a.shape[along], axis=along))
        at += a.shape[along]
    return tuple(done)


def side_by_side(arrays, axis, dim, along):
    widths = [a.shape[along] for a in arrays]
    both = jnp.concatenate(arrays, axis=along)
    whole = lax.all_gather(both, axis, axis=dim, tiled=True)
    return tuple(jnp.split(whole, [sum(widths[:k]) for k in range(1, len(widths))], axis=along))


def in_blocks(shard, dim, size):
    before, after = (shard.shape[:dim], shard.shape[dim + 1 :])
    return jnp.moveaxis(shard.reshape(*before, size, -1, *after), dim, 0)


def sent_and_summed(shard, axis, dim):
    blocks = in_blocks(shard, dim, lax.axis_size(axis))
    arrived = lax.all_to_all(blocks, axis, split_axis=0, concat_axis=0, tiled=True)
    return arrived.astype(jnp.float32).sum(axis=0)


def laid_out(blocks, dim):
    dims = list(blocks.shape[1:])
    dims[dim] *= blocks.shape[0]
    return jnp.moveaxis(blocks, 0, dim).reshape(dims)


def gathered_copies(shard, axis, dim):
    blocks = sent_to_all(shard, axis)
    return laid_out(blocks, dim)


def reduced_to_own(blocks, axes, order):
    inside = blocks.shape[1:]
    blocks = blocks.reshape(*(lax.axis_size(a) for a in axes), *inside)
    blocks = jnp.moveaxis(blocks, order, range(len(axes))).reshape(-1, *inside)
    for k in order:
        blocks = lax.psum_scatter(blocks, axes[k], scatter_dimension=0, tiled=True)
    return blocks[0]


def summed_rows(shard, axes, order, dim):
    size = lax.axis_size(axes)
    return reduced_to_own(in_blocks(shard, dim, size), axes, order)


def gathered_by_type(shard, axis):
    leaves, found = (jax.tree.leaves(shard), {})
    for initial, a in enumerate(leaves):
        if initial not in found:
            alike = [k for k, b in enumerate(leaves) if b.dtype == a.dtype]
            got = (
                collected_together([leaves[k] for k in alike], axis)
                if len(alike) > 1
                else [sent_to_all(a, axis)]
            )
            for k, b in zip(alike, got):
                found[k] = b
    numbers = iter(range(len(leaves)))
    return jax.tree.map(lambda _: found[next(numbers)], shard)


def entering_3(shard, axis, combine, identity):
    size, position = (lax.axis_size(axis), lax.axis_index(axis))
    passed = jnp.arange(size) > position

    def kept(part, zero, own):
        part = jnp.where(
            passed.reshape(-1, *(1 for _ in own.shape)), part, jnp.asarray(zero, own.dtype)
        )
        return part[::-1]

    pieces = gathered_by_type(shard, axis)
    return folded_in_pairs(jax.tree.map(kept, pieces, identity, shard), combine)


def mixer_pass(queries, key_rows, value_rows, log_decay, state_in):
    length = queries.shape[0]
    blocks = length // BLOCK
    nheads = state_in.shape[0]
    query_blocks = queries.reshape(blocks, BLOCK, nheads, KEY_CHANNELS)
    key_blocks = key_rows.reshape(blocks, BLOCK, nheads, KEY_CHANNELS) * KEY_CHANNELS ** (-0.5)
    value_blocks = value_rows.reshape(blocks, BLOCK, nheads, VAL_DIM)
    decays = log_decay.reshape(blocks, BLOCK, nheads, KEY_CHANNELS)
    cumulative = jnp.cumsum(decays, axis=1)
    closing = cumulative[:, -1]
    query_scaled = query_blocks * jnp.exp(cumulative)
    key_scaled = key_blocks * jnp.exp(-cumulative)
    causal = jnp.tril(jnp.ones((BLOCK, BLOCK), jnp.float32))
    scores = jnp.einsum("nthd,nshd->nhts", query_scaled, key_scaled) * causal
    within = jnp.einsum("nhts,nshv->nthv", scores, value_blocks)
    key_tail = key_blocks * jnp.exp(closing[:, None] - cumulative)
    additions = jnp.einsum("nshd,nshv->nhdv", key_tail, value_blocks)

    def advance(state_now, pieces):
        return (jnp.exp(pieces[0])[..., None] * state_now + pieces[1], state_now)

    state_out, entering = lax.scan(advance, state_in, (closing, additions))
    carried = jnp.einsum("nthd,nhdv->nthv", query_scaled, entering)
    return (within + carried).reshape(length, nheads * VAL_DIM)


def carry_terms(key_full, value_full, decay_full):
    length = key_full.shape[0]
    blocks = length // BLOCK
    nheads = key_full.shape[1] // KEY_CHANNELS
    key_blocks = key_full.reshape(blocks, BLOCK, nheads, KEY_CHANNELS) * KEY_CHANNELS ** (-0.5)
    value_blocks = value_full.reshape(blocks, BLOCK, nheads, VAL_DIM)
    cumulative = jnp.cumsum(decay_full.reshape(blocks, BLOCK, nheads, KEY_CHANNELS), axis=1)
    closing = cumulative[:, -1]
    key_tail = key_blocks * jnp.exp(closing[:, None] - cumulative)
    additions = jnp.einsum("nshd,nshv->nhdv", key_tail, value_blocks)
    log_total = jnp.sum(closing, axis=0)
    remaining = log_total[None] - jnp.cumsum(closing, axis=0)
    increment = jnp.einsum("nhd,nhdv->hdv", jnp.exp(remaining), additions)
    return (log_total, increment)


def chain_step(earlier, latter):
    return (earlier[0] + latter[0], jnp.exp(latter[0])[..., None] * earlier[1] + latter[1])


def body(
    moe_input,
    out_grad,
    routes,
    route_weight,
    w_gate,
    w_up,
    w_down,
    w_out,
    queries,
    key_rows,
    value_rows,
    log_decay,
):
    sp_count = lax.axis_size(SP)
    token_count = out_grad.shape[0]
    pair_count = token_count * TOP
    capacity = 5 * token_count * TOP // (4 * sp_count)
    query_full = queries.astype(jnp.float32)
    key_full = key_rows.astype(jnp.float32)
    value_full = value_rows.astype(jnp.float32)
    (log_total, increment), pull_carry = jax.vjp(carry_terms, key_full, value_full, log_decay)
    state_in = entering_2(
        (log_total, increment),
        SP,
        chain_step,
        (jnp.zeros_like(log_total), jnp.zeros_like(increment)),
    )[1]
    mixer_raw, pull_mixer = jax.vjp(
        mixer_pass, query_full, key_full, value_full, log_decay, state_in
    )
    mixer_out = mixer_raw.astype(jnp.bfloat16)
    flat_routes = routes.reshape(pair_count)
    onehot = (flat_routes[:, None] == jnp.arange(sp_count, dtype=jnp.int32)[None, :]).astype(
        jnp.int32
    )
    position = jnp.sum((jnp.cumsum(onehot, axis=0) - onehot) * onehot, axis=1)
    pair_slot = flat_routes * capacity + position
    slot_pair = (
        jnp.full((sp_count * capacity,), pair_count, jnp.int32)
        .at[pair_slot]
        .set(jnp.arange(pair_count, dtype=jnp.int32))
    )
    slot_token = slot_pair // TOP
    row_total = sp_count * capacity
    columns = out_grad.shape[1]
    weighted = (route_weight[:, :, None] * out_grad[:, None, :].astype(jnp.float32)).astype(
        jnp.bfloat16
    )
    weighted_pad = jnp.concatenate(
        [weighted.reshape(pair_count, columns), jnp.zeros((1, columns), jnp.bfloat16)], axis=0
    )
    inputs_pad = jnp.concatenate([moe_input, jnp.zeros((1, columns), jnp.bfloat16)], axis=0)
    send_in = jnp.take(inputs_pad, slot_token, axis=0).reshape(sp_count, capacity, columns)
    send_grad = jnp.take(weighted_pad, slot_pair, axis=0).reshape(sp_count, capacity, columns)
    send_in, send_grad = (send_in, send_grad)
    recv_in, recv_grad = sent_together((send_in, send_grad), SP, 0, 0, 1)
    rows_in, rows_grad = side_by_side(
        (recv_in.reshape(row_total, -1), recv_grad.reshape(row_total, -1)), "tp", 1, 0
    )
    gate_weight = w_gate[0]
    up_weight = w_up[0]
    down_weight = w_down[0]
    gate_pre = jnp.dot(rows_in, gate_weight, preferred_element_type=jnp.float32)
    up_pre = jnp.dot(rows_in, up_weight, preferred_element_type=jnp.float32)
    sigmoid_gate = jax.nn.sigmoid(gate_pre)
    activated = gate_pre * sigmoid_gate
    hidden = (activated * up_pre).astype(jnp.bfloat16)
    hidden_grad = lax.dot_general(
        rows_grad, down_weight, (((1,), (1,)), ((), ())), preferred_element_type=jnp.float32
    )
    down_part = lax.dot_general(
        hidden, rows_grad, (((0,), (0,)), ((), ())), preferred_element_type=jnp.float32
    ).astype(jnp.bfloat16)
    gate_grad = (
        hidden_grad * up_pre * sigmoid_gate * (1.0 + gate_pre * (1.0 - sigmoid_gate))
    ).astype(jnp.bfloat16)
    up_grad = (hidden_grad * activated).astype(jnp.bfloat16)
    gate_part = lax.dot_general(
        rows_in, gate_grad, (((0,), (0,)), ((), ())), preferred_element_type=jnp.float32
    ).astype(jnp.bfloat16)
    up_part = lax.dot_general(
        rows_in, up_grad, (((0,), (0,)), ((), ())), preferred_element_type=jnp.float32
    ).astype(jnp.bfloat16)
    partial_value = lax.dot_general(
        gate_grad, gate_weight, (((1,), (1,)), ((), ())), preferred_element_type=jnp.float32
    )
    partial_value = partial_value + lax.dot_general(
        up_grad, up_weight, (((1,), (1,)), ((), ())), preferred_element_type=jnp.float32
    )
    row_part = sent_and_summed(partial_value.astype(jnp.bfloat16), "tp", 1).astype(jnp.bfloat16)
    back_rows = lax.all_to_all(
        row_part.reshape(sp_count, capacity, -1), SP, split_axis=0, concat_axis=0, tiled=True
    ).reshape(row_total, -1)
    routed = jnp.sum(
        jnp.take(back_rows, pair_slot, axis=0).astype(jnp.float32).reshape(token_count, TOP, -1),
        axis=1,
    )
    residual_grad = (out_grad.astype(jnp.float32) + routed).astype(jnp.bfloat16)
    full_grad = gathered_copies(residual_grad, "tp", 1)
    grad_proj = summed_rows(
        lax.dot_general(
            full_grad, mixer_out, (((0,), (0,)), ((), ())), preferred_element_type=jnp.float32
        ).astype(jnp.bfloat16),
        SP,
        (1, 0),
        0,
    ).astype(jnp.float32)
    mixer_grad = jnp.dot(full_grad, w_out, preferred_element_type=jnp.float32)
    query_grad, key_grad, value_grad, decay_grad, state_grad = pull_mixer(mixer_grad)
    state_out_grad = entering_3(
        (log_total, state_grad),
        SP,
        chain_step,
        (jnp.zeros_like(log_total), jnp.zeros_like(state_grad)),
    )[1]
    total_grad = jnp.exp(log_total) * jnp.sum(state_out_grad * state_in, axis=2)
    key_extra, value_extra, decay_extra = pull_carry((total_grad, state_out_grad))
    return (
        gate_part[None],
        up_part[None],
        down_part[None],
        grad_proj,
        query_grad.astype(jnp.bfloat16),
        (key_grad + key_extra).astype(jnp.bfloat16),
        (value_grad + value_extra).astype(jnp.bfloat16),
        decay_grad + decay_extra,
    )


def solution(mesh):
    split = Mesh(mesh.devices.reshape(16, 2, mesh.shape["tp"]), ("sp_0", "sp_1", "tp"))
    placed = (
        P(SP, "tp"),
        P(SP, "tp"),
        P(SP, None),
        P(SP, None),
        P(SP, None, "tp"),
        P(SP, None, "tp"),
        P(SP, "tp", None),
        P(None, "tp"),
        P(SP, "tp"),
        P(SP, "tp"),
        P(SP, "tp"),
        P(SP, "tp"),
    )
    return jax.shard_map(
        body,
        mesh=split,
        in_specs=placed,
        out_specs=(
            P(SP, None, "tp"),
            P(SP, None, "tp"),
            P(SP, "tp", None),
            P(SP, "tp"),
            P(SP, "tp"),
            P(SP, "tp"),
            P(SP, "tp"),
            P(SP, "tp"),
        ),
        check_vma=False,
    )
```

profile of v0, /device:TPU:2, one launch (start us, length us, event | category | flops | bytes accessed | tf_op | source)
XLA Modules:
  0.0 358.1 jit_solution(17696580023732887906)
XLA Ops:
  9.4 1.2 reduce-window.6
  10.9 2.4 scatter_custom_fusion
  14.4 0.9 mul.294
  15.5 2.0 gather_fusion.1
  18.5 2.0 gather_fusion
  21.1 40.9 %all_to_all.30 = bf16[32,40,128]{2,1,0:T(8,128)(2,1)S(1)} all-to-all(bf16[32,40,128]{2,1,0:T(8,128)(2,1)S(1)} %pad_maximum_fusion), channel_id=1, replica_groups=mesh['sp_0'=16,'sp_1'=2,'tp'=16] {'sp_0','sp_1'}, dimensions={0} | all-to-all | bytes 655360 | tf_op jit(solution)/shard_map/all_to_all | solution.py:63
  66.0 1.1 broadcast_in_dim.171
  67.1 3.9 %all-to-all-start.4 = ((f32[32,65,64]{1,2,0:T(8,128)}), f32[32,65,64]{1,2,0:T(8,128)S(1)}, u32[]{:S(2)}, u32[]{:S(2)}) async-start(f32[32,65,64]{1,2,0:T(8,128)} %broadcast_in_dim.171), calls=%async_computation.4 | async-start | bytes 2097152 | tf_op jit(solution)/shard_map/all_to_all | solution.py:16
  72.8 1.0 copy.190
  75.6 0.9 convolution_multiply_fusion.1
  76.5 51.1 %all-to-all-done.4 = f32[32,65,64]{1,2,0:T(8,128)S(1)} async-done(((f32[32,65,64]{1,2,0:T(8,128)}), f32[32,65,64]{1,2,0:T(8,128)S(1)}, u32[]{:S(2)}, u32[]{:S(2)}) %all-to-all-start.4) | async-done | bytes 532512 | tf_op jit(solution)/shard_map/all_to_all | solution.py:16
  129.0 2.2 all-gather.2.cloned.1.call-done
  131.2 2.7 fusion.14
  135.6 0.9 multiply_convert_fusion.1
  137.4 0.9 fusion.11
  138.3 2.1 copy.263
  140.4 5.7 %all-to-all-start.1 = ((bf16[16,640,128]{2,1,0:T(8,128)(2,1)}), bf16[16,640,128]{2,1,0:T(8,128)(2,1)S(1)}, u32[]{:S(2)}, u32[]{:S(2)}) async-start(bf16[16,640,128]{2,1,0:T(8,128)(2,1)} %bitcast.219), calls=%async_computation.1 | async-start | bytes 5242880 | tf_op jit(solution)/shard_map/all_to_all | solution.py:87
  146.7 2.5 copy.225
  150.1 1.4 broadcast_select_fusion.1
  151.4 0.9 slice_add_fusion
  153.4 25.1 %all-to-all-done.1 = bf16[16,640,128]{2,1,0:T(8,128)(2,1)S(1)} async-done(((bf16[16,640,128]{2,1,0:T(8,128)(2,1)}), bf16[16,640,128]{2,1,0:T(8,128)(2,1)S(1)}, u32[]{:S(2)}, u32[]{:S(2)}) %all-to-all-start.1) | async-done | bytes 2621472 | tf_op jit(solution)/shard_map/all_to_all | solution.py:87
  178.5 1.1 reduce_sum.117
  179.6 1.7 reshape.285
  181.3 12.0 %all-to-all-start.2 = ((bf16[32,20,128]{2,1,0:T(8,128)(2,1)}), bf16[32,20,128]{2,1,0:T(8,128)(2,1)S(1)}, u32[]{:S(2)}, u32[]{:S(2)}) async-start(bf16[32,20,128]{2,1,0:T(8,128)(2,1)} %reshape.285), calls=%async_computation.2 | async-start | bytes 393216 | tf_op jit(solution)/shard_map/all_to_all | solution.py:283
  193.3 8.1 %while.37 = (s32[]{:T(128)}, f32[2,32,64]{2,1,0:T(8,128)S(1)}, f32[4,2,32,64]{3,2,1,0:T(8,128)}, f32[4,2,32]{2,1,0:T(2,128)S(1)}, f32[4,2,32,1]{2,1,3,0:T(2,128)...) while((s32[]{:T(128)}, f32[2,32,64]{2,1,0:T(8,128)S(1)}, f32[4,2,32,64]{3,2,1,0:T(8,128)}, ...), condition=%wide.region_10.11_spmd.clone, body=%wide.region_9.10_spmd.sunk.clone | while | flops 8194 | bytes 103013 | solution.py:167
  201.5 11.8 %all-to-all-done.2 = bf16[32,20,128]{2,1,0:T(8,128)(2,1)S(1)} async-done(((bf16[32,20,128]{2,1,0:T(8,128)(2,1)}), bf16[32,20,128]{2,1,0:T(8,128)(2,1)S(1)}, u32[]{:S(2)}, u32[]{:S(2)}) %all-to-all-start.2) | async-done | bytes 163872 | tf_op jit(solution)/shard_map/all_to_all | solution.py:283
  213.3 1.5 gather_fusion.2
  214.8 1.2 convert_reduce_fusion
  216.1 0.9 add_convert_fusion.1
  216.9 1.2 broadcast_in_dim.167
  218.1 7.7 %all-to-all-start.3 = ((bf16[16,256,128]{2,1,0:T(8,128)(2,1)}), bf16[16,256,128]{2,1,0:T(8,128)(2,1)S(1)}, u32[]{:S(2)}, u32[]{:S(2)}) async-start(bf16[16,256,128]{2,1,0:T(8,128)(2,1)} %broadcast_in_dim.167), calls=%async_computation.3 | async-start | bytes 2097152 | tf_op jit(solution)/shard_map/all_to_all | solution.py:16
  226.6 3.4 fusion.5
  230.0 3.2 fusion.7
  233.2 8.0 %all-to-all-done.3 = bf16[16,256,128]{2,1,0:T(8,128)(2,1)S(1)} async-done(((bf16[16,256,128]{2,1,0:T(8,128)(2,1)}), bf16[16,256,128]{2,1,0:T(8,128)(2,1)S(1)}, u32[]{:S(2)}, u32[]{:S(2)}) %all-to-all-start.3) | async-done | bytes 1048608 | tf_op jit(solution)/shard_map/all_to_all | solution.py:16
  243.7 1.3 reshape.335
  245.0 1.8 convolution_bitcast_fusion.2
  247.0 3.2 while.38
  250.4 1.1 broadcast_in_dim.177
  251.6 4.1 %all-to-all-start.5 = ((f32[32,65,64]{1,2,0:T(8,128)}), f32[32,65,64]{1,2,0:T(8,128)S(1)}, u32[]{:S(2)}, u32[]{:S(2)}) async-start(f32[32,65,64]{1,2,0:T(8,128)} %broadcast_in_dim.177), calls=%async_computation.7 | async-start | bytes 2097152 | tf_op jit(solution)/shard_map/all_to_all | solution.py:16
  255.9 3.4 fusion.6
  263.1 0.9 convolution_add_fusion.1
  264.1 72.6 %reduce-scatter.5.cloned.1.call-done = bf16[1,64,128]{2,1,0:T(8,128)(2,1)} async-done(((bf16[16,64,128]{2,1,0:T(8,128)(2,1)}), bf16[1,64,128]{2,1,0:T(8,128)(2,1)}) %reduce-scatter.5.cloned.1.call-update) | async-done | bytes 16400 | tf_op jit(solution)/shard_map/reduce_scatter | solution.py:107
  336.7 1.3 bitcast_convert_fusion
  341.1 1.3 pad_add_fusion.1
  344.1 1.3 fusion.21
  346.4 1.1 fusion.79
  347.6 1.1 fusion.37
  349.4 1.1 fusion.80
  (249 shorter events, 45.1 us)
Async XLA Ops:
  7.2 124.0 %copy-start = (bf16[1,2048,128]{2,1,0:T(8,128)(2,1)S(1)}, bf16[1,2048,128]{2,1,0:T(8,128)(2,1)}, u32[]{:S(2)}) copy-start(bf16[1,2048,128]{2,1,0:T(8,128)(2,1)} %param.20) | copy-start | bytes 1572868
  7.2 124.0 %all-gather.2.cloned.1.call-start = ((), (), s32[]{:S(2)}) async-start(), calls=%async_computation.8 | async-start | bytes 5570560 | tf_op jit(solution)/shard_map/all_gather | solution.py:76
  9.1 53.8 %copy-start.23 = (f32[256,64]{0,1:T(8,128)S(1)}, f32[256,64]{0,1:T(8,128)}, u32[]{:S(2)}) copy-start(f32[256,64]{0,1:T(8,128)} %param.27) | copy-start | bytes 196612
  15.5 48.2 %copy-start.25 = (bf16[256,64]{0,1:T(8,128)(2,1)S(1)}, bf16[256,64]{0,1:T(8,128)(2,1)}, u32[]{:S(2)}) copy-start(bf16[256,64]{0,1:T(8,128)(2,1)} %param.24) | copy-start | bytes 98308
  15.5 48.3 %copy-start.26 = (bf16[256,64]{0,1:T(8,128)(2,1)S(1)}, bf16[256,64]{0,1:T(8,128)(2,1)}, u32[]{:S(2)}) copy-start(bf16[256,64]{0,1:T(8,128)(2,1)} %param.25) | copy-start | bytes 98308
  15.5 48.4 %copy-start.24 = (bf16[256,128]{1,0:T(8,128)(2,1)S(1)}, bf16[256,128]{1,0:T(8,128)(2,1)}, u32[]{:S(2)}) copy-start(bf16[256,128]{1,0:T(8,128)(2,1)} %param.26) | copy-start | bytes 196612
  21.0 51.1 %copy-start.27 = (s32[256,2]{0,1:T(2,128)S(1)}, s32[256,2]{0,1:T(2,128)}, u32[]{:S(2)}) copy-start(s32[256,2]{0,1:T(2,128)} %param.18) | copy-start | bytes 6148
  21.1 51.8 %copy-start.15 = (bf16[2048,128]{1,0:T(8,128)(2,1)S(1)}, bf16[2048,128]{1,0:T(8,128)(2,1)}, u32[]{:S(2)}) copy-start(bf16[2048,128]{1,0:T(8,128)(2,1)} %param.23) | copy-start | bytes 1572868
  63.4 70.5 %copy-start.28 = (f32[2,32]{1,0:T(2,128)}, f32[2,32]{1,0:T(2,128)S(1)}, u32[]{:S(2)}) copy-start(f32[2,32]{1,0:T(2,128)S(1)} %get-tuple-element.302) | copy-start | bytes 772
  63.8 3.3 copy-start.5
  64.0 70.0 %copy-start.2 = (f32[4,64,2,32]{1,0,3,2:T(4,128)}, f32[4,64,2,32]{1,0,3,2:T(4,128)S(1)}, u32[]{:S(2)}) copy-start(f32[4,64,2,32]{1,0,3,2:T(4,128)S(1)} %mul.306) | copy-start | bytes 196612
  64.2 0.6 copy-start.8
  65.0 0.7 copy-start.10
  67.1 60.4 %all-to-all-start.4 = ((f32[32,65,64]{1,2,0:T(8,128)}), f32[32,65,64]{1,2,0:T(8,128)S(1)}, u32[]{:S(2)}, u32[]{:S(2)}) async-start(f32[32,65,64]{1,2,0:T(8,128)} %broadcast_in_dim.171), calls=%async_computation.4 | async-start | bytes 2097152 | tf_op jit(solution)/shard_map/all_to_all | solution.py:16
  71.0 62.9 %copy-start.14 = (bf16[1,2048,128]{2,1,0:T(8,128)(2,1)S(1)}, bf16[1,2048,128]{2,1,0:T(8,128)(2,1)}, u32[]{:S(2)}) copy-start(bf16[1,2048,128]{2,1,0:T(8,128)(2,1)} %param.21) | copy-start | bytes 1572868
  73.8 61.5 %copy-start.31 = (pred[32]{0:T(512)(128)(4,1)}, pred[32]{0:T(512)(128)(4,1)S(1)}, u32[]{:S(2)}) copy-start(pred[32]{0:T(512)(128)(4,1)S(1)} %iota_compare_fusion.4) | copy-start | bytes 100
  74.9 0.6 copy-start.16
  127.5 7.8 %copy-start.1 = (f32[32,65,64]{1,2,0:T(8,128)}, f32[32,65,64]{1,2,0:T(8,128)S(1)}, u32[]{:S(2)}) copy-start(f32[32,65,64]{1,2,0:T(8,128)S(1)} %all-to-all-done.4) | copy-start | bytes 1597444
  131.2 3.3 copy-start.32
  134.5 2.0 copy-start.34
  134.5 1.2 copy-start.33
  135.6 1.7 copy-start.36
  136.5 1.7 copy-start.18
  136.5 1.7 copy-start.20
  138.3 7.9 %copy-start.22 = (f32[32,2,32]{2,1,0:T(2,128)S(1)}, f32[32,2,32]{2,1,0:T(2,128)}, u32[]{:S(2)}) copy-start(f32[32,2,32]{2,1,0:T(2,128)} %broadcast_select_fusion.6) | copy-start | bytes 24580
  140.4 38.1 %all-to-all-start.1 = ((bf16[16,640,128]{2,1,0:T(8,128)(2,1)}), bf16[16,640,128]{2,1,0:T(8,128)(2,1)S(1)}, u32[]{:S(2)}, u32[]{:S(2)}) async-start(bf16[16,640,128]{2,1,0:T(8,128)(2,1)} %bitcast.219), calls=%async_computation.1 | async-start | bytes 5242880 | tf_op jit(solution)/shard_map/all_to_all | solution.py:87
  152.7 0.6 copy-start.11
  179.6 46.5 %copy-start.7 = (bf16[4,2,64,64]{3,2,1,0:T(8,128)(2,1)S(1)}, bf16[4,2,64,64]{3,2,1,0:T(8,128)(2,1)}, u32[]{:S(2)}) copy-start(bf16[4,2,64,64]{3,2,1,0:T(8,128)(2,1)} %convolution_multiply_fusion.1) | copy-start | bytes 196612
  179.6 46.9 %copy-start.19 = (bf16[640,128]{1,0:T(8,128)(2,1)S(1)}, bf16[640,128]{1,0:T(8,128)(2,1)}, u32[]{:S(2)}) copy-start(bf16[640,128]{1,0:T(8,128)(2,1)} %copy-done.18) | copy-start | bytes 491524
  181.3 32.0 %all-to-all-start.2 = ((bf16[32,20,128]{2,1,0:T(8,128)(2,1)}), bf16[32,20,128]{2,1,0:T(8,128)(2,1)S(1)}, u32[]{:S(2)}, u32[]{:S(2)}) async-start(bf16[32,20,128]{2,1,0:T(8,128)(2,1)} %reshape.285), calls=%async_computation.2 | async-start | bytes 393216 | tf_op jit(solution)/shard_map/all_to_all | solution.py:283
  201.5 24.4 %copy-start.4 = (f32[4,2,32,64]{3,2,1,0:T(8,128)S(1)}, f32[4,2,32,64]{3,2,1,0:T(8,128)}, u32[]{:S(2)}) copy-start(f32[4,2,32,64]{3,2,1,0:T(8,128)} %get-tuple-element.499) | copy-start | bytes 196612
  218.1 11.8 %copy-start.35 = (f32[640,128]{1,0:T(8,128)S(1)}, f32[640,128]{1,0:T(8,128)}, u32[]{:S(2)}) copy-start(f32[640,128]{1,0:T(8,128)} %copy-done.34) | copy-start | bytes 983044
  218.1 11.8 %copy-start.37 = (f32[640,128]{1,0:T(8,128)S(1)}, f32[640,128]{1,0:T(8,128)}, u32[]{:S(2)}) copy-start(f32[640,128]{1,0:T(8,128)} %copy-done.36) | copy-start | bytes 983044
  218.1 23.0 %all-to-all-start.3 = ((bf16[16,256,128]{2,1,0:T(8,128)(2,1)}), bf16[16,256,128]{2,1,0:T(8,128)(2,1)S(1)}, u32[]{:S(2)}, u32[]{:S(2)}) async-start(bf16[16,256,128]{2,1,0:T(8,128)(2,1)} %broadcast_in_dim.167), calls=%async_computation.3 | async-start | bytes 2097152 | tf_op jit(solution)/shard_map/all_to_all | solution.py:16
  225.8 36.3 %reduce-scatter.3.cloned.1.call-start = ((), (), s32[]{:S(2)}) async-start(), calls=%async_computation.9 | async-start | bytes 786432 | tf_op jit(solution)/shard_map/reduce_scatter | solution.py:107
  241.7 5.3 %copy-start.13 = (bf16[4,2,32,64]{3,2,1,0:T(8,128)(2,1)S(1)}, bf16[4,2,32,64]{3,2,1,0:T(8,128)(2,1)}, u32[]{:S(2)}) copy-start(bf16[4,2,32,64]{3,2,1,0:T(8,128)(2,1)} %broadcast_convert_fusion) | copy-start | bytes 98308
  241.7 8.6 %copy-start.21 = (f32[1,64]{0,1:T(8,128)S(1)}, f32[1,64]{0,1:T(8,128)}, u32[]{:S(2)}) copy-start(f32[1,64]{0,1:T(8,128)} %copy.197) | copy-start | bytes 772
  250.4 8.9 %copy-start.17 = (f32[64,64]{1,0:T(8,128)S(1)}, f32[64,64]{1,0:T(8,128)}, u32[]{:S(2)}) copy-start(f32[64,64]{1,0:T(8,128)} %copy-done.16) | copy-start | bytes 49156
  251.6 9.7 %copy-start.3 = (f32[4,64,2,32]{1,0,3,2:T(4,128)S(1)}, f32[4,64,2,32]{1,0,3,2:T(4,128)}, u32[]{:S(2)}) copy-start(f32[4,64,2,32]{1,0,3,2:T(4,128)} %copy-done.2) | copy-start | bytes 196612
  251.6 86.5 %all-to-all-start.5 = ((f32[32,65,64]{1,2,0:T(8,128)}), f32[32,65,64]{1,2,0:T(8,128)S(1)}, u32[]{:S(2)}, u32[]{:S(2)}) async-start(f32[32,65,64]{1,2,0:T(8,128)} %broadcast_in_dim.177), calls=%async_computation.7 | async-start | bytes 2097152 | tf_op jit(solution)/shard_map/all_to_all | solution.py:16
  255.6 7.3 %copy-start.9 = (bf16[4,64,2,32]{1,3,2,0:T(8,128)(2,1)S(1)}, bf16[4,64,2,32]{1,3,2,0:T(8,128)(2,1)}, u32[]{:S(2)}) copy-start(bf16[4,64,2,32]{1,3,2,0:T(8,128)(2,1)} %copy-done.8) | copy-start | bytes 98308
  255.7 82.7 %copy-start.30 = (pred[32]{0:T(512)(128)(4,1)S(1)}, pred[32]{0:T(512)(128)(4,1)}, u32[]{:S(2)}) copy-start(pred[32]{0:T(512)(128)(4,1)} %iota_compare_fusion.3) | copy-start | bytes 100
  255.7 81.0 %reduce-scatter.5.cloned.1.call-start = ((), (), s32[]{:S(2)}) async-start(), calls=%async_computation.10 | async-start | bytes 278528 | tf_op jit(solution)/shard_map/reduce_scatter | solution.py:107
  338.1 2.7 copy-start.12
  338.1 3.1 copy-start.6
  338.5 10.4 %copy-start.29 = (f32[2,32]{1,0:T(2,128)S(1)}, f32[2,32]{1,0:T(2,128)}, u32[]{:S(2)}) copy-start(f32[2,32]{1,0:T(2,128)} %copy-done.28) | copy-start | bytes 772
Sparse Core Ops, SparseCore 0:
  63.0 68.1 all-gather.1
  243.2 8.8 reduce-scatter.2
  262.2 74.4 reduce-scatter.4
where the time goes:
time: 360 us; the launch traced here: 358 us
  waiting for transfers between devices  171 us (48%)
  local copies, waits for them, and re-layouts  46.8 us (13%)
  blocking collectives  40.9 us (11%)
  starting transfers between devices  33.7 us (9%)
  matrix products  28 us (8%)
  other arithmetic  22.7 us (6%)
  between operations  14.8 us (4%)
    reduce_scatter x2, waiting for transfers between devices, reduced_to_own(): blocks = lax.psum_scatter(blocks, axes[k], scatter_dimension=0, tiled=True)  72.6 us
    all_to_all x3, waiting for transfers between devices, sent_to_all(): lax.all_to_all(jnp.broadcast_to(shard[None], (size, *shard.shape)), axis,...  59.1 us
    all_to_all x1, blocking collectives, sent_together(): lax.all_to_all(both, axis, split_axis=split_dim, concat_axis=concat_dim,...  40.9 us
    all_to_all x1, waiting for transfers between devices, sent_and_summed(): lax.all_to_all(blocks, axis, split_axis=0, concat_axis=0, tiled=True)  25.1 us
    all_to_all x3, starting transfers between devices, sent_to_all(): lax.all_to_all(jnp.broadcast_to(shard[None], (size, *shard.shape)), axis,...  15.6 us
    all_to_all x1, starting transfers between devices, body(): lax.all_to_all(row_part.reshape(sp_count, capacity, -1), SP, split_axis=0...  12 us
    all_to_all x1, waiting for transfers between devices, body(): lax.all_to_all(row_part.reshape(sp_count, capacity, -1), SP, split_axis=0...  11.8 us
    unnamed x81, local copies, waits for them, and re-layouts  8.39 us
  transfers between devices with their start and end apart: 8, of which 6 were waited for; matrix products, arithmetic and copies ran while one was open for 14% of the time, Pallas kernels for 0%

commit v1 on v0

v1 whole, which is shorter than its diff:
```python
import jax
import jax.numpy as jnp
from jax import lax
from jax.experimental import pallas as pl
from jax.experimental.pallas import tpu as pltpu
from jax.sharding import Mesh
from jax.sharding import PartitionSpec as P

KEY_CHANNELS = 32
VAL_DIM = 64
TOP = 2
BLOCK = 64
CAP = 20
PAD = 24
SP = ("sp_0", "sp_1")
N_SP = 32
N_TP = 16
TOK = 256
ROWS = N_SP * CAP
SLOTS = N_SP * PAD
NBLK = TOK // BLOCK
BF = jnp.bfloat16
F32 = jnp.float32
HI = lax.Precision.HIGHEST
SCALE = KEY_CHANNELS ** (-0.5)

NN = (((1,), (0,)), ((), ()))
NT = (((1,), (1,)), ((), ()))
TN = (((0,), (0,)), ((), ()))


def mm(a, b, dims=NN):
    return lax.dot_general(a.astype(BF), b.astype(BF), dims, preferred_element_type=F32)


def mm_exact(a, b, dims=NN):
    return lax.dot_general(a, b, dims, precision=HI, preferred_element_type=F32)


def iota(shape, dim):
    return lax.broadcasted_iota(jnp.int32, shape, dim)


def call(fn, outs, *args, name, scratch=(), smem=()):
    return pl.pallas_call(
        fn,
        out_shape=tuple(jax.ShapeDtypeStruct(s, d) for s, d in outs),
        in_specs=[
            pl.BlockSpec(memory_space=pltpu.SMEM if k in smem else pltpu.VMEM)
            for k in range(len(args))
        ],
        out_specs=tuple(pl.BlockSpec(memory_space=pltpu.VMEM) for _ in outs),
        scratch_shapes=scratch,
        name=name,
        compiler_params=pltpu.CompilerParams(vmem_limit_bytes=56 * 1024 * 1024),
    )(*args)


def dispatch_kernel(routes_ref, weight_ref, x_ref, g_ref, sx_ref, sg_ref, pick_ref):
    routes = routes_ref[...]
    expert = iota((N_SP, TOK), 0)
    hot = [(expert == routes[j : j + 1, :]) for j in range(TOP)]
    both = (hot[0] | hot[1]).astype(F32)
    before = (iota((TOK, TOK), 0) < iota((TOK, TOK), 1)).astype(F32)
    place = mm(both, before)
    spread = (iota((SLOTS, N_SP), 0) // PAD == iota((SLOTS, N_SP), 1)).astype(F32)
    slot_place = (iota((SLOTS, TOK), 0) % PAD).astype(F32)
    picks = [(mm(spread, jnp.where(h, place, -1.0)) == slot_place).astype(F32) for h in hot]
    pick = (picks[0] + picks[1]).astype(BF)
    pick_ref[...] = pick
    sx_ref[...] = mm(pick, x_ref[...]).astype(BF).reshape(N_SP, PAD, 128)
    grad = g_ref[...].astype(F32)
    weight = jnp.concatenate([weight_ref[...], jnp.zeros((6, TOK), F32)], axis=0).T
    rows = [(weight[:, j : j + 1] * grad).astype(BF) for j in range(TOP)]
    sent = mm(picks[0], rows[0]) + mm(picks[1], rows[1])
    sg_ref[...] = sent.astype(BF).reshape(N_SP, PAD, 128)


def turned_kernel(pick_ref, out_ref):
    out_ref[...] = pick_ref[...].astype(F32).T.astype(BF)


def copies_kernel(rows_ref, out_ref, packed):
    for e in range(N_SP):
        packed[e * CAP : (e + 1) * CAP, :] = rows_ref[e].astype(F32)[:CAP]
    out = packed[...].astype(BF)
    for k in range(N_TP):
        out_ref[k] = out


STEP = 128


def wide(ref, at, size):
    return jnp.concatenate([ref[k, at : at + size, :] for k in range(N_TP)], axis=1)


def pre_kernel(x_ref, wg_ref, wu_ref, pre_ref):
    weight = jnp.concatenate([wg_ref[...], wu_ref[...]], axis=1)
    for at in range(0, ROWS, STEP):
        pre_ref[at : at + STEP, :] = mm(wide(x_ref, at, STEP), weight)


def partial_kernel(g_ref, pre_ref, wg_ref, wu_ref, wd_ref, part_ref, grads_ref, hidden_ref):
    weight = jnp.concatenate([wg_ref[...], wu_ref[...]], axis=1)
    down = wd_ref[...]
    for at in range(0, ROWS, STEP):
        here = slice(at, at + STEP)
        hidden_grad = mm(wide(g_ref, at, STEP), down, NT)
        gate_pre, up_pre = pre_ref[here, :128], pre_ref[here, 128:]
        sigmoid = jax.nn.sigmoid(gate_pre)
        activated = gate_pre * sigmoid
        hidden_ref[here, :] = (activated * up_pre).astype(BF)
        gate = hidden_grad * up_pre * sigmoid * (1.0 + gate_pre * (1.0 - sigmoid))
        up = hidden_grad * activated
        grads = jnp.concatenate([gate.astype(BF), up.astype(BF)], axis=1)
        grads_ref[here, :] = grads
        part = mm(grads, weight, NT).astype(BF)
        for k in range(N_TP):
            part_ref[k, here, :] = part[:, k * 128 : (k + 1) * 128]


def weight_grads_kernel(x_ref, g_ref, grads_ref, hidden_ref, gate_ref, up_ref, down_ref):
    grads = grads_ref[...]
    hidden = hidden_ref[...]
    for k in range(N_TP):
        both = mm(x_ref[k], grads, TN)
        gate_ref[k * 128 : (k + 1) * 128, :] = both[:, :128].astype(BF)
        up_ref[k * 128 : (k + 1) * 128, :] = both[:, 128:].astype(BF)
        down_ref[:, k * 128 : (k + 1) * 128] = mm(hidden, g_ref[k], TN).astype(BF)


def row_sum_kernel(part_ref, out_ref, total):
    acc = part_ref[0].astype(F32)
    for k in range(1, N_TP):
        acc = acc + part_ref[k].astype(F32)
    total[:ROWS, :] = acc
    total[ROWS:, :] = jnp.zeros((8, 128), F32)
    keep = iota((PAD, 128), 0) < CAP
    for e in range(N_SP):
        out_ref[e] = jnp.where(keep, total[e * CAP : e * CAP + PAD, :], 0.0).astype(BF)


def residual_kernel(back_ref, turned_ref, g_ref, out_ref):
    routed = mm(turned_ref[...], back_ref[...].reshape(SLOTS, 128))
    residual = (g_ref[...].astype(F32) + routed).astype(BF)
    for k in range(N_TP):
        out_ref[k] = residual


def head_masks():
    key_lane = iota((1, 64), 1) // KEY_CHANNELS
    val_lane = iota((1, 128), 1) // VAL_DIM
    keys = [(key_lane == h).astype(F32) for h in range(2)]
    vals = [(val_lane == h).astype(F32) for h in range(2)]
    own = (iota((128, 64), 0) // VAL_DIM == iota((128, 64), 1) // KEY_CHANNELS).astype(F32)
    return keys, vals, own


def packed_state(state):
    both = state[:64] + state[64:]
    return jnp.concatenate([both[:32], both[32:]], axis=1)


def opened_state(packed, own):
    both = jnp.concatenate([packed[:, :64], packed[:, 64:]], axis=0)
    return jnp.concatenate([both, both], axis=0) * own


def block_sums(decay):
    row, col = iota((TOK, TOK), 0), iota((TOK, TOK), 1)
    within = ((row // BLOCK == col // BLOCK) & (col <= row)).astype(F32)
    return mm_exact(within, decay)


def whole_sums(cumulative):
    offset, parts = jnp.zeros((1, 64), F32), []
    for n in range(NBLK):
        block = cumulative[n * BLOCK : (n + 1) * BLOCK]
        parts.append(block + offset)
        offset = offset + block[BLOCK - 1 :]
    return jnp.concatenate(parts, axis=0), offset


def closings(cumulative):
    return [cumulative[(n + 1) * BLOCK - 1 : (n + 1) * BLOCK] for n in range(NBLK)]


def per_block(rows):
    return jnp.concatenate([jnp.broadcast_to(r, (BLOCK, r.shape[1])) for r in rows], axis=0)


def span_kernel(k_ref, v_ref, decay_ref, out_ref):
    _, _, own = head_masks()
    keys = k_ref[...].astype(F32).T * SCALE
    so_far, total = whole_sums(block_sums(decay_ref[...].T))
    state = mm(v_ref[...], keys * jnp.exp(total - so_far), TN) * own
    last = jnp.concatenate([total, jnp.zeros((1, 64), F32)], axis=1)
    rows = jnp.concatenate([packed_state(state), last, jnp.zeros((7, 128), F32)], axis=0)
    for s in range(N_SP):
        out_ref[s] = rows


def scores_of(queries, keys, mask, causal):
    return jnp.where(causal, mm(queries * mask, keys, NT), 0.0)


def causal_blocks():
    row, col = iota((TOK, TOK), 0), iota((TOK, TOK), 1)
    return (row // BLOCK == col // BLOCK) & (col <= row)


def forward_kernel(
    me_ref, spans_ref, q_ref, k_ref, v_ref, decay_ref, out_ref, entering_ref, reach_ref
):
    key_mask, val_mask, own = head_masks()
    me = me_ref[0]
    totals = jnp.concatenate([spans_ref[s, 32:33, :] for s in range(N_SP)], axis=0)[:, :64]
    start, between = iota((N_SP, N_SP), 0), iota((N_SP, N_SP), 1)
    passed = ((start < between) & (between < me)).astype(F32)
    reach = jnp.where(iota((N_SP, 64), 0) < me, jnp.exp(mm_exact(passed, totals)), 0.0)
    reach = jnp.concatenate([reach, reach], axis=1)
    reach_ref[...] = reach
    packed = jnp.zeros((32, 128), F32)
    for s in range(N_SP):
        packed = packed + reach[s : s + 1] * spans_ref[s, :32, :]
    state = opened_state(packed, own)
    queries = q_ref[...].astype(F32).T
    keys = k_ref[...].astype(F32).T * SCALE
    values = v_ref[...].astype(F32)
    cumulative = block_sums(decay_ref[...].T)
    closing = closings(cumulative)
    scaled_q = queries * jnp.exp(cumulative)
    scaled_k = keys * jnp.exp(-cumulative)
    tail = keys * jnp.exp(per_block(closing) - cumulative)
    causal = causal_blocks()
    within = jnp.zeros((TOK, 128), F32)
    for h in range(2):
        scores = scores_of(scaled_q, scaled_k, key_mask[h], causal)
        within = within + mm(scores, values * val_mask[h])
    for n in range(NBLK):
        here = slice(n * BLOCK, (n + 1) * BLOCK)
        entering_ref[n] = state
        out_ref[here, :] = (within[here] + mm(scaled_q[here], state, NT)).astype(BF)
        state = jnp.exp(closing[n]) * state + mm(values[here], tail[here], TN) * own


def mixer_grad_kernel(full_ref, w_ref, q_ref, decay_ref, reach_ref, grad_ref, sent_ref):
    _, _, own = head_masks()
    grad = mm(wide(full_ref, 0, TOK), w_ref[...])
    grad_ref[...] = grad
    so_far, _ = whole_sums(block_sums(decay_ref[...].T))
    scaled = q_ref[...].astype(F32).T * jnp.exp(so_far)
    packed = packed_state(mm(grad, scaled, TN) * own)
    for s in range(N_SP):
        sent_ref[s] = (packed * reach_ref[s : s + 1, :]).astype(BF)


def proj_kernel(full_ref, mixed_ref, out_ref):
    mixed = mixed_ref[...]
    for k in range(N_TP):
        part = mm(full_ref[k], mixed, TN).astype(BF)
        out_ref[2 * k] = part[:64]
        out_ref[2 * k + 1] = part[64:]


def backward_kernel(
    later_ref, grad_ref, entering_ref, q_ref, k_ref, v_ref, decay_ref, gq_ref, gk_ref, gv_ref, gd_ref
):
    key_mask, val_mask, own = head_masks()
    packed = later_ref[0].astype(F32)
    for s in range(1, N_SP):
        packed = packed + later_ref[s].astype(F32)
    state_grad = opened_state(packed, own)
    grad = grad_ref[...]
    queries = q_ref[...].astype(F32).T
    keys = k_ref[...].astype(F32).T * SCALE
    values = v_ref[...].astype(F32)
    cumulative = block_sums(decay_ref[...].T)
    closing = closings(cumulative)
    grow, shrink = jnp.exp(cumulative), jnp.exp(-cumulative)
    rest = jnp.exp(per_block(closing) - cumulative)
    scaled_q, scaled_k, tail = queries * grow, keys * shrink, keys * rest
    causal = causal_blocks()
    value_grad = jnp.zeros((TOK, 128), F32)
    query_grad = jnp.zeros((TOK, 64), F32)
    key_grad = jnp.zeros((TOK, 64), F32)
    for h in range(2):
        scores = scores_of(scaled_q, scaled_k, key_mask[h], causal)
        score_grad = jnp.where(causal, mm(grad * val_mask[h], values, NT), 0.0)
        value_grad = value_grad + mm(scores, grad * val_mask[h], TN)
        query_grad = query_grad + mm(score_grad, scaled_k * key_mask[h])
        key_grad = key_grad + mm(score_grad, scaled_q * key_mask[h], TN)
    carried_v, carried_q, tail_grad, close_grad = ([None] * NBLK for _ in range(4))
    for n in reversed(range(NBLK)):
        here = slice(n * BLOCK, (n + 1) * BLOCK)
        entering = entering_ref[n]
        decay_out = jnp.exp(closing[n])
        carried_v[n] = mm(tail[here], state_grad, NT)
        carried_q[n] = mm(grad[here], entering)
        tail_grad[n] = mm(values[here], state_grad)
        close_grad[n] = decay_out * jnp.sum(state_grad * entering, axis=0, keepdims=True) + jnp.sum(
            tail_grad[n] * tail[here], axis=0, keepdims=True
        )
        state_grad = decay_out * state_grad + mm(grad[here], scaled_q[here], TN) * own
    value_grad = value_grad + jnp.concatenate(carried_v, axis=0)
    query_grad = query_grad + jnp.concatenate(carried_q, axis=0)
    tail_grad = jnp.concatenate(tail_grad, axis=0)
    change = query_grad * scaled_q - key_grad * scaled_k - tail_grad * tail
    row, col = iota((TOK, TOK), 0), iota((TOK, TOK), 1)
    onward = ((row // BLOCK == col // BLOCK) & (col >= row)).astype(F32)
    gd_ref[...] = (mm_exact(onward, change) + per_block(close_grad)).T
    gq_ref[...] = (query_grad * grow).T.astype(BF)
    gk_ref[...] = ((key_grad * shrink + tail_grad * rest) * SCALE).T.astype(BF)
    gv_ref[...] = value_grad.astype(BF)


def proj_sum_kernel(parts_ref, out_ref):
    acc = parts_ref[0].astype(F32)
    for s in range(1, N_SP):
        acc = acc + parts_ref[s].astype(F32)
    out_ref[...] = acc


def exchanged(blocks, axis):
    return lax.all_to_all(blocks, axis, split_axis=0, concat_axis=0, tiled=True)


def body(
    moe_input,
    out_grad,
    routes,
    route_weight,
    w_gate,
    w_up,
    w_down,
    w_out,
    queries,
    key_rows,
    value_rows,
    log_decay,
):
    gate_weight, up_weight, down_weight = w_gate[0], w_up[0], w_down[0]
    q_t, k_t, decay_t = queries.T, key_rows.T, log_decay.T
    me = lax.axis_index(SP).astype(jnp.int32).reshape(1)

    send_in, send_grad, pick = call(
        dispatch_kernel,
        [((N_SP, PAD, 128), BF), ((N_SP, PAD, 128), BF), ((SLOTS, TOK), BF)],
        routes.T,
        route_weight.T,
        moe_input,
        out_grad,
        name="dispatch",
    )
    recv_in = exchanged(send_in, SP)
    recv_grad = exchanged(send_grad, SP)
    (turned,) = call(turned_kernel, [((TOK, SLOTS), BF)], pick, name="turned")
    (spans,) = call(
        span_kernel, [((N_SP, 40, 128), F32)], k_t, value_rows, decay_t, name="span"
    )

    def copies(rows):
        return call(
            copies_kernel,
            [((N_TP, ROWS, 128), BF)],
            rows,
            name="copies",
            scratch=[pltpu.VMEM((ROWS, 128), F32)],
        )[0]

    rows_in = exchanged(copies(recv_in), "tp")
    rows_grad = exchanged(copies(recv_grad), "tp")
    spans = exchanged(spans, SP)
    mixer_out, entering, reach = call(
        forward_kernel,
        [((TOK, 128), BF), ((NBLK, 128, 64), F32), ((N_SP, 128), F32)],
        me,
        spans,
        q_t,
        k_t,
        value_rows,
        decay_t,
        name="forward",
        smem=(0,),
    )
    (pre,) = call(
        pre_kernel, [((ROWS, 256), F32)], rows_in, gate_weight, up_weight, name="pre"
    )
    partial_rows, grads, hidden = call(
        partial_kernel,
        [((N_TP, ROWS, 128), BF), ((ROWS, 256), BF), ((ROWS, 128), BF)],
        rows_grad,
        pre,
        gate_weight,
        up_weight,
        down_weight,
        name="partial",
    )
    arrived = exchanged(partial_rows, "tp")
    gate_part, up_part, down_part = call(
        weight_grads_kernel,
        [((2048, 128), BF), ((2048, 128), BF), ((128, 2048), BF)],
        rows_in,
        rows_grad,
        grads,
        hidden,
        name="weight_grads",
    )
    (returned,) = call(
        row_sum_kernel,
        [((N_SP, PAD, 128), BF)],
        arrived,
        name="row_sum",
        scratch=[pltpu.VMEM((ROWS + 8, 128), F32)],
    )
    back = exchanged(returned, SP)
    (residual,) = call(
        residual_kernel, [((N_TP, TOK, 128), BF)], back, turned, out_grad, name="residual"
    )
    full_grad = exchanged(residual, "tp")
    mixer_grad, state_sent = call(
        mixer_grad_kernel,
        [((TOK, 128), F32), ((N_SP, 32, 128), BF)],
        full_grad,
        w_out,
        q_t,
        decay_t,
        reach,
        name="mixer_grad",
    )
    later = exchanged(state_sent, SP)
    (proj,) = call(proj_kernel, [((N_SP, 64, 128), BF)], full_grad, mixer_out, name="proj")
    proj_parts = exchanged(proj, SP)
    gq, gk, gv, gd = call(
        backward_kernel,
        [((64, TOK), BF), ((64, TOK), BF), ((TOK, 128), BF), ((64, TOK), F32)],
        later,
        mixer_grad,
        entering,
        q_t,
        k_t,
        value_rows,
        decay_t,
        name="backward",
    )
    (grad_proj,) = call(proj_sum_kernel, [((64, 128), F32)], proj_parts, name="proj_sum")
    return (gate_part[None], up_part[None], down_part[None], grad_proj, gq.T, gk.T, gv, gd.T)


def solution(mesh):
    split = Mesh(mesh.devices.reshape(16, 2, mesh.shape["tp"]), ("sp_0", "sp_1", "tp"))
    placed = (
        P(SP, "tp"),
        P(SP, "tp"),
        P(SP, None),
        P(SP, None),
        P(SP, None, "tp"),
        P(SP, None, "tp"),
        P(SP, "tp", None),
        P(None, "tp"),
        P(SP, "tp"),
        P(SP, "tp"),
        P(SP, "tp"),
        P(SP, "tp"),
    )
    return jax.shard_map(
        body,
        mesh=split,
        in_specs=placed,
        out_specs=(
            P(SP, None, "tp"),
            P(SP, None, "tp"),
            P(SP, "tp", None),
            P(SP, "tp"),
            P(SP, "tp"),
            P(SP, "tp"),
            P(SP, "tp"),
            P(SP, "tp"),
        ),
        check_vma=False,
    )
```

time: 360 us -> 367 us (1.019)
  the two profiles are of different devices: /device:TPU:2 before, /device:TPU:1 now
where the time goes in v1:
time: 367 us; the launch traced here: 366 us
  waiting for transfers between devices  188 us (51%)
  blocking collectives  74.9 us (20%)
  starting transfers between devices  49.8 us (14%)
  Pallas kernels  48.1 us (13%)
  local copies, waits for them, and re-layouts  4.02 us (1%)
    all_to_all x8, waiting for transfers between devices, exchanged(): return lax.all_to_all(blocks, axis, split_axis=0, concat_axis=0, tiled=True)  188 us
    all_to_all x2, blocking collectives, exchanged(): return lax.all_to_all(blocks, axis, split_axis=0, concat_axis=0, tiled=True)  74.9 us
    all_to_all x8, starting transfers between devices, exchanged(): return lax.all_to_all(blocks, axis, split_axis=0, concat_axis=0, tiled=True)  49.8 us
    pallas_call x15, Pallas kernels, call(): pl.pallas_call(fn, out_shape=tuple((jax.ShapeDtypeStruct(s, d) for s, d i...  48.1 us
  transfers between devices with their start and end apart: 8, of which 8 were waited for; matrix products, arithmetic and copies ran while one was open for 0% of the time, Pallas kernels for 8%

profile of v1, /device:TPU:1, one launch (start us, length us, event | category | flops | bytes accessed | tf_op | source)
XLA Modules:
  0.0 365.6 jit_solution(9305581019509357704)
XLA Ops:
  0.6 2.7 dispatch.1
  3.4 35.6 %all_to_all.50.rows_ref = bf16[32,24,128]{2,1,0:T(8,128)(2,1)} all-to-all(bf16[32,24,128]{2,1,0:T(8,128)(2,1)} %get-tuple-element.26), channel_id=1, replica_groups=mesh['sp_0'=16,'sp_1'=2,'tp'=16] {'sp_0','sp_1'}, dimensions={0} | all-to-all | bytes 393216 | tf_op jit(solution)/shard_map/all_to_all | solution.py:326
  39.0 5.0 %all-to-all-start.2 = ((bf16[32,24,128]{2,1,0:T(8,128)(2,1)}), bf16[32,24,128]{2,1,0:T(8,128)(2,1)S(1)}, u32[]{:S(2)}, u32[]{:S(2)}) async-start(bf16[32,24,128]{2,1,0:T(8,128)(2,1)} %get-tuple-element.27), calls=%async_computation.2 | async-start | bytes 393216 | tf_op jit(solution)/shard_map/all_to_all | solution.py:326
  43.9 2.6 copies.2
  46.6 16.3 %all-to-all-done.2.rows_ref = bf16[32,24,128]{2,1,0:T(8,128)(2,1)S(1)} async-done(((bf16[32,24,128]{2,1,0:T(8,128)(2,1)}), bf16[32,24,128]{2,1,0:T(8,128)(2,1)S(1)}, u32[]{:S(2)}, u32[]{:S(2)}) %all-to-all-start.2) | async-done | bytes 196640 | tf_op jit(solution)/shard_map/all_to_all | solution.py:326
  62.9 0.0 copy-start.6
  62.9 0.7 copy-done.6
  63.6 6.8 %all-to-all-start.1 = ((bf16[16,640,128]{2,1,0:T(8,128)(2,1)}), bf16[16,640,128]{2,1,0:T(8,128)(2,1)S(1)}, u32[]{:S(2)}, u32[]{:S(2)}) async-start(bf16[16,640,128]{2,1,0:T(8,128)(2,1)} %copies.2), calls=%async_computation.1 | async-start | bytes 5242880 | tf_op jit(solution)/shard_map/all_to_all | solution.py:326
  70.4 2.6 copies.3
  73.0 34.0 %all-to-all-done.1.x_ref = bf16[16,640,128]{2,1,0:T(8,128)(2,1)S(1)} async-done(((bf16[16,640,128]{2,1,0:T(8,128)(2,1)}), bf16[16,640,128]{2,1,0:T(8,128)(2,1)S(1)}, u32[]{:S(2)}, u32[]{:S(2)}) %all-to-all-start.1) | async-done | bytes 2621472 | tf_op jit(solution)/shard_map/all_to_all | solution.py:326
  107.0 0.0 copy-start
  107.0 1.5 copy-done
  108.5 4.7 %all-to-all-start.3 = ((bf16[16,640,128]{2,1,0:T(8,128)(2,1)}), bf16[16,640,128]{2,1,0:T(8,128)(2,1)}, u32[]{:S(2)}, u32[]{:S(2)}) async-start(bf16[16,640,128]{2,1,0:T(8,128)(2,1)} %copies.3), calls=%async_computation.3 | async-start | bytes 5242880 | tf_op jit(solution)/shard_map/all_to_all | solution.py:326
  113.2 3.7 %pre.1.pre_ref = f32[640,256]{1,0:T(8,128)} custom-call(bf16[16,640,128]{2,1,0:T(8,128)(2,1)} %copy-done, bf16[2048,128]{1,0:T(8,128)(2,1)} %bitcast.15, bf16[2048,128]{1,0:T(8,128)(2,1)} %bitcast.17), custom_call_target="tpu_custom_call" | custom-call | tf_op jit(solution)/shard_map/pre/pallas_call | solution.py:45
  117.0 30.2 %all-to-all-done.3.g_ref = bf16[16,640,128]{2,1,0:T(8,128)(2,1)} async-done(((bf16[16,640,128]{2,1,0:T(8,128)(2,1)}), bf16[16,640,128]{2,1,0:T(8,128)(2,1)}, u32[]{:S(2)}, u32[]{:S(2)}) %all-to-all-start.3) | async-done | bytes 2621472 | tf_op jit(solution)/shard_map/all_to_all | solution.py:326
  147.1 6.7 %partial.1 = (bf16[16,640,128]{2,1,0:T(8,128)(2,1)}, bf16[640,256]{1,0:T(8,128)(2,1)}, bf16[640,128]{1,0:T(8,128)(2,1)}) custom-call(bf16[16,640,128]{2,1,0:T(8,128)(2,1)} %all-to-all-done.3.g_ref, f32[640,256]{1,0:T(8,128)} %pre.1.pre_ref, bf16[2048,128]{1,0:T(8,128)(2,1)} %bitcast.16, bf16[2048,128]{1,0:T(8,128)(2,1)} %bitcast.18, bf16[128,2048]{1,0:T(8,128)(2,1)} %bitcast.23), custom_call_target="tpu_custom_call" | custom-call | tf_op jit(solution)/shard_map/partial/pallas_call | solution.py:45
  153.9 39.2 %all_to_all.51.part_ref = bf16[16,640,128]{2,1,0:T(8,128)(2,1)} all-to-all(bf16[16,640,128]{2,1,0:T(8,128)(2,1)} %get-tuple-element.33), channel_id=1, replica_groups=mesh['sp_0'=16,'sp_1'=2,'tp'=16] {'tp'}, dimensions={0} | all-to-all | bytes 5242880 | tf_op jit(solution)/shard_map/all_to_all | solution.py:326
  193.1 2.9 row_sum.1
  196.0 14.1 %all-to-all-start.5 = ((bf16[32,24,128]{2,1,0:T(8,128)(2,1)}), bf16[32,24,128]{2,1,0:T(8,128)(2,1)S(1)}, u32[]{:S(2)}, u32[]{:S(2)}) async-start(bf16[32,24,128]{2,1,0:T(8,128)(2,1)} %row_sum.1), calls=%async_computation.5 | async-start | bytes 393216 | tf_op jit(solution)/shard_map/all_to_all | solution.py:326
  210.2 2.4 span.1
  212.6 16.4 %all-to-all-done.5.back_ref = bf16[32,24,128]{2,1,0:T(8,128)(2,1)S(1)} async-done(((bf16[32,24,128]{2,1,0:T(8,128)(2,1)}), bf16[32,24,128]{2,1,0:T(8,128)(2,1)S(1)}, u32[]{:S(2)}, u32[]{:S(2)}) %all-to-all-start.5) | async-done | bytes 196640 | tf_op jit(solution)/shard_map/all_to_all | solution.py:326
  229.0 0.0 copy-start.5
  229.0 5.0 %all-to-all-start.7 = ((f32[32,40,128]{2,1,0:T(8,128)}), f32[32,40,128]{2,1,0:T(8,128)S(1)}, u32[]{:S(2)}, u32[]{:S(2)}) async-start(f32[32,40,128]{2,1,0:T(8,128)} %span.1), calls=%async_computation.7 | async-start | bytes 1310720 | tf_op jit(solution)/shard_map/all_to_all | solution.py:326
  234.0 1.9 turned.1.turned_ref
  235.9 0.0 copy-done.5
  235.9 2.3 residual.1
  238.2 34.8 %all-to-all-done.7.spans_ref = f32[32,40,128]{2,1,0:T(8,128)S(1)} async-done(((f32[32,40,128]{2,1,0:T(8,128)}), f32[32,40,128]{2,1,0:T(8,128)S(1)}, u32[]{:S(2)}, u32[]{:S(2)}) %all-to-all-start.7) | async-done | bytes 655392 | tf_op jit(solution)/shard_map/all_to_all | solution.py:326
  273.0 0.0 copy-start.2
  273.0 3.7 all-to-all-start.6
  276.7 0.0 copy-done.2
  276.7 3.3 forward.1
  280.0 12.7 %all-to-all-done.6.full_ref = bf16[16,256,128]{2,1,0:T(8,128)(2,1)S(1)} async-done(((bf16[16,256,128]{2,1,0:T(8,128)(2,1)}), bf16[16,256,128]{2,1,0:T(8,128)(2,1)S(1)}, u32[]{:S(2)}, u32[]{:S(2)}) %all-to-all-start.6) | async-done | bytes 1048608 | tf_op jit(solution)/shard_map/all_to_all | solution.py:326
  292.7 0.0 copy-start.1
  292.7 1.0 copy-done.1
  293.7 3.0 mixer_grad.1
  296.7 6.4 %all-to-all-start.9 = ((bf16[32,32,128]{2,1,0:T(8,128)(2,1)}), bf16[32,32,128]{2,1,0:T(8,128)(2,1)S(1)}, u32[]{:S(2)}, u32[]{:S(2)}) async-start(bf16[32,32,128]{2,1,0:T(8,128)(2,1)} %get-tuple-element.37), calls=%async_computation.9 | async-start | bytes 524288 | tf_op jit(solution)/shard_map/all_to_all | solution.py:326
  303.1 2.5 proj.1
  305.6 19.7 %all-to-all-done.9.later_ref = bf16[32,32,128]{2,1,0:T(8,128)(2,1)S(1)} async-done(((bf16[32,32,128]{2,1,0:T(8,128)(2,1)}), bf16[32,32,128]{2,1,0:T(8,128)(2,1)S(1)}, u32[]{:S(2)}, u32[]{:S(2)}) %all-to-all-start.9) | async-done | bytes 262176 | tf_op jit(solution)/shard_map/all_to_all | solution.py:326
  325.3 0.0 copy-start.4
  325.3 4.2 %all-to-all-start.8 = ((bf16[32,64,128]{2,1,0:T(8,128)(2,1)}), bf16[32,64,128]{2,1,0:T(8,128)(2,1)S(1)}, u32[]{:S(2)}, u32[]{:S(2)}) async-start(bf16[32,64,128]{2,1,0:T(8,128)(2,1)} %proj.1), calls=%async_computation.8 | async-start | bytes 1048576 | tf_op jit(solution)/shard_map/all_to_all | solution.py:326
  329.6 5.5 %weight_grads.1 = (bf16[2048,128]{1,0:T(8,128)(2,1)}, bf16[2048,128]{1,0:T(8,128)(2,1)}, bf16[128,2048]{1,0:T(8,128)(2,1)}) custom-call(bf16[16,640,128]{2,1,0:T(8,128)(2,1)} %copy-done, bf16[16,640,128]{2,1,0:T(8,128)(2,1)} %all-to-all-done.3.g_ref, bf16[640,256]{1,0:T(8,128)(2,1)} %get-tuple-element.28.grads_ref, bf16[640,128]{1,0:T(8,128)(2,1)} %get-tuple-element.29.hidden_ref), custom_call_target="tpu_custom_call" | custom-call | tf_op jit(solution)/shard_map/weight_grads/pallas_call | solution.py:45
  335.1 0.0 copy-done.4
  335.1 4.0 %backward.1 = (bf16[64,256]{1,0:T(8,128)(2,1)}, bf16[64,256]{1,0:T(8,128)(2,1)}, bf16[256,128]{1,0:T(8,128)(2,1)}, f32[64,256]{1,0:T(8,128)}) custom-call(bf16[32,32,128]{2,1,0:T(8,128)(2,1)} %copy-done.4, f32[256,128]{1,0:T(8,128)} %get-tuple-element.38.grad_ref, f32[4,128,64]{2,1,0:T(8,128)} %get-tuple-element.39.entering_ref, bf16[64,256]{1,0:T(8,128)(2,1)} %bitcast.29, ...), custom_call_target="tpu_custom_call" | custom-call | tf_op jit(solution)/shard_map/backward/pallas_call | solution.py:45
  339.1 24.0 %all-to-all-done.8.parts_ref = bf16[32,64,128]{2,1,0:T(8,128)(2,1)S(1)} async-done(((bf16[32,64,128]{2,1,0:T(8,128)(2,1)}), bf16[32,64,128]{2,1,0:T(8,128)(2,1)S(1)}, u32[]{:S(2)}, u32[]{:S(2)}) %all-to-all-start.8) | async-done | bytes 524320 | tf_op jit(solution)/shard_map/all_to_all | solution.py:326
  363.1 0.0 copy-start.3
  363.1 0.8 copy-done.3
  363.9 1.7 proj_sum.1
Async XLA Ops:
  39.0 23.9 %all-to-all-start.2 = ((bf16[32,24,128]{2,1,0:T(8,128)(2,1)}), bf16[32,24,128]{2,1,0:T(8,128)(2,1)S(1)}, u32[]{:S(2)}, u32[]{:S(2)}) async-start(bf16[32,24,128]{2,1,0:T(8,128)(2,1)} %get-tuple-element.27), calls=%async_computation.2 | async-start | bytes 393216 | tf_op jit(solution)/shard_map/all_to_all | solution.py:326
  62.9 0.7 copy-start.6
  63.6 43.4 %all-to-all-start.1 = ((bf16[16,640,128]{2,1,0:T(8,128)(2,1)}), bf16[16,640,128]{2,1,0:T(8,128)(2,1)S(1)}, u32[]{:S(2)}, u32[]{:S(2)}) async-start(bf16[16,640,128]{2,1,0:T(8,128)(2,1)} %copies.2), calls=%async_computation.1 | async-start | bytes 5242880 | tf_op jit(solution)/shard_map/all_to_all | solution.py:326
  107.0 1.5 copy-start
  108.5 38.6 %all-to-all-start.3 = ((bf16[16,640,128]{2,1,0:T(8,128)(2,1)}), bf16[16,640,128]{2,1,0:T(8,128)(2,1)}, u32[]{:S(2)}, u32[]{:S(2)}) async-start(bf16[16,640,128]{2,1,0:T(8,128)(2,1)} %copies.3), calls=%async_computation.3 | async-start | bytes 5242880 | tf_op jit(solution)/shard_map/all_to_all | solution.py:326
  196.0 32.9 %all-to-all-start.5 = ((bf16[32,24,128]{2,1,0:T(8,128)(2,1)}), bf16[32,24,128]{2,1,0:T(8,128)(2,1)S(1)}, u32[]{:S(2)}, u32[]{:S(2)}) async-start(bf16[32,24,128]{2,1,0:T(8,128)(2,1)} %row_sum.1), calls=%async_computation.5 | async-start | bytes 393216 | tf_op jit(solution)/shard_map/all_to_all | solution.py:326
  229.0 6.9 %copy-start.5 = (bf16[32,24,128]{2,1,0:T(8,128)(2,1)}, bf16[32,24,128]{2,1,0:T(8,128)(2,1)S(1)}, u32[]{:S(2)}) copy-start(bf16[32,24,128]{2,1,0:T(8,128)(2,1)S(1)} %all-to-all-done.5.back_ref) | copy-start | bytes 589828
  229.0 44.0 %all-to-all-start.7 = ((f32[32,40,128]{2,1,0:T(8,128)}), f32[32,40,128]{2,1,0:T(8,128)S(1)}, u32[]{:S(2)}, u32[]{:S(2)}) async-start(f32[32,40,128]{2,1,0:T(8,128)} %span.1), calls=%async_computation.7 | async-start | bytes 1310720 | tf_op jit(solution)/shard_map/all_to_all | solution.py:326
  273.0 3.7 %copy-start.2 = (f32[32,40,128]{2,1,0:T(8,128)}, f32[32,40,128]{2,1,0:T(8,128)S(1)}, u32[]{:S(2)}) copy-start(f32[32,40,128]{2,1,0:T(8,128)S(1)} %all-to-all-done.7.spans_ref) | copy-start | bytes 1966084
  273.0 19.7 %all-to-all-start.6 = ((bf16[16,256,128]{2,1,0:T(8,128)(2,1)}), bf16[16,256,128]{2,1,0:T(8,128)(2,1)S(1)}, u32[]{:S(2)}, u32[]{:S(2)}) async-start(bf16[16,256,128]{2,1,0:T(8,128)(2,1)} %residual.1), calls=%async_computation.6 | async-start | bytes 2097152 | tf_op jit(solution)/shard_map/all_to_all | solution.py:326
  292.7 1.0 copy-start.1
  296.7 28.6 %all-to-all-start.9 = ((bf16[32,32,128]{2,1,0:T(8,128)(2,1)}), bf16[32,32,128]{2,1,0:T(8,128)(2,1)S(1)}, u32[]{:S(2)}, u32[]{:S(2)}) async-start(bf16[32,32,128]{2,1,0:T(8,128)(2,1)} %get-tuple-element.37), calls=%async_computation.9 | async-start | bytes 524288 | tf_op jit(solution)/shard_map/all_to_all | solution.py:326
  325.3 9.8 %copy-start.4 = (bf16[32,32,128]{2,1,0:T(8,128)(2,1)}, bf16[32,32,128]{2,1,0:T(8,128)(2,1)S(1)}, u32[]{:S(2)}) copy-start(bf16[32,32,128]{2,1,0:T(8,128)(2,1)S(1)} %all-to-all-done.9.later_ref) | copy-start | bytes 786436
  325.3 37.7 %all-to-all-start.8 = ((bf16[32,64,128]{2,1,0:T(8,128)(2,1)}), bf16[32,64,128]{2,1,0:T(8,128)(2,1)S(1)}, u32[]{:S(2)}, u32[]{:S(2)}) async-start(bf16[32,64,128]{2,1,0:T(8,128)(2,1)} %proj.1), calls=%async_computation.8 | async-start | bytes 1048576 | tf_op jit(solution)/shard_map/all_to_all | solution.py:326
  363.1 0.8 copy-start.3

commit v2 on v1

v2 whole, which is shorter than its diff:
```python
import jax
import jax.numpy as jnp
from jax import lax
from jax.experimental import pallas as pl
from jax.experimental.pallas import tpu as pltpu
from jax.sharding import Mesh
from jax.sharding import PartitionSpec as P

KEY_CHANNELS = 32
VAL_DIM = 64
TOP = 2
BLOCK = 64
CAP = 20
PAD = 24
SP = ("sp_0", "sp_1")
N_SP = 32
N_TP = 16
TOK = 256
ROWS = N_SP * CAP
SLOTS = N_SP * PAD
HALF = ROWS // 2
NBLK = TOK // BLOCK
BF = jnp.bfloat16
F32 = jnp.float32
HI = lax.Precision.HIGHEST
SCALE = KEY_CHANNELS ** (-0.5)

NN = (((1,), (0,)), ((), ()))
NT = (((1,), (1,)), ((), ()))
TN = (((0,), (0,)), ((), ()))


def mm(a, b, dims=NN):
    return lax.dot_general(a.astype(BF), b.astype(BF), dims, preferred_element_type=F32)


def mm_exact(a, b, dims=NN):
    return lax.dot_general(a, b, dims, precision=HI, preferred_element_type=F32)


def iota(shape, dim):
    return lax.broadcasted_iota(jnp.int32, shape, dim)


def call(fn, outs, *args, name, scratch=(), smem=(), near=(), near_out=(), after=()):
    spaces = [pltpu.VMEM if k in near else pltpu.HBM for k in range(len(args))]
    args = [
        a if k in smem else pltpu.with_memory_space_constraint(a, spaces[k])
        for k, a in enumerate(args)
    ]
    after = [pltpu.with_memory_space_constraint(a, pltpu.HBM) for a in after]
    count = len(args)

    def run(*refs):
        fn(*refs[:count], *refs[count + len(after) :])

    return pl.pallas_call(
        run,
        out_shape=tuple(
            (pltpu.VMEM if k in near_out else pltpu.HBM)(s, d) for k, (s, d) in enumerate(outs)
        ),
        in_specs=[
            pl.BlockSpec(memory_space=pltpu.SMEM if k in smem else pltpu.VMEM)
            for k in range(count)
        ]
        + [pl.BlockSpec(memory_space=pltpu.HBM) for _ in after],
        out_specs=tuple(pl.BlockSpec(memory_space=pltpu.VMEM) for _ in outs),
        scratch_shapes=scratch,
        name=name,
        compiler_params=pltpu.CompilerParams(vmem_limit_bytes=24 * 1024 * 1024),
    )(*args, *after)


def head_masks():
    key_lane = iota((1, 64), 1) // KEY_CHANNELS
    val_lane = iota((1, 128), 1) // VAL_DIM
    keys = [(key_lane == h).astype(F32) for h in range(2)]
    vals = [(val_lane == h).astype(F32) for h in range(2)]
    own = (iota((128, 64), 0) // VAL_DIM == iota((128, 64), 1) // KEY_CHANNELS).astype(F32)
    return keys, vals, own


def packed_state(state):
    both = state[:64] + state[64:]
    return jnp.concatenate([both[:32], both[32:]], axis=1)


def opened_state(packed, own):
    both = jnp.concatenate([packed[:, :64], packed[:, 64:]], axis=0)
    return jnp.concatenate([both, both], axis=0) * own


def block_sums(decay):
    row, col = iota((TOK, TOK), 0), iota((TOK, TOK), 1)
    within = ((row // BLOCK == col // BLOCK) & (col <= row)).astype(F32)
    return mm_exact(within, decay)


def whole_sums(cumulative):
    offset, parts = jnp.zeros((1, 64), F32), []
    for n in range(NBLK):
        block = cumulative[n * BLOCK : (n + 1) * BLOCK]
        parts.append(block + offset)
        offset = offset + block[BLOCK - 1 :]
    return jnp.concatenate(parts, axis=0), offset


def closings(cumulative):
    return [cumulative[(n + 1) * BLOCK - 1 : (n + 1) * BLOCK] for n in range(NBLK)]


def per_block(rows):
    return jnp.concatenate([jnp.broadcast_to(r, (BLOCK, r.shape[1])) for r in rows], axis=0)


def two_parts(values):
    high = values.astype(BF).astype(F32)
    return high, values - high


def dispatch_kernel(
    routes_ref, weight_ref, x_ref, g_ref, k_ref, v_ref, decay_ref, sent_ref, pick_ref
):
    routes = routes_ref[...]
    expert = iota((N_SP, TOK), 0)
    hot = [(expert == routes[j : j + 1, :]) for j in range(TOP)]
    both = (hot[0] | hot[1]).astype(F32)
    before = (iota((TOK, TOK), 0) < iota((TOK, TOK), 1)).astype(F32)
    place = mm(both, before)
    owner, row = iota((SLOTS, N_SP), 0) // PAD, iota((SLOTS, N_SP), 0) % PAD
    mine = owner == iota((SLOTS, N_SP), 1)
    spread = mine.astype(F32)
    slot_place = (iota((SLOTS, TOK), 0) % PAD).astype(F32)
    picks = [(mm(spread, jnp.where(h, place, -1.0)) == slot_place).astype(F32) for h in hot]
    pick = picks[0] + picks[1]
    pick_ref[...] = pick.astype(BF)

    _, _, own = head_masks()
    keys = k_ref[...].astype(F32).T * SCALE
    so_far, total = whole_sums(block_sums(decay_ref[...].T))
    state = mm(v_ref[...], keys * jnp.exp(total - so_far), TN) * own
    state_high, state_low = two_parts(packed_state(state))
    total_row = jnp.concatenate(two_parts(total), axis=1)

    first = (mine & (row == CAP)).astype(F32)
    second = (mine & (row == CAP + 1)).astype(F32)
    chosen = jnp.concatenate([pick, first, second], axis=1)
    rows = jnp.concatenate([x_ref[...].astype(F32), state_high, state_low], axis=0)
    sent_ref[:, :PAD, :] = mm(chosen, rows).astype(BF).reshape(N_SP, PAD, 128)

    grad = g_ref[...].astype(F32)
    weight = jnp.concatenate([weight_ref[...], jnp.zeros((6, TOK), F32)], axis=0).T
    rows = [(weight[:, j : j + 1] * grad).astype(BF) for j in range(TOP)]
    sent = mm(picks[0], rows[0]) + mm(picks[1], rows[1])
    sent = jnp.where(iota((SLOTS, 128), 0) % PAD == CAP, total_row, sent)
    sent_ref[:, PAD:, :] = sent.astype(BF).reshape(N_SP, PAD, 128)


def turned_kernel(pick_ref, out_ref):
    out_ref[...] = pick_ref[...].astype(F32).T.astype(BF)


def copies_kernel(place_ref, recv_ref, out_ref, states_ref, reach_ref, packed):
    for e in range(N_SP):
        block = recv_ref[e].astype(F32)
        at = e * CAP if e < N_SP // 2 else ROWS + (e - N_SP // 2) * CAP
        packed[at : at + CAP, :] = block[:CAP]
        packed[at + HALF : at + HALF + CAP, :] = block[PAD : PAD + CAP]
    for p in range(2):
        out = packed[p * ROWS : (p + 1) * ROWS, :].astype(BF)
        for k in range(p, N_TP, 2):
            out_ref[k] = out

    chip = place_ref[2]
    totals = [recv_ref[s, PAD + CAP : PAD + CAP + 1, :].astype(F32) for s in range(N_SP)]
    totals = jnp.concatenate(totals, axis=0)
    totals = totals[:, :64] + totals[:, 64:]
    double = jnp.concatenate([totals, totals], axis=1)
    decays = jnp.exp(double)
    state = jnp.zeros((1, 128), F32)
    for s in range(N_SP):
        states_ref[s : s + 1, :] = state
        pair = recv_ref[s, CAP : CAP + 2, :].astype(F32)
        state = decays[s : s + 1] * state + pair[0:1] + pair[1:2]
    target, between = iota((16, N_SP), 0), iota((16, N_SP), 1)
    passed = ((between >= 2 * target + 2) & (between < 2 * chip)).astype(F32)
    reach = jnp.exp(mm_exact(passed, double))
    reach_ref[:16, :] = jnp.where(iota((16, 128), 0) < chip, reach, 0.0)
    here = iota((N_SP, 128), 0)
    even = jnp.sum(jnp.where(here == 2 * chip, decays, 0.0), axis=0, keepdims=True)
    odd = jnp.sum(jnp.where(here == 2 * chip + 1, decays, 0.0), axis=0, keepdims=True)
    reach_ref[16:, :] = jnp.concatenate([even, odd, jnp.zeros((6, 128), F32)], axis=0)


def wide(ref, at, size):
    return jnp.concatenate([ref[k, at : at + size, :] for k in range(N_TP)], axis=1)


def partial_kernel(
    rows_ref, wg_ref, wu_ref, wd_ref, pg_ref, pu_ref, pd_ref, part_ref, grads_ref, hidden_ref
):
    weight = jnp.concatenate([wg_ref[...], wu_ref[...], pg_ref[...], pu_ref[...]], axis=1)
    down = jnp.concatenate([wd_ref[...], pd_ref[...]], axis=0)
    pre = mm(wide(rows_ref, 0, HALF), weight)
    hidden_grad = mm(wide(rows_ref, HALF, HALF), down, NT)
    grads = []
    for b in range(2):
        gate_pre, up_pre = pre[:, 256 * b : 256 * b + 128], pre[:, 256 * b + 128 : 256 * b + 256]
        upper = hidden_grad[:, 128 * b : 128 * b + 128]
        sigmoid = jax.nn.sigmoid(gate_pre)
        activated = gate_pre * sigmoid
        hidden_ref[:, 128 * b : 128 * b + 128] = (activated * up_pre).astype(BF)
        gate = upper * up_pre * sigmoid * (1.0 + gate_pre * (1.0 - sigmoid))
        grads += [gate.astype(BF), (upper * activated).astype(BF)]
    grads = jnp.concatenate(grads, axis=1)
    grads_ref[...] = grads
    for k in range(0, N_TP, 2):
        part = mm(grads, weight[k * 128 : (k + 2) * 128], NT).astype(BF)
        part_ref[k] = part[:, :128]
        part_ref[k + 1] = part[:, 128:]


def weight_grads_kernel(rows_ref, grads_ref, hidden_ref, own_ref, sent_ref):
    grads = grads_ref[...]
    hidden = hidden_ref[...]
    for k in range(0, N_TP, 2):
        x = jnp.concatenate([rows_ref[k, :HALF, :], rows_ref[k + 1, :HALF, :]], axis=1)
        g = jnp.concatenate([rows_ref[k, HALF:, :], rows_ref[k + 1, HALF:, :]], axis=1)
        both = mm(x, grads, TN)
        down = mm(hidden, g, TN)
        here = slice(k * 128, (k + 2) * 128)
        own_ref[0, here, :] = both[:, :128]
        own_ref[1, here, :] = both[:, 128:256]
        sent_ref[0, here, :] = both[:, 256:384].astype(BF)
        sent_ref[1, here, :] = both[:, 384:].astype(BF)
        for n in range(2):
            block = slice((k + n) * 128, (k + n + 1) * 128)
            own_ref[2, block, :] = down[:128, n * 128 : (n + 1) * 128]
            sent_ref[2, block, :] = down[128:, n * 128 : (n + 1) * 128].astype(BF)


def grad_sum_kernel(own_ref, recv_ref, gate_ref, up_ref, down_ref):
    gate_ref[...] = (own_ref[0] + recv_ref[0].astype(F32)).astype(BF)
    up_ref[...] = (own_ref[1] + recv_ref[1].astype(F32)).astype(BF)
    for k in range(N_TP):
        here = slice(k * 128, (k + 1) * 128)
        down_ref[:, here] = (own_ref[2, here, :] + recv_ref[2, here, :].astype(F32)).astype(BF)


def row_sum_kernel(part_ref, states_ref, out_ref, total):
    for p in range(2):
        acc = part_ref[p].astype(F32)
        for k in range(p + 2, N_TP, 2):
            acc = acc + part_ref[k].astype(F32)
        total[p * HALF : (p + 1) * HALF, :] = acc
    total[ROWS:, :] = jnp.zeros((8, 128), F32)
    row = iota((PAD, 128), 0)
    high, low = two_parts(states_ref[...])
    for e in range(N_SP):
        rows = jnp.where(row < CAP, total[e * CAP : e * CAP + PAD, :], 0.0)
        rows = jnp.where(row == CAP, high[e : e + 1], rows)
        rows = jnp.where(row == CAP + 1, low[e : e + 1], rows)
        out_ref[e] = rows.astype(BF)


def residual_kernel(back_ref, turned_ref, g_ref, out_ref):
    routed = mm(turned_ref[...], back_ref[...].reshape(SLOTS, 128))
    residual = (g_ref[...].astype(F32) + routed).astype(BF)
    for k in range(N_TP):
        out_ref[k] = residual


def scores_of(queries, keys, mask, causal):
    return jnp.where(causal, mm(queries * mask, keys, NT), 0.0)


def causal_blocks():
    row, col = iota((TOK, TOK), 0), iota((TOK, TOK), 1)
    return (row // BLOCK == col // BLOCK) & (col <= row)


def forward_kernel(back_ref, q_ref, k_ref, v_ref, decay_ref, out_ref, entering_ref):
    key_mask, val_mask, own = head_masks()
    rows = [back_ref[s, CAP : CAP + 2, :].astype(F32) for s in range(N_SP)]
    packed = jnp.concatenate([r[0:1] + r[1:2] for r in rows], axis=0)
    state = opened_state(packed, own)
    queries = q_ref[...].astype(F32).T
    keys = k_ref[...].astype(F32).T * SCALE
    values = v_ref[...].astype(F32)
    cumulative = block_sums(decay_ref[...].T)
    closing = closings(cumulative)
    scaled_q = queries * jnp.exp(cumulative)
    scaled_k = keys * jnp.exp(-cumulative)
    tail = keys * jnp.exp(per_block(closing) - cumulative)
    causal = causal_blocks()
    within = jnp.zeros((TOK, 128), F32)
    for h in range(2):
        scores = scores_of(scaled_q, scaled_k, key_mask[h], causal)
        within = within + mm(scores, values * val_mask[h])
    for n in range(NBLK):
        here = slice(n * BLOCK, (n + 1) * BLOCK)
        entering_ref[n] = state
        out_ref[here, :] = (within[here] + mm(scaled_q[here], state, NT)).astype(BF)
        state = jnp.exp(closing[n]) * state + mm(values[here], tail[here], TN) * own


def mixer_grad_kernel(
    place_ref, full_ref, w_ref, mixed_ref, q_ref, decay_ref, grad_ref, span_ref, sent_ref, kept_ref
):
    _, _, own = head_masks()
    grad = mm(wide(full_ref, 0, TOK), w_ref[...])
    grad_ref[...] = grad
    so_far, _ = whole_sums(block_sums(decay_ref[...].T))
    scaled = q_ref[...].astype(F32).T * jnp.exp(so_far)
    packed = packed_state(mm(grad, scaled, TN) * own)
    span_ref[...] = packed
    high, low = two_parts(packed)
    sent_ref[1024:1056, :] = high.astype(BF)
    sent_ref[1056:, :] = low.astype(BF)
    mixed = mixed_ref[...]
    first = place_ref[1] == 0
    for k in range(0, N_TP, 2):
        rows = jnp.concatenate([full_ref[k], full_ref[k + 1]], axis=1)
        part = mm(rows, mixed, TN)
        for n in range(2):
            low, high = part[n * 128 : n * 128 + 64], part[n * 128 + 64 : n * 128 + 128]
            here = slice((k + n) * 64, (k + n + 1) * 64)
            kept_ref[here, :] = jnp.where(first, low, high)
            sent_ref[here, :] = jnp.where(first, high, low).astype(BF)


def chip_kernel(place_ref, recv_ref, kept_ref, span_ref, reach_ref, sent_ref, other_ref):
    other = recv_ref[1024:1056, :].astype(F32) + recv_ref[1056:, :].astype(F32)
    other_ref[...] = other
    first = place_ref[1] == 0
    mine = span_ref[...]
    both = jnp.where(first, mine, other) + reach_ref[16:17, :] * jnp.where(first, other, mine)
    for z in range(16):
        here = slice(z * 64, (z + 1) * 64)
        sent_ref[z, :32, :] = (both * reach_ref[z : z + 1, :]).astype(BF)
        sent_ref[z, 32:, :] = (kept_ref[here, :] + recv_ref[here, :].astype(F32)).astype(BF)


def backward_kernel(
    place_ref,
    later_ref,
    other_ref,
    reach_ref,
    grad_ref,
    entering_ref,
    q_ref,
    k_ref,
    v_ref,
    decay_ref,
    gp_ref,
    gq_ref,
    gk_ref,
    gv_ref,
    gd_ref,
):
    key_mask, val_mask, own = head_masks()
    sums = later_ref[0].astype(F32)
    for z in range(1, 16):
        sums = sums + later_ref[z].astype(F32)
    gp_ref[...] = sums[32:]
    packed = sums[:32]
    packed = jnp.where(place_ref[1] == 0, reach_ref[17:18, :] * packed + other_ref[...], packed)
    state_grad = opened_state(packed, own)
    grad = grad_ref[...]
    queries = q_ref[...].astype(F32).T
    keys = k_ref[...].astype(F32).T * SCALE
    values = v_ref[...].astype(F32)
    cumulative = block_sums(decay_ref[...].T)
    closing = closings(cumulative)
    grow, shrink = jnp.exp(cumulative), jnp.exp(-cumulative)
    rest = jnp.exp(per_block(closing) - cumulative)
    scaled_q, scaled_k, tail = queries * grow, keys * shrink, keys * rest
    causal = causal_blocks()
    value_grad = jnp.zeros((TOK, 128), F32)
    query_grad = jnp.zeros((TOK, 64), F32)
    key_grad = jnp.zeros((TOK, 64), F32)
    for h in range(2):
        scores = scores_of(scaled_q, scaled_k, key_mask[h], causal)
        score_grad = jnp.where(causal, mm(grad * val_mask[h], values, NT), 0.0)
        value_grad = value_grad + mm(scores, grad * val_mask[h], TN)
        query_grad = query_grad + mm(score_grad, scaled_k * key_mask[h])
        key_grad = key_grad + mm(score_grad, scaled_q * key_mask[h], TN)
    carried_v, carried_q, tail_grad, close_grad = ([None] * NBLK for _ in range(4))
    for n in reversed(range(NBLK)):
        here = slice(n * BLOCK, (n + 1) * BLOCK)
        entering = entering_ref[n]
        decay_out = jnp.exp(closing[n])
        carried_v[n] = mm(tail[here], state_grad, NT)
        carried_q[n] = mm(grad[here], entering)
        tail_grad[n] = mm(values[here], state_grad)
        close_grad[n] = decay_out * jnp.sum(state_grad * entering, axis=0, keepdims=True) + jnp.sum(
            tail_grad[n] * tail[here], axis=0, keepdims=True
        )
        state_grad = decay_out * state_grad + mm(grad[here], scaled_q[here], TN) * own
    value_grad = value_grad + jnp.concatenate(carried_v, axis=0)
    query_grad = query_grad + jnp.concatenate(carried_q, axis=0)
    tail_grad = jnp.concatenate(tail_grad, axis=0)
    change = query_grad * scaled_q - key_grad * scaled_k - tail_grad * tail
    row, col = iota((TOK, TOK), 0), iota((TOK, TOK), 1)
    onward = ((row // BLOCK == col // BLOCK) & (col >= row)).astype(F32)
    gd_ref[...] = (mm_exact(onward, change) + per_block(close_grad)).T
    gq_ref[...] = (query_grad * grow).T.astype(BF)
    gk_ref[...] = ((key_grad * shrink + tail_grad * rest) * SCALE).T.astype(BF)
    gv_ref[...] = value_grad.astype(BF)


def exchanged(blocks, axis):
    return lax.all_to_all(blocks, axis, split_axis=0, concat_axis=0, tiled=True)


PARTNERS = [(k, k ^ 1) for k in range(N_TP)]


def body(
    moe_input,
    out_grad,
    routes,
    route_weight,
    w_gate,
    w_up,
    w_down,
    w_out,
    queries,
    key_rows,
    value_rows,
    log_decay,
):
    weights = (w_gate[0], w_up[0], w_down[0])
    with jax.named_scope("partner_weights"):
        partner_weights = tuple(lax.ppermute(w, "tp", PARTNERS) for w in weights)
    q_t, k_t, decay_t = queries.T, key_rows.T, log_decay.T
    place = jnp.stack(
        [lax.axis_index(SP), lax.axis_index("sp_1"), lax.axis_index("sp_0")]
    ).astype(jnp.int32)

    sent, pick = call(
        dispatch_kernel,
        [((N_SP, 2 * PAD, 128), BF), ((SLOTS, TOK), BF)],
        routes.T,
        route_weight.T,
        moe_input,
        out_grad,
        k_t,
        value_rows,
        decay_t,
        name="dispatch",
    )
    recv = exchanged(sent, SP)
    (turned,) = call(turned_kernel, [((TOK, SLOTS), BF)], pick, name="turned")
    copies, states, reach = call(
        copies_kernel,
        [((N_TP, ROWS, 128), BF), ((N_SP, 128), F32), ((24, 128), F32)],
        place,
        recv,
        name="copies",
        scratch=[pltpu.VMEM((2 * ROWS, 128), F32)],
        smem=(0,),
        near=(1,),
        near_out=(0,),
        after=partner_weights,
    )
    rows = exchanged(copies, "tp")
    partial_rows, grads, hidden = call(
        partial_kernel,
        [((N_TP, HALF, 128), BF), ((HALF, 512), BF), ((HALF, 256), BF)],
        rows,
        *weights,
        *partner_weights,
        name="partial",
        near=(0,),
        near_out=(0,),
    )
    arrived = exchanged(partial_rows, "tp")
    (returned,) = call(
        row_sum_kernel,
        [((N_SP, PAD, 128), BF)],
        arrived,
        states,
        name="row_sum",
        near=(0,),
        scratch=[pltpu.VMEM((ROWS + 8, 128), F32)],
    )
    own_grads, sent_grads = call(
        weight_grads_kernel,
        [((3, 2048, 128), F32), ((3, 2048, 128), BF)],
        rows,
        grads,
        hidden,
        name="weight_grads",
        near=(0,),
        after=(returned,),
    )
    with jax.named_scope("partner_grads"):
        partner_grads = lax.ppermute(sent_grads, "tp", PARTNERS)
    back = exchanged(returned, SP)
    (residual,) = call(
        residual_kernel,
        [((N_TP, TOK, 128), BF)],
        back,
        turned,
        out_grad,
        name="residual",
        near=(0,),
        after=(own_grads,),
    )
    full_grad = exchanged(residual, "tp")
    mixer_out, entering = call(
        forward_kernel,
        [((TOK, 128), BF), ((NBLK, 128, 64), F32)],
        back,
        q_t,
        k_t,
        value_rows,
        decay_t,
        name="forward",
        near=(0,),
        after=(residual,),
    )
    mixer_grad, span_grad, to_other, kept = call(
        mixer_grad_kernel,
        [((TOK, 128), F32), ((32, 128), F32), ((1088, 128), BF), ((1024, 128), F32)],
        place,
        full_grad,
        w_out,
        mixer_out,
        q_t,
        decay_t,
        name="mixer_grad",
        smem=(0,),
        near=(1,),
        near_out=(2, 3),
    )
    with jax.named_scope("cores"):
        from_other = lax.ppermute(to_other, "sp_1", [(0, 1), (1, 0)])
    chip_sent, other_grad = call(
        chip_kernel,
        [((16, 96, 128), BF), ((32, 128), F32)],
        place,
        from_other,
        kept,
        span_grad,
        reach,
        name="chip",
        smem=(0,),
        near=(1, 2),
    )
    later = exchanged(chip_sent, "sp_0")
    grad_proj, gq, gk, gv, gd = call(
        backward_kernel,
        [((64, 128), F32), ((64, TOK), BF), ((64, TOK), BF), ((TOK, 128), BF), ((64, TOK), F32)],
        place,
        later,
        other_grad,
        reach,
        mixer_grad,
        entering,
        q_t,
        k_t,
        value_rows,
        decay_t,
        name="backward",
        smem=(0,),
        near=(1,),
    )
    gate_part, up_part, down_part = call(
        grad_sum_kernel,
        [((2048, 128), BF), ((2048, 128), BF), ((128, 2048), BF)],
        own_grads,
        partner_grads,
        name="grad_sum",
    )
    return (gate_part[None], up_part[None], down_part[None], grad_proj, gq.T, gk.T, gv, gd.T)


def solution(mesh):
    split = Mesh(mesh.devices.reshape(16, 2, mesh.shape["tp"]), ("sp_0", "sp_1", "tp"))
    placed = (
        P(SP, "tp"),
        P(SP, "tp"),
        P(SP, None),
        P(SP, None),
        P(SP, None, "tp"),
        P(SP, None, "tp"),
        P(SP, "tp", None),
        P(None, "tp"),
        P(SP, "tp"),
        P(SP, "tp"),
        P(SP, "tp"),
        P(SP, "tp"),
    )
    return jax.shard_map(
        body,
        mesh=split,
        in_specs=placed,
        out_specs=(
            P(SP, None, "tp"),
            P(SP, None, "tp"),
            P(SP, "tp", None),
            P(SP, "tp"),
            P(SP, "tp"),
            P(SP, "tp"),
            P(SP, "tp"),
            P(SP, "tp"),
        ),
        check_vma=False,
    )
```

time: 367 us -> 238 us (0.65)
  waiting for transfers between devices: 188 us -> 84.4 us
  blocking collectives: 74.9 us -> 60.2 us
  Pallas kernels: 48.1 us -> 35.5 us
  starting transfers between devices: 49.8 us -> 54.1 us
    all_to_all x8 -> x4, waiting for transfers between devices: 188 us -> 24.4 us  [exchanged(): return lax.all_to_all(blocks, axis, split_axis=0, concat_axis=0, tiled=True)]
    ppermute x0 -> x5, waiting for transfers between devices: none -> 60 us  [the longest x1 30.7 us: body(): partner_grads = lax.ppermute(sent_grads, 'tp', PARTNERS)]
    ppermute x0 -> x5, starting transfers between devices: none -> 15.2 us  [the longest x3 8.41 us: body(): partner_weights = tuple((lax.ppermute(w, 'tp', PARTNERS) for w in weights))]
    all_to_all x2, blocking collectives: 74.9 us -> 60.2 us  [exchanged(): return lax.all_to_all(blocks, axis, split_axis=0, concat_axis=0, tiled=True)]
    pallas_call x15 -> x12, Pallas kernels: 48.1 us -> 35.5 us  [call(): pl.pallas_call(run, out_shape=tuple(((pltpu.VMEM if k in near_out else pl...]
    all_to_all x8 -> x4, starting transfers between devices: 49.8 us -> 38.9 us  [exchanged(): return lax.all_to_all(blocks, axis, split_axis=0, concat_axis=0, tiled=True)]
  transfers between devices with their start and end apart: 8 -> 9, of which waited for: 8 -> 6; matrix products, arithmetic and copies ran while one was open for 0% -> 0% of each run, Pallas kernels for 8% -> 6%
where the time goes in v2:
time: 238 us; the launch traced here: 237 us
  waiting for transfers between devices  84.4 us (35%)
  blocking collectives  60.2 us (25%)
  starting transfers between devices  54.1 us (23%)
  Pallas kernels  35.5 us (15%)
    all_to_all x2, blocking collectives, exchanged(): return lax.all_to_all(blocks, axis, split_axis=0, concat_axis=0, tiled=True)  60.2 us
    all_to_all x4, starting transfers between devices, exchanged(): return lax.all_to_all(blocks, axis, split_axis=0, concat_axis=0, tiled=True)  38.9 us
    pallas_call x12, Pallas kernels, call(): pl.pallas_call(run, out_shape=tuple(((pltpu.VMEM if k in near_out else pl...  35.5 us
    ppermute x1, waiting for transfers between devices, body(): partner_grads = lax.ppermute(sent_grads, 'tp', PARTNERS)  30.7 us
    ppermute x3, waiting for transfers between devices, body(): partner_weights = tuple((lax.ppermute(w, 'tp', PARTNERS) for w in weights))  29.3 us
    all_to_all x4, waiting for transfers between devices, exchanged(): return lax.all_to_all(blocks, axis, split_axis=0, concat_axis=0, tiled=True)  24.4 us
    ppermute x3, starting transfers between devices, body(): partner_weights = tuple((lax.ppermute(w, 'tp', PARTNERS) for w in weights))  8.41 us
    ppermute x1, starting transfers between devices, body(): from_other = lax.ppermute(to_other, 'sp_1', [(0, 1), (1, 0)])  4.86 us
  transfers between devices with their start and end apart: 9, of which 6 were waited for; matrix products, arithmetic and copies ran while one was open for 0% of the time, Pallas kernels for 6%

profile of v2, /device:TPU:1, one launch (start us, length us, event | category | flops | bytes accessed | tf_op | source)
XLA Modules:
  0.0 236.9 jit_solution(15470984765195054631)
XLA Ops:
  0.6 3.8 %dispatch.1 = (bf16[32,48,128]{2,1,0:T(8,128)(2,1)}, bf16[768,256]{1,0:T(8,128)(2,1)}) custom-call(s32[2,256]{1,0:T(2,128)} %bitcast.33, f32[2,256]{1,0:T(2,128)} %bitcast.34, bf16[256,128]{1,0:T(8,128)(2,1)} %refs_2_.3, bf16[256,128]{1,0:T(8,128)(2,1)} %refs_2_.4, bf16[64,256]{1,0:T(8,128)(2,1)} %bitcast.27, bf16[256,128]{1,0:T(8,128)(2,1)} %refs_8_.1, ...), custom_call_target="tpu_custom_call" | custom-call | tf_op jit(solution)/shard_map/dispatch/pallas_call | solution.py:57
  4.4 16.7 %all-to-all-start = ((bf16[32,48,128]{2,1,0:T(8,128)(2,1)}), bf16[32,48,128]{2,1,0:T(8,128)(2,1)S(1)}, u32[]{:S(2)}, u32[]{:S(2)}) async-start(bf16[32,48,128]{2,1,0:T(8,128)(2,1)} %get-tuple-element.34), calls=%async_computation | async-start | bytes 786432 | tf_op jit(solution)/shard_map/all_to_all | solution.py:413
  21.2 3.1 %collective-permute-start = (bf16[2048,128]{1,0:T(8,128)(2,1)}, bf16[2048,128]{1,0:T(8,128)(2,1)S(1)}, u32[]{:S(2)}, u32[]{:S(2)}) collective-permute-start(bf16[2048,128]{1,0:T(8,128)(2,1)} %bitcast.21), channel_id=1, source_target_pairs={{0,1},{1,0},{2,3},{3,2},{4,5},{5,4},{6,7},{7,6},{8,9},{9,8},{10,11... | collective-permute-start | bytes 1572872 | tf_op jit(solution)/shard_map/partner_weights/ppermute | solution.py:435
  24.3 2.2 collective-permute-start.1
  26.5 3.1 %collective-permute-start.2 = (bf16[128,2048]{1,0:T(8,128)(2,1)}, bf16[128,2048]{1,0:T(8,128)(2,1)S(1)}, u32[]{:S(2)}, u32[]{:S(2)}) collective-permute-start(bf16[128,2048]{1,0:T(8,128)(2,1)} %bitcast.25), channel_id=1, source_target_pairs={{0,1},{1,0},{2,3},{3,2},{4,5},{5,4},{6,7},{7,6},{8,9},{9,8},{10,11... | collective-permute-start | bytes 1572872 | tf_op jit(solution)/shard_map/partner_weights/ppermute | solution.py:435
  29.6 0.1 pad_add_fusion.refs_0_
  29.7 6.8 %collective-permute-done.refs_2_.refs_4_ = bf16[2048,128]{1,0:T(8,128)(2,1)S(1)} collective-permute-done((bf16[2048,128]{1,0:T(8,128)(2,1)}, bf16[2048,128]{1,0:T(8,128)(2,1)S(1)}, u32[]{:S(2)}, u32[]{:S(2)}) %collective-permute-start) | collective-permute-done | bytes 524320 | tf_op jit(solution)/shard_map/partner_weights/ppermute | solution.py:435
  36.5 0.0 copy-start
  36.5 11.2 %collective-permute-done.1.refs_3_.refs_5_ = bf16[2048,128]{1,0:T(8,128)(2,1)S(1)} collective-permute-done((bf16[2048,128]{1,0:T(8,128)(2,1)}, bf16[2048,128]{1,0:T(8,128)(2,1)S(1)}, u32[]{:S(2)}, u32[]{:S(2)}) %collective-permute-start.1) | collective-permute-done | bytes 524320 | tf_op jit(solution)/shard_map/partner_weights/ppermute | solution.py:435
  47.8 0.0 copy-start.1
  47.8 11.2 %collective-permute-done.2.refs_4_.refs_6_ = bf16[128,2048]{1,0:T(8,128)(2,1)S(1)} collective-permute-done((bf16[128,2048]{1,0:T(8,128)(2,1)}, bf16[128,2048]{1,0:T(8,128)(2,1)S(1)}, u32[]{:S(2)}, u32[]{:S(2)}) %collective-permute-start.2) | collective-permute-done | bytes 524320 | tf_op jit(solution)/shard_map/partner_weights/ppermute | solution.py:435
  59.0 0.0 copy-start.2
  59.0 0.0 all-to-all-done.refs_1_
  59.0 0.0 copy-done
  59.0 0.0 copy-done.1
  59.0 0.8 copy-done.2
  59.8 1.6 copies.1
  61.4 39.3 %all_to_all.30.refs_0_ = bf16[16,640,128]{2,1,0:T(8,128)(2,1)S(1)} all-to-all(bf16[16,640,128]{2,1,0:T(8,128)(2,1)S(1)} %get-tuple-element.35), channel_id=1, replica_groups=mesh['sp_0'=16,'sp_1'=2,'tp'=16] {'tp'}, dimensions={0} | all-to-all | bytes 5242880 | tf_op jit(solution)/shard_map/all_to_all | solution.py:413
  100.7 4.4 %partial.1 = (bf16[16,320,128]{2,1,0:T(8,128)(2,1)S(1)}, bf16[320,512]{1,0:T(8,128)(2,1)}, bf16[320,256]{1,0:T(8,128)(2,1)}) custom-call(bf16[16,640,128]{2,1,0:T(8,128)(2,1)S(1)} %all_to_all.30.refs_0_, bf16[2048,128]{1,0:T(8,128)(2,1)} %bitcast.22, bf16[2048,128]{1,0:T(8,128)(2,1)} %bitcast.24, bf16[128,2048]{1,0:T(8,128)(2,1)} %bitcast.26, ...), custom_call_target="tpu_custom_call" | custom-call | tf_op jit(solution)/shard_map/partial/pallas_call | solution.py:57
  105.1 20.9 %all_to_all.31.refs_0_ = bf16[16,320,128]{2,1,0:T(8,128)(2,1)S(1)} all-to-all(bf16[16,320,128]{2,1,0:T(8,128)(2,1)S(1)} %get-tuple-element.38), channel_id=1, replica_groups=mesh['sp_0'=16,'sp_1'=2,'tp'=16] {'tp'}, dimensions={0} | all-to-all | bytes 2621440 | tf_op jit(solution)/shard_map/all_to_all | solution.py:413
  126.0 1.6 row_sum.1.refs_3_
  127.6 14.9 %all-to-all-start.3 = ((bf16[32,24,128]{2,1,0:T(8,128)(2,1)}), bf16[32,24,128]{2,1,0:T(8,128)(2,1)S(1)}, u32[]{:S(2)}, u32[]{:S(2)}) async-start(bf16[32,24,128]{2,1,0:T(8,128)(2,1)} %row_sum.1.refs_3_), calls=%async_computation.3 | async-start | bytes 393216 | tf_op jit(solution)/shard_map/all_to_all | solution.py:413
  142.5 1.9 turned.1.refs_1_
  144.5 5.0 %weight_grads.1 = (f32[3,2048,128]{2,1,0:T(8,128)}, bf16[3,2048,128]{2,1,0:T(8,128)(2,1)}) custom-call(bf16[16,640,128]{2,1,0:T(8,128)(2,1)S(1)} %all_to_all.30.refs_0_, bf16[320,512]{1,0:T(8,128)(2,1)} %get-tuple-element.36.refs_1_, bf16[320,256]{1,0:T(8,128)(2,1)} %get-tuple-element.37.refs_2_, bf16[32,24,128]{2,1,0:T(8,128)(2,1)} %row_sum.1.refs_3_), custom_call_target="tpu_custom_call" | custom-call | tf_op jit(solution)/shard_map/weight_grads/pallas_call | solution.py:57
  149.4 11.9 %all-to-all-done.3.refs_0_ = bf16[32,24,128]{2,1,0:T(8,128)(2,1)S(1)} async-done(((bf16[32,24,128]{2,1,0:T(8,128)(2,1)}), bf16[32,24,128]{2,1,0:T(8,128)(2,1)S(1)}, u32[]{:S(2)}, u32[]{:S(2)}) %all-to-all-start.3) | async-done | bytes 196640 | tf_op jit(solution)/shard_map/all_to_all | solution.py:413
  161.3 2.3 residual.1.refs_5_
  163.6 3.7 %all-to-all-start.4 = ((bf16[16,256,128]{2,1,0:T(8,128)(2,1)}), bf16[16,256,128]{2,1,0:T(8,128)(2,1)S(1)}, u32[]{:S(2)}, u32[]{:S(2)}) async-start(bf16[16,256,128]{2,1,0:T(8,128)(2,1)} %residual.1.refs_5_), calls=%async_computation.4 | async-start | bytes 2097152 | tf_op jit(solution)/shard_map/all_to_all | solution.py:413
  167.3 3.0 %forward.1 = (bf16[256,128]{1,0:T(8,128)(2,1)}, f32[4,128,64]{2,1,0:T(8,128)}) custom-call(bf16[32,24,128]{2,1,0:T(8,128)(2,1)S(1)} %all-to-all-done.3.refs_0_, bf16[64,256]{1,0:T(8,128)(2,1)} %bitcast.30, bf16[64,256]{1,0:T(8,128)(2,1)} %bitcast.28, bf16[256,128]{1,0:T(8,128)(2,1)} %refs_8_.1, f32[64,256]{1,0:T(8,128)} %bitcast.18, ...), custom_call_target="tpu_custom_call" | custom-call | tf_op jit(solution)/shard_map/forward/pallas_call | solution.py:57
  170.3 0.0 copy-start.4
  170.3 12.5 %all-to-all-done.4.refs_1_ = bf16[16,256,128]{2,1,0:T(8,128)(2,1)S(1)} async-done(((bf16[16,256,128]{2,1,0:T(8,128)(2,1)}), bf16[16,256,128]{2,1,0:T(8,128)(2,1)S(1)}, u32[]{:S(2)}, u32[]{:S(2)}) %all-to-all-start.4) | async-done | bytes 1048608 | tf_op jit(solution)/shard_map/all_to_all | solution.py:413
  182.8 2.8 %mixer_grad.1 = (f32[256,128]{1,0:T(8,128)}, f32[32,128]{1,0:T(8,128)}, bf16[1088,128]{1,0:T(8,128)(2,1)S(1)}, f32[1024,128]{1,0:T(8,128)S(1)}) custom-call(s32[3]{0:T(128)S(1)} %pad_add_fusion.refs_0_, bf16[16,256,128]{2,1,0:T(8,128)(2,1)S(1)} %all-to-all-done.4.refs_1_, bf16[2048,128]{1,0:T(8,128)(2,1)} %refs_2_.5, ...), custom_call_target="tpu_custom_call" | custom-call | tf_op jit(solution)/shard_map/mixer_grad/pallas_call | solution.py:57
  185.6 4.9 %collective-permute-start.4 = (bf16[1088,128]{1,0:T(8,128)(2,1)S(1)}, bf16[1088,128]{1,0:T(8,128)(2,1)S(1)}, u32[]{:S(2)}, u32[]{:S(2)}) collective-permute-start(bf16[1088,128]{1,0:T(8,128)(2,1)S(1)} %get-tuple-element.47), channel_id=1, source_target_pairs={{0,16},{16,0},{1,17},{17,1},{2,18},{18,2},{3,19},{19,3},{4,20},{20... | collective-permute-start | bytes 835592 | tf_op jit(solution)/shard_map/cores/ppermute | solution.py:539
  190.4 0.0 copy-done.4
  190.4 1.9 collective-permute-start.3
  192.4 0.0 collective-permute-done.4.refs_1_
  192.4 1.6 chip.1
  193.9 3.6 %all-to-all-start.5 = ((bf16[16,96,128]{2,1,0:T(8,128)(2,1)}), bf16[16,96,128]{2,1,0:T(8,128)(2,1)S(1)}, u32[]{:S(2)}, u32[]{:S(2)}) async-start(bf16[16,96,128]{2,1,0:T(8,128)(2,1)} %get-tuple-element.51), calls=%async_computation.5 | async-start | bytes 786432 | tf_op jit(solution)/shard_map/all_to_all | solution.py:413
  197.6 30.7 %collective-permute-done.3.refs_1_ = bf16[3,2048,128]{2,1,0:T(8,128)(2,1)S(1)} collective-permute-done((bf16[3,2048,128]{2,1,0:T(8,128)(2,1)S(1)}, bf16[3,2048,128]{2,1,0:T(8,128)(2,1)S(1)}, u32[]{:S(2)}, u32[]{:S(2)}) %collective-permute-start.3) | collective-permute-done | bytes 1572896 | tf_op jit(solution)/shard_map/partner_grads/ppermute | solution.py:499
  228.3 0.0 copy-start.3
  228.3 1.2 copy-done.3
  229.5 3.6 %grad_sum.1 = (bf16[2048,128]{1,0:T(8,128)(2,1)}, bf16[2048,128]{1,0:T(8,128)(2,1)}, bf16[128,2048]{1,0:T(8,128)(2,1)}) custom-call(f32[3,2048,128]{2,1,0:T(8,128)} %get-tuple-element.40.refs_0_.refs_3_, bf16[3,2048,128]{2,1,0:T(8,128)(2,1)} %copy-done.3), custom_call_target="tpu_custom_call" | custom-call | tf_op jit(solution)/shard_map/grad_sum/pallas_call | solution.py:57
  233.0 0.0 all-to-all-done.5.refs_1_
  233.0 3.9 %backward.1 = (f32[64,128]{1,0:T(8,128)}, bf16[64,256]{1,0:T(8,128)(2,1)}, bf16[64,256]{1,0:T(8,128)(2,1)}, bf16[256,128]{1,0:T(8,128)(2,1)}, f32[64,256]{1,0:T(8,128)}) custom-call(s32[3]{0:T(128)S(1)} %pad_add_fusion.refs_0_, bf16[16,96,128]{2,1,0:T(8,128)(2,1)S(1)} %all-to-all-done.5.refs_1_, f32[32,128]{1,0:T(8,128)} %get-tuple-element.52.refs_2_, ...), custom_call_target="tpu_custom_call" | custom-call | tf_op jit(solution)/shard_map/backward/pallas_call | solution.py:57
Async XLA Ops:
  4.4 54.6 %all-to-all-start = ((bf16[32,48,128]{2,1,0:T(8,128)(2,1)}), bf16[32,48,128]{2,1,0:T(8,128)(2,1)S(1)}, u32[]{:S(2)}, u32[]{:S(2)}) async-start(bf16[32,48,128]{2,1,0:T(8,128)(2,1)} %get-tuple-element.34), calls=%async_computation | async-start | bytes 786432 | tf_op jit(solution)/shard_map/all_to_all | solution.py:413
  21.2 15.4 %collective-permute-start = (bf16[2048,128]{1,0:T(8,128)(2,1)}, bf16[2048,128]{1,0:T(8,128)(2,1)S(1)}, u32[]{:S(2)}, u32[]{:S(2)}) collective-permute-start(bf16[2048,128]{1,0:T(8,128)(2,1)} %bitcast.21), channel_id=1, source_target_pairs={{0,1},{1,0},{2,3},{3,2},{4,5},{5,4},{6,7},{7,6},{8,9},{9,8},{10,11... | collective-permute-start | bytes 1572872 | tf_op jit(solution)/shard_map/partner_weights/ppermute | solution.py:435
  24.3 23.5 %collective-permute-start.1 = (bf16[2048,128]{1,0:T(8,128)(2,1)}, bf16[2048,128]{1,0:T(8,128)(2,1)S(1)}, u32[]{:S(2)}, u32[]{:S(2)}) collective-permute-start(bf16[2048,128]{1,0:T(8,128)(2,1)} %bitcast.23), channel_id=1, source_target_pairs={{0,1},{1,0},{2,3},{3,2},{4,5},{5,4},{6,7},{7,6},{8,9},{9,8},{10,11... | collective-permute-start | bytes 1572872 | tf_op jit(solution)/shard_map/partner_weights/ppermute | solution.py:435
  26.5 32.5 %collective-permute-start.2 = (bf16[128,2048]{1,0:T(8,128)(2,1)}, bf16[128,2048]{1,0:T(8,128)(2,1)S(1)}, u32[]{:S(2)}, u32[]{:S(2)}) collective-permute-start(bf16[128,2048]{1,0:T(8,128)(2,1)} %bitcast.25), channel_id=1, source_target_pairs={{0,1},{1,0},{2,3},{3,2},{4,5},{5,4},{6,7},{7,6},{8,9},{9,8},{10,11... | collective-permute-start | bytes 1572872 | tf_op jit(solution)/shard_map/partner_weights/ppermute | solution.py:435
  36.5 22.5 %copy-start = (bf16[2048,128]{1,0:T(8,128)(2,1)}, bf16[2048,128]{1,0:T(8,128)(2,1)S(1)}, u32[]{:S(2)}) copy-start(bf16[2048,128]{1,0:T(8,128)(2,1)S(1)} %collective-permute-done.refs_2_.refs_4_) | copy-start | bytes 1572868
  47.8 11.2 %copy-start.1 = (bf16[2048,128]{1,0:T(8,128)(2,1)}, bf16[2048,128]{1,0:T(8,128)(2,1)S(1)}, u32[]{:S(2)}) copy-start(bf16[2048,128]{1,0:T(8,128)(2,1)S(1)} %collective-permute-done.1.refs_3_.refs_5_) | copy-start | bytes 1572868
  59.0 0.8 copy-start.2
  127.6 33.7 %all-to-all-start.3 = ((bf16[32,24,128]{2,1,0:T(8,128)(2,1)}), bf16[32,24,128]{2,1,0:T(8,128)(2,1)S(1)}, u32[]{:S(2)}, u32[]{:S(2)}) async-start(bf16[32,24,128]{2,1,0:T(8,128)(2,1)} %row_sum.1.refs_3_), calls=%async_computation.3 | async-start | bytes 393216 | tf_op jit(solution)/shard_map/all_to_all | solution.py:413
  163.6 19.2 %all-to-all-start.4 = ((bf16[16,256,128]{2,1,0:T(8,128)(2,1)}), bf16[16,256,128]{2,1,0:T(8,128)(2,1)S(1)}, u32[]{:S(2)}, u32[]{:S(2)}) async-start(bf16[16,256,128]{2,1,0:T(8,128)(2,1)} %residual.1.refs_5_), calls=%async_computation.4 | async-start | bytes 2097152 | tf_op jit(solution)/shard_map/all_to_all | solution.py:413
  170.3 20.1 %copy-start.4 = (bf16[3,2048,128]{2,1,0:T(8,128)(2,1)S(1)}, bf16[3,2048,128]{2,1,0:T(8,128)(2,1)}, u32[]{:S(2)}) copy-start(bf16[3,2048,128]{2,1,0:T(8,128)(2,1)} %get-tuple-element.41) | copy-start | bytes 4718596
  185.6 6.8 %collective-permute-start.4 = (bf16[1088,128]{1,0:T(8,128)(2,1)S(1)}, bf16[1088,128]{1,0:T(8,128)(2,1)S(1)}, u32[]{:S(2)}, u32[]{:S(2)}) collective-permute-start(bf16[1088,128]{1,0:T(8,128)(2,1)S(1)} %get-tuple-element.47), channel_id=1, source_target_pairs={{0,16},{16,0},{1,17},{17,1},{2,18},{18,2},{3,19},{19,3},{4,20},{20... | collective-permute-start | bytes 835592 | tf_op jit(solution)/shard_map/cores/ppermute | solution.py:539
  190.4 37.8 %collective-permute-start.3 = (bf16[3,2048,128]{2,1,0:T(8,128)(2,1)S(1)}, bf16[3,2048,128]{2,1,0:T(8,128)(2,1)S(1)}, u32[]{:S(2)}, u32[]{:S(2)}) collective-permute-start(bf16[3,2048,128]{2,1,0:T(8,128)(2,1)S(1)} %copy-done.4), channel_id=1, source_target_pairs={{0,1},{1,0},{2,3},{3,2},{4,5},{5,4},{6,7},{7,6},{8,9},{9,8},{10,11... | collective-permute-start | bytes 4718600 | tf_op jit(solution)/shard_map/partner_grads/ppermute | solution.py:499
  193.9 39.1 %all-to-all-start.5 = ((bf16[16,96,128]{2,1,0:T(8,128)(2,1)}), bf16[16,96,128]{2,1,0:T(8,128)(2,1)S(1)}, u32[]{:S(2)}, u32[]{:S(2)}) async-start(bf16[16,96,128]{2,1,0:T(8,128)(2,1)} %get-tuple-element.51), calls=%async_computation.5 | async-start | bytes 786432 | tf_op jit(solution)/shard_map/all_to_all | solution.py:413
  228.3 1.2 copy-start.3

commit v3 on v2

--- a/solution.py
+++ b/solution.py
@@ -5,6 +5,7 @@
 from jax.experimental.pallas import tpu as pltpu
 from jax.sharding import Mesh
 from jax.sharding import PartitionSpec as P
+
 
 KEY_CHANNELS = 32
 VAL_DIM = 64
@@ -18,7 +19,8 @@
 TOK = 256
 ROWS = N_SP * CAP
 SLOTS = N_SP * PAD
-HALF = ROWS // 2
+PART = ROWS // 4
+WEIGHT_ROWS = 3 * 2048
 NBLK = TOK // BLOCK
 BF = jnp.bfloat16
 F32 = jnp.float32
@@ -42,7 +44,7 @@
     return lax.broadcasted_iota(jnp.int32, shape, dim)
 
 
-def call(fn, outs, *args, name, scratch=(), smem=(), near=(), near_out=(), after=()):
+def call(fn, outs, *args, scratch=(), smem=(), near=(), near_out=(), after=()):
     spaces = [pltpu.VMEM if k in near else pltpu.HBM for k in range(len(args))]
     args = [
         a if k in smem else pltpu.with_memory_space_constraint(a, spaces[k])
@@ -66,7 +68,6 @@
         + [pl.BlockSpec(memory_space=pltpu.HBM) for _ in after],
         out_specs=tuple(pl.BlockSpec(memory_space=pltpu.VMEM) for _ in outs),
         scratch_shapes=scratch,
-        name=name,
         compiler_params=pltpu.CompilerParams(vmem_limit_bytes=24 * 1024 * 1024),
     )(*args, *after)
 
@@ -160,17 +161,20 @@
     out_ref[...] = pick_ref[...].astype(F32).T.astype(BF)
 
 
-def copies_kernel(place_ref, recv_ref, out_ref, states_ref, reach_ref, packed):
+def quarter_of(place_ref, k):
+    return jnp.where(place_ref[1] == 0, k % 4, k // 4)
+
+
+def copies_kernel(place_ref, recv_ref, out_ref, states_ref, reach_ref, packed, rounded):
     for e in range(N_SP):
         block = recv_ref[e].astype(F32)
-        at = e * CAP if e < N_SP // 2 else ROWS + (e - N_SP // 2) * CAP
+        at = (e // 8) * 2 * PART + (e % 8) * CAP
         packed[at : at + CAP, :] = block[:CAP]
-        packed[at + HALF : at + HALF + CAP, :] = block[PAD : PAD + CAP]
-    for p in range(2):
-        out = packed[p * ROWS : (p + 1) * ROWS, :].astype(BF)
-        for k in range(p, N_TP, 2):
-            out_ref[k] = out
-
+        packed[at + PART : at + PART + CAP, :] = block[PAD : PAD + CAP]
+    for q in range(4):
+        rounded[q] = packed[q * 2 * PART : (q + 1) * 2 * PART, :].astype(BF)
+    for k in range(N_TP):
+        out_ref[k] = rounded[quarter_of(place_ref, k)]
     chip = place_ref[2]
     totals = [recv_ref[s, PAD + CAP : PAD + CAP + 1, :].astype(F32) for s in range(N_SP)]
     totals = jnp.concatenate(totals, axis=0)
@@ -192,19 +196,33 @@
     reach_ref[16:, :] = jnp.concatenate([even, odd, jnp.zeros((6, 128), F32)], axis=0)
 
 
+def pack_kernel(wg_ref, wu_ref, wd_ref, out_ref):
+    out_ref[:2048, :] = wg_ref[...]
+    out_ref[2048:4096, :] = wu_ref[...]
+    for k in range(N_TP):
+        at = 4096 + k * 128
+        out_ref[at : at + 128, :] = wd_ref[:, k * 128 : (k + 1) * 128]
+
+
 def wide(ref, at, size):
     return jnp.concatenate([ref[k, at : at + size, :] for k in range(N_TP)], axis=1)
 
 
 def partial_kernel(
-    rows_ref, wg_ref, wu_ref, wd_ref, pg_ref, pu_ref, pd_ref, part_ref, grads_ref, hidden_ref
+    rows_ref, own_ref, left_ref, right_ref, far_a_ref, far_b_ref, part_ref, grads_ref, hidden_ref
 ):
-    weight = jnp.concatenate([wg_ref[...], wu_ref[...], pg_ref[...], pu_ref[...]], axis=1)
-    down = jnp.concatenate([wd_ref[...], pd_ref[...]], axis=0)
-    pre = mm(wide(rows_ref, 0, HALF), weight)
-    hidden_grad = mm(wide(rows_ref, HALF, HALF), down, NT)
+    gates, downs = [], []
+    for ref in (own_ref, left_ref, right_ref):
+        gates += [ref[:2048, :], ref[2048:4096, :]]
+        downs.append([ref[4096 + k * 128 : 4224 + k * 128, :] for k in range(N_TP)])
+    gates += [far_a_ref[:2048, :], jnp.concatenate([far_a_ref[2048:, :], far_b_ref[:1024, :]], axis=0)]
+    downs.append([far_b_ref[1024 + k * 128 : 1152 + k * 128, :] for k in range(N_TP)])
+    weight = jnp.concatenate(gates, axis=1)
+    down = jnp.concatenate([jnp.concatenate(d, axis=1) for d in downs], axis=0)
+    pre = mm(wide(rows_ref, 0, PART), weight)
+    hidden_grad = mm(wide(rows_ref, PART, PART), down, NT)
     grads = []
-    for b in range(2):
+    for b in range(4):
         gate_pre, up_pre = pre[:, 256 * b : 256 * b + 128], pre[:, 256 * b + 128 : 256 * b + 256]
         upper = hidden_grad[:, 128 * b : 128 * b + 128]
         sigmoid = jax.nn.sigmoid(gate_pre)
@@ -220,39 +238,45 @@
         part_ref[k + 1] = part[:, 128:]
 
 
-def weight_grads_kernel(rows_ref, grads_ref, hidden_ref, own_ref, sent_ref):
+def weight_grads_kernel(rows_ref, grads_ref, hidden_ref, *out_refs):
     grads = grads_ref[...]
     hidden = hidden_ref[...]
     for k in range(0, N_TP, 2):
-        x = jnp.concatenate([rows_ref[k, :HALF, :], rows_ref[k + 1, :HALF, :]], axis=1)
-        g = jnp.concatenate([rows_ref[k, HALF:, :], rows_ref[k + 1, HALF:, :]], axis=1)
+        x = jnp.concatenate([rows_ref[k, :PART, :], rows_ref[k + 1, :PART, :]], axis=1)
+        g = jnp.concatenate([rows_ref[k, PART:, :], rows_ref[k + 1, PART:, :]], axis=1)
         both = mm(x, grads, TN)
         down = mm(hidden, g, TN)
-        here = slice(k * 128, (k + 2) * 128)
-        own_ref[0, here, :] = both[:, :128]
-        own_ref[1, here, :] = both[:, 128:256]
-        sent_ref[0, here, :] = both[:, 256:384].astype(BF)
-        sent_ref[1, here, :] = both[:, 384:].astype(BF)
-        for n in range(2):
-            block = slice((k + n) * 128, (k + n + 1) * 128)
-            own_ref[2, block, :] = down[:128, n * 128 : (n + 1) * 128]
-            sent_ref[2, block, :] = down[128:, n * 128 : (n + 1) * 128].astype(BF)
-
-
-def grad_sum_kernel(own_ref, recv_ref, gate_ref, up_ref, down_ref):
-    gate_ref[...] = (own_ref[0] + recv_ref[0].astype(F32)).astype(BF)
-    up_ref[...] = (own_ref[1] + recv_ref[1].astype(F32)).astype(BF)
+        at = k * 128
+        for b, ref in enumerate(out_refs):
+            kind = ref.dtype
+            ref[at : at + 256, :] = both[:, 256 * b : 256 * b + 128].astype(kind)
+            ref[2048 + at : 2304 + at, :] = both[:, 256 * b + 128 : 256 * b + 256].astype(kind)
+            for n in range(2):
+                block = 4096 + at + n * 128
+                ref[block : block + 128, :] = down[
+                    128 * b : 128 * b + 128, n * 128 : (n + 1) * 128
+                ].astype(kind)
+
+
+def grad_sum_kernel(own_ref, a_ref, b_ref, c_ref, gate_ref, up_ref, down_ref):
+    def total(at, size):
+        parts = [r[at : at + size, :].astype(F32) for r in (a_ref, b_ref, c_ref)]
+        return (own_ref[at : at + size, :] + parts[0] + parts[1] + parts[2]).astype(BF)
+
     for k in range(N_TP):
         here = slice(k * 128, (k + 1) * 128)
-        down_ref[:, here] = (own_ref[2, here, :] + recv_ref[2, here, :].astype(F32)).astype(BF)
-
-
-def row_sum_kernel(part_ref, states_ref, out_ref, total):
-    for p in range(2):
-        acc = part_ref[p].astype(F32)
-        for k in range(p + 2, N_TP, 2):
-            acc = acc + part_ref[k].astype(F32)
-        total[p * HALF : (p + 1) * HALF, :] = acc
+        gate_ref[here, :] = total(k * 128, 128)
+        up_ref[here, :] = total(2048 + k * 128, 128)
+        down_ref[:, here] = total(4096 + k * 128, 128)
+
+
+def row_sum_kernel(place_ref, part_ref, states_ref, out_ref, total):
+    for q in range(4):
+        acc = jnp.zeros((PART, 128), F32)
+        for j in range(4):
+            source = jnp.where(place_ref[1] == 0, 4 * j + q, 4 * q + j)
+            acc = acc + part_ref[source].astype(F32)
+        total[q * PART : (q + 1) * PART, :] = acc
     total[ROWS:, :] = jnp.zeros((8, 128), F32)
     row = iota((PAD, 128), 0)
     high, low = two_parts(states_ref[...])
@@ -413,7 +437,17 @@
     return lax.all_to_all(blocks, axis, split_axis=0, concat_axis=0, tiled=True)
 
 
-PARTNERS = [(k, k ^ 1) for k in range(N_TP)]
+def ring_step(step):
+    pairs = []
+    for t in range(N_TP):
+        y, x = t // 4, t % 4
+        pairs.append((t, 4 * y + (x + step) % 4))
+        pairs.append((N_TP + t, N_TP + 4 * ((y + step) % 4) + x))
+    return pairs
+
+
+def passed_on(array, step):
+    return lax.ppermute(array, ("sp_1", "tp"), ring_step(step))
 
 
 def body(
@@ -430,9 +464,6 @@
     value_rows,
     log_decay,
 ):
-    weights = (w_gate[0], w_up[0], w_down[0])
-    with jax.named_scope("partner_weights"):
-        partner_weights = tuple(lax.ppermute(w, "tp", PARTNERS) for w in weights)
     q_t, k_t, decay_t = queries.T, key_rows.T, log_decay.T
     place = jnp.stack(
         [lax.axis_index(SP), lax.axis_index("sp_1"), lax.axis_index("sp_0")]
@@ -448,30 +479,31 @@
         k_t,
         value_rows,
         decay_t,
-        name="dispatch",
     )
     recv = exchanged(sent, SP)
-    (turned,) = call(turned_kernel, [((TOK, SLOTS), BF)], pick, name="turned")
+    (packed,) = call(pack_kernel, [((WEIGHT_ROWS, 128), BF)], w_gate[0], w_up[0], w_down[0])
+    left = passed_on(packed, 1)
+    right = passed_on(packed, -1)
+    far_a = passed_on(left[: WEIGHT_ROWS // 2], 1)
+    far_b = passed_on(right[WEIGHT_ROWS // 2 :], -1)
+    weights = (packed, left, right, far_a, far_b)
+    (turned,) = call(turned_kernel, [((TOK, SLOTS), BF)], pick)
     copies, states, reach = call(
         copies_kernel,
-        [((N_TP, ROWS, 128), BF), ((N_SP, 128), F32), ((24, 128), F32)],
+        [((N_TP, 2 * PART, 128), BF), ((N_SP, 128), F32), ((24, 128), F32)],
         place,
         recv,
-        name="copies",
-        scratch=[pltpu.VMEM((2 * ROWS, 128), F32)],
+        scratch=[pltpu.VMEM((2 * ROWS, 128), F32), pltpu.VMEM((4, 2 * PART, 128), BF)],
         smem=(0,),
         near=(1,),
         near_out=(0,),
-        after=partner_weights,
     )
     rows = exchanged(copies, "tp")
     partial_rows, grads, hidden = call(
         partial_kernel,
-        [((N_TP, HALF, 128), BF), ((HALF, 512), BF), ((HALF, 256), BF)],
+        [((N_TP, PART, 128), BF), ((PART, 1024), BF), ((PART, 512), BF)],
         rows,
         *weights,
-        *partner_weights,
-        name="partial",
         near=(0,),
         near_out=(0,),
     )
@@ -479,24 +511,23 @@
     (returned,) = call(
         row_sum_kernel,
         [((N_SP, PAD, 128), BF)],
+        place,
         arrived,
         states,
-        name="row_sum",
-        near=(0,),
+        smem=(0,),
+        near=(1,),
         scratch=[pltpu.VMEM((ROWS + 8, 128), F32)],
     )
-    own_grads, sent_grads = call(
+    own_grads, grads_a, grads_b, grads_c = call(
         weight_grads_kernel,
-        [((3, 2048, 128), F32), ((3, 2048, 128), BF)],
+        [((WEIGHT_ROWS, 128), F32)] + 3 * [((WEIGHT_ROWS, 128), BF)],
         rows,
         grads,
         hidden,
-        name="weight_grads",
         near=(0,),
         after=(returned,),
     )
-    with jax.named_scope("partner_grads"):
-        partner_grads = lax.ppermute(sent_grads, "tp", PARTNERS)
+    other_grads = (passed_on(grads_a, -1), passed_on(grads_b, 1), passed_on(grads_c, 2))
     back = exchanged(returned, SP)
     (residual,) = call(
         residual_kernel,
@@ -504,7 +535,6 @@
         back,
         turned,
         out_grad,
-        name="residual",
         near=(0,),
         after=(own_grads,),
     )
@@ -517,7 +547,6 @@
         k_t,
         value_rows,
         decay_t,
-        name="forward",
         near=(0,),
         after=(residual,),
     )
@@ -530,13 +559,11 @@
         mixer_out,
         q_t,
         decay_t,
-        name="mixer_grad",
         smem=(0,),
         near=(1,),
         near_out=(2, 3),
     )
-    with jax.named_scope("cores"):
-        from_other = lax.ppermute(to_other, "sp_1", [(0, 1), (1, 0)])
+    from_other = lax.ppermute(to_other, "sp_1", [(0, 1), (1, 0)])
     chip_sent, other_grad = call(
         chip_kernel,
         [((16, 96, 128), BF), ((32, 128), F32)],
@@ -545,7 +572,6 @@
         kept,
         span_grad,
         reach,
-        name="chip",
         smem=(0,),
         near=(1, 2),
     )
@@ -563,7 +589,6 @@
         k_t,
         value_rows,
         decay_t,
-        name="backward",
         smem=(0,),
         near=(1,),
     )
@@ -571,8 +596,7 @@
         grad_sum_kernel,
         [((2048, 128), BF), ((2048, 128), BF), ((128, 2048), BF)],
         own_grads,
-        partner_grads,
-        name="grad_sum",
+        *other_grads,
     )
     return (gate_part[None], up_part[None], down_part[None], grad_proj, gq.T, gk.T, gv, gd.T)
 

time: 238 us -> 215 us (0.903)
  blocking collectives: 60.2 us -> 15.5 us
  starting transfers between devices: 54.1 us -> 63.7 us
  Pallas kernels: 35.5 us -> 42.2 us
  waiting for transfers between devices: 84.4 us -> 88.5 us
    all_to_all x2 -> x1, blocking collectives: 60.2 us -> 15.5 us  [exchanged(): return lax.all_to_all(blocks, axis, split_axis=0, concat_axis=0, tiled=True)]
    all_to_all x4 -> x5, waiting for transfers between devices: 24.4 us -> 42.2 us  [exchanged(): return lax.all_to_all(blocks, axis, split_axis=0, concat_axis=0, tiled=True)]
    ppermute x4 -> x7, waiting for transfers between devices: 60 us -> 46.3 us  [passed_on(): return lax.ppermute(array, ('sp_1', 'tp'), ring_step(step))]
    ppermute x4 -> x7, starting transfers between devices: 10.3 us -> 20.8 us  [passed_on(): return lax.ppermute(array, ('sp_1', 'tp'), ring_step(step))]
    pallas_call x12 -> x13, Pallas kernels: 35.5 us -> 42.2 us  [call(): pl.pallas_call(run, out_shape=tuple(((pltpu.VMEM if k in near_out else pl...]
    all_to_all x4 -> x5, starting transfers between devices: 38.9 us -> 38.1 us  [exchanged(): return lax.all_to_all(blocks, axis, split_axis=0, concat_axis=0, tiled=True)]
  transfers between devices with their start and end apart: 9 -> 13, of which waited for: 6 -> 6; matrix products, arithmetic and copies ran while one was open for 0% -> 1% of each run, Pallas kernels for 6% -> 10%
where the time goes in v3:
time: 215 us; the launch traced here: 214 us
  waiting for transfers between devices  88.5 us (41%)
  starting transfers between devices  63.7 us (30%)
  Pallas kernels  42.2 us (20%)
  blocking collectives  15.5 us (7%)
  local copies, waits for them, and re-layouts  3.35 us (2%)
    ppermute x7, waiting for transfers between devices, passed_on(): return lax.ppermute(array, ('sp_1', 'tp'), ring_step(step))  46.3 us
    all_to_all x5, waiting for transfers between devices, exchanged(): return lax.all_to_all(blocks, axis, split_axis=0, concat_axis=0, tiled=True)  42.2 us
    pallas_call x13, Pallas kernels, call(): pl.pallas_call(run, out_shape=tuple(((pltpu.VMEM if k in near_out else pl...  42.2 us
    all_to_all x5, starting transfers between devices, exchanged(): return lax.all_to_all(blocks, axis, split_axis=0, concat_axis=0, tiled=True)  38.1 us
    ppermute x7, starting transfers between devices, passed_on(): return lax.ppermute(array, ('sp_1', 'tp'), ring_step(step))  20.8 us
    all_to_all x1, blocking collectives, exchanged(): return lax.all_to_all(blocks, axis, split_axis=0, concat_axis=0, tiled=True)  15.5 us
    ppermute x1, starting transfers between devices, body(): from_other = lax.ppermute(to_other, 'sp_1', [(0, 1), (1, 0)])  4.82 us
  transfers between devices with their start and end apart: 13, of which 6 were waited for; matrix products, arithmetic and copies ran while one was open for 1% of the time, Pallas kernels for 10%

profile of v3, /device:TPU:1, one launch (start us, length us, event | category | flops | bytes accessed | tf_op | source)
XLA Modules:
  0.0 214.1 jit_solution(14270834848376056386)
XLA Ops:
  0.6 3.8 %shard_map.179 = (bf16[32,48,128]{2,1,0:T(8,128)(2,1)}, bf16[768,256]{1,0:T(8,128)(2,1)}) custom-call(s32[2,256]{1,0:T(2,128)} %bitcast.30, f32[2,256]{1,0:T(2,128)} %bitcast.31, bf16[256,128]{1,0:T(8,128)(2,1)} %refs_2_.3, bf16[256,128]{1,0:T(8,128)(2,1)} %refs_2_.4, bf16[64,256]{1,0:T(8,128)(2,1)} %bitcast.24, bf16[256,128]{1,0:T(8,128)(2,1)} %refs_8_.1, ...), custom_call_target="tpu_custom_call" | custom-call | tf_op jit(solution)/shard_map/pallas_call | solution.py:59
  4.4 16.7 %all-to-all-start = ((bf16[32,48,128]{2,1,0:T(8,128)(2,1)}), bf16[32,48,128]{2,1,0:T(8,128)(2,1)S(1)}, u32[]{:S(2)}, u32[]{:S(2)}) async-start(bf16[32,48,128]{2,1,0:T(8,128)(2,1)} %get-tuple-element.36), calls=%async_computation | async-start | bytes 786432 | tf_op jit(solution)/shard_map/all_to_all | solution.py:437
  21.2 2.7 %shard_map.181.refs_1_ = bf16[6144,128]{1,0:T(8,128)(2,1)} custom-call(bf16[2048,128]{1,0:T(8,128)(2,1)} %bitcast.21, bf16[2048,128]{1,0:T(8,128)(2,1)} %bitcast.22, bf16[128,2048]{1,0:T(8,128)(2,1)} %bitcast.23), custom_call_target="tpu_custom_call" | custom-call | tf_op jit(solution)/shard_map/pallas_call | solution.py:59
  23.9 3.2 %collective-permute-start = (bf16[6144,128]{1,0:T(8,128)(2,1)}, bf16[6144,128]{1,0:T(8,128)(2,1)S(1)}, u32[]{:S(2)}, u32[]{:S(2)}) collective-permute-start(bf16[6144,128]{1,0:T(8,128)(2,1)} %shard_map.181.refs_1_), channel_id=1, source_target_pairs={{0,1},{16,20},{1,2},{17,21},{2,3},{18,22},{3,0},{19,23},{4,5},{20,... | collective-permute-start | bytes 4718600 | tf_op jit(solution)/shard_map/ppermute | solution.py:450
  27.1 3.4 %collective-permute-start.1 = (bf16[6144,128]{1,0:T(8,128)(2,1)}, bf16[6144,128]{1,0:T(8,128)(2,1)}, u32[]{:S(2)}, u32[]{:S(2)}) collective-permute-start(bf16[6144,128]{1,0:T(8,128)(2,1)} %shard_map.181.refs_1_), channel_id=1, source_target_pairs={{0,3},{16,28},{1,0},{17,29},{2,1},{18,30},{3,2},{19,31},{4,7},{20,... | collective-permute-start | bytes 4718600 | tf_op jit(solution)/shard_map/ppermute | solution.py:450
  30.5 0.1 pad_add_fusion.refs_0_
  30.6 18.4 %all-to-all-done.refs_1_ = bf16[32,48,128]{2,1,0:T(8,128)(2,1)S(1)} async-done(((bf16[32,48,128]{2,1,0:T(8,128)(2,1)}), bf16[32,48,128]{2,1,0:T(8,128)(2,1)S(1)}, u32[]{:S(2)}, u32[]{:S(2)}) %all-to-all-start) | async-done | bytes 393248 | tf_op jit(solution)/shard_map/all_to_all | solution.py:437
  48.9 2.0 shard_map.180
  51.0 6.8 %all-to-all-start.1 = ((bf16[16,320,128]{2,1,0:T(8,128)(2,1)}), bf16[16,320,128]{2,1,0:T(8,128)(2,1)S(1)}, u32[]{:S(2)}, u32[]{:S(2)}) async-start(bf16[16,320,128]{2,1,0:T(8,128)(2,1)} %get-tuple-element.37), calls=%async_computation.1 | async-start | bytes 2621440 | tf_op jit(solution)/shard_map/all_to_all | solution.py:437
  57.7 0.0 collective-permute-done.refs_2_
  57.7 0.0 copy-start
  57.7 0.1 slice.8
  57.8 3.3 %collective-permute-start.2 = (bf16[3072,128]{1,0:T(8,128)(2,1)S(1)}, bf16[3072,128]{1,0:T(8,128)(2,1)S(1)}, u32[]{:S(2)}, u32[]{:S(2)}) collective-permute-start(bf16[3072,128]{1,0:T(8,128)(2,1)S(1)} %slice.8), channel_id=1, source_target_pairs={{0,1},{16,20},{1,2},{17,21},{2,3},{18,22},{3,0},{19,23},{4,5},{20,... | collective-permute-start | bytes 2359304 | tf_op jit(solution)/shard_map/ppermute | solution.py:450
  61.1 0.0 collective-permute-done.1.refs_3_
  61.1 1.2 slice.9
  62.3 0.0 copy-done
  62.3 3.2 %collective-permute-start.3 = (bf16[3072,128]{1,0:T(8,128)(2,1)S(1)}, bf16[3072,128]{1,0:T(8,128)(2,1)}, u32[]{:S(2)}, u32[]{:S(2)}) collective-permute-start(bf16[3072,128]{1,0:T(8,128)(2,1)S(1)} %slice.9), channel_id=1, source_target_pairs={{0,3},{16,28},{1,0},{17,29},{2,1},{18,30},{3,2},{19,31},{4,7},{20,... | collective-permute-start | bytes 2359304 | tf_op jit(solution)/shard_map/ppermute | solution.py:450
  65.5 18.7 %collective-permute-done.2.refs_4_ = bf16[3072,128]{1,0:T(8,128)(2,1)S(1)} collective-permute-done((bf16[3072,128]{1,0:T(8,128)(2,1)S(1)}, bf16[3072,128]{1,0:T(8,128)(2,1)S(1)}, u32[]{:S(2)}, u32[]{:S(2)}) %collective-permute-start.2) | collective-permute-done | bytes 786464 | tf_op jit(solution)/shard_map/ppermute | solution.py:450
  84.2 0.9 copy-done.3
  85.1 0.0 collective-permute-done.3.refs_5_
  85.1 0.0 all-to-all-done.1.refs_0_
  85.1 5.8 %shard_map.182 = (bf16[16,160,128]{2,1,0:T(8,128)(2,1)S(1)}, bf16[160,1024]{1,0:T(8,128)(2,1)}, bf16[160,512]{1,0:T(8,128)(2,1)}) custom-call(bf16[16,320,128]{2,1,0:T(8,128)(2,1)S(1)} %all-to-all-done.1.refs_0_, bf16[6144,128]{1,0:T(8,128)(2,1)} %shard_map.181.refs_1_, bf16[6144,128]{1,0:T(8,128)(2,1)} %copy-done, ...), custom_call_target="tpu_custom_call" | custom-call | tf_op jit(solution)/shard_map/pallas_call | solution.py:59
  90.9 15.5 %all_to_all.30.refs_1_ = bf16[16,160,128]{2,1,0:T(8,128)(2,1)S(1)} all-to-all(bf16[16,160,128]{2,1,0:T(8,128)(2,1)S(1)} %get-tuple-element.40), channel_id=1, replica_groups=mesh['sp_0'=16,'sp_1'=2,'tp'=16] {'tp'}, dimensions={0} | all-to-all | bytes 1310720 | tf_op jit(solution)/shard_map/all_to_all | solution.py:437
  106.4 1.6 shard_map.183.refs_3_
  108.0 6.2 %all-to-all-start.3 = ((bf16[32,24,128]{2,1,0:T(8,128)(2,1)}), bf16[32,24,128]{2,1,0:T(8,128)(2,1)S(1)}, u32[]{:S(2)}, u32[]{:S(2)}) async-start(bf16[32,24,128]{2,1,0:T(8,128)(2,1)} %shard_map.183.refs_3_), calls=%async_computation.3 | async-start | bytes 393216 | tf_op jit(solution)/shard_map/all_to_all | solution.py:437
  114.2 1.9 shard_map.186.refs_1_
  116.1 5.8 %shard_map.184 = (f32[6144,128]{1,0:T(8,128)}, bf16[6144,128]{1,0:T(8,128)(2,1)}, bf16[6144,128]{1,0:T(8,128)(2,1)}, bf16[6144,128]{1,0:T(8,128)(2,1)}) custom-call(bf16[16,320,128]{2,1,0:T(8,128)(2,1)S(1)} %all-to-all-done.1.refs_0_, bf16[160,1024]{1,0:T(8,128)(2,1)} %get-tuple-element.38.refs_1_, bf16[160,512]{1,0:T(8,128)(2,1)} %get-tuple-element.39.refs_2_, ...), custom_call_target="tpu_custom_call" | custom-call | tf_op jit(solution)/shard_map/pallas_call | solution.py:59
  121.9 11.2 %all-to-all-done.3.refs_0_ = bf16[32,24,128]{2,1,0:T(8,128)(2,1)S(1)} async-done(((bf16[32,24,128]{2,1,0:T(8,128)(2,1)}), bf16[32,24,128]{2,1,0:T(8,128)(2,1)S(1)}, u32[]{:S(2)}, u32[]{:S(2)}) %all-to-all-start.3) | async-done | bytes 196640 | tf_op jit(solution)/shard_map/all_to_all | solution.py:437
  133.1 2.4 %shard_map.187.refs_5_ = bf16[16,256,128]{2,1,0:T(8,128)(2,1)} custom-call(bf16[32,24,128]{2,1,0:T(8,128)(2,1)S(1)} %all-to-all-done.3.refs_0_, bf16[256,768]{1,0:T(8,128)(2,1)} %shard_map.186.refs_1_, bf16[256,128]{1,0:T(8,128)(2,1)} %refs_2_.4, f32[6144,128]{1,0:T(8,128)} %get-tuple-element.42.refs_0_.refs_3_), custom_call_target="tpu_custom_call" | custom-call | tf_op jit(solution)/shard_map/pallas_call | solution.py:59
  135.5 3.7 %all-to-all-start.4 = ((bf16[16,256,128]{2,1,0:T(8,128)(2,1)}), bf16[16,256,128]{2,1,0:T(8,128)(2,1)S(1)}, u32[]{:S(2)}, u32[]{:S(2)}) async-start(bf16[16,256,128]{2,1,0:T(8,128)(2,1)} %shard_map.187.refs_5_), calls=%async_computation.4 | async-start | bytes 2097152 | tf_op jit(solution)/shard_map/all_to_all | solution.py:437
  139.2 3.0 %shard_map.188 = (bf16[256,128]{1,0:T(8,128)(2,1)}, f32[4,128,64]{2,1,0:T(8,128)}) custom-call(bf16[32,24,128]{2,1,0:T(8,128)(2,1)S(1)} %all-to-all-done.3.refs_0_, bf16[64,256]{1,0:T(8,128)(2,1)} %bitcast.27, bf16[64,256]{1,0:T(8,128)(2,1)} %bitcast.25, bf16[256,128]{1,0:T(8,128)(2,1)} %refs_8_.1, f32[64,256]{1,0:T(8,128)} %bitcast.18, ...), custom_call_target="tpu_custom_call" | custom-call | tf_op jit(solution)/shard_map/pallas_call | solution.py:59
  142.2 12.6 %all-to-all-done.4.refs_1_ = bf16[16,256,128]{2,1,0:T(8,128)(2,1)S(1)} async-done(((bf16[16,256,128]{2,1,0:T(8,128)(2,1)}), bf16[16,256,128]{2,1,0:T(8,128)(2,1)S(1)}, u32[]{:S(2)}, u32[]{:S(2)}) %all-to-all-start.4) | async-done | bytes 1048608 | tf_op jit(solution)/shard_map/all_to_all | solution.py:437
  154.8 2.8 %shard_map.189 = (f32[256,128]{1,0:T(8,128)}, f32[32,128]{1,0:T(8,128)}, bf16[1088,128]{1,0:T(8,128)(2,1)S(1)}, f32[1024,128]{1,0:T(8,128)S(1)}) custom-call(s32[3]{0:T(128)S(1)} %pad_add_fusion.refs_0_, bf16[16,256,128]{2,1,0:T(8,128)(2,1)S(1)} %all-to-all-done.4.refs_1_, bf16[2048,128]{1,0:T(8,128)(2,1)} %refs_2_.5, ...), custom_call_target="tpu_custom_call" | custom-call | tf_op jit(solution)/shard_map/pallas_call | solution.py:59
  157.6 4.8 %collective-permute-start.7 = (bf16[1088,128]{1,0:T(8,128)(2,1)S(1)}, bf16[1088,128]{1,0:T(8,128)(2,1)S(1)}, u32[]{:S(2)}, u32[]{:S(2)}) collective-permute-start(bf16[1088,128]{1,0:T(8,128)(2,1)S(1)} %get-tuple-element.51), channel_id=1, source_target_pairs={{0,16},{16,0},{1,17},{17,1},{2,18},{18,2},{3,19},{19,3},{4,20},{20... | collective-permute-start | bytes 835592 | tf_op jit(solution)/shard_map/ppermute | solution.py:566
  162.4 2.0 collective-permute-start.4
  164.4 3.3 %collective-permute-start.5 = (bf16[6144,128]{1,0:T(8,128)(2,1)}, bf16[6144,128]{1,0:T(8,128)(2,1)S(1)}, u32[]{:S(2)}, u32[]{:S(2)}) collective-permute-start(bf16[6144,128]{1,0:T(8,128)(2,1)} %get-tuple-element.44), channel_id=1, source_target_pairs={{0,1},{16,20},{1,2},{17,21},{2,3},{18,22},{3,0},{19,23},{4,5},{20,... | collective-permute-start | bytes 4718600 | tf_op jit(solution)/shard_map/ppermute | solution.py:450
  167.7 2.4 %collective-permute-start.6 = (bf16[6144,128]{1,0:T(8,128)(2,1)}, bf16[6144,128]{1,0:T(8,128)(2,1)}, u32[]{:S(2)}, u32[]{:S(2)}) collective-permute-start(bf16[6144,128]{1,0:T(8,128)(2,1)} %get-tuple-element.45), channel_id=1, source_target_pairs={{0,2},{16,24},{1,3},{17,25},{2,0},{18,26},{3,1},{19,27},{4,6},{20,... | collective-permute-start | bytes 4718600 | tf_op jit(solution)/shard_map/ppermute | solution.py:450
  170.1 0.0 collective-permute-done.7.refs_1_
  170.1 1.6 shard_map.190
  171.7 4.8 %all-to-all-start.5 = ((bf16[16,96,128]{2,1,0:T(8,128)(2,1)}), bf16[16,96,128]{2,1,0:T(8,128)(2,1)S(1)}, u32[]{:S(2)}, u32[]{:S(2)}) async-start(bf16[16,96,128]{2,1,0:T(8,128)(2,1)} %get-tuple-element.55), calls=%async_computation.5 | async-start | bytes 786432 | tf_op jit(solution)/shard_map/all_to_all | solution.py:437
  176.5 7.5 %collective-permute-done.4.refs_1_ = bf16[6144,128]{1,0:T(8,128)(2,1)S(1)} collective-permute-done((bf16[6144,128]{1,0:T(8,128)(2,1)}, bf16[6144,128]{1,0:T(8,128)(2,1)S(1)}, u32[]{:S(2)}, u32[]{:S(2)}) %collective-permute-start.4) | collective-permute-done | bytes 1572896 | tf_op jit(solution)/shard_map/ppermute | solution.py:450
  184.1 20.1 %collective-permute-done.5.refs_2_ = bf16[6144,128]{1,0:T(8,128)(2,1)S(1)} collective-permute-done((bf16[6144,128]{1,0:T(8,128)(2,1)}, bf16[6144,128]{1,0:T(8,128)(2,1)S(1)}, u32[]{:S(2)}, u32[]{:S(2)}) %collective-permute-start.5) | collective-permute-done | bytes 1572896 | tf_op jit(solution)/shard_map/ppermute | solution.py:450
  204.1 0.0 collective-permute-done.6.refs_3_
  204.1 0.0 copy-done.1
  204.1 1.2 copy-done.2
  205.3 4.9 %shard_map.185 = (bf16[2048,128]{1,0:T(8,128)(2,1)}, bf16[2048,128]{1,0:T(8,128)(2,1)}, bf16[128,2048]{1,0:T(8,128)(2,1)}) custom-call(f32[6144,128]{1,0:T(8,128)} %get-tuple-element.42.refs_0_.refs_3_, bf16[6144,128]{1,0:T(8,128)(2,1)} %copy-done.1, bf16[6144,128]{1,0:T(8,128)(2,1)} %copy-done.2, bf16[6144,128]{1,0:T(8,128)(2,1)} %collective-permute-done.6.refs_3_), custom_call_target="tpu_custom_call" | custom-call | tf_op jit(solution)/shard_map/pallas_call | solution.py:59
  210.3 0.0 all-to-all-done.5.refs_1_
  210.3 3.9 %shard_map.191 = (f32[64,128]{1,0:T(8,128)}, bf16[64,256]{1,0:T(8,128)(2,1)}, bf16[64,256]{1,0:T(8,128)(2,1)}, bf16[256,128]{1,0:T(8,128)(2,1)}, f32[64,256]{1,0:T(8,128)}) custom-call(s32[3]{0:T(128)S(1)} %pad_add_fusion.refs_0_, bf16[16,96,128]{2,1,0:T(8,128)(2,1)S(1)} %all-to-all-done.5.refs_1_, f32[32,128]{1,0:T(8,128)} %get-tuple-element.56.refs_2_, ...), custom_call_target="tpu_custom_call" | custom-call | tf_op jit(solution)/shard_map/pallas_call | solution.py:59
  (3 shorter events, 0.0 us)
Async XLA Ops:
  4.4 44.5 %all-to-all-start = ((bf16[32,48,128]{2,1,0:T(8,128)(2,1)}), bf16[32,48,128]{2,1,0:T(8,128)(2,1)S(1)}, u32[]{:S(2)}, u32[]{:S(2)}) async-start(bf16[32,48,128]{2,1,0:T(8,128)(2,1)} %get-tuple-element.36), calls=%async_computation | async-start | bytes 786432 | tf_op jit(solution)/shard_map/all_to_all | solution.py:437
  23.9 33.8 %collective-permute-start = (bf16[6144,128]{1,0:T(8,128)(2,1)}, bf16[6144,128]{1,0:T(8,128)(2,1)S(1)}, u32[]{:S(2)}, u32[]{:S(2)}) collective-permute-start(bf16[6144,128]{1,0:T(8,128)(2,1)} %shard_map.181.refs_1_), channel_id=1, source_target_pairs={{0,1},{16,20},{1,2},{17,21},{2,3},{18,22},{3,0},{19,23},{4,5},{20,... | collective-permute-start | bytes 4718600 | tf_op jit(solution)/shard_map/ppermute | solution.py:450
  27.1 34.0 %collective-permute-start.1 = (bf16[6144,128]{1,0:T(8,128)(2,1)}, bf16[6144,128]{1,0:T(8,128)(2,1)}, u32[]{:S(2)}, u32[]{:S(2)}) collective-permute-start(bf16[6144,128]{1,0:T(8,128)(2,1)} %shard_map.181.refs_1_), channel_id=1, source_target_pairs={{0,3},{16,28},{1,0},{17,29},{2,1},{18,30},{3,2},{19,31},{4,7},{20,... | collective-permute-start | bytes 4718600 | tf_op jit(solution)/shard_map/ppermute | solution.py:450
  51.0 34.2 %all-to-all-start.1 = ((bf16[16,320,128]{2,1,0:T(8,128)(2,1)}), bf16[16,320,128]{2,1,0:T(8,128)(2,1)S(1)}, u32[]{:S(2)}, u32[]{:S(2)}) async-start(bf16[16,320,128]{2,1,0:T(8,128)(2,1)} %get-tuple-element.37), calls=%async_computation.1 | async-start | bytes 2621440 | tf_op jit(solution)/shard_map/all_to_all | solution.py:437
  57.7 4.6 %copy-start = (bf16[6144,128]{1,0:T(8,128)(2,1)}, bf16[6144,128]{1,0:T(8,128)(2,1)S(1)}, u32[]{:S(2)}) copy-start(bf16[6144,128]{1,0:T(8,128)(2,1)S(1)} %collective-permute-done.refs_2_) | copy-start | bytes 4718596
  57.8 26.4 %collective-permute-start.2 = (bf16[3072,128]{1,0:T(8,128)(2,1)S(1)}, bf16[3072,128]{1,0:T(8,128)(2,1)S(1)}, u32[]{:S(2)}, u32[]{:S(2)}) collective-permute-start(bf16[3072,128]{1,0:T(8,128)(2,1)S(1)} %slice.8), channel_id=1, source_target_pairs={{0,1},{16,20},{1,2},{17,21},{2,3},{18,22},{3,0},{19,23},{4,5},{20,... | collective-permute-start | bytes 2359304 | tf_op jit(solution)/shard_map/ppermute | solution.py:450
  62.3 22.8 %collective-permute-start.3 = (bf16[3072,128]{1,0:T(8,128)(2,1)S(1)}, bf16[3072,128]{1,0:T(8,128)(2,1)}, u32[]{:S(2)}, u32[]{:S(2)}) collective-permute-start(bf16[3072,128]{1,0:T(8,128)(2,1)S(1)} %slice.9), channel_id=1, source_target_pairs={{0,3},{16,28},{1,0},{17,29},{2,1},{18,30},{3,2},{19,31},{4,7},{20,... | collective-permute-start | bytes 2359304 | tf_op jit(solution)/shard_map/ppermute | solution.py:450
  84.2 0.9 copy-start.3
  108.0 25.2 %all-to-all-start.3 = ((bf16[32,24,128]{2,1,0:T(8,128)(2,1)}), bf16[32,24,128]{2,1,0:T(8,128)(2,1)S(1)}, u32[]{:S(2)}, u32[]{:S(2)}) async-start(bf16[32,24,128]{2,1,0:T(8,128)(2,1)} %shard_map.183.refs_3_), calls=%async_computation.3 | async-start | bytes 393216 | tf_op jit(solution)/shard_map/all_to_all | solution.py:437
  135.5 19.3 %all-to-all-start.4 = ((bf16[16,256,128]{2,1,0:T(8,128)(2,1)}), bf16[16,256,128]{2,1,0:T(8,128)(2,1)S(1)}, u32[]{:S(2)}, u32[]{:S(2)}) async-start(bf16[16,256,128]{2,1,0:T(8,128)(2,1)} %shard_map.187.refs_5_), calls=%async_computation.4 | async-start | bytes 2097152 | tf_op jit(solution)/shard_map/all_to_all | solution.py:437
  157.6 12.6 %collective-permute-start.7 = (bf16[1088,128]{1,0:T(8,128)(2,1)S(1)}, bf16[1088,128]{1,0:T(8,128)(2,1)S(1)}, u32[]{:S(2)}, u32[]{:S(2)}) collective-permute-start(bf16[1088,128]{1,0:T(8,128)(2,1)S(1)} %get-tuple-element.51), channel_id=1, source_target_pairs={{0,16},{16,0},{1,17},{17,1},{2,18},{18,2},{3,19},{19,3},{4,20},{20... | collective-permute-start | bytes 835592 | tf_op jit(solution)/shard_map/ppermute | solution.py:566
  162.4 21.7 %collective-permute-start.4 = (bf16[6144,128]{1,0:T(8,128)(2,1)}, bf16[6144,128]{1,0:T(8,128)(2,1)S(1)}, u32[]{:S(2)}, u32[]{:S(2)}) collective-permute-start(bf16[6144,128]{1,0:T(8,128)(2,1)} %get-tuple-element.43), channel_id=1, source_target_pairs={{0,3},{16,28},{1,0},{17,29},{2,1},{18,30},{3,2},{19,31},{4,7},{20,... | collective-permute-start | bytes 4718600 | tf_op jit(solution)/shard_map/ppermute | solution.py:450
  164.4 39.7 %collective-permute-start.5 = (bf16[6144,128]{1,0:T(8,128)(2,1)}, bf16[6144,128]{1,0:T(8,128)(2,1)S(1)}, u32[]{:S(2)}, u32[]{:S(2)}) collective-permute-start(bf16[6144,128]{1,0:T(8,128)(2,1)} %get-tuple-element.44), channel_id=1, source_target_pairs={{0,1},{16,20},{1,2},{17,21},{2,3},{18,22},{3,0},{19,23},{4,5},{20,... | collective-permute-start | bytes 4718600 | tf_op jit(solution)/shard_map/ppermute | solution.py:450
  167.7 36.4 %collective-permute-start.6 = (bf16[6144,128]{1,0:T(8,128)(2,1)}, bf16[6144,128]{1,0:T(8,128)(2,1)}, u32[]{:S(2)}, u32[]{:S(2)}) collective-permute-start(bf16[6144,128]{1,0:T(8,128)(2,1)} %get-tuple-element.45), channel_id=1, source_target_pairs={{0,2},{16,24},{1,3},{17,25},{2,0},{18,26},{3,1},{19,27},{4,6},{20,... | collective-permute-start | bytes 4718600 | tf_op jit(solution)/shard_map/ppermute | solution.py:450
  171.7 38.5 %all-to-all-start.5 = ((bf16[16,96,128]{2,1,0:T(8,128)(2,1)}), bf16[16,96,128]{2,1,0:T(8,128)(2,1)S(1)}, u32[]{:S(2)}, u32[]{:S(2)}) async-start(bf16[16,96,128]{2,1,0:T(8,128)(2,1)} %get-tuple-element.55), calls=%async_computation.5 | async-start | bytes 786432 | tf_op jit(solution)/shard_map/all_to_all | solution.py:437
  184.1 20.1 %copy-start.1 = (bf16[6144,128]{1,0:T(8,128)(2,1)}, bf16[6144,128]{1,0:T(8,128)(2,1)S(1)}, u32[]{:S(2)}) copy-start(bf16[6144,128]{1,0:T(8,128)(2,1)S(1)} %collective-permute-done.4.refs_1_) | copy-start | bytes 4718596
  204.1 1.2 copy-start.2

commit v4 on v3

--- a/solution.py
+++ b/solution.py
@@ -20,7 +20,7 @@
 ROWS = N_SP * CAP
 SLOTS = N_SP * PAD
 PART = ROWS // 4
-WEIGHT_ROWS = 3 * 2048
+LOT = 3 * 1024
 NBLK = TOK // BLOCK
 BF = jnp.bfloat16
 F32 = jnp.float32
@@ -196,27 +196,24 @@
     reach_ref[16:, :] = jnp.concatenate([even, odd, jnp.zeros((6, 128), F32)], axis=0)
 
 
-def pack_kernel(wg_ref, wu_ref, wd_ref, out_ref):
-    out_ref[:2048, :] = wg_ref[...]
-    out_ref[2048:4096, :] = wu_ref[...]
+def pack_kernel(wg_ref, wu_ref, wd_ref, a_ref, b_ref):
+    a_ref[:2048, :] = wg_ref[...]
+    a_ref[2048:, :] = wu_ref[:1024, :]
+    b_ref[:1024, :] = wu_ref[1024:, :]
     for k in range(N_TP):
-        at = 4096 + k * 128
-        out_ref[at : at + 128, :] = wd_ref[:, k * 128 : (k + 1) * 128]
+        b_ref[1024 + k * 128 : 1152 + k * 128, :] = wd_ref[:, k * 128 : (k + 1) * 128]
 
 
 def wide(ref, at, size):
     return jnp.concatenate([ref[k, at : at + size, :] for k in range(N_TP)], axis=1)
 
 
-def partial_kernel(
-    rows_ref, own_ref, left_ref, right_ref, far_a_ref, far_b_ref, part_ref, grads_ref, hidden_ref
-):
+def partial_kernel(rows_ref, *refs):
+    lots, (part_ref, grads_ref, hidden_ref) = refs[:8], refs[8:]
     gates, downs = [], []
-    for ref in (own_ref, left_ref, right_ref):
-        gates += [ref[:2048, :], ref[2048:4096, :]]
-        downs.append([ref[4096 + k * 128 : 4224 + k * 128, :] for k in range(N_TP)])
-    gates += [far_a_ref[:2048, :], jnp.concatenate([far_a_ref[2048:, :], far_b_ref[:1024, :]], axis=0)]
-    downs.append([far_b_ref[1024 + k * 128 : 1152 + k * 128, :] for k in range(N_TP)])
+    for a_ref, b_ref in zip(lots[::2], lots[1::2]):
+        gates += [a_ref[:2048, :], jnp.concatenate([a_ref[2048:, :], b_ref[:1024, :]], axis=0)]
+        downs.append([b_ref[1024 + k * 128 : 1152 + k * 128, :] for k in range(N_TP)])
     weight = jnp.concatenate(gates, axis=1)
     down = jnp.concatenate([jnp.concatenate(d, axis=1) for d in downs], axis=0)
     pre = mm(wide(rows_ref, 0, PART), weight)
@@ -247,21 +244,36 @@
         both = mm(x, grads, TN)
         down = mm(hidden, g, TN)
         at = k * 128
-        for b, ref in enumerate(out_refs):
-            kind = ref.dtype
-            ref[at : at + 256, :] = both[:, 256 * b : 256 * b + 128].astype(kind)
-            ref[2048 + at : 2304 + at, :] = both[:, 256 * b + 128 : 256 * b + 256].astype(kind)
+        for b in range(4):
+            a_ref, b_ref = out_refs[2 * b : 2 * b + 2]
+            kind = a_ref.dtype
+            up = both[:, 256 * b + 128 : 256 * b + 256].astype(kind)
+            a_ref[at : at + 256, :] = both[:, 256 * b : 256 * b + 128].astype(kind)
+            if k < N_TP // 2:
+                a_ref[2048 + at : 2304 + at, :] = up
+            else:
+                b_ref[at - 1024 : at - 768, :] = up
             for n in range(2):
-                block = 4096 + at + n * 128
-                ref[block : block + 128, :] = down[
+                block = 1024 + at + n * 128
+                b_ref[block : block + 128, :] = down[
                     128 * b : 128 * b + 128, n * 128 : (n + 1) * 128
                 ].astype(kind)
 
 
-def grad_sum_kernel(own_ref, a_ref, b_ref, c_ref, gate_ref, up_ref, down_ref):
+def relay_kernel(
+    left_a_ref, left_b_ref, right_a_ref, right_b_ref, far_a_ref, far_b_ref, left_ref, right_ref
+):
+    right_ref[:LOT, :] = (right_a_ref[...].astype(F32) + far_a_ref[...].astype(F32)).astype(BF)
+    right_ref[LOT:, :] = right_b_ref[...]
+    left_ref[:LOT, :] = left_a_ref[...]
+    left_ref[LOT:, :] = (left_b_ref[...].astype(F32) + far_b_ref[...].astype(F32)).astype(BF)
+
+
+def grad_sum_kernel(own_a_ref, own_b_ref, x_ref, y_ref, gate_ref, up_ref, down_ref):
     def total(at, size):
-        parts = [r[at : at + size, :].astype(F32) for r in (a_ref, b_ref, c_ref)]
-        return (own_ref[at : at + size, :] + parts[0] + parts[1] + parts[2]).astype(BF)
+        ref, start = (own_a_ref, at) if at < LOT else (own_b_ref, at - LOT)
+        other = x_ref[at : at + size, :].astype(F32) + y_ref[at : at + size, :].astype(F32)
+        return (ref[start : start + size, :] + other).astype(BF)
 
     for k in range(N_TP):
         here = slice(k * 128, (k + 1) * 128)
@@ -481,12 +493,16 @@
         decay_t,
     )
     recv = exchanged(sent, SP)
-    (packed,) = call(pack_kernel, [((WEIGHT_ROWS, 128), BF)], w_gate[0], w_up[0], w_down[0])
-    left = passed_on(packed, 1)
-    right = passed_on(packed, -1)
-    far_a = passed_on(left[: WEIGHT_ROWS // 2], 1)
-    far_b = passed_on(right[WEIGHT_ROWS // 2 :], -1)
-    weights = (packed, left, right, far_a, far_b)
+    own_a, own_b = call(
+        pack_kernel, [((LOT, 128), BF), ((LOT, 128), BF)], w_gate[0], w_up[0], w_down[0]
+    )
+    left_a = passed_on(own_a, 1)
+    right_b = passed_on(own_b, -1)
+    left_b = passed_on(own_b, 1)
+    right_a = passed_on(own_a, -1)
+    far_a = passed_on(left_a, 1)
+    far_b = passed_on(right_b, -1)
+    weights = (own_a, own_b, left_a, left_b, right_a, right_b, far_a, far_b)
     (turned,) = call(turned_kernel, [((TOK, SLOTS), BF)], pick)
     copies, states, reach = call(
         copies_kernel,
@@ -518,16 +534,17 @@
         near=(1,),
         scratch=[pltpu.VMEM((ROWS + 8, 128), F32)],
     )
-    own_grads, grads_a, grads_b, grads_c = call(
+    own_grad_a, own_grad_b, *lots = call(
         weight_grads_kernel,
-        [((WEIGHT_ROWS, 128), F32)] + 3 * [((WEIGHT_ROWS, 128), BF)],
+        2 * [((LOT, 128), F32)] + 6 * [((LOT, 128), BF)],
         rows,
         grads,
         hidden,
         near=(0,),
         after=(returned,),
     )
-    other_grads = (passed_on(grads_a, -1), passed_on(grads_b, 1), passed_on(grads_c, 2))
+    via_right = passed_on(lots[4], 1)
+    via_left = passed_on(lots[5], -1)
     back = exchanged(returned, SP)
     (residual,) = call(
         residual_kernel,
@@ -536,7 +553,7 @@
         turned,
         out_grad,
         near=(0,),
-        after=(own_grads,),
+        after=(own_grad_a,),
     )
     full_grad = exchanged(residual, "tp")
     mixer_out, entering = call(
@@ -550,6 +567,9 @@
         near=(0,),
         after=(residual,),
     )
+    to_left, to_right = call(
+        relay_kernel, 2 * [((2 * LOT, 128), BF)], *lots[:4], via_right, via_left, after=(residual,)
+    )
     mixer_grad, span_grad, to_other, kept = call(
         mixer_grad_kernel,
         [((TOK, 128), F32), ((32, 128), F32), ((1088, 128), BF), ((1024, 128), F32)],
@@ -560,6 +580,7 @@
         q_t,
         decay_t,
         smem=(0,),
+        after=(to_left,),
         near=(1,),
         near_out=(2, 3),
     )
@@ -592,11 +613,15 @@
         smem=(0,),
         near=(1,),
     )
+    from_right = passed_on(to_left, -1)
+    from_left = passed_on(to_right, 1)
     gate_part, up_part, down_part = call(
         grad_sum_kernel,
         [((2048, 128), BF), ((2048, 128), BF), ((128, 2048), BF)],
-        own_grads,
-        *other_grads,
+        own_grad_a,
+        own_grad_b,
+        from_left,
+        from_right,
     )
     return (gate_part[None], up_part[None], down_part[None], grad_proj, gq.T, gk.T, gv, gd.T)
 

time: 215 us -> 223 us (1.037)
  the two profiles are of different devices: /device:TPU:1 before, /device:TPU:4 now
where the time goes in v4:
time: 223 us; the launch traced here: 222 us
  waiting for transfers between devices  87 us (39%)
  starting transfers between devices  69.7 us (31%)
  Pallas kernels  45.7 us (20%)
  blocking collectives  16.8 us (8%)
    ppermute x10, waiting for transfers between devices, passed_on(): return lax.ppermute(array, ('sp_1', 'tp'), ring_step(step))  47.2 us
    pallas_call x14, Pallas kernels, call(): pl.pallas_call(run, out_shape=tuple(((pltpu.VMEM if k in near_out else pl...  45.7 us
    all_to_all x5, waiting for transfers between devices, exchanged(): return lax.all_to_all(blocks, axis, split_axis=0, concat_axis=0, tiled=True)  39.8 us
    all_to_all x5, starting transfers between devices, exchanged(): return lax.all_to_all(blocks, axis, split_axis=0, concat_axis=0, tiled=True)  36.7 us
    ppermute x10, starting transfers between devices, passed_on(): return lax.ppermute(array, ('sp_1', 'tp'), ring_step(step))  29.5 us
    all_to_all x1, blocking collectives, exchanged(): return lax.all_to_all(blocks, axis, split_axis=0, concat_axis=0, tiled=True)  16.8 us
  transfers between devices with their start and end apart: 16, of which 9 were waited for; matrix products, arithmetic and copies ran while one was open for 0% of the time, Pallas kernels for 12%

profile of v4, /device:TPU:4, one launch (start us, length us, event | category | flops | bytes accessed | tf_op | source)
XLA Modules:
  0.0 222.0 jit_solution(10283851461887531851)
XLA Ops:
  0.6 3.8 %shard_map.179 = (bf16[32,48,128]{2,1,0:T(8,128)(2,1)}, bf16[768,256]{1,0:T(8,128)(2,1)}) custom-call(s32[2,256]{1,0:T(2,128)} %bitcast.30, f32[2,256]{1,0:T(2,128)} %bitcast.31, bf16[256,128]{1,0:T(8,128)(2,1)} %refs_2_.3, bf16[256,128]{1,0:T(8,128)(2,1)} %refs_2_.4, bf16[64,256]{1,0:T(8,128)(2,1)} %bitcast.27, bf16[256,128]{1,0:T(8,128)(2,1)} %refs_8_.1, ...), custom_call_target="tpu_custom_call" | custom-call | tf_op jit(solution)/shard_map/pallas_call | solution.py:59
  4.4 15.5 %all-to-all-start = ((bf16[32,48,128]{2,1,0:T(8,128)(2,1)}), bf16[32,48,128]{2,1,0:T(8,128)(2,1)S(1)}, u32[]{:S(2)}, u32[]{:S(2)}) async-start(bf16[32,48,128]{2,1,0:T(8,128)(2,1)} %get-tuple-element.44), calls=%async_computation | async-start | bytes 786432 | tf_op jit(solution)/shard_map/all_to_all | solution.py:449
  19.9 2.6 %shard_map.181 = (bf16[3072,128]{1,0:T(8,128)(2,1)}, bf16[3072,128]{1,0:T(8,128)(2,1)}) custom-call(bf16[2048,128]{1,0:T(8,128)(2,1)} %bitcast.21, bf16[2048,128]{1,0:T(8,128)(2,1)} %bitcast.22, bf16[128,2048]{1,0:T(8,128)(2,1)} %bitcast.23), custom_call_target="tpu_custom_call" | custom-call | tf_op jit(solution)/shard_map/pallas_call | solution.py:59
  22.5 3.2 %collective-permute-start = (bf16[3072,128]{1,0:T(8,128)(2,1)}, bf16[3072,128]{1,0:T(8,128)(2,1)}, u32[]{:S(2)}, u32[]{:S(2)}) collective-permute-start(bf16[3072,128]{1,0:T(8,128)(2,1)} %get-tuple-element.46.refs_1_), channel_id=1, source_target_pairs={{0,1},{16,20},{1,2},{17,21},{2,3},{18,22},{3,0},{19,23},{4,5},{20,... | collective-permute-start | bytes 2359304 | tf_op jit(solution)/shard_map/ppermute | solution.py:462
  25.7 2.7 %collective-permute-start.3 = (bf16[3072,128]{1,0:T(8,128)(2,1)}, bf16[3072,128]{1,0:T(8,128)(2,1)}, u32[]{:S(2)}, u32[]{:S(2)}) collective-permute-start(bf16[3072,128]{1,0:T(8,128)(2,1)} %get-tuple-element.47.refs_2_), channel_id=1, source_target_pairs={{0,3},{16,28},{1,0},{17,29},{2,1},{18,30},{3,2},{19,31},{4,7},{20,... | collective-permute-start | bytes 2359304 | tf_op jit(solution)/shard_map/ppermute | solution.py:462
  28.5 0.1 pad_add_fusion.refs_0_
  28.6 19.6 %all-to-all-done.refs_1_ = bf16[32,48,128]{2,1,0:T(8,128)(2,1)S(1)} async-done(((bf16[32,48,128]{2,1,0:T(8,128)(2,1)}), bf16[32,48,128]{2,1,0:T(8,128)(2,1)S(1)}, u32[]{:S(2)}, u32[]{:S(2)}) %all-to-all-start) | async-done | bytes 393248 | tf_op jit(solution)/shard_map/all_to_all | solution.py:449
  48.1 2.0 shard_map.180
  50.1 7.4 %all-to-all-start.1 = ((bf16[16,320,128]{2,1,0:T(8,128)(2,1)}), bf16[16,320,128]{2,1,0:T(8,128)(2,1)S(1)}, u32[]{:S(2)}, u32[]{:S(2)}) async-start(bf16[16,320,128]{2,1,0:T(8,128)(2,1)} %get-tuple-element.45), calls=%async_computation.1 | async-start | bytes 2621440 | tf_op jit(solution)/shard_map/all_to_all | solution.py:449
  57.6 3.1 %collective-permute-start.1 = (bf16[3072,128]{1,0:T(8,128)(2,1)S(1)}, bf16[3072,128]{1,0:T(8,128)(2,1)S(1)}, u32[]{:S(2)}, u32[]{:S(2)}) collective-permute-start(bf16[3072,128]{1,0:T(8,128)(2,1)S(1)} %copy-done.2), channel_id=1, source_target_pairs={{0,1},{16,20},{1,2},{17,21},{2,3},{18,22},{3,0},{19,23},{4,5},{20,... | collective-permute-start | bytes 2359304 | tf_op jit(solution)/shard_map/ppermute | solution.py:462
  60.7 2.8 %collective-permute-start.2 = (bf16[3072,128]{1,0:T(8,128)(2,1)S(1)}, bf16[3072,128]{1,0:T(8,128)(2,1)S(1)}, u32[]{:S(2)}, u32[]{:S(2)}) collective-permute-start(bf16[3072,128]{1,0:T(8,128)(2,1)S(1)} %copy-done.1), channel_id=1, source_target_pairs={{0,3},{16,28},{1,0},{17,29},{2,1},{18,30},{3,2},{19,31},{4,7},{20,... | collective-permute-start | bytes 2359304 | tf_op jit(solution)/shard_map/ppermute | solution.py:462
  63.5 3.1 %collective-permute-start.4 = (bf16[3072,128]{1,0:T(8,128)(2,1)}, bf16[3072,128]{1,0:T(8,128)(2,1)S(1)}, u32[]{:S(2)}, u32[]{:S(2)}) collective-permute-start(bf16[3072,128]{1,0:T(8,128)(2,1)} %collective-permute-done.refs_3_), channel_id=1, source_target_pairs={{0,1},{16,20},{1,2},{17,21},{2,3},{18,22},{3,0},{19,23},{4,5},{20,... | collective-permute-start | bytes 2359304 | tf_op jit(solution)/shard_map/ppermute | solution.py:462
  66.6 0.0 collective-permute-done.3.refs_6_
  66.6 2.8 %collective-permute-start.5 = (bf16[3072,128]{1,0:T(8,128)(2,1)}, bf16[3072,128]{1,0:T(8,128)(2,1)}, u32[]{:S(2)}, u32[]{:S(2)}) collective-permute-start(bf16[3072,128]{1,0:T(8,128)(2,1)} %collective-permute-done.3.refs_6_), channel_id=1, source_target_pairs={{0,3},{16,28},{1,0},{17,29},{2,1},{18,30},{3,2},{19,31},{4,7},{20,... | collective-permute-start | bytes 2359304 | tf_op jit(solution)/shard_map/ppermute | solution.py:462
  69.3 13.0 %collective-permute-done.1.refs_4_ = bf16[3072,128]{1,0:T(8,128)(2,1)S(1)} collective-permute-done((bf16[3072,128]{1,0:T(8,128)(2,1)S(1)}, bf16[3072,128]{1,0:T(8,128)(2,1)S(1)}, u32[]{:S(2)}, u32[]{:S(2)}) %collective-permute-start.1) | collective-permute-done | bytes 786464 | tf_op jit(solution)/shard_map/ppermute | solution.py:462
  82.3 0.0 collective-permute-done.2.refs_5_
  82.3 8.4 %collective-permute-done.4.refs_7_ = bf16[3072,128]{1,0:T(8,128)(2,1)S(1)} collective-permute-done((bf16[3072,128]{1,0:T(8,128)(2,1)}, bf16[3072,128]{1,0:T(8,128)(2,1)S(1)}, u32[]{:S(2)}, u32[]{:S(2)}) %collective-permute-start.4) | collective-permute-done | bytes 786464 | tf_op jit(solution)/shard_map/ppermute | solution.py:462
  90.7 0.9 copy-done.5
  91.6 0.0 all-to-all-done.1.refs_0_
  91.6 5.8 %shard_map.182 = (bf16[16,160,128]{2,1,0:T(8,128)(2,1)S(1)}, bf16[160,1024]{1,0:T(8,128)(2,1)}, bf16[160,512]{1,0:T(8,128)(2,1)}) custom-call(bf16[16,320,128]{2,1,0:T(8,128)(2,1)S(1)} %all-to-all-done.1.refs_0_, bf16[3072,128]{1,0:T(8,128)(2,1)} %get-tuple-element.46.refs_1_, bf16[3072,128]{1,0:T(8,128)(2,1)} %get-tuple-element.47.refs_2_, ...), custom_call_target="tpu_custom_call" | custom-call | tf_op jit(solution)/shard_map/pallas_call | solution.py:59
  97.4 16.8 %all_to_all.30.refs_1_ = bf16[16,160,128]{2,1,0:T(8,128)(2,1)S(1)} all-to-all(bf16[16,160,128]{2,1,0:T(8,128)(2,1)S(1)} %get-tuple-element.50), channel_id=1, replica_groups=mesh['sp_0'=16,'sp_1'=2,'tp'=16] {'tp'}, dimensions={0} | all-to-all | bytes 1310720 | tf_op jit(solution)/shard_map/all_to_all | solution.py:449
  114.2 1.5 shard_map.183.refs_3_
  115.7 3.9 %all-to-all-start.3 = ((bf16[32,24,128]{2,1,0:T(8,128)(2,1)}), bf16[32,24,128]{2,1,0:T(8,128)(2,1)S(1)}, u32[]{:S(2)}, u32[]{:S(2)}) async-start(bf16[32,24,128]{2,1,0:T(8,128)(2,1)} %shard_map.183.refs_3_), calls=%async_computation.3 | async-start | bytes 393216 | tf_op jit(solution)/shard_map/all_to_all | solution.py:449
  119.6 1.9 shard_map.185.refs_1_
  121.5 6.0 %shard_map.184 = (f32[3072,128]{1,0:T(8,128)}, f32[3072,128]{1,0:T(8,128)}, bf16[3072,128]{1,0:T(8,128)(2,1)}, bf16[3072,128]{1,0:T(8,128)(2,1)}, bf16[3072,128]...) custom-call(bf16[16,320,128]{2,1,0:T(8,128)(2,1)S(1)} %all-to-all-done.1.refs_0_, ...), custom_call_target="tpu_custom_call" | custom-call | tf_op jit(solution)/shard_map/pallas_call | solution.py:59
  127.5 12.1 %all-to-all-done.3.refs_0_ = bf16[32,24,128]{2,1,0:T(8,128)(2,1)S(1)} async-done(((bf16[32,24,128]{2,1,0:T(8,128)(2,1)}), bf16[32,24,128]{2,1,0:T(8,128)(2,1)S(1)}, u32[]{:S(2)}, u32[]{:S(2)}) %all-to-all-start.3) | async-done | bytes 196640 | tf_op jit(solution)/shard_map/all_to_all | solution.py:449
  139.6 2.3 %shard_map.186.refs_6_.refs_5_ = bf16[16,256,128]{2,1,0:T(8,128)(2,1)} custom-call(bf16[32,24,128]{2,1,0:T(8,128)(2,1)S(1)} %all-to-all-done.3.refs_0_, bf16[256,768]{1,0:T(8,128)(2,1)} %shard_map.185.refs_1_, bf16[256,128]{1,0:T(8,128)(2,1)} %refs_2_.4, f32[3072,128]{1,0:T(8,128)} %get-tuple-element.52.refs_3_.refs_0_), custom_call_target="tpu_custom_call" | custom-call | tf_op jit(solution)/shard_map/pallas_call | solution.py:59
  141.8 5.9 %all-to-all-start.4 = ((bf16[16,256,128]{2,1,0:T(8,128)(2,1)}), bf16[16,256,128]{2,1,0:T(8,128)(2,1)S(1)}, u32[]{:S(2)}, u32[]{:S(2)}) async-start(bf16[16,256,128]{2,1,0:T(8,128)(2,1)} %shard_map.186.refs_6_.refs_5_), calls=%async_computation.4 | async-start | bytes 2097152 | tf_op jit(solution)/shard_map/all_to_all | solution.py:449
  147.8 3.1 %collective-permute-start.6 = (bf16[3072,128]{1,0:T(8,128)(2,1)S(1)}, bf16[3072,128]{1,0:T(8,128)(2,1)S(1)}, u32[]{:S(2)}, u32[]{:S(2)}) collective-permute-start(bf16[3072,128]{1,0:T(8,128)(2,1)S(1)} %copy-done.9), channel_id=1, source_target_pairs={{0,1},{16,20},{1,2},{17,21},{2,3},{18,22},{3,0},{19,23},{4,5},{20,... | collective-permute-start | bytes 2359304 | tf_op jit(solution)/shard_map/ppermute | solution.py:462
  150.9 2.9 %collective-permute-start.7 = (bf16[3072,128]{1,0:T(8,128)(2,1)S(1)}, bf16[3072,128]{1,0:T(8,128)(2,1)S(1)}, u32[]{:S(2)}, u32[]{:S(2)}) collective-permute-start(bf16[3072,128]{1,0:T(8,128)(2,1)S(1)} %copy-done.8), channel_id=1, source_target_pairs={{0,3},{16,28},{1,0},{17,29},{2,1},{18,30},{3,2},{19,31},{4,7},{20,... | collective-permute-start | bytes 2359304 | tf_op jit(solution)/shard_map/ppermute | solution.py:462
  153.8 3.0 %shard_map.189 = (bf16[256,128]{1,0:T(8,128)(2,1)}, f32[4,128,64]{2,1,0:T(8,128)}) custom-call(bf16[32,24,128]{2,1,0:T(8,128)(2,1)S(1)} %all-to-all-done.3.refs_0_, bf16[64,256]{1,0:T(8,128)(2,1)} %bitcast.24, bf16[64,256]{1,0:T(8,128)(2,1)} %bitcast.28, bf16[256,128]{1,0:T(8,128)(2,1)} %refs_8_.1, f32[64,256]{1,0:T(8,128)} %bitcast.18, ...), custom_call_target="tpu_custom_call" | custom-call | tf_op jit(solution)/shard_map/pallas_call | solution.py:59
  156.8 11.2 %collective-permute-done.6.refs_4_ = bf16[3072,128]{1,0:T(8,128)(2,1)S(1)} collective-permute-done((bf16[3072,128]{1,0:T(8,128)(2,1)S(1)}, bf16[3072,128]{1,0:T(8,128)(2,1)S(1)}, u32[]{:S(2)}, u32[]{:S(2)}) %collective-permute-start.6) | collective-permute-done | bytes 786464 | tf_op jit(solution)/shard_map/ppermute | solution.py:462
  168.0 0.5 collective-permute-done.7.refs_5_
  168.6 0.4 copy-done.6
  168.9 0.5 copy-done.7
  169.5 4.2 %shard_map.187 = (bf16[6144,128]{1,0:T(8,128)(2,1)}, bf16[6144,128]{1,0:T(8,128)(2,1)}) custom-call(bf16[3072,128]{1,0:T(8,128)(2,1)} %get-tuple-element.54.refs_0_, bf16[3072,128]{1,0:T(8,128)(2,1)} %get-tuple-element.55.refs_1_, bf16[3072,128]{1,0:T(8,128)(2,1)} %get-tuple-element.56.refs_2_, bf16[3072,128]{1,0:T(8,128)(2,1)} %get-tuple-element.57.refs_3_, ...), custom_call_target="tpu_custom_call" | custom-call | tf_op jit(solution)/shard_map/pallas_call | solution.py:59
  173.7 0.0 all-to-all-done.4.refs_1_
  173.7 2.9 %shard_map.190 = (f32[256,128]{1,0:T(8,128)}, f32[32,128]{1,0:T(8,128)}, bf16[1088,128]{1,0:T(8,128)(2,1)S(1)}, f32[1024,128]{1,0:T(8,128)S(1)}) custom-call(s32[3]{0:T(128)S(1)} %pad_add_fusion.refs_0_, bf16[16,256,128]{2,1,0:T(8,128)(2,1)S(1)} %all-to-all-done.4.refs_1_, bf16[2048,128]{1,0:T(8,128)(2,1)} %refs_2_.5, ...), custom_call_target="tpu_custom_call" | custom-call | tf_op jit(solution)/shard_map/pallas_call | solution.py:59
  176.6 3.5 %collective-permute-start.10 = (bf16[1088,128]{1,0:T(8,128)(2,1)S(1)}, bf16[1088,128]{1,0:T(8,128)(2,1)S(1)}, u32[]{:S(2)}, u32[]{:S(2)}) collective-permute-start(bf16[1088,128]{1,0:T(8,128)(2,1)S(1)} %get-tuple-element.67), channel_id=1, source_target_pairs={{0,16},{16,0},{1,17},{17,1},{2,18},{18,2},{3,19},{19,3},{4,20},{20... | collective-permute-start | bytes 835592 | tf_op jit(solution)/shard_map/ppermute | solution.py:587
  180.1 3.1 %collective-permute-start.8 = (bf16[6144,128]{1,0:T(8,128)(2,1)}, bf16[6144,128]{1,0:T(8,128)(2,1)}, u32[]{:S(2)}, u32[]{:S(2)}) collective-permute-start(bf16[6144,128]{1,0:T(8,128)(2,1)} %get-tuple-element.61), channel_id=1, source_target_pairs={{0,1},{16,20},{1,2},{17,21},{2,3},{18,22},{3,0},{19,23},{4,5},{20,... | collective-permute-start | bytes 4718600 | tf_op jit(solution)/shard_map/ppermute | solution.py:462
  183.3 2.7 %collective-permute-start.9 = (bf16[6144,128]{1,0:T(8,128)(2,1)S(1)}, bf16[6144,128]{1,0:T(8,128)(2,1)}, u32[]{:S(2)}, u32[]{:S(2)}) collective-permute-start(bf16[6144,128]{1,0:T(8,128)(2,1)S(1)} %copy-done), channel_id=1, source_target_pairs={{0,3},{16,28},{1,0},{17,29},{2,1},{18,30},{3,2},{19,31},{4,7},{20,... | collective-permute-start | bytes 4718600 | tf_op jit(solution)/shard_map/ppermute | solution.py:462
  186.0 1.6 shard_map.191
  187.6 4.0 %all-to-all-start.5 = ((bf16[16,96,128]{2,1,0:T(8,128)(2,1)}), bf16[16,96,128]{2,1,0:T(8,128)(2,1)S(1)}, u32[]{:S(2)}, u32[]{:S(2)}) async-start(bf16[16,96,128]{2,1,0:T(8,128)(2,1)} %get-tuple-element.71), calls=%async_computation.5 | async-start | bytes 786432 | tf_op jit(solution)/shard_map/all_to_all | solution.py:449
  191.6 11.1 %collective-permute-done.8.refs_2_ = bf16[6144,128]{1,0:T(8,128)(2,1)} collective-permute-done((bf16[6144,128]{1,0:T(8,128)(2,1)}, bf16[6144,128]{1,0:T(8,128)(2,1)}, u32[]{:S(2)}, u32[]{:S(2)}) %collective-permute-start.8) | collective-permute-done | bytes 1572896 | tf_op jit(solution)/shard_map/ppermute | solution.py:462
  202.8 2.9 %collective-permute-done.9.refs_3_ = bf16[6144,128]{1,0:T(8,128)(2,1)} collective-permute-done((bf16[6144,128]{1,0:T(8,128)(2,1)S(1)}, bf16[6144,128]{1,0:T(8,128)(2,1)}, u32[]{:S(2)}, u32[]{:S(2)}) %collective-permute-start.9) | collective-permute-done | bytes 1572896 | tf_op jit(solution)/shard_map/ppermute | solution.py:462
  205.7 4.3 %shard_map.188 = (bf16[2048,128]{1,0:T(8,128)(2,1)}, bf16[2048,128]{1,0:T(8,128)(2,1)}, bf16[128,2048]{1,0:T(8,128)(2,1)}) custom-call(f32[3072,128]{1,0:T(8,128)} %get-tuple-element.52.refs_3_.refs_0_, f32[3072,128]{1,0:T(8,128)} %get-tuple-element.53.refs_1_, bf16[6144,128]{1,0:T(8,128)(2,1)} %collective-permute-done.8.refs_2_, ...), custom_call_target="tpu_custom_call" | custom-call | tf_op jit(solution)/shard_map/pallas_call | solution.py:59
  210.0 8.2 %all-to-all-done.5.refs_1_ = bf16[16,96,128]{2,1,0:T(8,128)(2,1)S(1)} async-done(((bf16[16,96,128]{2,1,0:T(8,128)(2,1)}), bf16[16,96,128]{2,1,0:T(8,128)(2,1)S(1)}, u32[]{:S(2)}, u32[]{:S(2)}) %all-to-all-start.5) | async-done | bytes 393248 | tf_op jit(solution)/shard_map/all_to_all | solution.py:449
  218.1 3.9 %shard_map.192 = (f32[64,128]{1,0:T(8,128)}, bf16[64,256]{1,0:T(8,128)(2,1)}, bf16[64,256]{1,0:T(8,128)(2,1)}, bf16[256,128]{1,0:T(8,128)(2,1)}, f32[64,256]{1,0:T(8,128)}) custom-call(s32[3]{0:T(128)S(1)} %pad_add_fusion.refs_0_, bf16[16,96,128]{2,1,0:T(8,128)(2,1)S(1)} %all-to-all-done.5.refs_1_, f32[32,128]{1,0:T(8,128)} %get-tuple-element.72.refs_2_, ...), custom_call_target="tpu_custom_call" | custom-call | tf_op jit(solution)/shard_map/pallas_call | solution.py:59
  (20 shorter events, 0.0 us)
Async XLA Ops:
  4.4 43.7 %all-to-all-start = ((bf16[32,48,128]{2,1,0:T(8,128)(2,1)}), bf16[32,48,128]{2,1,0:T(8,128)(2,1)S(1)}, u32[]{:S(2)}, u32[]{:S(2)}) async-start(bf16[32,48,128]{2,1,0:T(8,128)(2,1)} %get-tuple-element.44), calls=%async_computation | async-start | bytes 786432 | tf_op jit(solution)/shard_map/all_to_all | solution.py:449
  22.5 35.1 %copy-start.2 = (bf16[3072,128]{1,0:T(8,128)(2,1)S(1)}, bf16[3072,128]{1,0:T(8,128)(2,1)}, u32[]{:S(2)}) copy-start(bf16[3072,128]{1,0:T(8,128)(2,1)} %get-tuple-element.47.refs_2_) | copy-start | bytes 2359300
  22.5 38.2 %copy-start.1 = (bf16[3072,128]{1,0:T(8,128)(2,1)S(1)}, bf16[3072,128]{1,0:T(8,128)(2,1)}, u32[]{:S(2)}) copy-start(bf16[3072,128]{1,0:T(8,128)(2,1)} %get-tuple-element.46.refs_1_) | copy-start | bytes 2359300
  22.5 41.0 %collective-permute-start = (bf16[3072,128]{1,0:T(8,128)(2,1)}, bf16[3072,128]{1,0:T(8,128)(2,1)}, u32[]{:S(2)}, u32[]{:S(2)}) collective-permute-start(bf16[3072,128]{1,0:T(8,128)(2,1)} %get-tuple-element.46.refs_1_), channel_id=1, source_target_pairs={{0,1},{16,20},{1,2},{17,21},{2,3},{18,22},{3,0},{19,23},{4,5},{20,... | collective-permute-start | bytes 2359304 | tf_op jit(solution)/shard_map/ppermute | solution.py:462
  25.7 40.8 %collective-permute-start.3 = (bf16[3072,128]{1,0:T(8,128)(2,1)}, bf16[3072,128]{1,0:T(8,128)(2,1)}, u32[]{:S(2)}, u32[]{:S(2)}) collective-permute-start(bf16[3072,128]{1,0:T(8,128)(2,1)} %get-tuple-element.47.refs_2_), channel_id=1, source_target_pairs={{0,3},{16,28},{1,0},{17,29},{2,1},{18,30},{3,2},{19,31},{4,7},{20,... | collective-permute-start | bytes 2359304 | tf_op jit(solution)/shard_map/ppermute | solution.py:462
  50.1 41.5 %all-to-all-start.1 = ((bf16[16,320,128]{2,1,0:T(8,128)(2,1)}), bf16[16,320,128]{2,1,0:T(8,128)(2,1)S(1)}, u32[]{:S(2)}, u32[]{:S(2)}) async-start(bf16[16,320,128]{2,1,0:T(8,128)(2,1)} %get-tuple-element.45), calls=%async_computation.1 | async-start | bytes 2621440 | tf_op jit(solution)/shard_map/all_to_all | solution.py:449
  57.6 24.7 %collective-permute-start.1 = (bf16[3072,128]{1,0:T(8,128)(2,1)S(1)}, bf16[3072,128]{1,0:T(8,128)(2,1)S(1)}, u32[]{:S(2)}, u32[]{:S(2)}) collective-permute-start(bf16[3072,128]{1,0:T(8,128)(2,1)S(1)} %copy-done.2), channel_id=1, source_target_pairs={{0,1},{16,20},{1,2},{17,21},{2,3},{18,22},{3,0},{19,23},{4,5},{20,... | collective-permute-start | bytes 2359304 | tf_op jit(solution)/shard_map/ppermute | solution.py:462
  60.7 21.6 %collective-permute-start.2 = (bf16[3072,128]{1,0:T(8,128)(2,1)S(1)}, bf16[3072,128]{1,0:T(8,128)(2,1)S(1)}, u32[]{:S(2)}, u32[]{:S(2)}) collective-permute-start(bf16[3072,128]{1,0:T(8,128)(2,1)S(1)} %copy-done.1), channel_id=1, source_target_pairs={{0,3},{16,28},{1,0},{17,29},{2,1},{18,30},{3,2},{19,31},{4,7},{20,... | collective-permute-start | bytes 2359304 | tf_op jit(solution)/shard_map/ppermute | solution.py:462
  63.5 27.3 %collective-permute-start.4 = (bf16[3072,128]{1,0:T(8,128)(2,1)}, bf16[3072,128]{1,0:T(8,128)(2,1)S(1)}, u32[]{:S(2)}, u32[]{:S(2)}) collective-permute-start(bf16[3072,128]{1,0:T(8,128)(2,1)} %collective-permute-done.refs_3_), channel_id=1, source_target_pairs={{0,1},{16,20},{1,2},{17,21},{2,3},{18,22},{3,0},{19,23},{4,5},{20,... | collective-permute-start | bytes 2359304 | tf_op jit(solution)/shard_map/ppermute | solution.py:462
  66.6 25.1 %collective-permute-start.5 = (bf16[3072,128]{1,0:T(8,128)(2,1)}, bf16[3072,128]{1,0:T(8,128)(2,1)}, u32[]{:S(2)}, u32[]{:S(2)}) collective-permute-start(bf16[3072,128]{1,0:T(8,128)(2,1)} %collective-permute-done.3.refs_6_), channel_id=1, source_target_pairs={{0,3},{16,28},{1,0},{17,29},{2,1},{18,30},{3,2},{19,31},{4,7},{20,... | collective-permute-start | bytes 2359304 | tf_op jit(solution)/shard_map/ppermute | solution.py:462
  82.3 8.4 %copy-start.3 = (bf16[3072,128]{1,0:T(8,128)(2,1)}, bf16[3072,128]{1,0:T(8,128)(2,1)S(1)}, u32[]{:S(2)}) copy-start(bf16[3072,128]{1,0:T(8,128)(2,1)S(1)} %collective-permute-done.1.refs_4_) | copy-start | bytes 2359300
  82.3 8.4 %copy-start.4 = (bf16[3072,128]{1,0:T(8,128)(2,1)}, bf16[3072,128]{1,0:T(8,128)(2,1)S(1)}, u32[]{:S(2)}) copy-start(bf16[3072,128]{1,0:T(8,128)(2,1)S(1)} %collective-permute-done.2.refs_5_) | copy-start | bytes 2359300
  90.7 0.9 copy-start.5
  115.7 23.8 %all-to-all-start.3 = ((bf16[32,24,128]{2,1,0:T(8,128)(2,1)}), bf16[32,24,128]{2,1,0:T(8,128)(2,1)S(1)}, u32[]{:S(2)}, u32[]{:S(2)}) async-start(bf16[32,24,128]{2,1,0:T(8,128)(2,1)} %shard_map.183.refs_3_), calls=%async_computation.3 | async-start | bytes 393216 | tf_op jit(solution)/shard_map/all_to_all | solution.py:449
  141.8 5.9 %copy-start.9 = (bf16[3072,128]{1,0:T(8,128)(2,1)S(1)}, bf16[3072,128]{1,0:T(8,128)(2,1)}, u32[]{:S(2)}) copy-start(bf16[3072,128]{1,0:T(8,128)(2,1)} %get-tuple-element.58) | copy-start | bytes 2359300
  141.8 9.0 %copy-start.8 = (bf16[3072,128]{1,0:T(8,128)(2,1)S(1)}, bf16[3072,128]{1,0:T(8,128)(2,1)}, u32[]{:S(2)}) copy-start(bf16[3072,128]{1,0:T(8,128)(2,1)} %get-tuple-element.59) | copy-start | bytes 2359300
  141.8 31.9 %all-to-all-start.4 = ((bf16[16,256,128]{2,1,0:T(8,128)(2,1)}), bf16[16,256,128]{2,1,0:T(8,128)(2,1)S(1)}, u32[]{:S(2)}, u32[]{:S(2)}) async-start(bf16[16,256,128]{2,1,0:T(8,128)(2,1)} %shard_map.186.refs_6_.refs_5_), calls=%async_computation.4 | async-start | bytes 2097152 | tf_op jit(solution)/shard_map/all_to_all | solution.py:449
  147.8 20.3 %collective-permute-start.6 = (bf16[3072,128]{1,0:T(8,128)(2,1)S(1)}, bf16[3072,128]{1,0:T(8,128)(2,1)S(1)}, u32[]{:S(2)}, u32[]{:S(2)}) collective-permute-start(bf16[3072,128]{1,0:T(8,128)(2,1)S(1)} %copy-done.9), channel_id=1, source_target_pairs={{0,1},{16,20},{1,2},{17,21},{2,3},{18,22},{3,0},{19,23},{4,5},{20,... | collective-permute-start | bytes 2359304 | tf_op jit(solution)/shard_map/ppermute | solution.py:462
  150.9 17.7 %collective-permute-start.7 = (bf16[3072,128]{1,0:T(8,128)(2,1)S(1)}, bf16[3072,128]{1,0:T(8,128)(2,1)S(1)}, u32[]{:S(2)}, u32[]{:S(2)}) collective-permute-start(bf16[3072,128]{1,0:T(8,128)(2,1)S(1)} %copy-done.8), channel_id=1, source_target_pairs={{0,3},{16,28},{1,0},{17,29},{2,1},{18,30},{3,2},{19,31},{4,7},{20,... | collective-permute-start | bytes 2359304 | tf_op jit(solution)/shard_map/ppermute | solution.py:462
  168.0 0.9 copy-start.6
  168.6 0.9 copy-start.7
  173.7 9.6 %copy-start = (bf16[6144,128]{1,0:T(8,128)(2,1)S(1)}, bf16[6144,128]{1,0:T(8,128)(2,1)}, u32[]{:S(2)}) copy-start(bf16[6144,128]{1,0:T(8,128)(2,1)} %get-tuple-element.62.refs_6_) | copy-start | bytes 4718596
  176.6 9.4 %collective-permute-start.10 = (bf16[1088,128]{1,0:T(8,128)(2,1)S(1)}, bf16[1088,128]{1,0:T(8,128)(2,1)S(1)}, u32[]{:S(2)}, u32[]{:S(2)}) collective-permute-start(bf16[1088,128]{1,0:T(8,128)(2,1)S(1)} %get-tuple-element.67), channel_id=1, source_target_pairs={{0,16},{16,0},{1,17},{17,1},{2,18},{18,2},{3,19},{19,3},{4,20},{20... | collective-permute-start | bytes 835592 | tf_op jit(solution)/shard_map/ppermute | solution.py:587
  180.1 22.6 %collective-permute-start.8 = (bf16[6144,128]{1,0:T(8,128)(2,1)}, bf16[6144,128]{1,0:T(8,128)(2,1)}, u32[]{:S(2)}, u32[]{:S(2)}) collective-permute-start(bf16[6144,128]{1,0:T(8,128)(2,1)} %get-tuple-element.61), channel_id=1, source_target_pairs={{0,1},{16,20},{1,2},{17,21},{2,3},{18,22},{3,0},{19,23},{4,5},{20,... | collective-permute-start | bytes 4718600 | tf_op jit(solution)/shard_map/ppermute | solution.py:462
  183.3 22.4 %collective-permute-start.9 = (bf16[6144,128]{1,0:T(8,128)(2,1)S(1)}, bf16[6144,128]{1,0:T(8,128)(2,1)}, u32[]{:S(2)}, u32[]{:S(2)}) collective-permute-start(bf16[6144,128]{1,0:T(8,128)(2,1)S(1)} %copy-done), channel_id=1, source_target_pairs={{0,3},{16,28},{1,0},{17,29},{2,1},{18,30},{3,2},{19,31},{4,7},{20,... | collective-permute-start | bytes 4718600 | tf_op jit(solution)/shard_map/ppermute | solution.py:462
  187.6 30.5 %all-to-all-start.5 = ((bf16[16,96,128]{2,1,0:T(8,128)(2,1)}), bf16[16,96,128]{2,1,0:T(8,128)(2,1)S(1)}, u32[]{:S(2)}, u32[]{:S(2)}) async-start(bf16[16,96,128]{2,1,0:T(8,128)(2,1)} %get-tuple-element.71), calls=%async_computation.5 | async-start | bytes 786432 | tf_op jit(solution)/shard_map/all_to_all | solution.py:449

commit v5 on v4

--- a/solution.py
+++ b/solution.py
@@ -244,36 +244,57 @@
         both = mm(x, grads, TN)
         down = mm(hidden, g, TN)
         at = k * 128
-        for b in range(4):
-            a_ref, b_ref = out_refs[2 * b : 2 * b + 2]
+        for b, (a_part, b_part) in enumerate(lots_of(out_refs)):
+            (a_ref, a_at), (b_ref, b_at) = a_part, b_part
             kind = a_ref.dtype
             up = both[:, 256 * b + 128 : 256 * b + 256].astype(kind)
-            a_ref[at : at + 256, :] = both[:, 256 * b : 256 * b + 128].astype(kind)
+            a_ref[a_at + at : a_at + at + 256, :] = both[:, 256 * b : 256 * b + 128].astype(kind)
             if k < N_TP // 2:
-                a_ref[2048 + at : 2304 + at, :] = up
+                a_ref[a_at + 2048 + at : a_at + 2304 + at, :] = up
             else:
-                b_ref[at - 1024 : at - 768, :] = up
+                b_ref[b_at + at - 1024 : b_at + at - 768, :] = up
             for n in range(2):
-                block = 1024 + at + n * 128
+                block = b_at + 1024 + at + n * 128
                 b_ref[block : block + 128, :] = down[
                     128 * b : 128 * b + 128, n * 128 : (n + 1) * 128
                 ].astype(kind)
 
 
-def relay_kernel(
-    left_a_ref, left_b_ref, right_a_ref, right_b_ref, far_a_ref, far_b_ref, left_ref, right_ref
+def lots_of(refs):
+    own_a, own_b, to_left, to_right, left_b, right_a = refs
+    return (
+        ((own_a, 0), (own_b, 0)),
+        ((to_left, 0), (left_b, 0)),
+        ((right_a, 0), (to_right, LOT)),
+        ((to_right, 0), (to_left, LOT)),
+    )
+
+
+def relay_kernel(left_b_ref, right_a_ref, from_right_ref, from_left_ref, to_left_ref, to_right_ref):
+    far_a, far_b = from_left_ref[:LOT, :].astype(F32), from_right_ref[LOT:, :].astype(F32)
+    to_right_ref[...] = (right_a_ref[...].astype(F32) + far_a).astype(BF)
+    to_left_ref[...] = (left_b_ref[...].astype(F32) + far_b).astype(BF)
+
+
+def grad_sum_kernel(
+    own_a_ref,
+    own_b_ref,
+    from_right_ref,
+    from_left_ref,
+    last_a_ref,
+    last_b_ref,
+    gate_ref,
+    up_ref,
+    down_ref,
 ):
-    right_ref[:LOT, :] = (right_a_ref[...].astype(F32) + far_a_ref[...].astype(F32)).astype(BF)
-    right_ref[LOT:, :] = right_b_ref[...]
-    left_ref[:LOT, :] = left_a_ref[...]
-    left_ref[LOT:, :] = (left_b_ref[...].astype(F32) + far_b_ref[...].astype(F32)).astype(BF)
-
-
-def grad_sum_kernel(own_a_ref, own_b_ref, x_ref, y_ref, gate_ref, up_ref, down_ref):
     def total(at, size):
-        ref, start = (own_a_ref, at) if at < LOT else (own_b_ref, at - LOT)
-        other = x_ref[at : at + size, :].astype(F32) + y_ref[at : at + size, :].astype(F32)
-        return (ref[start : start + size, :] + other).astype(BF)
+        if at < LOT:
+            refs = (own_a_ref, from_right_ref, last_a_ref)
+            rows = [r[at : at + size, :].astype(F32) for r in refs]
+        else:
+            own, last = (r[at - LOT : at - LOT + size, :] for r in (own_b_ref, last_b_ref))
+            rows = [own, from_left_ref[at : at + size, :].astype(F32), last.astype(F32)]
+        return (rows[0] + rows[1] + rows[2]).astype(BF)
 
     for k in range(N_TP):
         here = slice(k * 128, (k + 1) * 128)
@@ -494,7 +515,12 @@
     )
     recv = exchanged(sent, SP)
     own_a, own_b = call(
-        pack_kernel, [((LOT, 128), BF), ((LOT, 128), BF)], w_gate[0], w_up[0], w_down[0]
+        pack_kernel,
+        [((LOT, 128), BF), ((LOT, 128), BF)],
+        w_gate[0],
+        w_up[0],
+        w_down[0],
+        near_out=(0, 1),
     )
     left_a = passed_on(own_a, 1)
     right_b = passed_on(own_b, -1)
@@ -503,7 +529,6 @@
     far_a = passed_on(left_a, 1)
     far_b = passed_on(right_b, -1)
     weights = (own_a, own_b, left_a, left_b, right_a, right_b, far_a, far_b)
-    (turned,) = call(turned_kernel, [((TOK, SLOTS), BF)], pick)
     copies, states, reach = call(
         copies_kernel,
         [((N_TP, 2 * PART, 128), BF), ((N_SP, 128), F32), ((24, 128), F32)],
@@ -515,15 +540,39 @@
         near_out=(0,),
     )
     rows = exchanged(copies, "tp")
+    (turned,) = call(turned_kernel, [((TOK, SLOTS), BF)], pick, after=(copies,))
     partial_rows, grads, hidden = call(
         partial_kernel,
         [((N_TP, PART, 128), BF), ((PART, 1024), BF), ((PART, 512), BF)],
         rows,
         *weights,
-        near=(0,),
-        near_out=(0,),
+        near=tuple(range(9)),
+        near_out=(1, 2),
     )
     arrived = exchanged(partial_rows, "tp")
+    own_grad_a, own_grad_b, to_left, to_right, left_lot, right_lot = call(
+        weight_grads_kernel,
+        2 * [((LOT, 128), F32)] + 2 * [((2 * LOT, 128), BF)] + 2 * [((LOT, 128), BF)],
+        rows,
+        grads,
+        hidden,
+        near=(0, 1, 2),
+        near_out=(2, 3),
+    )
+    from_left = passed_on(to_right, 1)
+    from_right = passed_on(to_left, -1)
+    lot_left, lot_right = call(
+        relay_kernel,
+        2 * [((LOT, 128), BF)],
+        left_lot,
+        right_lot,
+        from_right,
+        from_left,
+        near=(2, 3),
+        near_out=(0, 1),
+    )
+    last_a = passed_on(lot_right, 1)
+    last_b = passed_on(lot_left, -1)
     (returned,) = call(
         row_sum_kernel,
         [((N_SP, PAD, 128), BF)],
@@ -534,27 +583,8 @@
         near=(1,),
         scratch=[pltpu.VMEM((ROWS + 8, 128), F32)],
     )
-    own_grad_a, own_grad_b, *lots = call(
-        weight_grads_kernel,
-        2 * [((LOT, 128), F32)] + 6 * [((LOT, 128), BF)],
-        rows,
-        grads,
-        hidden,
-        near=(0,),
-        after=(returned,),
-    )
-    via_right = passed_on(lots[4], 1)
-    via_left = passed_on(lots[5], -1)
     back = exchanged(returned, SP)
-    (residual,) = call(
-        residual_kernel,
-        [((N_TP, TOK, 128), BF)],
-        back,
-        turned,
-        out_grad,
-        near=(0,),
-        after=(own_grad_a,),
-    )
+    (residual,) = call(residual_kernel, [((N_TP, TOK, 128), BF)], back, turned, out_grad, near=(0,))
     full_grad = exchanged(residual, "tp")
     mixer_out, entering = call(
         forward_kernel,
@@ -565,10 +595,8 @@
         value_rows,
         decay_t,
         near=(0,),
+        near_out=(0,),
         after=(residual,),
-    )
-    to_left, to_right = call(
-        relay_kernel, 2 * [((2 * LOT, 128), BF)], *lots[:4], via_right, via_left, after=(residual,)
     )
     mixer_grad, span_grad, to_other, kept = call(
         mixer_grad_kernel,
@@ -580,9 +608,8 @@
         q_t,
         decay_t,
         smem=(0,),
-        after=(to_left,),
-        near=(1,),
-        near_out=(2, 3),
+        near=(1, 3),
+        near_out=(0, 1, 2, 3),
     )
     from_other = lax.ppermute(to_other, "sp_1", [(0, 1), (1, 0)])
     chip_sent, other_grad = call(
@@ -594,7 +621,8 @@
         span_grad,
         reach,
         smem=(0,),
-        near=(1, 2),
+        near=(1, 2, 3),
+        near_out=(1,),
     )
     later = exchanged(chip_sent, "sp_0")
     grad_proj, gq, gk, gv, gd = call(
@@ -611,17 +639,19 @@
         value_rows,
         decay_t,
         smem=(0,),
-        near=(1,),
-    )
-    from_right = passed_on(to_left, -1)
-    from_left = passed_on(to_right, 1)
+        near=(1, 2, 4),
+    )
     gate_part, up_part, down_part = call(
         grad_sum_kernel,
         [((2048, 128), BF), ((2048, 128), BF), ((128, 2048), BF)],
         own_grad_a,
         own_grad_b,
+        from_right,
         from_left,
-        from_right,
+        last_a,
+        last_b,
+        near=(2, 3, 4, 5),
+        after=(residual,),
     )
     return (gate_part[None], up_part[None], down_part[None], grad_proj, gq.T, gk.T, gv, gd.T)
 

time: 223 us -> 217 us (0.973)
  the two profiles are of different devices: /device:TPU:4 before, /device:TPU:1 now
where the time goes in v5:
time: 217 us; the launch traced here: 213 us
  starting transfers between devices  75.5 us (35%)
  waiting for transfers between devices  70.7 us (33%)
  Pallas kernels  39.7 us (18%)
  blocking collectives  15.2 us (7%)
  local copies, waits for them, and re-layouts  11.1 us (5%)
    pallas_call x14, Pallas kernels, call(): pl.pallas_call(run, out_shape=tuple(((pltpu.VMEM if k in near_out else pl...  39.7 us
    all_to_all x5, starting transfers between devices, exchanged(): return lax.all_to_all(blocks, axis, split_axis=0, concat_axis=0, tiled=True)  38.3 us
    all_to_all x5, waiting for transfers between devices, exchanged(): return lax.all_to_all(blocks, axis, split_axis=0, concat_axis=0, tiled=True)  38.1 us
    ppermute x10, starting transfers between devices, passed_on(): return lax.ppermute(array, ('sp_1', 'tp'), ring_step(step))  32.2 us
    ppermute x10, waiting for transfers between devices, passed_on(): return lax.ppermute(array, ('sp_1', 'tp'), ring_step(step))  31.5 us
    all_to_all x1, blocking collectives, exchanged(): return lax.all_to_all(blocks, axis, split_axis=0, concat_axis=0, tiled=True)  15.2 us
    unnamed x28, local copies, waits for them, and re-layouts  11.1 us
    ppermute x1, starting transfers between devices, body(): from_other = lax.ppermute(to_other, 'sp_1', [(0, 1), (1, 0)])  5.02 us
  transfers between devices with their start and end apart: 16, of which 11 were waited for; matrix products, arithmetic and copies ran while one was open for 0% of the time, Pallas kernels for 11%

profile of v5, /device:TPU:1, one launch (start us, length us, event | category | flops | bytes accessed | tf_op | source)
XLA Modules:
  0.0 213.2 jit_solution(1050378377794748726)
XLA Ops:
  0.6 3.8 %shard_map.179 = (bf16[32,48,128]{2,1,0:T(8,128)(2,1)}, bf16[768,256]{1,0:T(8,128)(2,1)}) custom-call(s32[2,256]{1,0:T(2,128)} %bitcast.30, f32[2,256]{1,0:T(2,128)} %bitcast.31, bf16[256,128]{1,0:T(8,128)(2,1)} %refs_2_.3, bf16[256,128]{1,0:T(8,128)(2,1)} %refs_2_.4, bf16[64,256]{1,0:T(8,128)(2,1)} %bitcast.24, bf16[256,128]{1,0:T(8,128)(2,1)} %refs_8_.1, ...), custom_call_target="tpu_custom_call" | custom-call | tf_op jit(solution)/shard_map/pallas_call | solution.py:59
  4.4 16.7 %all-to-all-start = ((bf16[32,48,128]{2,1,0:T(8,128)(2,1)}), bf16[32,48,128]{2,1,0:T(8,128)(2,1)S(1)}, u32[]{:S(2)}, u32[]{:S(2)}) async-start(bf16[32,48,128]{2,1,0:T(8,128)(2,1)} %get-tuple-element.42), calls=%async_computation | async-start | bytes 786432 | tf_op jit(solution)/shard_map/all_to_all | solution.py:470
  21.2 1.5 shard_map.181
  22.7 3.2 %collective-permute-start = (bf16[3072,128]{1,0:T(8,128)(2,1)S(1)}, bf16[3072,128]{1,0:T(8,128)(2,1)}, u32[]{:S(2)}, u32[]{:S(2)}) collective-permute-start(bf16[3072,128]{1,0:T(8,128)(2,1)S(1)} %get-tuple-element.44.refs_1_), channel_id=1, source_target_pairs={{0,1},{16,20},{1,2},{17,21},{2,3},{18,22},{3,0},{19,23},{4,5},{20,... | collective-permute-start | bytes 2359304 | tf_op jit(solution)/shard_map/ppermute | solution.py:483
  25.9 3.4 %collective-permute-start.3 = (bf16[3072,128]{1,0:T(8,128)(2,1)S(1)}, bf16[3072,128]{1,0:T(8,128)(2,1)}, u32[]{:S(2)}, u32[]{:S(2)}) collective-permute-start(bf16[3072,128]{1,0:T(8,128)(2,1)S(1)} %get-tuple-element.45.refs_2_), channel_id=1, source_target_pairs={{0,3},{16,28},{1,0},{17,29},{2,1},{18,30},{3,2},{19,31},{4,7},{20,... | collective-permute-start | bytes 2359304 | tf_op jit(solution)/shard_map/ppermute | solution.py:483
  29.4 19.6 %all-to-all-done.refs_1_ = bf16[32,48,128]{2,1,0:T(8,128)(2,1)S(1)} async-done(((bf16[32,48,128]{2,1,0:T(8,128)(2,1)}), bf16[32,48,128]{2,1,0:T(8,128)(2,1)S(1)}, u32[]{:S(2)}, u32[]{:S(2)}) %all-to-all-start) | async-done | bytes 393248 | tf_op jit(solution)/shard_map/all_to_all | solution.py:470
  48.9 2.0 shard_map.180
  51.0 6.8 %all-to-all-start.1 = ((bf16[16,320,128]{2,1,0:T(8,128)(2,1)}), bf16[16,320,128]{2,1,0:T(8,128)(2,1)S(1)}, u32[]{:S(2)}, u32[]{:S(2)}) async-start(bf16[16,320,128]{2,1,0:T(8,128)(2,1)} %get-tuple-element.43.refs_1_), calls=%async_computation.1 | async-start | bytes 2621440 | tf_op jit(solution)/shard_map/all_to_all | solution.py:470
  57.7 4.5 %collective-permute-start.2 = (bf16[3072,128]{1,0:T(8,128)(2,1)S(1)}, bf16[3072,128]{1,0:T(8,128)(2,1)S(1)}, u32[]{:S(2)}, u32[]{:S(2)}) collective-permute-start(bf16[3072,128]{1,0:T(8,128)(2,1)S(1)} %get-tuple-element.44.refs_1_), channel_id=1, source_target_pairs={{0,3},{16,28},{1,0},{17,29},{2,1},{18,30},{3,2},{19,31},{4,7},{20,... | collective-permute-start | bytes 2359304 | tf_op jit(solution)/shard_map/ppermute | solution.py:483
  62.2 1.9 collective-permute-start.1
  64.2 2.1 %collective-permute-start.4 = (bf16[3072,128]{1,0:T(8,128)(2,1)}, bf16[3072,128]{1,0:T(8,128)(2,1)S(1)}, u32[]{:S(2)}, u32[]{:S(2)}) collective-permute-start(bf16[3072,128]{1,0:T(8,128)(2,1)} %collective-permute-done.refs_3_), channel_id=1, source_target_pairs={{0,1},{16,20},{1,2},{17,21},{2,3},{18,22},{3,0},{19,23},{4,5},{20,... | collective-permute-start | bytes 2359304 | tf_op jit(solution)/shard_map/ppermute | solution.py:483
  66.3 4.3 %collective-permute-start.5 = (bf16[3072,128]{1,0:T(8,128)(2,1)}, bf16[3072,128]{1,0:T(8,128)(2,1)S(1)}, u32[]{:S(2)}, u32[]{:S(2)}) collective-permute-start(bf16[3072,128]{1,0:T(8,128)(2,1)} %collective-permute-done.3.refs_6_), channel_id=1, source_target_pairs={{0,3},{16,28},{1,0},{17,29},{2,1},{18,30},{3,2},{19,31},{4,7},{20,... | collective-permute-start | bytes 2359304 | tf_op jit(solution)/shard_map/ppermute | solution.py:483
  70.7 12.3 %collective-permute-done.2.refs_5_ = bf16[3072,128]{1,0:T(8,128)(2,1)S(1)} collective-permute-done((bf16[3072,128]{1,0:T(8,128)(2,1)S(1)}, bf16[3072,128]{1,0:T(8,128)(2,1)S(1)}, u32[]{:S(2)}, u32[]{:S(2)}) %collective-permute-start.2) | collective-permute-done | bytes 786464 | tf_op jit(solution)/shard_map/ppermute | solution.py:483
  83.0 0.9 copy-done
  85.4 7.2 %collective-permute-done.4.refs_7_ = bf16[3072,128]{1,0:T(8,128)(2,1)S(1)} collective-permute-done((bf16[3072,128]{1,0:T(8,128)(2,1)}, bf16[3072,128]{1,0:T(8,128)(2,1)S(1)}, u32[]{:S(2)}, u32[]{:S(2)}) %collective-permute-start.4) | collective-permute-done | bytes 786464 | tf_op jit(solution)/shard_map/ppermute | solution.py:483
  92.7 0.9 copy-done.4
  93.6 0.9 copy-done.6
  94.5 1.1 copy-done.1
  95.6 1.1 copy-done.3
  96.7 1.1 copy-done.5
  97.9 1.1 copy-done.7
  99.0 5.2 %shard_map.182 = (bf16[16,160,128]{2,1,0:T(8,128)(2,1)}, bf16[160,1024]{1,0:T(8,128)(2,1)S(1)}, bf16[160,512]{1,0:T(8,128)(2,1)S(1)}) custom-call(bf16[16,320,128]{2,1,0:T(8,128)(2,1)S(1)} %all-to-all-done.1.refs_0_, bf16[3072,128]{1,0:T(8,128)(2,1)S(1)} %get-tuple-element.44.refs_1_, bf16[3072,128]{1,0:T(8,128)(2,1)S(1)} %get-tuple-element.45.refs_2_, ...), custom_call_target="tpu_custom_call" | custom-call | tf_op jit(solution)/shard_map/pallas_call | solution.py:59
  104.9 15.2 %all_to_all.30.refs_1_ = bf16[16,160,128]{2,1,0:T(8,128)(2,1)S(1)} all-to-all(bf16[16,160,128]{2,1,0:T(8,128)(2,1)} %get-tuple-element.56), channel_id=1, replica_groups=mesh['sp_0'=16,'sp_1'=2,'tp'=16] {'tp'}, dimensions={0} | all-to-all | bytes 1310720 | tf_op jit(solution)/shard_map/all_to_all | solution.py:470
  120.2 1.5 shard_map.185
  121.7 6.6 %all-to-all-start.3 = ((bf16[32,24,128]{2,1,0:T(8,128)(2,1)}), bf16[32,24,128]{2,1,0:T(8,128)(2,1)S(1)}, u32[]{:S(2)}, u32[]{:S(2)}) async-start(bf16[32,24,128]{2,1,0:T(8,128)(2,1)} %shard_map.185), calls=%async_computation.3 | async-start | bytes 393216 | tf_op jit(solution)/shard_map/all_to_all | solution.py:470
  128.3 1.9 shard_map.186.refs_1_
  130.2 17.0 %all-to-all-done.3.refs_0_ = bf16[32,24,128]{2,1,0:T(8,128)(2,1)S(1)} async-done(((bf16[32,24,128]{2,1,0:T(8,128)(2,1)}), bf16[32,24,128]{2,1,0:T(8,128)(2,1)S(1)}, u32[]{:S(2)}, u32[]{:S(2)}) %all-to-all-start.3) | async-done | bytes 196640 | tf_op jit(solution)/shard_map/all_to_all | solution.py:470
  147.3 2.3 %shard_map.187.refs_6_.refs_5_ = bf16[16,256,128]{2,1,0:T(8,128)(2,1)} custom-call(bf16[32,24,128]{2,1,0:T(8,128)(2,1)S(1)} %all-to-all-done.3.refs_0_, bf16[256,768]{1,0:T(8,128)(2,1)} %shard_map.186.refs_1_, bf16[256,128]{1,0:T(8,128)(2,1)} %refs_2_.4), custom_call_target="tpu_custom_call" | custom-call | tf_op jit(solution)/shard_map/pallas_call | solution.py:59
  149.6 4.3 %all-to-all-start.4 = ((bf16[16,256,128]{2,1,0:T(8,128)(2,1)}), bf16[16,256,128]{2,1,0:T(8,128)(2,1)}, u32[]{:S(2)}, u32[]{:S(2)}) async-start(bf16[16,256,128]{2,1,0:T(8,128)(2,1)} %shard_map.187.refs_6_.refs_5_), calls=%async_computation.4 | async-start | bytes 2097152 | tf_op jit(solution)/shard_map/all_to_all | solution.py:470
  153.9 4.9 %shard_map.183 = (f32[3072,128]{1,0:T(8,128)}, f32[3072,128]{1,0:T(8,128)}, bf16[6144,128]{1,0:T(8,128)(2,1)}, bf16[6144,128]{1,0:T(8,128)(2,1)}, bf16[3072,128]{1,0:T(8,128)(2,1)}, /*index=5*/bf16[3072,128]{1,0:T(8,128)(2,1)}) custom-call(bf16[16,320,128]{2,1,0:T(8,128)(2,1)S(1)} %all-to-all-done.1.refs_0_, bf16[160,1024]{1,0:T(8,128)(2,1)S(1)} %copy-done.9, ...), custom_call_target="tpu_custom_call" | custom-call | tf_op jit(solution)/shard_map/pallas_call | solution.py:59
  158.8 4.4 %collective-permute-start.6 = (bf16[6144,128]{1,0:T(8,128)(2,1)}, bf16[6144,128]{1,0:T(8,128)(2,1)S(1)}, u32[]{:S(2)}, u32[]{:S(2)}) collective-permute-start(bf16[6144,128]{1,0:T(8,128)(2,1)} %get-tuple-element.50), channel_id=1, source_target_pairs={{0,3},{16,28},{1,0},{17,29},{2,1},{18,30},{3,2},{19,31},{4,7},{20,... | collective-permute-start | bytes 4718600 | tf_op jit(solution)/shard_map/ppermute | solution.py:483
  163.2 1.9 collective-permute-start.7
  165.1 3.0 %shard_map.189 = (bf16[256,128]{1,0:T(8,128)(2,1)S(1)}, f32[4,128,64]{2,1,0:T(8,128)}) custom-call(bf16[32,24,128]{2,1,0:T(8,128)(2,1)S(1)} %all-to-all-done.3.refs_0_, bf16[64,256]{1,0:T(8,128)(2,1)} %bitcast.27, bf16[64,256]{1,0:T(8,128)(2,1)} %bitcast.25, bf16[256,128]{1,0:T(8,128)(2,1)} %refs_8_.1, f32[64,256]{1,0:T(8,128)} %bitcast.18, ...), custom_call_target="tpu_custom_call" | custom-call | tf_op jit(solution)/shard_map/pallas_call | solution.py:59
  168.1 1.5 all-to-all-done.4.refs_1_
  169.6 2.9 %shard_map.190 = (f32[256,128]{1,0:T(8,128)S(1)}, f32[32,128]{1,0:T(8,128)S(1)}, bf16[1088,128]{1,0:T(8,128)(2,1)S(1)}, f32[1024,128]{1,0:T(8,128)S(1)}) custom-call(s32[3]{0:T(128)S(1)} %pad_add_fusion.refs_0_, bf16[16,256,128]{2,1,0:T(8,128)(2,1)} %all-to-all-done.4.refs_1_, bf16[2048,128]{1,0:T(8,128)(2,1)} %refs_2_.5, ...), custom_call_target="tpu_custom_call" | custom-call | tf_op jit(solution)/shard_map/pallas_call | solution.py:59
  172.5 5.0 %collective-permute-start.10 = (bf16[1088,128]{1,0:T(8,128)(2,1)S(1)}, bf16[1088,128]{1,0:T(8,128)(2,1)S(1)}, u32[]{:S(2)}, u32[]{:S(2)}) collective-permute-start(bf16[1088,128]{1,0:T(8,128)(2,1)S(1)} %get-tuple-element.63), channel_id=1, source_target_pairs={{0,16},{16,0},{1,17},{17,1},{2,18},{18,2},{3,19},{19,3},{4,20},{20... | collective-permute-start | bytes 835592 | tf_op jit(solution)/shard_map/ppermute | solution.py:614
  177.5 1.2 collective-permute-done.10.refs_1_
  178.7 1.6 shard_map.191
  180.8 3.9 %all-to-all-start.5 = ((bf16[16,96,128]{2,1,0:T(8,128)(2,1)}), bf16[16,96,128]{2,1,0:T(8,128)(2,1)S(1)}, u32[]{:S(2)}, u32[]{:S(2)}) async-start(bf16[16,96,128]{2,1,0:T(8,128)(2,1)} %get-tuple-element.67), calls=%async_computation.5 | async-start | bytes 786432 | tf_op jit(solution)/shard_map/all_to_all | solution.py:470
  185.0 2.0 collective-permute-done.7.refs_3_
  187.0 1.9 shard_map.184
  188.9 1.9 collective-permute-start.8
  190.9 4.6 %collective-permute-start.9 = (bf16[3072,128]{1,0:T(8,128)(2,1)S(1)}, bf16[3072,128]{1,0:T(8,128)(2,1)S(1)}, u32[]{:S(2)}, u32[]{:S(2)}) collective-permute-start(bf16[3072,128]{1,0:T(8,128)(2,1)S(1)} %get-tuple-element.55), channel_id=1, source_target_pairs={{0,3},{16,28},{1,0},{17,29},{2,1},{18,30},{3,2},{19,31},{4,7},{20,... | collective-permute-start | bytes 2359304 | tf_op jit(solution)/shard_map/ppermute | solution.py:483
  195.4 7.7 %collective-permute-done.8.refs_4_ = bf16[3072,128]{1,0:T(8,128)(2,1)S(1)} collective-permute-done((bf16[3072,128]{1,0:T(8,128)(2,1)S(1)}, bf16[3072,128]{1,0:T(8,128)(2,1)S(1)}, u32[]{:S(2)}, u32[]{:S(2)}) %collective-permute-start.8) | collective-permute-done | bytes 786464 | tf_op jit(solution)/shard_map/ppermute | solution.py:483
  203.2 1.2 collective-permute-done.9.refs_5_
  204.3 3.4 %shard_map.188 = (bf16[2048,128]{1,0:T(8,128)(2,1)}, bf16[2048,128]{1,0:T(8,128)(2,1)}, bf16[128,2048]{1,0:T(8,128)(2,1)}) custom-call(f32[3072,128]{1,0:T(8,128)} %get-tuple-element.48.refs_0_, f32[3072,128]{1,0:T(8,128)} %get-tuple-element.49.refs_1_, bf16[6144,128]{1,0:T(8,128)(2,1)S(1)} %collective-permute-done.6.refs_2_, ...), custom_call_target="tpu_custom_call" | custom-call | tf_op jit(solution)/shard_map/pallas_call | solution.py:59
  207.7 0.9 copy-done.11
  209.4 3.8 %shard_map.192 = (f32[64,128]{1,0:T(8,128)}, bf16[64,256]{1,0:T(8,128)(2,1)}, bf16[64,256]{1,0:T(8,128)(2,1)}, bf16[256,128]{1,0:T(8,128)(2,1)}, f32[64,256]{1,0:T(8,128)}) custom-call(s32[3]{0:T(128)S(1)} %pad_add_fusion.refs_0_, bf16[16,96,128]{2,1,0:T(8,128)(2,1)S(1)} %all-to-all-done.5.refs_1_, f32[32,128]{1,0:T(8,128)S(1)} %copy-done.13, ...), custom_call_target="tpu_custom_call" | custom-call | tf_op jit(solution)/shard_map/pallas_call | solution.py:59
  (28 shorter events, 4.0 us)
Async XLA Ops:
  4.4 44.5 %all-to-all-start = ((bf16[32,48,128]{2,1,0:T(8,128)(2,1)}), bf16[32,48,128]{2,1,0:T(8,128)(2,1)S(1)}, u32[]{:S(2)}, u32[]{:S(2)}) async-start(bf16[32,48,128]{2,1,0:T(8,128)(2,1)} %get-tuple-element.42), calls=%async_computation | async-start | bytes 786432 | tf_op jit(solution)/shard_map/all_to_all | solution.py:470
  22.7 41.4 %collective-permute-start = (bf16[3072,128]{1,0:T(8,128)(2,1)S(1)}, bf16[3072,128]{1,0:T(8,128)(2,1)}, u32[]{:S(2)}, u32[]{:S(2)}) collective-permute-start(bf16[3072,128]{1,0:T(8,128)(2,1)S(1)} %get-tuple-element.44.refs_1_), channel_id=1, source_target_pairs={{0,1},{16,20},{1,2},{17,21},{2,3},{18,22},{3,0},{19,23},{4,5},{20,... | collective-permute-start | bytes 2359304 | tf_op jit(solution)/shard_map/ppermute | solution.py:483
  25.9 40.4 %collective-permute-start.3 = (bf16[3072,128]{1,0:T(8,128)(2,1)S(1)}, bf16[3072,128]{1,0:T(8,128)(2,1)}, u32[]{:S(2)}, u32[]{:S(2)}) collective-permute-start(bf16[3072,128]{1,0:T(8,128)(2,1)S(1)} %get-tuple-element.45.refs_2_), channel_id=1, source_target_pairs={{0,3},{16,28},{1,0},{17,29},{2,1},{18,30},{3,2},{19,31},{4,7},{20,... | collective-permute-start | bytes 2359304 | tf_op jit(solution)/shard_map/ppermute | solution.py:483
  51.0 43.5 %all-to-all-start.1 = ((bf16[16,320,128]{2,1,0:T(8,128)(2,1)}), bf16[16,320,128]{2,1,0:T(8,128)(2,1)S(1)}, u32[]{:S(2)}, u32[]{:S(2)}) async-start(bf16[16,320,128]{2,1,0:T(8,128)(2,1)} %get-tuple-element.43.refs_1_), calls=%async_computation.1 | async-start | bytes 2621440 | tf_op jit(solution)/shard_map/all_to_all | solution.py:470
  57.7 25.3 %collective-permute-start.2 = (bf16[3072,128]{1,0:T(8,128)(2,1)S(1)}, bf16[3072,128]{1,0:T(8,128)(2,1)S(1)}, u32[]{:S(2)}, u32[]{:S(2)}) collective-permute-start(bf16[3072,128]{1,0:T(8,128)(2,1)S(1)} %get-tuple-element.44.refs_1_), channel_id=1, source_target_pairs={{0,3},{16,28},{1,0},{17,29},{2,1},{18,30},{3,2},{19,31},{4,7},{20,... | collective-permute-start | bytes 2359304 | tf_op jit(solution)/shard_map/ppermute | solution.py:483
  62.2 22.3 %collective-permute-start.1 = (bf16[3072,128]{1,0:T(8,128)(2,1)S(1)}, bf16[3072,128]{1,0:T(8,128)(2,1)S(1)}, u32[]{:S(2)}, u32[]{:S(2)}) collective-permute-start(bf16[3072,128]{1,0:T(8,128)(2,1)S(1)} %get-tuple-element.45.refs_2_), channel_id=1, source_target_pairs={{0,1},{16,20},{1,2},{17,21},{2,3},{18,22},{3,0},{19,23},{4,5},{20,... | collective-permute-start | bytes 2359304 | tf_op jit(solution)/shard_map/ppermute | solution.py:483
  64.2 28.5 %collective-permute-start.4 = (bf16[3072,128]{1,0:T(8,128)(2,1)}, bf16[3072,128]{1,0:T(8,128)(2,1)S(1)}, u32[]{:S(2)}, u32[]{:S(2)}) collective-permute-start(bf16[3072,128]{1,0:T(8,128)(2,1)} %collective-permute-done.refs_3_), channel_id=1, source_target_pairs={{0,1},{16,20},{1,2},{17,21},{2,3},{18,22},{3,0},{19,23},{4,5},{20,... | collective-permute-start | bytes 2359304 | tf_op jit(solution)/shard_map/ppermute | solution.py:483
  66.3 27.3 %collective-permute-start.5 = (bf16[3072,128]{1,0:T(8,128)(2,1)}, bf16[3072,128]{1,0:T(8,128)(2,1)S(1)}, u32[]{:S(2)}, u32[]{:S(2)}) collective-permute-start(bf16[3072,128]{1,0:T(8,128)(2,1)} %collective-permute-done.3.refs_6_), channel_id=1, source_target_pairs={{0,3},{16,28},{1,0},{17,29},{2,1},{18,30},{3,2},{19,31},{4,7},{20,... | collective-permute-start | bytes 2359304 | tf_op jit(solution)/shard_map/ppermute | solution.py:483
  83.0 0.9 copy-start
  84.5 0.9 copy-start.2
  92.7 0.9 copy-start.4
  93.6 0.9 copy-start.6
  94.5 1.1 copy-start.1
  95.6 1.1 copy-start.3
  96.7 1.1 copy-start.5
  97.9 1.1 copy-start.7
  104.2 0.7 copy-start.8
  121.7 25.6 %all-to-all-start.3 = ((bf16[32,24,128]{2,1,0:T(8,128)(2,1)}), bf16[32,24,128]{2,1,0:T(8,128)(2,1)S(1)}, u32[]{:S(2)}, u32[]{:S(2)}) async-start(bf16[32,24,128]{2,1,0:T(8,128)(2,1)} %shard_map.185), calls=%async_computation.3 | async-start | bytes 393216 | tf_op jit(solution)/shard_map/all_to_all | solution.py:470
  130.2 23.7 %copy-start.9 = (bf16[160,1024]{1,0:T(8,128)(2,1)S(1)}, bf16[160,1024]{1,0:T(8,128)(2,1)}, u32[]{:S(2)}) copy-start(bf16[160,1024]{1,0:T(8,128)(2,1)} %copy-done.8) | copy-start | bytes 983044
  149.6 20.0 %all-to-all-start.4 = ((bf16[16,256,128]{2,1,0:T(8,128)(2,1)}), bf16[16,256,128]{2,1,0:T(8,128)(2,1)}, u32[]{:S(2)}, u32[]{:S(2)}) async-start(bf16[16,256,128]{2,1,0:T(8,128)(2,1)} %shard_map.187.refs_6_.refs_5_), calls=%async_computation.4 | async-start | bytes 2097152 | tf_op jit(solution)/shard_map/all_to_all | solution.py:470
  158.8 26.2 %collective-permute-start.6 = (bf16[6144,128]{1,0:T(8,128)(2,1)}, bf16[6144,128]{1,0:T(8,128)(2,1)S(1)}, u32[]{:S(2)}, u32[]{:S(2)}) collective-permute-start(bf16[6144,128]{1,0:T(8,128)(2,1)} %get-tuple-element.50), channel_id=1, source_target_pairs={{0,3},{16,28},{1,0},{17,29},{2,1},{18,30},{3,2},{19,31},{4,7},{20,... | collective-permute-start | bytes 4718600 | tf_op jit(solution)/shard_map/ppermute | solution.py:483
  163.2 23.8 %collective-permute-start.7 = (bf16[6144,128]{1,0:T(8,128)(2,1)}, bf16[6144,128]{1,0:T(8,128)(2,1)S(1)}, u32[]{:S(2)}, u32[]{:S(2)}) collective-permute-start(bf16[6144,128]{1,0:T(8,128)(2,1)} %get-tuple-element.51), channel_id=1, source_target_pairs={{0,1},{16,20},{1,2},{17,21},{2,3},{18,22},{3,0},{19,23},{4,5},{20,... | collective-permute-start | bytes 4718600 | tf_op jit(solution)/shard_map/ppermute | solution.py:483
  172.5 7.8 %copy-start.10 = (f32[256,128]{1,0:T(8,128)}, f32[256,128]{1,0:T(8,128)S(1)}, u32[]{:S(2)}) copy-start(f32[256,128]{1,0:T(8,128)S(1)} %get-tuple-element.69.refs_4_) | copy-start | bytes 393220
  172.5 6.2 %collective-permute-start.10 = (bf16[1088,128]{1,0:T(8,128)(2,1)S(1)}, bf16[1088,128]{1,0:T(8,128)(2,1)S(1)}, u32[]{:S(2)}, u32[]{:S(2)}) collective-permute-start(bf16[1088,128]{1,0:T(8,128)(2,1)S(1)} %get-tuple-element.63), channel_id=1, source_target_pairs={{0,16},{16,0},{1,17},{17,1},{2,18},{18,2},{3,19},{19,3},{4,20},{20... | collective-permute-start | bytes 835592 | tf_op jit(solution)/shard_map/ppermute | solution.py:614
  180.2 0.6 copy-start.12
  180.8 26.9 %all-to-all-start.5 = ((bf16[16,96,128]{2,1,0:T(8,128)(2,1)}), bf16[16,96,128]{2,1,0:T(8,128)(2,1)S(1)}, u32[]{:S(2)}, u32[]{:S(2)}) async-start(bf16[16,96,128]{2,1,0:T(8,128)(2,1)} %get-tuple-element.67), calls=%async_computation.5 | async-start | bytes 786432 | tf_op jit(solution)/shard_map/all_to_all | solution.py:470
  188.9 14.2 %collective-permute-start.8 = (bf16[3072,128]{1,0:T(8,128)(2,1)S(1)}, bf16[3072,128]{1,0:T(8,128)(2,1)S(1)}, u32[]{:S(2)}, u32[]{:S(2)}) collective-permute-start(bf16[3072,128]{1,0:T(8,128)(2,1)S(1)} %get-tuple-element.54), channel_id=1, source_target_pairs={{0,1},{16,20},{1,2},{17,21},{2,3},{18,22},{3,0},{19,23},{4,5},{20,... | collective-permute-start | bytes 2359304 | tf_op jit(solution)/shard_map/ppermute | solution.py:483
  190.9 13.5 %collective-permute-start.9 = (bf16[3072,128]{1,0:T(8,128)(2,1)S(1)}, bf16[3072,128]{1,0:T(8,128)(2,1)S(1)}, u32[]{:S(2)}, u32[]{:S(2)}) collective-permute-start(bf16[3072,128]{1,0:T(8,128)(2,1)S(1)} %get-tuple-element.55), channel_id=1, source_target_pairs={{0,3},{16,28},{1,0},{17,29},{2,1},{18,30},{3,2},{19,31},{4,7},{20,... | collective-permute-start | bytes 2359304 | tf_op jit(solution)/shard_map/ppermute | solution.py:483
  207.7 0.9 copy-start.11
  208.6 0.7 copy-start.13

commit v6 on v5

--- a/solution.py
+++ b/solution.py
@@ -44,7 +44,7 @@
     return lax.broadcasted_iota(jnp.int32, shape, dim)
 
 
-def call(fn, outs, *args, scratch=(), smem=(), near=(), near_out=(), after=()):
+def call(fn, outs, *args, scratch=(), smem=(), near=(), near_out=(), after=(), raw=()):
     spaces = [pltpu.VMEM if k in near else pltpu.HBM for k in range(len(args))]
     args = [
         a if k in smem else pltpu.with_memory_space_constraint(a, spaces[k])
@@ -62,7 +62,9 @@
             (pltpu.VMEM if k in near_out else pltpu.HBM)(s, d) for k, (s, d) in enumerate(outs)
         ),
         in_specs=[
-            pl.BlockSpec(memory_space=pltpu.SMEM if k in smem else pltpu.VMEM)
+            pl.BlockSpec(
+                memory_space=pltpu.SMEM if k in smem else pltpu.HBM if k in raw else pltpu.VMEM
+            )
             for k in range(count)
         ]
         + [pl.BlockSpec(memory_space=pltpu.HBM) for _ in after],
@@ -91,10 +93,17 @@
     return jnp.concatenate([both, both], axis=0) * own
 
 
+def picked_sums(mask, values):
+    high = values.astype(BF).astype(F32)
+    middle = (values - high).astype(BF).astype(F32)
+    sums = mm(mask, jnp.concatenate([high, middle, values - high - middle], axis=1))
+    return sums[:, :64] + sums[:, 64:128] + sums[:, 128:192]
+
+
 def block_sums(decay):
     row, col = iota((TOK, TOK), 0), iota((TOK, TOK), 1)
     within = ((row // BLOCK == col // BLOCK) & (col <= row)).astype(F32)
-    return mm_exact(within, decay)
+    return picked_sums(within, decay)
 
 
 def whole_sums(cumulative):
@@ -209,28 +218,39 @@
 
 
 def partial_kernel(rows_ref, *refs):
-    lots, (part_ref, grads_ref, hidden_ref) = refs[:8], refs[8:]
-    gates, downs = [], []
-    for a_ref, b_ref in zip(lots[::2], lots[1::2]):
-        gates += [a_ref[:2048, :], jnp.concatenate([a_ref[2048:, :], b_ref[:1024, :]], axis=0)]
-        downs.append([b_ref[1024 + k * 128 : 1152 + k * 128, :] for k in range(N_TP)])
-    weight = jnp.concatenate(gates, axis=1)
-    down = jnp.concatenate([jnp.concatenate(d, axis=1) for d in downs], axis=0)
-    pre = mm(wide(rows_ref, 0, PART), weight)
-    hidden_grad = mm(wide(rows_ref, PART, PART), down, NT)
-    grads = []
+    lots, (part_ref, grads_ref, hidden_ref, held, done) = refs[:8], refs[8:]
+    copies = [pltpu.make_async_copy(lots[i], held.at[i], done.at[i]) for i in range(8)]
+    for copy in copies:
+        copy.start()
+    x, g = wide(rows_ref, 0, PART), wide(rows_ref, PART, PART)
     for b in range(4):
-        gate_pre, up_pre = pre[:, 256 * b : 256 * b + 128], pre[:, 256 * b + 128 : 256 * b + 256]
-        upper = hidden_grad[:, 128 * b : 128 * b + 128]
+        copies[2 * b].wait()
+        copies[2 * b + 1].wait()
+        gate_weight = held[2 * b, :2048, :]
+        up_weight = jnp.concatenate([held[2 * b, 2048:, :], held[2 * b + 1, :1024, :]], axis=0)
+        blocks = [held[2 * b + 1, 1024 + k * 128 : 1152 + k * 128, :] for k in range(N_TP)]
+        pre = mm(x, jnp.concatenate([gate_weight, up_weight], axis=1))
+        upper = mm(g, jnp.concatenate(blocks, axis=1), NT)
+        gate_pre, up_pre = pre[:, :128], pre[:, 128:]
         sigmoid = jax.nn.sigmoid(gate_pre)
         activated = gate_pre * sigmoid
         hidden_ref[:, 128 * b : 128 * b + 128] = (activated * up_pre).astype(BF)
         gate = upper * up_pre * sigmoid * (1.0 + gate_pre * (1.0 - sigmoid))
-        grads += [gate.astype(BF), (upper * activated).astype(BF)]
-    grads = jnp.concatenate(grads, axis=1)
-    grads_ref[...] = grads
+        grads_ref[:, 256 * b : 256 * b + 128] = gate.astype(BF)
+        grads_ref[:, 256 * b + 128 : 256 * b + 256] = (upper * activated).astype(BF)
+    grads = grads_ref[...]
+
+    def up_rows(b, at):
+        if at < 1024:
+            return held[2 * b, 2048 + at : 2304 + at, :]
+        return held[2 * b + 1, at - 1024 : at - 768, :]
+
     for k in range(0, N_TP, 2):
-        part = mm(grads, weight[k * 128 : (k + 2) * 128], NT).astype(BF)
+        at = k * 128
+        weight = []
+        for b in range(4):
+            weight += [held[2 * b, at : at + 256, :], up_rows(b, at)]
+        part = mm(grads, jnp.concatenate(weight, axis=1), NT).astype(BF)
         part_ref[k] = part[:, :128]
         part_ref[k + 1] = part[:, 128:]
 
@@ -398,31 +418,23 @@
         sent_ref[z, 32:, :] = (kept_ref[here, :] + recv_ref[here, :].astype(F32)).astype(BF)
 
 
-def backward_kernel(
-    place_ref,
-    later_ref,
-    other_ref,
-    reach_ref,
+def local_backward_kernel(
     grad_ref,
     entering_ref,
     q_ref,
     k_ref,
     v_ref,
     decay_ref,
-    gp_ref,
     gq_ref,
-    gk_ref,
-    gv_ref,
-    gd_ref,
+    value_ref,
+    keys_ref,
+    change_ref,
+    tail_ref,
+    reach_ref,
+    rest_ref,
+    leave_ref,
 ):
     key_mask, val_mask, own = head_masks()
-    sums = later_ref[0].astype(F32)
-    for z in range(1, 16):
-        sums = sums + later_ref[z].astype(F32)
-    gp_ref[...] = sums[32:]
-    packed = sums[:32]
-    packed = jnp.where(place_ref[1] == 0, reach_ref[17:18, :] * packed + other_ref[...], packed)
-    state_grad = opened_state(packed, own)
     grad = grad_ref[...]
     queries = q_ref[...].astype(F32).T
     keys = k_ref[...].astype(F32).T * SCALE
@@ -442,11 +454,15 @@
         value_grad = value_grad + mm(scores, grad * val_mask[h], TN)
         query_grad = query_grad + mm(score_grad, scaled_k * key_mask[h])
         key_grad = key_grad + mm(score_grad, scaled_q * key_mask[h], TN)
-    carried_v, carried_q, tail_grad, close_grad = ([None] * NBLK for _ in range(4))
+    carried_v, carried_q, tail_grad, close_grad, reach = ([None] * NBLK for _ in range(5))
+    state_grad, later = jnp.zeros((128, 64), F32), jnp.zeros((1, 64), F32)
     for n in reversed(range(NBLK)):
         here = slice(n * BLOCK, (n + 1) * BLOCK)
         entering = entering_ref[n]
         decay_out = jnp.exp(closing[n])
+        reach[n] = jnp.exp(later)
+        later = later + closing[n]
+        leave_ref[n : n + 1, :] = jnp.exp(later)
         carried_v[n] = mm(tail[here], state_grad, NT)
         carried_q[n] = mm(grad[here], entering)
         tail_grad[n] = mm(values[here], state_grad)
@@ -454,16 +470,59 @@
             tail_grad[n] * tail[here], axis=0, keepdims=True
         )
         state_grad = decay_out * state_grad + mm(grad[here], scaled_q[here], TN) * own
-    value_grad = value_grad + jnp.concatenate(carried_v, axis=0)
+    value_ref[...] = value_grad + jnp.concatenate(carried_v, axis=0)
     query_grad = query_grad + jnp.concatenate(carried_q, axis=0)
     tail_grad = jnp.concatenate(tail_grad, axis=0)
     change = query_grad * scaled_q - key_grad * scaled_k - tail_grad * tail
     row, col = iota((TOK, TOK), 0), iota((TOK, TOK), 1)
     onward = ((row // BLOCK == col // BLOCK) & (col >= row)).astype(F32)
-    gd_ref[...] = (mm_exact(onward, change) + per_block(close_grad)).T
+    change_ref[...] = picked_sums(onward, change) + per_block(close_grad)
     gq_ref[...] = (query_grad * grow).T.astype(BF)
-    gk_ref[...] = ((key_grad * shrink + tail_grad * rest) * SCALE).T.astype(BF)
-    gv_ref[...] = value_grad.astype(BF)
+    keys_ref[...] = (key_grad * shrink + tail_grad * rest) * SCALE
+    tail_ref[...] = tail
+    reach_ref[...] = per_block(reach)
+    rest_ref[...] = rest * SCALE
+
+
+def backward_kernel(
+    place_ref,
+    later_ref,
+    other_ref,
+    chips_ref,
+    entering_ref,
+    v_ref,
+    value_ref,
+    keys_ref,
+    change_ref,
+    tail_ref,
+    reach_ref,
+    rest_ref,
+    leave_ref,
+    gp_ref,
+    gk_ref,
+    gv_ref,
+    gd_ref,
+):
+    _, _, own = head_masks()
+    sums = later_ref[0].astype(F32)
+    for z in range(1, 16):
+        sums = sums + later_ref[z].astype(F32)
+    gp_ref[...] = sums[32:]
+    packed = sums[:32]
+    packed = jnp.where(place_ref[1] == 0, chips_ref[17:18, :] * packed + other_ref[...], packed)
+    state_grad = opened_state(packed, own)
+    tail, reach = tail_ref[...], reach_ref[...]
+    gv_ref[...] = (value_ref[...] + mm(tail * reach, state_grad, NT)).astype(BF)
+    tail_grad = mm(v_ref[...], state_grad) * reach
+    gk_ref[...] = (keys_ref[...] + tail_grad * rest_ref[...]).T.astype(BF)
+    row, col = iota((TOK, TOK), 0), iota((TOK, TOK), 1)
+    ahead = ((row // BLOCK == col // BLOCK) & (col < row)).astype(F32)
+    passed = [
+        leave_ref[n : n + 1, :] * jnp.sum(state_grad * entering_ref[n], axis=0, keepdims=True)
+        for n in range(NBLK)
+    ]
+    change = change_ref[...] + picked_sums(ahead, tail_grad * tail) + per_block(passed)
+    gd_ref[...] = change.T
 
 
 def exchanged(blocks, axis):
@@ -515,12 +574,7 @@
     )
     recv = exchanged(sent, SP)
     own_a, own_b = call(
-        pack_kernel,
-        [((LOT, 128), BF), ((LOT, 128), BF)],
-        w_gate[0],
-        w_up[0],
-        w_down[0],
-        near_out=(0, 1),
+        pack_kernel, [((LOT, 128), BF), ((LOT, 128), BF)], w_gate[0], w_up[0], w_down[0]
     )
     left_a = passed_on(own_a, 1)
     right_b = passed_on(own_b, -1)
@@ -546,8 +600,10 @@
         [((N_TP, PART, 128), BF), ((PART, 1024), BF), ((PART, 512), BF)],
         rows,
         *weights,
-        near=tuple(range(9)),
+        scratch=[pltpu.VMEM((8, LOT, 128), BF), pltpu.SemaphoreType.DMA((8,))],
+        near=(0,),
         near_out=(1, 2),
+        raw=tuple(range(1, 9)),
     )
     arrived = exchanged(partial_rows, "tp")
     own_grad_a, own_grad_b, to_left, to_right, left_lot, right_lot = call(
@@ -561,6 +617,20 @@
     )
     from_left = passed_on(to_right, 1)
     from_right = passed_on(to_left, -1)
+    (returned,) = call(
+        row_sum_kernel,
+        [((N_SP, PAD, 128), BF)],
+        place,
+        arrived,
+        states,
+        near_out=(0,),
+        smem=(0,),
+        near=(1,),
+        scratch=[pltpu.VMEM((ROWS + 8, 128), F32)],
+    )
+    back = exchanged(returned, SP)
+    (residual,) = call(residual_kernel, [((N_TP, TOK, 128), BF)], back, turned, out_grad, near=(0,))
+    full_grad = exchanged(residual, "tp")
     lot_left, lot_right = call(
         relay_kernel,
         2 * [((LOT, 128), BF)],
@@ -568,24 +638,12 @@
         right_lot,
         from_right,
         from_left,
+        after=(residual,),
         near=(2, 3),
         near_out=(0, 1),
     )
     last_a = passed_on(lot_right, 1)
     last_b = passed_on(lot_left, -1)
-    (returned,) = call(
-        row_sum_kernel,
-        [((N_SP, PAD, 128), BF)],
-        place,
-        arrived,
-        states,
-        smem=(0,),
-        near=(1,),
-        scratch=[pltpu.VMEM((ROWS + 8, 128), F32)],
-    )
-    back = exchanged(returned, SP)
-    (residual,) = call(residual_kernel, [((N_TP, TOK, 128), BF)], back, turned, out_grad, near=(0,))
-    full_grad = exchanged(residual, "tp")
     mixer_out, entering = call(
         forward_kernel,
         [((TOK, 128), BF), ((NBLK, 128, 64), F32)],
@@ -609,7 +667,7 @@
         decay_t,
         smem=(0,),
         near=(1, 3),
-        near_out=(0, 1, 2, 3),
+        near_out=(1, 2, 3),
     )
     from_other = lax.ppermute(to_other, "sp_1", [(0, 1), (1, 0)])
     chip_sent, other_grad = call(
@@ -622,24 +680,40 @@
         reach,
         smem=(0,),
         near=(1, 2, 3),
-        near_out=(1,),
     )
     later = exchanged(chip_sent, "sp_0")
-    grad_proj, gq, gk, gv, gd = call(
-        backward_kernel,
-        [((64, 128), F32), ((64, TOK), BF), ((64, TOK), BF), ((TOK, 128), BF), ((64, TOK), F32)],
-        place,
-        later,
-        other_grad,
-        reach,
+    gq, *local = call(
+        local_backward_kernel,
+        [
+            ((64, TOK), BF),
+            ((TOK, 128), F32),
+            ((TOK, 64), F32),
+            ((TOK, 64), F32),
+            ((TOK, 64), F32),
+            ((TOK, 64), F32),
+            ((TOK, 64), F32),
+            ((NBLK, 64), F32),
+        ],
         mixer_grad,
         entering,
         q_t,
         k_t,
         value_rows,
         decay_t,
+        after=(chip_sent,),
+    )
+    grad_proj, gk, gv, gd = call(
+        backward_kernel,
+        [((64, 128), F32), ((64, TOK), BF), ((TOK, 128), BF), ((64, TOK), F32)],
+        place,
+        later,
+        other_grad,
+        reach,
+        entering,
+        value_rows,
+        *local,
         smem=(0,),
-        near=(1, 2, 4),
+        near=(1,),
     )
     gate_part, up_part, down_part = call(
         grad_sum_kernel,
@@ -651,7 +725,7 @@
         last_a,
         last_b,
         near=(2, 3, 4, 5),
-        after=(residual,),
+        after=(chip_sent,),
     )
     return (gate_part[None], up_part[None], down_part[None], grad_proj, gq.T, gk.T, gv, gd.T)
 

time: 217 us -> 208 us (0.959)
  local copies, waits for them, and re-layouts: 11.1 us -> 0.93 us
  Pallas kernels: 39.7 us -> 43 us
  waiting for transfers between devices: 70.7 us -> 68.1 us
    unnamed x28 -> x10, local copies, waits for them, and re-layouts: 11.1 us -> 0.93 us
    pallas_call x14 -> x15, Pallas kernels: 39.7 us -> 43 us  [call(): pl.pallas_call(run, out_shape=tuple(((pltpu.VMEM if k in near_out else pl...]
  transfers between devices with their start and end apart: 16 -> 16, of which waited for: 11 -> 11; matrix products, arithmetic and copies ran while one was open for 0% -> 0% of each run, Pallas kernels for 11% -> 13%
where the time goes in v6:
time: 208 us; the launch traced here: 204 us
  starting transfers between devices  75.6 us (36%)
  waiting for transfers between devices  68.1 us (33%)
  Pallas kernels  43 us (21%)
  blocking collectives  15.7 us (8%)
    pallas_call x15, Pallas kernels, call(): pl.pallas_call(run, out_shape=tuple(((pltpu.VMEM if k in near_out else pl...  43 us
    all_to_all x5, starting transfers between devices, exchanged(): return lax.all_to_all(blocks, axis, split_axis=0, concat_axis=0, tiled=True)  38 us
    all_to_all x5, waiting for transfers between devices, exchanged(): return lax.all_to_all(blocks, axis, split_axis=0, concat_axis=0, tiled=True)  37.2 us
    ppermute x10, starting transfers between devices, passed_on(): return lax.ppermute(array, ('sp_1', 'tp'), ring_step(step))  32.5 us
    ppermute x10, waiting for transfers between devices, passed_on(): return lax.ppermute(array, ('sp_1', 'tp'), ring_step(step))  29.7 us
    all_to_all x1, blocking collectives, exchanged(): return lax.all_to_all(blocks, axis, split_axis=0, concat_axis=0, tiled=True)  15.7 us
    ppermute x1, starting transfers between devices, body(): from_other = lax.ppermute(to_other, 'sp_1', [(0, 1), (1, 0)])  5.03 us
  transfers between devices with their start and end apart: 16, of which 11 were waited for; matrix products, arithmetic and copies ran while one was open for 0% of the time, Pallas kernels for 13%

profile of v6, /device:TPU:1, one launch (start us, length us, event | category | flops | bytes accessed | tf_op | source)
XLA Modules:
  0.0 204.4 jit_solution(1589761846454140808)
XLA Ops:
  0.6 3.5 %shard_map.179 = (bf16[32,48,128]{2,1,0:T(8,128)(2,1)}, bf16[768,256]{1,0:T(8,128)(2,1)}) custom-call(s32[2,256]{1,0:T(2,128)} %bitcast.30, f32[2,256]{1,0:T(2,128)} %bitcast.31, bf16[256,128]{1,0:T(8,128)(2,1)} %refs_2_.3, bf16[256,128]{1,0:T(8,128)(2,1)} %refs_2_.4, bf16[64,256]{1,0:T(8,128)(2,1)} %bitcast.24, bf16[256,128]{1,0:T(8,128)(2,1)} %refs_5_.3, ...), custom_call_target="tpu_custom_call" | custom-call | tf_op jit(solution)/shard_map/pallas_call | solution.py:59
  4.2 16.7 %all-to-all-start = ((bf16[32,48,128]{2,1,0:T(8,128)(2,1)}), bf16[32,48,128]{2,1,0:T(8,128)(2,1)S(1)}, u32[]{:S(2)}, u32[]{:S(2)}) async-start(bf16[32,48,128]{2,1,0:T(8,128)(2,1)} %get-tuple-element.49), calls=%async_computation | async-start | bytes 786432 | tf_op jit(solution)/shard_map/all_to_all | solution.py:529
  20.9 2.5 %shard_map.181 = (bf16[3072,128]{1,0:T(8,128)(2,1)}, bf16[3072,128]{1,0:T(8,128)(2,1)}) custom-call(bf16[2048,128]{1,0:T(8,128)(2,1)} %bitcast.21, bf16[2048,128]{1,0:T(8,128)(2,1)} %bitcast.22, bf16[128,2048]{1,0:T(8,128)(2,1)} %bitcast.23), custom_call_target="tpu_custom_call" | custom-call | tf_op jit(solution)/shard_map/pallas_call | solution.py:59
  23.4 3.3 %collective-permute-start = (bf16[3072,128]{1,0:T(8,128)(2,1)}, bf16[3072,128]{1,0:T(8,128)(2,1)}, u32[]{:S(2)}, u32[]{:S(2)}) collective-permute-start(bf16[3072,128]{1,0:T(8,128)(2,1)} %get-tuple-element.51.refs_1_), channel_id=1, source_target_pairs={{0,1},{16,20},{1,2},{17,21},{2,3},{18,22},{3,0},{19,23},{4,5},{20,... | collective-permute-start | bytes 2359304 | tf_op jit(solution)/shard_map/ppermute | solution.py:542
  26.8 3.4 %collective-permute-start.3 = (bf16[3072,128]{1,0:T(8,128)(2,1)}, bf16[3072,128]{1,0:T(8,128)(2,1)}, u32[]{:S(2)}, u32[]{:S(2)}) collective-permute-start(bf16[3072,128]{1,0:T(8,128)(2,1)} %get-tuple-element.52.refs_2_), channel_id=1, source_target_pairs={{0,3},{16,28},{1,0},{17,29},{2,1},{18,30},{3,2},{19,31},{4,7},{20,... | collective-permute-start | bytes 2359304 | tf_op jit(solution)/shard_map/ppermute | solution.py:542
  30.2 0.1 pad_add_fusion.refs_0_
  30.2 18.4 %all-to-all-done.refs_1_ = bf16[32,48,128]{2,1,0:T(8,128)(2,1)S(1)} async-done(((bf16[32,48,128]{2,1,0:T(8,128)(2,1)}), bf16[32,48,128]{2,1,0:T(8,128)(2,1)S(1)}, u32[]{:S(2)}, u32[]{:S(2)}) %all-to-all-start) | async-done | bytes 393248 | tf_op jit(solution)/shard_map/all_to_all | solution.py:529
  48.7 2.0 shard_map.180
  50.6 6.8 %all-to-all-start.1 = ((bf16[16,320,128]{2,1,0:T(8,128)(2,1)}), bf16[16,320,128]{2,1,0:T(8,128)(2,1)S(1)}, u32[]{:S(2)}, u32[]{:S(2)}) async-start(bf16[16,320,128]{2,1,0:T(8,128)(2,1)} %get-tuple-element.50.refs_1_), calls=%async_computation.1 | async-start | bytes 2621440 | tf_op jit(solution)/shard_map/all_to_all | solution.py:529
  57.4 4.5 %collective-permute-start.2 = (bf16[3072,128]{1,0:T(8,128)(2,1)S(1)}, bf16[3072,128]{1,0:T(8,128)(2,1)S(1)}, u32[]{:S(2)}, u32[]{:S(2)}) collective-permute-start(bf16[3072,128]{1,0:T(8,128)(2,1)S(1)} %copy-done), channel_id=1, source_target_pairs={{0,3},{16,28},{1,0},{17,29},{2,1},{18,30},{3,2},{19,31},{4,7},{20,... | collective-permute-start | bytes 2359304 | tf_op jit(solution)/shard_map/ppermute | solution.py:542
  61.9 1.9 collective-permute-start.1
  63.9 0.0 collective-permute-done.refs_3_
  63.9 2.1 %collective-permute-start.4 = (bf16[3072,128]{1,0:T(8,128)(2,1)}, bf16[3072,128]{1,0:T(8,128)(2,1)S(1)}, u32[]{:S(2)}, u32[]{:S(2)}) collective-permute-start(bf16[3072,128]{1,0:T(8,128)(2,1)} %collective-permute-done.refs_3_), channel_id=1, source_target_pairs={{0,1},{16,20},{1,2},{17,21},{2,3},{18,22},{3,0},{19,23},{4,5},{20,... | collective-permute-start | bytes 2359304 | tf_op jit(solution)/shard_map/ppermute | solution.py:542
  66.0 0.0 collective-permute-done.3.refs_6_
  66.0 4.3 %collective-permute-start.5 = (bf16[3072,128]{1,0:T(8,128)(2,1)}, bf16[3072,128]{1,0:T(8,128)(2,1)}, u32[]{:S(2)}, u32[]{:S(2)}) collective-permute-start(bf16[3072,128]{1,0:T(8,128)(2,1)} %collective-permute-done.3.refs_6_), channel_id=1, source_target_pairs={{0,3},{16,28},{1,0},{17,29},{2,1},{18,30},{3,2},{19,31},{4,7},{20,... | collective-permute-start | bytes 2359304 | tf_op jit(solution)/shard_map/ppermute | solution.py:542
  70.4 12.3 %collective-permute-done.2.refs_5_ = bf16[3072,128]{1,0:T(8,128)(2,1)S(1)} collective-permute-done((bf16[3072,128]{1,0:T(8,128)(2,1)S(1)}, bf16[3072,128]{1,0:T(8,128)(2,1)S(1)}, u32[]{:S(2)}, u32[]{:S(2)}) %collective-permute-start.2) | collective-permute-done | bytes 786464 | tf_op jit(solution)/shard_map/ppermute | solution.py:542
  82.7 1.5 collective-permute-done.1.refs_4_
  84.2 8.1 %collective-permute-done.4.refs_7_ = bf16[3072,128]{1,0:T(8,128)(2,1)S(1)} collective-permute-done((bf16[3072,128]{1,0:T(8,128)(2,1)}, bf16[3072,128]{1,0:T(8,128)(2,1)S(1)}, u32[]{:S(2)}, u32[]{:S(2)}) %collective-permute-start.4) | collective-permute-done | bytes 786464 | tf_op jit(solution)/shard_map/ppermute | solution.py:542
  92.3 0.9 copy-done.4
  93.3 0.0 collective-permute-done.5.refs_8_
  93.3 5.8 %shard_map.182 = (bf16[16,160,128]{2,1,0:T(8,128)(2,1)}, bf16[160,1024]{1,0:T(8,128)(2,1)S(1)}, bf16[160,512]{1,0:T(8,128)(2,1)S(1)}) custom-call(bf16[16,320,128]{2,1,0:T(8,128)(2,1)S(1)} %all-to-all-done.1.refs_0_, bf16[3072,128]{1,0:T(8,128)(2,1)} %get-tuple-element.51.refs_1_, bf16[3072,128]{1,0:T(8,128)(2,1)} %get-tuple-element.52.refs_2_, ...), custom_call_target="tpu_custom_call" | custom-call | tf_op jit(solution)/shard_map/pallas_call | solution.py:59
  99.1 15.7 %all_to_all.30.refs_1_ = bf16[16,160,128]{2,1,0:T(8,128)(2,1)S(1)} all-to-all(bf16[16,160,128]{2,1,0:T(8,128)(2,1)} %get-tuple-element.61), channel_id=1, replica_groups=mesh['sp_0'=16,'sp_1'=2,'tp'=16] {'tp'}, dimensions={0} | all-to-all | bytes 1310720 | tf_op jit(solution)/shard_map/all_to_all | solution.py:529
  114.8 1.5 shard_map.184
  116.3 6.2 %all-to-all-start.3 = ((bf16[32,24,128]{2,1,0:T(8,128)(2,1)}), bf16[32,24,128]{2,1,0:T(8,128)(2,1)S(1)}, u32[]{:S(2)}, u32[]{:S(2)}) async-start(bf16[32,24,128]{2,1,0:T(8,128)(2,1)} %shard_map.184), calls=%async_computation.3 | async-start | bytes 393216 | tf_op jit(solution)/shard_map/all_to_all | solution.py:529
  122.5 1.9 shard_map.185.refs_1_
  124.5 17.0 %all-to-all-done.3.refs_0_ = bf16[32,24,128]{2,1,0:T(8,128)(2,1)S(1)} async-done(((bf16[32,24,128]{2,1,0:T(8,128)(2,1)}), bf16[32,24,128]{2,1,0:T(8,128)(2,1)S(1)}, u32[]{:S(2)}, u32[]{:S(2)}) %all-to-all-start.3) | async-done | bytes 196640 | tf_op jit(solution)/shard_map/all_to_all | solution.py:529
  141.5 2.2 %shard_map.186.refs_4_.refs_5_ = bf16[16,256,128]{2,1,0:T(8,128)(2,1)} custom-call(bf16[32,24,128]{2,1,0:T(8,128)(2,1)S(1)} %all-to-all-done.3.refs_0_, bf16[256,768]{1,0:T(8,128)(2,1)} %shard_map.185.refs_1_, bf16[256,128]{1,0:T(8,128)(2,1)} %refs_2_.4), custom_call_target="tpu_custom_call" | custom-call | tf_op jit(solution)/shard_map/pallas_call | solution.py:59
  143.7 4.3 %all-to-all-start.4 = ((bf16[16,256,128]{2,1,0:T(8,128)(2,1)}), bf16[16,256,128]{2,1,0:T(8,128)(2,1)}, u32[]{:S(2)}, u32[]{:S(2)}) async-start(bf16[16,256,128]{2,1,0:T(8,128)(2,1)} %shard_map.186.refs_4_.refs_5_), calls=%async_computation.4 | async-start | bytes 2097152 | tf_op jit(solution)/shard_map/all_to_all | solution.py:529
  148.1 4.9 %shard_map.183 = (f32[3072,128]{1,0:T(8,128)}, f32[3072,128]{1,0:T(8,128)}, bf16[6144,128]{1,0:T(8,128)(2,1)}, bf16[6144,128]{1,0:T(8,128)(2,1)}, bf16[3072,128]{1,0:T(8,128)(2,1)}, /*index=5*/bf16[3072,128]{1,0:T(8,128)(2,1)}) custom-call(bf16[16,320,128]{2,1,0:T(8,128)(2,1)S(1)} %all-to-all-done.1.refs_0_, ...), custom_call_target="tpu_custom_call" | custom-call | tf_op jit(solution)/shard_map/pallas_call | solution.py:59
  153.0 4.4 %collective-permute-start.6 = (bf16[6144,128]{1,0:T(8,128)(2,1)}, bf16[6144,128]{1,0:T(8,128)(2,1)S(1)}, u32[]{:S(2)}, u32[]{:S(2)}) collective-permute-start(bf16[6144,128]{1,0:T(8,128)(2,1)} %get-tuple-element.57), channel_id=1, source_target_pairs={{0,3},{16,28},{1,0},{17,29},{2,1},{18,30},{3,2},{19,31},{4,7},{20,... | collective-permute-start | bytes 4718600 | tf_op jit(solution)/shard_map/ppermute | solution.py:542
  157.4 1.9 collective-permute-start.7
  159.3 2.6 %shard_map.188 = (bf16[256,128]{1,0:T(8,128)(2,1)S(1)}, f32[4,128,64]{2,1,0:T(8,128)}) custom-call(bf16[32,24,128]{2,1,0:T(8,128)(2,1)S(1)} %all-to-all-done.3.refs_0_, bf16[64,256]{1,0:T(8,128)(2,1)} %bitcast.27, bf16[64,256]{1,0:T(8,128)(2,1)} %bitcast.25, bf16[256,128]{1,0:T(8,128)(2,1)} %refs_5_.3, f32[64,256]{1,0:T(8,128)} %bitcast.18, ...), custom_call_target="tpu_custom_call" | custom-call | tf_op jit(solution)/shard_map/pallas_call | solution.py:59
  162.0 1.8 all-to-all-done.4.refs_1_
  163.7 2.9 %shard_map.189 = (f32[256,128]{1,0:T(8,128)}, f32[32,128]{1,0:T(8,128)S(1)}, bf16[1088,128]{1,0:T(8,128)(2,1)S(1)}, f32[1024,128]{1,0:T(8,128)S(1)}) custom-call(s32[3]{0:T(128)S(1)} %pad_add_fusion.refs_0_, bf16[16,256,128]{2,1,0:T(8,128)(2,1)} %all-to-all-done.4.refs_1_, bf16[2048,128]{1,0:T(8,128)(2,1)} %refs_2_.5, ...), custom_call_target="tpu_custom_call" | custom-call | tf_op jit(solution)/shard_map/pallas_call | solution.py:59
  166.6 5.0 %collective-permute-start.10 = (bf16[1088,128]{1,0:T(8,128)(2,1)S(1)}, bf16[1088,128]{1,0:T(8,128)(2,1)S(1)}, u32[]{:S(2)}, u32[]{:S(2)}) collective-permute-start(bf16[1088,128]{1,0:T(8,128)(2,1)S(1)} %get-tuple-element.67), channel_id=1, source_target_pairs={{0,16},{16,0},{1,17},{17,1},{2,18},{18,2},{3,19},{19,3},{4,20},{20... | collective-permute-start | bytes 835592 | tf_op jit(solution)/shard_map/ppermute | solution.py:672
  171.7 1.2 collective-permute-done.10.refs_1_
  172.8 1.5 shard_map.190
  174.4 4.0 %all-to-all-start.5 = ((bf16[16,96,128]{2,1,0:T(8,128)(2,1)}), bf16[16,96,128]{2,1,0:T(8,128)(2,1)S(1)}, u32[]{:S(2)}, u32[]{:S(2)}) async-start(bf16[16,96,128]{2,1,0:T(8,128)(2,1)} %get-tuple-element.71.refs_6_), calls=%async_computation.5 | async-start | bytes 786432 | tf_op jit(solution)/shard_map/all_to_all | solution.py:529
  178.4 0.9 collective-permute-done.6.refs_2_
  179.2 2.0 collective-permute-done.7.refs_3_
  181.2 1.7 shard_map.187
  183.0 1.9 collective-permute-start.8
  184.9 4.8 %collective-permute-start.9 = (bf16[3072,128]{1,0:T(8,128)(2,1)S(1)}, bf16[3072,128]{1,0:T(8,128)(2,1)S(1)}, u32[]{:S(2)}, u32[]{:S(2)}) collective-permute-start(bf16[3072,128]{1,0:T(8,128)(2,1)S(1)} %get-tuple-element.65), channel_id=1, source_target_pairs={{0,3},{16,28},{1,0},{17,29},{2,1},{18,30},{3,2},{19,31},{4,7},{20,... | collective-permute-start | bytes 2359304 | tf_op jit(solution)/shard_map/ppermute | solution.py:542
  189.6 3.8 %shard_map.192 = (bf16[64,256]{1,0:T(8,128)(2,1)}, f32[256,128]{1,0:T(8,128)}, f32[256,64]{1,0:T(8,128)}, f32[256,64]{1,0:T(8,128)}, f32[256,64]{1,0:T(8,128)}, ...) custom-call(f32[256,128]{1,0:T(8,128)} %get-tuple-element.77.refs_0_, ...), custom_call_target="tpu_custom_call" | custom-call | tf_op jit(solution)/shard_map/pallas_call | solution.py:59
  193.4 3.8 %collective-permute-done.8.refs_4_ = bf16[3072,128]{1,0:T(8,128)(2,1)S(1)} collective-permute-done((bf16[3072,128]{1,0:T(8,128)(2,1)S(1)}, bf16[3072,128]{1,0:T(8,128)(2,1)S(1)}, u32[]{:S(2)}, u32[]{:S(2)}) %collective-permute-start.8) | collective-permute-done | bytes 786464 | tf_op jit(solution)/shard_map/ppermute | solution.py:542
  197.2 1.2 collective-permute-done.9.refs_5_
  198.4 3.3 %shard_map.191 = (bf16[2048,128]{1,0:T(8,128)(2,1)}, bf16[2048,128]{1,0:T(8,128)(2,1)}, bf16[128,2048]{1,0:T(8,128)(2,1)}) custom-call(f32[3072,128]{1,0:T(8,128)} %get-tuple-element.55.refs_0_, f32[3072,128]{1,0:T(8,128)} %get-tuple-element.56.refs_1_, bf16[6144,128]{1,0:T(8,128)(2,1)S(1)} %collective-permute-done.6.refs_2_, ...), custom_call_target="tpu_custom_call" | custom-call | tf_op jit(solution)/shard_map/pallas_call | solution.py:59
  201.7 2.6 %shard_map.193 = (f32[64,128]{1,0:T(8,128)}, bf16[64,256]{1,0:T(8,128)(2,1)}, bf16[256,128]{1,0:T(8,128)(2,1)}, f32[64,256]{1,0:T(8,128)}) custom-call(s32[3]{0:T(128)S(1)} %pad_add_fusion.refs_0_, bf16[16,96,128]{2,1,0:T(8,128)(2,1)S(1)} %all-to-all-done.5.refs_1_, f32[32,128]{1,0:T(8,128)} %get-tuple-element.75.refs_2_, ...), custom_call_target="tpu_custom_call" | custom-call | tf_op jit(solution)/shard_map/pallas_call | solution.py:59
  (11 shorter events, 0.0 us)
Async XLA Ops:
  4.2 44.5 %all-to-all-start = ((bf16[32,48,128]{2,1,0:T(8,128)(2,1)}), bf16[32,48,128]{2,1,0:T(8,128)(2,1)S(1)}, u32[]{:S(2)}, u32[]{:S(2)}) async-start(bf16[32,48,128]{2,1,0:T(8,128)(2,1)} %get-tuple-element.49), calls=%async_computation | async-start | bytes 786432 | tf_op jit(solution)/shard_map/all_to_all | solution.py:529
  23.4 34.0 %copy-start = (bf16[3072,128]{1,0:T(8,128)(2,1)S(1)}, bf16[3072,128]{1,0:T(8,128)(2,1)}, u32[]{:S(2)}) copy-start(bf16[3072,128]{1,0:T(8,128)(2,1)} %get-tuple-element.51.refs_1_) | copy-start | bytes 2359300
  23.4 38.5 %copy-start.1 = (bf16[3072,128]{1,0:T(8,128)(2,1)S(1)}, bf16[3072,128]{1,0:T(8,128)(2,1)}, u32[]{:S(2)}) copy-start(bf16[3072,128]{1,0:T(8,128)(2,1)} %get-tuple-element.52.refs_2_) | copy-start | bytes 2359300
  23.4 40.4 %collective-permute-start = (bf16[3072,128]{1,0:T(8,128)(2,1)}, bf16[3072,128]{1,0:T(8,128)(2,1)}, u32[]{:S(2)}, u32[]{:S(2)}) collective-permute-start(bf16[3072,128]{1,0:T(8,128)(2,1)} %get-tuple-element.51.refs_1_), channel_id=1, source_target_pairs={{0,1},{16,20},{1,2},{17,21},{2,3},{18,22},{3,0},{19,23},{4,5},{20,... | collective-permute-start | bytes 2359304 | tf_op jit(solution)/shard_map/ppermute | solution.py:542
  26.8 39.2 %collective-permute-start.3 = (bf16[3072,128]{1,0:T(8,128)(2,1)}, bf16[3072,128]{1,0:T(8,128)(2,1)}, u32[]{:S(2)}, u32[]{:S(2)}) collective-permute-start(bf16[3072,128]{1,0:T(8,128)(2,1)} %get-tuple-element.52.refs_2_), channel_id=1, source_target_pairs={{0,3},{16,28},{1,0},{17,29},{2,1},{18,30},{3,2},{19,31},{4,7},{20,... | collective-permute-start | bytes 2359304 | tf_op jit(solution)/shard_map/ppermute | solution.py:542
  50.6 42.6 %all-to-all-start.1 = ((bf16[16,320,128]{2,1,0:T(8,128)(2,1)}), bf16[16,320,128]{2,1,0:T(8,128)(2,1)S(1)}, u32[]{:S(2)}, u32[]{:S(2)}) async-start(bf16[16,320,128]{2,1,0:T(8,128)(2,1)} %get-tuple-element.50.refs_1_), calls=%async_computation.1 | async-start | bytes 2621440 | tf_op jit(solution)/shard_map/all_to_all | solution.py:529
  57.4 25.3 %collective-permute-start.2 = (bf16[3072,128]{1,0:T(8,128)(2,1)S(1)}, bf16[3072,128]{1,0:T(8,128)(2,1)S(1)}, u32[]{:S(2)}, u32[]{:S(2)}) collective-permute-start(bf16[3072,128]{1,0:T(8,128)(2,1)S(1)} %copy-done), channel_id=1, source_target_pairs={{0,3},{16,28},{1,0},{17,29},{2,1},{18,30},{3,2},{19,31},{4,7},{20,... | collective-permute-start | bytes 2359304 | tf_op jit(solution)/shard_map/ppermute | solution.py:542
  61.9 22.3 %collective-permute-start.1 = (bf16[3072,128]{1,0:T(8,128)(2,1)S(1)}, bf16[3072,128]{1,0:T(8,128)(2,1)S(1)}, u32[]{:S(2)}, u32[]{:S(2)}) collective-permute-start(bf16[3072,128]{1,0:T(8,128)(2,1)S(1)} %copy-done.1), channel_id=1, source_target_pairs={{0,1},{16,20},{1,2},{17,21},{2,3},{18,22},{3,0},{19,23},{4,5},{20,... | collective-permute-start | bytes 2359304 | tf_op jit(solution)/shard_map/ppermute | solution.py:542
  63.9 28.5 %collective-permute-start.4 = (bf16[3072,128]{1,0:T(8,128)(2,1)}, bf16[3072,128]{1,0:T(8,128)(2,1)S(1)}, u32[]{:S(2)}, u32[]{:S(2)}) collective-permute-start(bf16[3072,128]{1,0:T(8,128)(2,1)} %collective-permute-done.refs_3_), channel_id=1, source_target_pairs={{0,1},{16,20},{1,2},{17,21},{2,3},{18,22},{3,0},{19,23},{4,5},{20,... | collective-permute-start | bytes 2359304 | tf_op jit(solution)/shard_map/ppermute | solution.py:542
  66.0 27.2 %collective-permute-start.5 = (bf16[3072,128]{1,0:T(8,128)(2,1)}, bf16[3072,128]{1,0:T(8,128)(2,1)}, u32[]{:S(2)}, u32[]{:S(2)}) collective-permute-start(bf16[3072,128]{1,0:T(8,128)(2,1)} %collective-permute-done.3.refs_6_), channel_id=1, source_target_pairs={{0,3},{16,28},{1,0},{17,29},{2,1},{18,30},{3,2},{19,31},{4,7},{20,... | collective-permute-start | bytes 2359304 | tf_op jit(solution)/shard_map/ppermute | solution.py:542
  82.7 9.6 %copy-start.2 = (bf16[3072,128]{1,0:T(8,128)(2,1)}, bf16[3072,128]{1,0:T(8,128)(2,1)S(1)}, u32[]{:S(2)}) copy-start(bf16[3072,128]{1,0:T(8,128)(2,1)S(1)} %collective-permute-done.2.refs_5_) | copy-start | bytes 2359300
  84.2 8.1 %copy-start.3 = (bf16[3072,128]{1,0:T(8,128)(2,1)}, bf16[3072,128]{1,0:T(8,128)(2,1)S(1)}, u32[]{:S(2)}) copy-start(bf16[3072,128]{1,0:T(8,128)(2,1)S(1)} %collective-permute-done.1.refs_4_) | copy-start | bytes 2359300
  92.3 0.9 copy-start.4
  116.3 25.2 %all-to-all-start.3 = ((bf16[32,24,128]{2,1,0:T(8,128)(2,1)}), bf16[32,24,128]{2,1,0:T(8,128)(2,1)S(1)}, u32[]{:S(2)}, u32[]{:S(2)}) async-start(bf16[32,24,128]{2,1,0:T(8,128)(2,1)} %shard_map.184), calls=%async_computation.3 | async-start | bytes 393216 | tf_op jit(solution)/shard_map/all_to_all | solution.py:529
  143.7 20.0 %all-to-all-start.4 = ((bf16[16,256,128]{2,1,0:T(8,128)(2,1)}), bf16[16,256,128]{2,1,0:T(8,128)(2,1)}, u32[]{:S(2)}, u32[]{:S(2)}) async-start(bf16[16,256,128]{2,1,0:T(8,128)(2,1)} %shard_map.186.refs_4_.refs_5_), calls=%async_computation.4 | async-start | bytes 2097152 | tf_op jit(solution)/shard_map/all_to_all | solution.py:529
  153.0 26.2 %collective-permute-start.6 = (bf16[6144,128]{1,0:T(8,128)(2,1)}, bf16[6144,128]{1,0:T(8,128)(2,1)S(1)}, u32[]{:S(2)}, u32[]{:S(2)}) collective-permute-start(bf16[6144,128]{1,0:T(8,128)(2,1)} %get-tuple-element.57), channel_id=1, source_target_pairs={{0,3},{16,28},{1,0},{17,29},{2,1},{18,30},{3,2},{19,31},{4,7},{20,... | collective-permute-start | bytes 4718600 | tf_op jit(solution)/shard_map/ppermute | solution.py:542
  157.4 23.8 %collective-permute-start.7 = (bf16[6144,128]{1,0:T(8,128)(2,1)}, bf16[6144,128]{1,0:T(8,128)(2,1)S(1)}, u32[]{:S(2)}, u32[]{:S(2)}) collective-permute-start(bf16[6144,128]{1,0:T(8,128)(2,1)} %get-tuple-element.58), channel_id=1, source_target_pairs={{0,1},{16,20},{1,2},{17,21},{2,3},{18,22},{3,0},{19,23},{4,5},{20,... | collective-permute-start | bytes 4718600 | tf_op jit(solution)/shard_map/ppermute | solution.py:542
  166.6 6.2 %collective-permute-start.10 = (bf16[1088,128]{1,0:T(8,128)(2,1)S(1)}, bf16[1088,128]{1,0:T(8,128)(2,1)S(1)}, u32[]{:S(2)}, u32[]{:S(2)}) collective-permute-start(bf16[1088,128]{1,0:T(8,128)(2,1)S(1)} %get-tuple-element.67), channel_id=1, source_target_pairs={{0,16},{16,0},{1,17},{17,1},{2,18},{18,2},{3,19},{19,3},{4,20},{20... | collective-permute-start | bytes 835592 | tf_op jit(solution)/shard_map/ppermute | solution.py:672
  174.4 27.4 %all-to-all-start.5 = ((bf16[16,96,128]{2,1,0:T(8,128)(2,1)}), bf16[16,96,128]{2,1,0:T(8,128)(2,1)S(1)}, u32[]{:S(2)}, u32[]{:S(2)}) async-start(bf16[16,96,128]{2,1,0:T(8,128)(2,1)} %get-tuple-element.71.refs_6_), calls=%async_computation.5 | async-start | bytes 786432 | tf_op jit(solution)/shard_map/all_to_all | solution.py:529
  183.0 14.2 %collective-permute-start.8 = (bf16[3072,128]{1,0:T(8,128)(2,1)S(1)}, bf16[3072,128]{1,0:T(8,128)(2,1)S(1)}, u32[]{:S(2)}, u32[]{:S(2)}) collective-permute-start(bf16[3072,128]{1,0:T(8,128)(2,1)S(1)} %get-tuple-element.64), channel_id=1, source_target_pairs={{0,1},{16,20},{1,2},{17,21},{2,3},{18,22},{3,0},{19,23},{4,5},{20,... | collective-permute-start | bytes 2359304 | tf_op jit(solution)/shard_map/ppermute | solution.py:542
  184.9 13.5 %collective-permute-start.9 = (bf16[3072,128]{1,0:T(8,128)(2,1)S(1)}, bf16[3072,128]{1,0:T(8,128)(2,1)S(1)}, u32[]{:S(2)}, u32[]{:S(2)}) collective-permute-start(bf16[3072,128]{1,0:T(8,128)(2,1)S(1)} %get-tuple-element.65), channel_id=1, source_target_pairs={{0,3},{16,28},{1,0},{17,29},{2,1},{18,30},{3,2},{19,31},{4,7},{20,... | collective-permute-start | bytes 2359304 | tf_op jit(solution)/shard_map/ppermute | solution.py:542

commit v7 on v6

--- a/solution.py
+++ b/solution.py
@@ -223,21 +223,29 @@
     for copy in copies:
         copy.start()
     x, g = wide(rows_ref, 0, PART), wide(rows_ref, PART, PART)
-    for b in range(4):
-        copies[2 * b].wait()
-        copies[2 * b + 1].wait()
-        gate_weight = held[2 * b, :2048, :]
-        up_weight = jnp.concatenate([held[2 * b, 2048:, :], held[2 * b + 1, :1024, :]], axis=0)
-        blocks = [held[2 * b + 1, 1024 + k * 128 : 1152 + k * 128, :] for k in range(N_TP)]
-        pre = mm(x, jnp.concatenate([gate_weight, up_weight], axis=1))
-        upper = mm(g, jnp.concatenate(blocks, axis=1), NT)
-        gate_pre, up_pre = pre[:, :128], pre[:, 128:]
-        sigmoid = jax.nn.sigmoid(gate_pre)
-        activated = gate_pre * sigmoid
-        hidden_ref[:, 128 * b : 128 * b + 128] = (activated * up_pre).astype(BF)
-        gate = upper * up_pre * sigmoid * (1.0 + gate_pre * (1.0 - sigmoid))
-        grads_ref[:, 256 * b : 256 * b + 128] = gate.astype(BF)
-        grads_ref[:, 256 * b + 128 : 256 * b + 256] = (upper * activated).astype(BF)
+    for pair in range(2):
+        gates, downs = [], []
+        for b in (2 * pair, 2 * pair + 1):
+            copies[2 * b].wait()
+            copies[2 * b + 1].wait()
+            gates.append(held[2 * b, :2048, :])
+            gates.append(
+                jnp.concatenate([held[2 * b, 2048:, :], held[2 * b + 1, :1024, :]], axis=0)
+            )
+            blocks = [held[2 * b + 1, 1024 + k * 128 : 1152 + k * 128, :] for k in range(N_TP)]
+            downs.append(jnp.concatenate(blocks, axis=1))
+        pres = mm(x, jnp.concatenate(gates, axis=1))
+        uppers = mm(g, jnp.concatenate(downs, axis=0), NT)
+        for n in range(2):
+            b = 2 * pair + n
+            gate_pre, up_pre = pres[:, 256 * n : 256 * n + 128], pres[:, 256 * n + 128 : 256 * n + 256]
+            upper = uppers[:, 128 * n : 128 * n + 128]
+            sigmoid = jax.nn.sigmoid(gate_pre)
+            activated = gate_pre * sigmoid
+            hidden_ref[:, 128 * b : 128 * b + 128] = (activated * up_pre).astype(BF)
+            gate = upper * up_pre * sigmoid * (1.0 + gate_pre * (1.0 - sigmoid))
+            grads_ref[:, 256 * b : 256 * b + 128] = gate.astype(BF)
+            grads_ref[:, 256 * b + 128 : 256 * b + 256] = (upper * activated).astype(BF)
     grads = grads_ref[...]
 
     def up_rows(b, at):
@@ -613,7 +621,6 @@
         grads,
         hidden,
         near=(0, 1, 2),
-        near_out=(2, 3),
     )
     from_left = passed_on(to_right, 1)
     from_right = passed_on(to_left, -1)
@@ -623,7 +630,6 @@
         place,
         arrived,
         states,
-        near_out=(0,),
         smem=(0,),
         near=(1,),
         scratch=[pltpu.VMEM((ROWS + 8, 128), F32)],
@@ -640,7 +646,6 @@
         from_left,
         after=(residual,),
         near=(2, 3),
-        near_out=(0, 1),
     )
     last_a = passed_on(lot_right, 1)
     last_b = passed_on(lot_left, -1)

time: 208 us -> 210 us (level)
  transfers between devices with their start and end apart: 16 -> 16, of which waited for: 11 -> 11; matrix products, arithmetic and copies ran while one was open for 0% -> 0% of each run, Pallas kernels for 13% -> 14%
where the time goes in v7:
time: 210 us; the launch traced here: 207 us
  starting transfers between devices  75.6 us (36%)
  waiting for transfers between devices  68.6 us (33%)
  Pallas kernels  44.7 us (21%)
  blocking collectives  15.7 us (7%)
    pallas_call x15, Pallas kernels, call(): pl.pallas_call(run, out_shape=tuple(((pltpu.VMEM if k in near_out else pl...  44.7 us
    all_to_all x5, starting transfers between devices, exchanged(): return lax.all_to_all(blocks, axis, split_axis=0, concat_axis=0, tiled=True)  38 us
    all_to_all x5, waiting for transfers between devices, exchanged(): return lax.all_to_all(blocks, axis, split_axis=0, concat_axis=0, tiled=True)  37.2 us
    ppermute x10, starting transfers between devices, passed_on(): return lax.ppermute(array, ('sp_1', 'tp'), ring_step(step))  32.5 us
    ppermute x10, waiting for transfers between devices, passed_on(): return lax.ppermute(array, ('sp_1', 'tp'), ring_step(step))  30.2 us
    all_to_all x1, blocking collectives, exchanged(): return lax.all_to_all(blocks, axis, split_axis=0, concat_axis=0, tiled=True)  15.7 us
    ppermute x1, starting transfers between devices, body(): from_other = lax.ppermute(to_other, 'sp_1', [(0, 1), (1, 0)])  5.03 us
  transfers between devices with their start and end apart: 16, of which 11 were waited for; matrix products, arithmetic and copies ran while one was open for 0% of the time, Pallas kernels for 14%

profile of v7, /device:TPU:1, one launch (start us, length us, event | category | flops | bytes accessed | tf_op | source)
XLA Modules:
  0.0 206.5 jit_solution(8133286550824538214)
XLA Ops:
  0.6 3.5 %shard_map.179 = (bf16[32,48,128]{2,1,0:T(8,128)(2,1)}, bf16[768,256]{1,0:T(8,128)(2,1)}) custom-call(s32[2,256]{1,0:T(2,128)} %bitcast.30, f32[2,256]{1,0:T(2,128)} %bitcast.31, bf16[256,128]{1,0:T(8,128)(2,1)} %refs_2_.3, bf16[256,128]{1,0:T(8,128)(2,1)} %refs_2_.4, bf16[64,256]{1,0:T(8,128)(2,1)} %bitcast.24, bf16[256,128]{1,0:T(8,128)(2,1)} %refs_5_.3, ...), custom_call_target="tpu_custom_call" | custom-call | tf_op jit(solution)/shard_map/pallas_call | solution.py:59
  4.2 16.7 %all-to-all-start = ((bf16[32,48,128]{2,1,0:T(8,128)(2,1)}), bf16[32,48,128]{2,1,0:T(8,128)(2,1)S(1)}, u32[]{:S(2)}, u32[]{:S(2)}) async-start(bf16[32,48,128]{2,1,0:T(8,128)(2,1)} %get-tuple-element.49), calls=%async_computation | async-start | bytes 786432 | tf_op jit(solution)/shard_map/all_to_all | solution.py:537
  20.9 2.5 %shard_map.181 = (bf16[3072,128]{1,0:T(8,128)(2,1)}, bf16[3072,128]{1,0:T(8,128)(2,1)}) custom-call(bf16[2048,128]{1,0:T(8,128)(2,1)} %bitcast.21, bf16[2048,128]{1,0:T(8,128)(2,1)} %bitcast.22, bf16[128,2048]{1,0:T(8,128)(2,1)} %bitcast.23), custom_call_target="tpu_custom_call" | custom-call | tf_op jit(solution)/shard_map/pallas_call | solution.py:59
  23.4 3.3 %collective-permute-start = (bf16[3072,128]{1,0:T(8,128)(2,1)}, bf16[3072,128]{1,0:T(8,128)(2,1)}, u32[]{:S(2)}, u32[]{:S(2)}) collective-permute-start(bf16[3072,128]{1,0:T(8,128)(2,1)} %get-tuple-element.51.refs_1_), channel_id=1, source_target_pairs={{0,1},{16,20},{1,2},{17,21},{2,3},{18,22},{3,0},{19,23},{4,5},{20,... | collective-permute-start | bytes 2359304 | tf_op jit(solution)/shard_map/ppermute | solution.py:550
  26.8 3.4 %collective-permute-start.3 = (bf16[3072,128]{1,0:T(8,128)(2,1)}, bf16[3072,128]{1,0:T(8,128)(2,1)}, u32[]{:S(2)}, u32[]{:S(2)}) collective-permute-start(bf16[3072,128]{1,0:T(8,128)(2,1)} %get-tuple-element.52.refs_2_), channel_id=1, source_target_pairs={{0,3},{16,28},{1,0},{17,29},{2,1},{18,30},{3,2},{19,31},{4,7},{20,... | collective-permute-start | bytes 2359304 | tf_op jit(solution)/shard_map/ppermute | solution.py:550
  30.2 0.1 pad_add_fusion.refs_0_
  30.2 18.4 %all-to-all-done.refs_1_ = bf16[32,48,128]{2,1,0:T(8,128)(2,1)S(1)} async-done(((bf16[32,48,128]{2,1,0:T(8,128)(2,1)}), bf16[32,48,128]{2,1,0:T(8,128)(2,1)S(1)}, u32[]{:S(2)}, u32[]{:S(2)}) %all-to-all-start) | async-done | bytes 393248 | tf_op jit(solution)/shard_map/all_to_all | solution.py:537
  48.7 2.0 shard_map.180
  50.6 6.8 %all-to-all-start.1 = ((bf16[16,320,128]{2,1,0:T(8,128)(2,1)}), bf16[16,320,128]{2,1,0:T(8,128)(2,1)S(1)}, u32[]{:S(2)}, u32[]{:S(2)}) async-start(bf16[16,320,128]{2,1,0:T(8,128)(2,1)} %get-tuple-element.50.refs_1_), calls=%async_computation.1 | async-start | bytes 2621440 | tf_op jit(solution)/shard_map/all_to_all | solution.py:537
  57.4 4.5 %collective-permute-start.2 = (bf16[3072,128]{1,0:T(8,128)(2,1)S(1)}, bf16[3072,128]{1,0:T(8,128)(2,1)S(1)}, u32[]{:S(2)}, u32[]{:S(2)}) collective-permute-start(bf16[3072,128]{1,0:T(8,128)(2,1)S(1)} %copy-done), channel_id=1, source_target_pairs={{0,3},{16,28},{1,0},{17,29},{2,1},{18,30},{3,2},{19,31},{4,7},{20,... | collective-permute-start | bytes 2359304 | tf_op jit(solution)/shard_map/ppermute | solution.py:550
  61.9 1.9 collective-permute-start.1
  63.9 0.0 collective-permute-done.refs_3_
  63.9 2.1 %collective-permute-start.4 = (bf16[3072,128]{1,0:T(8,128)(2,1)}, bf16[3072,128]{1,0:T(8,128)(2,1)S(1)}, u32[]{:S(2)}, u32[]{:S(2)}) collective-permute-start(bf16[3072,128]{1,0:T(8,128)(2,1)} %collective-permute-done.refs_3_), channel_id=1, source_target_pairs={{0,1},{16,20},{1,2},{17,21},{2,3},{18,22},{3,0},{19,23},{4,5},{20,... | collective-permute-start | bytes 2359304 | tf_op jit(solution)/shard_map/ppermute | solution.py:550
  66.0 0.0 collective-permute-done.3.refs_6_
  66.0 4.3 %collective-permute-start.5 = (bf16[3072,128]{1,0:T(8,128)(2,1)}, bf16[3072,128]{1,0:T(8,128)(2,1)}, u32[]{:S(2)}, u32[]{:S(2)}) collective-permute-start(bf16[3072,128]{1,0:T(8,128)(2,1)} %collective-permute-done.3.refs_6_), channel_id=1, source_target_pairs={{0,3},{16,28},{1,0},{17,29},{2,1},{18,30},{3,2},{19,31},{4,7},{20,... | collective-permute-start | bytes 2359304 | tf_op jit(solution)/shard_map/ppermute | solution.py:550
  70.4 12.3 %collective-permute-done.2.refs_5_ = bf16[3072,128]{1,0:T(8,128)(2,1)S(1)} collective-permute-done((bf16[3072,128]{1,0:T(8,128)(2,1)S(1)}, bf16[3072,128]{1,0:T(8,128)(2,1)S(1)}, u32[]{:S(2)}, u32[]{:S(2)}) %collective-permute-start.2) | collective-permute-done | bytes 786464 | tf_op jit(solution)/shard_map/ppermute | solution.py:550
  82.7 1.5 collective-permute-done.1.refs_4_
  84.2 8.1 %collective-permute-done.4.refs_7_ = bf16[3072,128]{1,0:T(8,128)(2,1)S(1)} collective-permute-done((bf16[3072,128]{1,0:T(8,128)(2,1)}, bf16[3072,128]{1,0:T(8,128)(2,1)S(1)}, u32[]{:S(2)}, u32[]{:S(2)}) %collective-permute-start.4) | collective-permute-done | bytes 786464 | tf_op jit(solution)/shard_map/ppermute | solution.py:550
  92.3 0.9 copy-done.4
  93.3 0.0 collective-permute-done.5.refs_8_
  93.3 6.4 %shard_map.182 = (bf16[16,160,128]{2,1,0:T(8,128)(2,1)}, bf16[160,1024]{1,0:T(8,128)(2,1)S(1)}, bf16[160,512]{1,0:T(8,128)(2,1)S(1)}) custom-call(bf16[16,320,128]{2,1,0:T(8,128)(2,1)S(1)} %all-to-all-done.1.refs_0_, bf16[3072,128]{1,0:T(8,128)(2,1)} %get-tuple-element.51.refs_1_, bf16[3072,128]{1,0:T(8,128)(2,1)} %get-tuple-element.52.refs_2_, ...), custom_call_target="tpu_custom_call" | custom-call | tf_op jit(solution)/shard_map/pallas_call | solution.py:59
  99.6 15.7 %all_to_all.30.refs_1_ = bf16[16,160,128]{2,1,0:T(8,128)(2,1)S(1)} all-to-all(bf16[16,160,128]{2,1,0:T(8,128)(2,1)} %get-tuple-element.61), channel_id=1, replica_groups=mesh['sp_0'=16,'sp_1'=2,'tp'=16] {'tp'}, dimensions={0} | all-to-all | bytes 1310720 | tf_op jit(solution)/shard_map/all_to_all | solution.py:537
  115.4 1.5 shard_map.184
  116.9 6.2 %all-to-all-start.3 = ((bf16[32,24,128]{2,1,0:T(8,128)(2,1)}), bf16[32,24,128]{2,1,0:T(8,128)(2,1)S(1)}, u32[]{:S(2)}, u32[]{:S(2)}) async-start(bf16[32,24,128]{2,1,0:T(8,128)(2,1)} %shard_map.184), calls=%async_computation.3 | async-start | bytes 393216 | tf_op jit(solution)/shard_map/all_to_all | solution.py:537
  123.1 1.9 shard_map.185.refs_1_
  125.0 17.0 %all-to-all-done.3.refs_0_ = bf16[32,24,128]{2,1,0:T(8,128)(2,1)S(1)} async-done(((bf16[32,24,128]{2,1,0:T(8,128)(2,1)}), bf16[32,24,128]{2,1,0:T(8,128)(2,1)S(1)}, u32[]{:S(2)}, u32[]{:S(2)}) %all-to-all-start.3) | async-done | bytes 196640 | tf_op jit(solution)/shard_map/all_to_all | solution.py:537
  142.1 2.2 %shard_map.186.refs_4_.refs_5_ = bf16[16,256,128]{2,1,0:T(8,128)(2,1)} custom-call(bf16[32,24,128]{2,1,0:T(8,128)(2,1)S(1)} %all-to-all-done.3.refs_0_, bf16[256,768]{1,0:T(8,128)(2,1)} %shard_map.185.refs_1_, bf16[256,128]{1,0:T(8,128)(2,1)} %refs_2_.4), custom_call_target="tpu_custom_call" | custom-call | tf_op jit(solution)/shard_map/pallas_call | solution.py:59
  144.3 4.3 %all-to-all-start.4 = ((bf16[16,256,128]{2,1,0:T(8,128)(2,1)}), bf16[16,256,128]{2,1,0:T(8,128)(2,1)}, u32[]{:S(2)}, u32[]{:S(2)}) async-start(bf16[16,256,128]{2,1,0:T(8,128)(2,1)} %shard_map.186.refs_4_.refs_5_), calls=%async_computation.4 | async-start | bytes 2097152 | tf_op jit(solution)/shard_map/all_to_all | solution.py:537
  148.7 4.9 %shard_map.183 = (f32[3072,128]{1,0:T(8,128)}, f32[3072,128]{1,0:T(8,128)}, bf16[6144,128]{1,0:T(8,128)(2,1)}, bf16[6144,128]{1,0:T(8,128)(2,1)}, bf16[3072,128]{1,0:T(8,128)(2,1)}, /*index=5*/bf16[3072,128]{1,0:T(8,128)(2,1)}) custom-call(bf16[16,320,128]{2,1,0:T(8,128)(2,1)S(1)} %all-to-all-done.1.refs_0_, ...), custom_call_target="tpu_custom_call" | custom-call | tf_op jit(solution)/shard_map/pallas_call | solution.py:59
  153.6 4.4 %collective-permute-start.6 = (bf16[6144,128]{1,0:T(8,128)(2,1)}, bf16[6144,128]{1,0:T(8,128)(2,1)S(1)}, u32[]{:S(2)}, u32[]{:S(2)}) collective-permute-start(bf16[6144,128]{1,0:T(8,128)(2,1)} %get-tuple-element.57), channel_id=1, source_target_pairs={{0,3},{16,28},{1,0},{17,29},{2,1},{18,30},{3,2},{19,31},{4,7},{20,... | collective-permute-start | bytes 4718600 | tf_op jit(solution)/shard_map/ppermute | solution.py:550
  158.0 1.9 collective-permute-start.7
  159.9 2.6 %shard_map.188 = (bf16[256,128]{1,0:T(8,128)(2,1)S(1)}, f32[4,128,64]{2,1,0:T(8,128)}) custom-call(bf16[32,24,128]{2,1,0:T(8,128)(2,1)S(1)} %all-to-all-done.3.refs_0_, bf16[64,256]{1,0:T(8,128)(2,1)} %bitcast.27, bf16[64,256]{1,0:T(8,128)(2,1)} %bitcast.25, bf16[256,128]{1,0:T(8,128)(2,1)} %refs_5_.3, f32[64,256]{1,0:T(8,128)} %bitcast.18, ...), custom_call_target="tpu_custom_call" | custom-call | tf_op jit(solution)/shard_map/pallas_call | solution.py:59
  162.5 1.8 all-to-all-done.4.refs_1_
  164.3 2.9 %shard_map.189 = (f32[256,128]{1,0:T(8,128)}, f32[32,128]{1,0:T(8,128)S(1)}, bf16[1088,128]{1,0:T(8,128)(2,1)S(1)}, f32[1024,128]{1,0:T(8,128)S(1)}) custom-call(s32[3]{0:T(128)S(1)} %pad_add_fusion.refs_0_, bf16[16,256,128]{2,1,0:T(8,128)(2,1)} %all-to-all-done.4.refs_1_, bf16[2048,128]{1,0:T(8,128)(2,1)} %refs_2_.5, ...), custom_call_target="tpu_custom_call" | custom-call | tf_op jit(solution)/shard_map/pallas_call | solution.py:59
  167.2 5.0 %collective-permute-start.10 = (bf16[1088,128]{1,0:T(8,128)(2,1)S(1)}, bf16[1088,128]{1,0:T(8,128)(2,1)S(1)}, u32[]{:S(2)}, u32[]{:S(2)}) collective-permute-start(bf16[1088,128]{1,0:T(8,128)(2,1)S(1)} %get-tuple-element.67), channel_id=1, source_target_pairs={{0,16},{16,0},{1,17},{17,1},{2,18},{18,2},{3,19},{19,3},{4,20},{20... | collective-permute-start | bytes 835592 | tf_op jit(solution)/shard_map/ppermute | solution.py:677
  172.2 1.2 collective-permute-done.10.refs_1_
  173.4 1.5 shard_map.190
  174.9 4.0 %all-to-all-start.5 = ((bf16[16,96,128]{2,1,0:T(8,128)(2,1)}), bf16[16,96,128]{2,1,0:T(8,128)(2,1)S(1)}, u32[]{:S(2)}, u32[]{:S(2)}) async-start(bf16[16,96,128]{2,1,0:T(8,128)(2,1)} %get-tuple-element.71.refs_6_), calls=%async_computation.5 | async-start | bytes 786432 | tf_op jit(solution)/shard_map/all_to_all | solution.py:537
  179.0 0.9 collective-permute-done.6.refs_2_
  179.8 2.0 collective-permute-done.7.refs_3_
  181.8 2.8 %shard_map.187 = (bf16[3072,128]{1,0:T(8,128)(2,1)}, bf16[3072,128]{1,0:T(8,128)(2,1)}) custom-call(bf16[3072,128]{1,0:T(8,128)(2,1)} %get-tuple-element.59.refs_0_, bf16[3072,128]{1,0:T(8,128)(2,1)} %get-tuple-element.60.refs_1_, bf16[6144,128]{1,0:T(8,128)(2,1)S(1)} %collective-permute-done.6.refs_2_, ...), custom_call_target="tpu_custom_call" | custom-call | tf_op jit(solution)/shard_map/pallas_call | solution.py:59
  184.6 2.1 %collective-permute-start.8 = (bf16[3072,128]{1,0:T(8,128)(2,1)}, bf16[3072,128]{1,0:T(8,128)(2,1)S(1)}, u32[]{:S(2)}, u32[]{:S(2)}) collective-permute-start(bf16[3072,128]{1,0:T(8,128)(2,1)} %get-tuple-element.64), channel_id=1, source_target_pairs={{0,1},{16,20},{1,2},{17,21},{2,3},{18,22},{3,0},{19,23},{4,5},{20,... | collective-permute-start | bytes 2359304 | tf_op jit(solution)/shard_map/ppermute | solution.py:550
  186.7 4.6 %collective-permute-start.9 = (bf16[3072,128]{1,0:T(8,128)(2,1)}, bf16[3072,128]{1,0:T(8,128)(2,1)S(1)}, u32[]{:S(2)}, u32[]{:S(2)}) collective-permute-start(bf16[3072,128]{1,0:T(8,128)(2,1)} %get-tuple-element.65), channel_id=1, source_target_pairs={{0,3},{16,28},{1,0},{17,29},{2,1},{18,30},{3,2},{19,31},{4,7},{20,... | collective-permute-start | bytes 2359304 | tf_op jit(solution)/shard_map/ppermute | solution.py:550
  191.3 3.8 %shard_map.192 = (bf16[64,256]{1,0:T(8,128)(2,1)}, f32[256,128]{1,0:T(8,128)}, f32[256,64]{1,0:T(8,128)}, f32[256,64]{1,0:T(8,128)}, f32[256,64]{1,0:T(8,128)}, ...) custom-call(f32[256,128]{1,0:T(8,128)} %get-tuple-element.77.refs_0_, ...), custom_call_target="tpu_custom_call" | custom-call | tf_op jit(solution)/shard_map/pallas_call | solution.py:59
  195.1 4.0 %collective-permute-done.8.refs_4_ = bf16[3072,128]{1,0:T(8,128)(2,1)S(1)} collective-permute-done((bf16[3072,128]{1,0:T(8,128)(2,1)}, bf16[3072,128]{1,0:T(8,128)(2,1)S(1)}, u32[]{:S(2)}, u32[]{:S(2)}) %collective-permute-start.8) | collective-permute-done | bytes 786464 | tf_op jit(solution)/shard_map/ppermute | solution.py:550
  199.1 1.5 collective-permute-done.9.refs_5_
  200.5 3.3 %shard_map.191 = (bf16[2048,128]{1,0:T(8,128)(2,1)}, bf16[2048,128]{1,0:T(8,128)(2,1)}, bf16[128,2048]{1,0:T(8,128)(2,1)}) custom-call(f32[3072,128]{1,0:T(8,128)} %get-tuple-element.55.refs_0_, f32[3072,128]{1,0:T(8,128)} %get-tuple-element.56.refs_1_, bf16[6144,128]{1,0:T(8,128)(2,1)S(1)} %collective-permute-done.6.refs_2_, ...), custom_call_target="tpu_custom_call" | custom-call | tf_op jit(solution)/shard_map/pallas_call | solution.py:59
  203.9 2.6 %shard_map.193 = (f32[64,128]{1,0:T(8,128)}, bf16[64,256]{1,0:T(8,128)(2,1)}, bf16[256,128]{1,0:T(8,128)(2,1)}, f32[64,256]{1,0:T(8,128)}) custom-call(s32[3]{0:T(128)S(1)} %pad_add_fusion.refs_0_, bf16[16,96,128]{2,1,0:T(8,128)(2,1)S(1)} %all-to-all-done.5.refs_1_, f32[32,128]{1,0:T(8,128)} %get-tuple-element.75.refs_2_, ...), custom_call_target="tpu_custom_call" | custom-call | tf_op jit(solution)/shard_map/pallas_call | solution.py:59
  (11 shorter events, 0.0 us)
Async XLA Ops:
  4.2 44.5 %all-to-all-start = ((bf16[32,48,128]{2,1,0:T(8,128)(2,1)}), bf16[32,48,128]{2,1,0:T(8,128)(2,1)S(1)}, u32[]{:S(2)}, u32[]{:S(2)}) async-start(bf16[32,48,128]{2,1,0:T(8,128)(2,1)} %get-tuple-element.49), calls=%async_computation | async-start | bytes 786432 | tf_op jit(solution)/shard_map/all_to_all | solution.py:537
  23.4 34.0 %copy-start = (bf16[3072,128]{1,0:T(8,128)(2,1)S(1)}, bf16[3072,128]{1,0:T(8,128)(2,1)}, u32[]{:S(2)}) copy-start(bf16[3072,128]{1,0:T(8,128)(2,1)} %get-tuple-element.51.refs_1_) | copy-start | bytes 2359300
  23.4 38.5 %copy-start.1 = (bf16[3072,128]{1,0:T(8,128)(2,1)S(1)}, bf16[3072,128]{1,0:T(8,128)(2,1)}, u32[]{:S(2)}) copy-start(bf16[3072,128]{1,0:T(8,128)(2,1)} %get-tuple-element.52.refs_2_) | copy-start | bytes 2359300
  23.4 40.4 %collective-permute-start = (bf16[3072,128]{1,0:T(8,128)(2,1)}, bf16[3072,128]{1,0:T(8,128)(2,1)}, u32[]{:S(2)}, u32[]{:S(2)}) collective-permute-start(bf16[3072,128]{1,0:T(8,128)(2,1)} %get-tuple-element.51.refs_1_), channel_id=1, source_target_pairs={{0,1},{16,20},{1,2},{17,21},{2,3},{18,22},{3,0},{19,23},{4,5},{20,... | collective-permute-start | bytes 2359304 | tf_op jit(solution)/shard_map/ppermute | solution.py:550
  26.8 39.2 %collective-permute-start.3 = (bf16[3072,128]{1,0:T(8,128)(2,1)}, bf16[3072,128]{1,0:T(8,128)(2,1)}, u32[]{:S(2)}, u32[]{:S(2)}) collective-permute-start(bf16[3072,128]{1,0:T(8,128)(2,1)} %get-tuple-element.52.refs_2_), channel_id=1, source_target_pairs={{0,3},{16,28},{1,0},{17,29},{2,1},{18,30},{3,2},{19,31},{4,7},{20,... | collective-permute-start | bytes 2359304 | tf_op jit(solution)/shard_map/ppermute | solution.py:550
  50.6 42.6 %all-to-all-start.1 = ((bf16[16,320,128]{2,1,0:T(8,128)(2,1)}), bf16[16,320,128]{2,1,0:T(8,128)(2,1)S(1)}, u32[]{:S(2)}, u32[]{:S(2)}) async-start(bf16[16,320,128]{2,1,0:T(8,128)(2,1)} %get-tuple-element.50.refs_1_), calls=%async_computation.1 | async-start | bytes 2621440 | tf_op jit(solution)/shard_map/all_to_all | solution.py:537
  57.4 25.3 %collective-permute-start.2 = (bf16[3072,128]{1,0:T(8,128)(2,1)S(1)}, bf16[3072,128]{1,0:T(8,128)(2,1)S(1)}, u32[]{:S(2)}, u32[]{:S(2)}) collective-permute-start(bf16[3072,128]{1,0:T(8,128)(2,1)S(1)} %copy-done), channel_id=1, source_target_pairs={{0,3},{16,28},{1,0},{17,29},{2,1},{18,30},{3,2},{19,31},{4,7},{20,... | collective-permute-start | bytes 2359304 | tf_op jit(solution)/shard_map/ppermute | solution.py:550
  61.9 22.3 %collective-permute-start.1 = (bf16[3072,128]{1,0:T(8,128)(2,1)S(1)}, bf16[3072,128]{1,0:T(8,128)(2,1)S(1)}, u32[]{:S(2)}, u32[]{:S(2)}) collective-permute-start(bf16[3072,128]{1,0:T(8,128)(2,1)S(1)} %copy-done.1), channel_id=1, source_target_pairs={{0,1},{16,20},{1,2},{17,21},{2,3},{18,22},{3,0},{19,23},{4,5},{20,... | collective-permute-start | bytes 2359304 | tf_op jit(solution)/shard_map/ppermute | solution.py:550
  63.9 28.5 %collective-permute-start.4 = (bf16[3072,128]{1,0:T(8,128)(2,1)}, bf16[3072,128]{1,0:T(8,128)(2,1)S(1)}, u32[]{:S(2)}, u32[]{:S(2)}) collective-permute-start(bf16[3072,128]{1,0:T(8,128)(2,1)} %collective-permute-done.refs_3_), channel_id=1, source_target_pairs={{0,1},{16,20},{1,2},{17,21},{2,3},{18,22},{3,0},{19,23},{4,5},{20,... | collective-permute-start | bytes 2359304 | tf_op jit(solution)/shard_map/ppermute | solution.py:550
  66.0 27.2 %collective-permute-start.5 = (bf16[3072,128]{1,0:T(8,128)(2,1)}, bf16[3072,128]{1,0:T(8,128)(2,1)}, u32[]{:S(2)}, u32[]{:S(2)}) collective-permute-start(bf16[3072,128]{1,0:T(8,128)(2,1)} %collective-permute-done.3.refs_6_), channel_id=1, source_target_pairs={{0,3},{16,28},{1,0},{17,29},{2,1},{18,30},{3,2},{19,31},{4,7},{20,... | collective-permute-start | bytes 2359304 | tf_op jit(solution)/shard_map/ppermute | solution.py:550
  82.7 9.6 %copy-start.2 = (bf16[3072,128]{1,0:T(8,128)(2,1)}, bf16[3072,128]{1,0:T(8,128)(2,1)S(1)}, u32[]{:S(2)}) copy-start(bf16[3072,128]{1,0:T(8,128)(2,1)S(1)} %collective-permute-done.2.refs_5_) | copy-start | bytes 2359300
  84.2 8.1 %copy-start.3 = (bf16[3072,128]{1,0:T(8,128)(2,1)}, bf16[3072,128]{1,0:T(8,128)(2,1)S(1)}, u32[]{:S(2)}) copy-start(bf16[3072,128]{1,0:T(8,128)(2,1)S(1)} %collective-permute-done.1.refs_4_) | copy-start | bytes 2359300
  92.3 0.9 copy-start.4
  116.9 25.2 %all-to-all-start.3 = ((bf16[32,24,128]{2,1,0:T(8,128)(2,1)}), bf16[32,24,128]{2,1,0:T(8,128)(2,1)S(1)}, u32[]{:S(2)}, u32[]{:S(2)}) async-start(bf16[32,24,128]{2,1,0:T(8,128)(2,1)} %shard_map.184), calls=%async_computation.3 | async-start | bytes 393216 | tf_op jit(solution)/shard_map/all_to_all | solution.py:537
  144.3 20.0 %all-to-all-start.4 = ((bf16[16,256,128]{2,1,0:T(8,128)(2,1)}), bf16[16,256,128]{2,1,0:T(8,128)(2,1)}, u32[]{:S(2)}, u32[]{:S(2)}) async-start(bf16[16,256,128]{2,1,0:T(8,128)(2,1)} %shard_map.186.refs_4_.refs_5_), calls=%async_computation.4 | async-start | bytes 2097152 | tf_op jit(solution)/shard_map/all_to_all | solution.py:537
  153.6 26.2 %collective-permute-start.6 = (bf16[6144,128]{1,0:T(8,128)(2,1)}, bf16[6144,128]{1,0:T(8,128)(2,1)S(1)}, u32[]{:S(2)}, u32[]{:S(2)}) collective-permute-start(bf16[6144,128]{1,0:T(8,128)(2,1)} %get-tuple-element.57), channel_id=1, source_target_pairs={{0,3},{16,28},{1,0},{17,29},{2,1},{18,30},{3,2},{19,31},{4,7},{20,... | collective-permute-start | bytes 4718600 | tf_op jit(solution)/shard_map/ppermute | solution.py:550
  158.0 23.8 %collective-permute-start.7 = (bf16[6144,128]{1,0:T(8,128)(2,1)}, bf16[6144,128]{1,0:T(8,128)(2,1)S(1)}, u32[]{:S(2)}, u32[]{:S(2)}) collective-permute-start(bf16[6144,128]{1,0:T(8,128)(2,1)} %get-tuple-element.58), channel_id=1, source_target_pairs={{0,1},{16,20},{1,2},{17,21},{2,3},{18,22},{3,0},{19,23},{4,5},{20,... | collective-permute-start | bytes 4718600 | tf_op jit(solution)/shard_map/ppermute | solution.py:550
  167.2 6.2 %collective-permute-start.10 = (bf16[1088,128]{1,0:T(8,128)(2,1)S(1)}, bf16[1088,128]{1,0:T(8,128)(2,1)S(1)}, u32[]{:S(2)}, u32[]{:S(2)}) collective-permute-start(bf16[1088,128]{1,0:T(8,128)(2,1)S(1)} %get-tuple-element.67), channel_id=1, source_target_pairs={{0,16},{16,0},{1,17},{17,1},{2,18},{18,2},{3,19},{19,3},{4,20},{20... | collective-permute-start | bytes 835592 | tf_op jit(solution)/shard_map/ppermute | solution.py:677
  174.9 28.9 %all-to-all-start.5 = ((bf16[16,96,128]{2,1,0:T(8,128)(2,1)}), bf16[16,96,128]{2,1,0:T(8,128)(2,1)S(1)}, u32[]{:S(2)}, u32[]{:S(2)}) async-start(bf16[16,96,128]{2,1,0:T(8,128)(2,1)} %get-tuple-element.71.refs_6_), calls=%async_computation.5 | async-start | bytes 786432 | tf_op jit(solution)/shard_map/all_to_all | solution.py:537
  184.6 14.4 %collective-permute-start.8 = (bf16[3072,128]{1,0:T(8,128)(2,1)}, bf16[3072,128]{1,0:T(8,128)(2,1)S(1)}, u32[]{:S(2)}, u32[]{:S(2)}) collective-permute-start(bf16[3072,128]{1,0:T(8,128)(2,1)} %get-tuple-element.64), channel_id=1, source_target_pairs={{0,1},{16,20},{1,2},{17,21},{2,3},{18,22},{3,0},{19,23},{4,5},{20,... | collective-permute-start | bytes 2359304 | tf_op jit(solution)/shard_map/ppermute | solution.py:550
  186.7 13.8 %collective-permute-start.9 = (bf16[3072,128]{1,0:T(8,128)(2,1)}, bf16[3072,128]{1,0:T(8,128)(2,1)S(1)}, u32[]{:S(2)}, u32[]{:S(2)}) collective-permute-start(bf16[3072,128]{1,0:T(8,128)(2,1)} %get-tuple-element.65), channel_id=1, source_target_pairs={{0,3},{16,28},{1,0},{17,29},{2,1},{18,30},{3,2},{19,31},{4,7},{20,... | collective-permute-start | bytes 2359304 | tf_op jit(solution)/shard_map/ppermute | solution.py:550

commit v8 on v6

--- a/solution.py
+++ b/solution.py
@@ -21,6 +21,7 @@
 SLOTS = N_SP * PAD
 PART = ROWS // 4
 LOT = 3 * 1024
+EARLY = LOT // 2
 NBLK = TOK // BLOCK
 BF = jnp.bfloat16
 F32 = jnp.float32
@@ -264,36 +265,53 @@
         both = mm(x, grads, TN)
         down = mm(hidden, g, TN)
         at = k * 128
-        for b, (a_part, b_part) in enumerate(lots_of(out_refs)):
-            (a_ref, a_at), (b_ref, b_at) = a_part, b_part
-            kind = a_ref.dtype
-            up = both[:, 256 * b + 128 : 256 * b + 256].astype(kind)
-            a_ref[a_at + at : a_at + at + 256, :] = both[:, 256 * b : 256 * b + 128].astype(kind)
+        for b in range(4):
+
+            def put(lot, row, value):
+                ref, start = place_of(out_refs, b, lot, row)
+                ref[start : start + len(value), :] = value.astype(ref.dtype)
+
+            put(0, at, both[:, 256 * b : 256 * b + 128])
+            up = both[:, 256 * b + 128 : 256 * b + 256]
             if k < N_TP // 2:
-                a_ref[a_at + 2048 + at : a_at + 2304 + at, :] = up
+                put(0, 2048 + at, up)
             else:
-                b_ref[b_at + at - 1024 : b_at + at - 768, :] = up
+                put(1, at - 1024, up)
             for n in range(2):
-                block = b_at + 1024 + at + n * 128
-                b_ref[block : block + 128, :] = down[
-                    128 * b : 128 * b + 128, n * 128 : (n + 1) * 128
-                ].astype(kind)
-
-
-def lots_of(refs):
-    own_a, own_b, to_left, to_right, left_b, right_a = refs
-    return (
-        ((own_a, 0), (own_b, 0)),
-        ((to_left, 0), (left_b, 0)),
-        ((right_a, 0), (to_right, LOT)),
-        ((to_right, 0), (to_left, LOT)),
-    )
-
-
-def relay_kernel(left_b_ref, right_a_ref, from_right_ref, from_left_ref, to_left_ref, to_right_ref):
-    far_a, far_b = from_left_ref[:LOT, :].astype(F32), from_right_ref[LOT:, :].astype(F32)
-    to_right_ref[...] = (right_a_ref[...].astype(F32) + far_a).astype(BF)
-    to_left_ref[...] = (left_b_ref[...].astype(F32) + far_b).astype(BF)
+                block = down[128 * b : 128 * b + 128, n * 128 : (n + 1) * 128]
+                put(1, 1024 + at + n * 128, block)
+
+
+def place_of(refs, device, lot, row):
+    own_a, own_b, to_left, to_right, left_b, left_late, right_a, right_late = refs
+    if device == 0:
+        return (own_a, own_b)[lot], row
+    if device == 3:
+        return ((to_right, row), (to_left, EARLY + row))[lot]
+    if device == 1:
+        if lot == 1:
+            return left_b, row
+        return (to_left, row) if row < EARLY else (left_late, row - EARLY)
+    if lot == 0:
+        return right_a, row
+    return (to_right, LOT + row) if row < EARLY else (right_late, row - EARLY)
+
+
+def relay_kernel(
+    left_b_ref,
+    left_late_ref,
+    right_a_ref,
+    right_late_ref,
+    from_right_ref,
+    from_left_ref,
+    to_left_ref,
+    to_right_ref,
+):
+    far_a, far_b = from_left_ref[:LOT, :].astype(F32), from_right_ref[EARLY:, :].astype(F32)
+    to_right_ref[:LOT, :] = (right_a_ref[...].astype(F32) + far_a).astype(BF)
+    to_right_ref[LOT:, :] = right_late_ref[...]
+    to_left_ref[:EARLY, :] = left_late_ref[...]
+    to_left_ref[EARLY:, :] = (left_b_ref[...].astype(F32) + far_b).astype(BF)
 
 
 def grad_sum_kernel(
@@ -301,26 +319,28 @@
     own_b_ref,
     from_right_ref,
     from_left_ref,
-    last_a_ref,
-    last_b_ref,
+    last_left_ref,
+    last_right_ref,
     gate_ref,
     up_ref,
     down_ref,
 ):
-    def total(at, size):
-        if at < LOT:
-            refs = (own_a_ref, from_right_ref, last_a_ref)
-            rows = [r[at : at + size, :].astype(F32) for r in refs]
+    def total(at):
+        lot, row = divmod(at, LOT)
+        if lot == 0:
+            own, summed = (own_a_ref, row), (last_left_ref, row)
+            single = (from_right_ref if row < EARLY else last_right_ref, row % EARLY)
         else:
-            own, last = (r[at - LOT : at - LOT + size, :] for r in (own_b_ref, last_b_ref))
-            rows = [own, from_left_ref[at : at + size, :].astype(F32), last.astype(F32)]
+            own, summed = (own_b_ref, row), (last_right_ref, EARLY + row)
+            single = (from_left_ref if row < EARLY else last_left_ref, LOT + row % EARLY)
+        rows = [r[start : start + 128, :].astype(F32) for r, start in (own, summed, single)]
         return (rows[0] + rows[1] + rows[2]).astype(BF)
 
     for k in range(N_TP):
         here = slice(k * 128, (k + 1) * 128)
-        gate_ref[here, :] = total(k * 128, 128)
-        up_ref[here, :] = total(2048 + k * 128, 128)
-        down_ref[:, here] = total(4096 + k * 128, 128)
+        gate_ref[here, :] = total(k * 128)
+        up_ref[here, :] = total(2048 + k * 128)
+        down_ref[:, here] = total(4096 + k * 128)
 
 
 def row_sum_kernel(place_ref, part_ref, states_ref, out_ref, total):
@@ -606,14 +626,15 @@
         raw=tuple(range(1, 9)),
     )
     arrived = exchanged(partial_rows, "tp")
-    own_grad_a, own_grad_b, to_left, to_right, left_lot, right_lot = call(
+    own_grad_a, own_grad_b, to_left, to_right, *held_back = call(
         weight_grads_kernel,
-        2 * [((LOT, 128), F32)] + 2 * [((2 * LOT, 128), BF)] + 2 * [((LOT, 128), BF)],
+        2 * [((LOT, 128), F32)]
+        + 2 * [((LOT + EARLY, 128), BF)]
+        + 2 * [((LOT, 128), BF), ((EARLY, 128), BF)],
         rows,
         grads,
         hidden,
         near=(0, 1, 2),
-        near_out=(2, 3),
     )
     from_left = passed_on(to_right, 1)
     from_right = passed_on(to_left, -1)
@@ -623,7 +644,6 @@
         place,
         arrived,
         states,
-        near_out=(0,),
         smem=(0,),
         near=(1,),
         scratch=[pltpu.VMEM((ROWS + 8, 128), F32)],
@@ -633,14 +653,12 @@
     full_grad = exchanged(residual, "tp")
     lot_left, lot_right = call(
         relay_kernel,
-        2 * [((LOT, 128), BF)],
-        left_lot,
-        right_lot,
+        2 * [((LOT + EARLY, 128), BF)],
+        *held_back,
         from_right,
         from_left,
         after=(residual,),
-        near=(2, 3),
-        near_out=(0, 1),
+        near=(4, 5),
     )
     last_a = passed_on(lot_right, 1)
     last_b = passed_on(lot_left, -1)

time: 208 us -> 209 us (level)
  transfers between devices with their start and end apart: 16 -> 16, of which waited for: 11 -> 9; matrix products, arithmetic and copies ran while one was open for 0% -> 0% of each run, Pallas kernels for 13% -> 14%
where the time goes in v8:
time: 209 us; the launch traced here: 206 us
  starting transfers between devices  75 us (36%)
  waiting for transfers between devices  69.9 us (33%)
  Pallas kernels  43.9 us (21%)
  blocking collectives  15.7 us (8%)
    pallas_call x15, Pallas kernels, call(): pl.pallas_call(run, out_shape=tuple(((pltpu.VMEM if k in near_out else pl...  43.9 us
    all_to_all x5, starting transfers between devices, exchanged(): return lax.all_to_all(blocks, axis, split_axis=0, concat_axis=0, tiled=True)  37.5 us
    all_to_all x5, waiting for transfers between devices, exchanged(): return lax.all_to_all(blocks, axis, split_axis=0, concat_axis=0, tiled=True)  37.3 us
    ppermute x10, starting transfers between devices, passed_on(): return lax.ppermute(array, ('sp_1', 'tp'), ring_step(step))  32.5 us
    ppermute x10, waiting for transfers between devices, passed_on(): return lax.ppermute(array, ('sp_1', 'tp'), ring_step(step))  31.4 us
    all_to_all x1, blocking collectives, exchanged(): return lax.all_to_all(blocks, axis, split_axis=0, concat_axis=0, tiled=True)  15.7 us
    ppermute x1, starting transfers between devices, body(): from_other = lax.ppermute(to_other, 'sp_1', [(0, 1), (1, 0)])  5.02 us
  transfers between devices with their start and end apart: 16, of which 9 were waited for; matrix products, arithmetic and copies ran while one was open for 0% of the time, Pallas kernels for 14%

profile of v8, /device:TPU:1, one launch (start us, length us, event | category | flops | bytes accessed | tf_op | source)
XLA Modules:
  0.0 206.4 jit_solution(3408229327626661700)
XLA Ops:
  0.6 3.5 %shard_map.179 = (bf16[32,48,128]{2,1,0:T(8,128)(2,1)}, bf16[768,256]{1,0:T(8,128)(2,1)}) custom-call(s32[2,256]{1,0:T(2,128)} %bitcast.30, f32[2,256]{1,0:T(2,128)} %bitcast.31, bf16[256,128]{1,0:T(8,128)(2,1)} %refs_2_.3, bf16[256,128]{1,0:T(8,128)(2,1)} %refs_2_.4, bf16[64,256]{1,0:T(8,128)(2,1)} %bitcast.24, bf16[256,128]{1,0:T(8,128)(2,1)} %refs_5_.3, ...), custom_call_target="tpu_custom_call" | custom-call | tf_op jit(solution)/shard_map/pallas_call | solution.py:60
  4.2 16.7 %all-to-all-start = ((bf16[32,48,128]{2,1,0:T(8,128)(2,1)}), bf16[32,48,128]{2,1,0:T(8,128)(2,1)S(1)}, u32[]{:S(2)}, u32[]{:S(2)}) async-start(bf16[32,48,128]{2,1,0:T(8,128)(2,1)} %get-tuple-element.51), calls=%async_computation | async-start | bytes 786432 | tf_op jit(solution)/shard_map/all_to_all | solution.py:549
  20.9 2.5 %shard_map.181 = (bf16[3072,128]{1,0:T(8,128)(2,1)}, bf16[3072,128]{1,0:T(8,128)(2,1)}) custom-call(bf16[2048,128]{1,0:T(8,128)(2,1)} %bitcast.21, bf16[2048,128]{1,0:T(8,128)(2,1)} %bitcast.22, bf16[128,2048]{1,0:T(8,128)(2,1)} %bitcast.23), custom_call_target="tpu_custom_call" | custom-call | tf_op jit(solution)/shard_map/pallas_call | solution.py:60
  23.4 3.2 %collective-permute-start = (bf16[3072,128]{1,0:T(8,128)(2,1)}, bf16[3072,128]{1,0:T(8,128)(2,1)}, u32[]{:S(2)}, u32[]{:S(2)}) collective-permute-start(bf16[3072,128]{1,0:T(8,128)(2,1)} %get-tuple-element.53.refs_1_), channel_id=1, source_target_pairs={{0,1},{16,20},{1,2},{17,21},{2,3},{18,22},{3,0},{19,23},{4,5},{20,... | collective-permute-start | bytes 2359304 | tf_op jit(solution)/shard_map/ppermute | solution.py:562
  26.6 3.4 %collective-permute-start.3 = (bf16[3072,128]{1,0:T(8,128)(2,1)}, bf16[3072,128]{1,0:T(8,128)(2,1)}, u32[]{:S(2)}, u32[]{:S(2)}) collective-permute-start(bf16[3072,128]{1,0:T(8,128)(2,1)} %get-tuple-element.54.refs_2_), channel_id=1, source_target_pairs={{0,3},{16,28},{1,0},{17,29},{2,1},{18,30},{3,2},{19,31},{4,7},{20,... | collective-permute-start | bytes 2359304 | tf_op jit(solution)/shard_map/ppermute | solution.py:562
  30.0 0.1 pad_add_fusion.refs_0_
  30.1 18.6 %all-to-all-done.refs_1_ = bf16[32,48,128]{2,1,0:T(8,128)(2,1)S(1)} async-done(((bf16[32,48,128]{2,1,0:T(8,128)(2,1)}), bf16[32,48,128]{2,1,0:T(8,128)(2,1)S(1)}, u32[]{:S(2)}, u32[]{:S(2)}) %all-to-all-start) | async-done | bytes 393248 | tf_op jit(solution)/shard_map/all_to_all | solution.py:549
  48.7 2.0 shard_map.180
  50.7 6.9 %all-to-all-start.1 = ((bf16[16,320,128]{2,1,0:T(8,128)(2,1)}), bf16[16,320,128]{2,1,0:T(8,128)(2,1)S(1)}, u32[]{:S(2)}, u32[]{:S(2)}) async-start(bf16[16,320,128]{2,1,0:T(8,128)(2,1)} %get-tuple-element.52.refs_1_), calls=%async_computation.1 | async-start | bytes 2621440 | tf_op jit(solution)/shard_map/all_to_all | solution.py:549
  57.6 4.5 %collective-permute-start.2 = (bf16[3072,128]{1,0:T(8,128)(2,1)S(1)}, bf16[3072,128]{1,0:T(8,128)(2,1)S(1)}, u32[]{:S(2)}, u32[]{:S(2)}) collective-permute-start(bf16[3072,128]{1,0:T(8,128)(2,1)S(1)} %copy-done.2), channel_id=1, source_target_pairs={{0,3},{16,28},{1,0},{17,29},{2,1},{18,30},{3,2},{19,31},{4,7},{20,... | collective-permute-start | bytes 2359304 | tf_op jit(solution)/shard_map/ppermute | solution.py:562
  62.1 1.9 collective-permute-start.1
  64.0 0.0 collective-permute-done.refs_3_
  64.0 2.1 %collective-permute-start.4 = (bf16[3072,128]{1,0:T(8,128)(2,1)}, bf16[3072,128]{1,0:T(8,128)(2,1)S(1)}, u32[]{:S(2)}, u32[]{:S(2)}) collective-permute-start(bf16[3072,128]{1,0:T(8,128)(2,1)} %collective-permute-done.refs_3_), channel_id=1, source_target_pairs={{0,1},{16,20},{1,2},{17,21},{2,3},{18,22},{3,0},{19,23},{4,5},{20,... | collective-permute-start | bytes 2359304 | tf_op jit(solution)/shard_map/ppermute | solution.py:562
  66.2 0.0 collective-permute-done.3.refs_6_
  66.2 4.3 %collective-permute-start.5 = (bf16[3072,128]{1,0:T(8,128)(2,1)}, bf16[3072,128]{1,0:T(8,128)(2,1)}, u32[]{:S(2)}, u32[]{:S(2)}) collective-permute-start(bf16[3072,128]{1,0:T(8,128)(2,1)} %collective-permute-done.3.refs_6_), channel_id=1, source_target_pairs={{0,3},{16,28},{1,0},{17,29},{2,1},{18,30},{3,2},{19,31},{4,7},{20,... | collective-permute-start | bytes 2359304 | tf_op jit(solution)/shard_map/ppermute | solution.py:562
  70.5 12.3 %collective-permute-done.2.refs_5_ = bf16[3072,128]{1,0:T(8,128)(2,1)S(1)} collective-permute-done((bf16[3072,128]{1,0:T(8,128)(2,1)S(1)}, bf16[3072,128]{1,0:T(8,128)(2,1)S(1)}, u32[]{:S(2)}, u32[]{:S(2)}) %collective-permute-start.2) | collective-permute-done | bytes 786464 | tf_op jit(solution)/shard_map/ppermute | solution.py:562
  82.8 1.5 collective-permute-done.1.refs_4_
  84.3 8.1 %collective-permute-done.4.refs_7_ = bf16[3072,128]{1,0:T(8,128)(2,1)S(1)} collective-permute-done((bf16[3072,128]{1,0:T(8,128)(2,1)}, bf16[3072,128]{1,0:T(8,128)(2,1)S(1)}, u32[]{:S(2)}, u32[]{:S(2)}) %collective-permute-start.4) | collective-permute-done | bytes 786464 | tf_op jit(solution)/shard_map/ppermute | solution.py:562
  92.5 0.9 copy-done.6
  93.4 0.0 collective-permute-done.5.refs_8_
  93.4 5.8 %shard_map.182 = (bf16[16,160,128]{2,1,0:T(8,128)(2,1)}, bf16[160,1024]{1,0:T(8,128)(2,1)S(1)}, bf16[160,512]{1,0:T(8,128)(2,1)S(1)}) custom-call(bf16[16,320,128]{2,1,0:T(8,128)(2,1)S(1)} %all-to-all-done.1.refs_0_, bf16[3072,128]{1,0:T(8,128)(2,1)} %get-tuple-element.53.refs_1_, bf16[3072,128]{1,0:T(8,128)(2,1)} %get-tuple-element.54.refs_2_, ...), custom_call_target="tpu_custom_call" | custom-call | tf_op jit(solution)/shard_map/pallas_call | solution.py:60
  99.2 15.7 %all_to_all.30.refs_1_ = bf16[16,160,128]{2,1,0:T(8,128)(2,1)S(1)} all-to-all(bf16[16,160,128]{2,1,0:T(8,128)(2,1)} %get-tuple-element.65), channel_id=1, replica_groups=mesh['sp_0'=16,'sp_1'=2,'tp'=16] {'tp'}, dimensions={0} | all-to-all | bytes 1310720 | tf_op jit(solution)/shard_map/all_to_all | solution.py:549
  114.9 1.5 shard_map.184
  116.4 6.2 %all-to-all-start.3 = ((bf16[32,24,128]{2,1,0:T(8,128)(2,1)}), bf16[32,24,128]{2,1,0:T(8,128)(2,1)S(1)}, u32[]{:S(2)}, u32[]{:S(2)}) async-start(bf16[32,24,128]{2,1,0:T(8,128)(2,1)} %shard_map.184), calls=%async_computation.3 | async-start | bytes 393216 | tf_op jit(solution)/shard_map/all_to_all | solution.py:549
  122.6 1.9 shard_map.185.refs_1_
  124.5 17.0 %all-to-all-done.3.refs_0_ = bf16[32,24,128]{2,1,0:T(8,128)(2,1)S(1)} async-done(((bf16[32,24,128]{2,1,0:T(8,128)(2,1)}), bf16[32,24,128]{2,1,0:T(8,128)(2,1)S(1)}, u32[]{:S(2)}, u32[]{:S(2)}) %all-to-all-start.3) | async-done | bytes 196640 | tf_op jit(solution)/shard_map/all_to_all | solution.py:549
  141.6 2.3 %shard_map.186.refs_6_.refs_5_ = bf16[16,256,128]{2,1,0:T(8,128)(2,1)} custom-call(bf16[32,24,128]{2,1,0:T(8,128)(2,1)S(1)} %all-to-all-done.3.refs_0_, bf16[256,768]{1,0:T(8,128)(2,1)} %shard_map.185.refs_1_, bf16[256,128]{1,0:T(8,128)(2,1)} %refs_2_.4), custom_call_target="tpu_custom_call" | custom-call | tf_op jit(solution)/shard_map/pallas_call | solution.py:60
  143.9 3.7 %all-to-all-start.4 = ((bf16[16,256,128]{2,1,0:T(8,128)(2,1)}), bf16[16,256,128]{2,1,0:T(8,128)(2,1)S(1)}, u32[]{:S(2)}, u32[]{:S(2)}) async-start(bf16[16,256,128]{2,1,0:T(8,128)(2,1)} %shard_map.186.refs_6_.refs_5_), calls=%async_computation.4 | async-start | bytes 2097152 | tf_op jit(solution)/shard_map/all_to_all | solution.py:549
  147.6 0.0 copy-start.1
  147.6 4.8 %shard_map.183 = (f32[3072,128]{1,0:T(8,128)}, f32[3072,128]{1,0:T(8,128)}, bf16[4608,128]{1,0:T(8,128)(2,1)}, bf16[4608,128]{1,0:T(8,128)(2,1)}, bf16[3072,128]...) custom-call(bf16[16,320,128]{2,1,0:T(8,128)(2,1)S(1)} %all-to-all-done.1.refs_0_, ...), custom_call_target="tpu_custom_call" | custom-call | tf_op jit(solution)/shard_map/pallas_call | solution.py:60
  152.4 4.4 %collective-permute-start.6 = (bf16[4608,128]{1,0:T(8,128)(2,1)}, bf16[4608,128]{1,0:T(8,128)(2,1)S(1)}, u32[]{:S(2)}, u32[]{:S(2)}) collective-permute-start(bf16[4608,128]{1,0:T(8,128)(2,1)} %get-tuple-element.59), channel_id=1, source_target_pairs={{0,3},{16,28},{1,0},{17,29},{2,1},{18,30},{3,2},{19,31},{4,7},{20,... | collective-permute-start | bytes 3538952 | tf_op jit(solution)/shard_map/ppermute | solution.py:562
  156.9 1.9 collective-permute-start.7
  158.8 2.7 %shard_map.188 = (bf16[256,128]{1,0:T(8,128)(2,1)S(1)}, f32[4,128,64]{2,1,0:T(8,128)}) custom-call(bf16[32,24,128]{2,1,0:T(8,128)(2,1)S(1)} %copy-done.1, bf16[64,256]{1,0:T(8,128)(2,1)} %bitcast.27, bf16[64,256]{1,0:T(8,128)(2,1)} %bitcast.25, bf16[256,128]{1,0:T(8,128)(2,1)} %refs_5_.3, f32[64,256]{1,0:T(8,128)} %bitcast.18, ...), custom_call_target="tpu_custom_call" | custom-call | tf_op jit(solution)/shard_map/pallas_call | solution.py:60
  161.5 1.7 all-to-all-done.4.refs_1_
  163.2 2.2 %shard_map.189 = (f32[256,128]{1,0:T(8,128)}, f32[32,128]{1,0:T(8,128)S(1)}, bf16[1088,128]{1,0:T(8,128)(2,1)S(1)}, f32[1024,128]{1,0:T(8,128)S(1)}) custom-call(s32[3]{0:T(128)S(1)} %pad_add_fusion.refs_0_, bf16[16,256,128]{2,1,0:T(8,128)(2,1)S(1)} %all-to-all-done.4.refs_1_, bf16[2048,128]{1,0:T(8,128)(2,1)} %refs_2_.5, ...), custom_call_target="tpu_custom_call" | custom-call | tf_op jit(solution)/shard_map/pallas_call | solution.py:60
  165.4 5.0 %collective-permute-start.10 = (bf16[1088,128]{1,0:T(8,128)(2,1)S(1)}, bf16[1088,128]{1,0:T(8,128)(2,1)S(1)}, u32[]{:S(2)}, u32[]{:S(2)}) collective-permute-start(bf16[1088,128]{1,0:T(8,128)(2,1)S(1)} %get-tuple-element.71), channel_id=1, source_target_pairs={{0,16},{16,0},{1,17},{17,1},{2,18},{18,2},{3,19},{19,3},{4,20},{20... | collective-permute-start | bytes 835592 | tf_op jit(solution)/shard_map/ppermute | solution.py:690
  170.4 1.2 collective-permute-done.10.refs_1_
  171.6 1.6 shard_map.190
  173.1 4.0 %all-to-all-start.5 = ((bf16[16,96,128]{2,1,0:T(8,128)(2,1)}), bf16[16,96,128]{2,1,0:T(8,128)(2,1)S(1)}, u32[]{:S(2)}, u32[]{:S(2)}) async-start(bf16[16,96,128]{2,1,0:T(8,128)(2,1)} %get-tuple-element.75.refs_6_), calls=%async_computation.5 | async-start | bytes 786432 | tf_op jit(solution)/shard_map/all_to_all | solution.py:549
  177.2 0.0 collective-permute-done.6.refs_4_.refs_2_
  177.2 3.3 %shard_map.187 = (bf16[4608,128]{1,0:T(8,128)(2,1)}, bf16[4608,128]{1,0:T(8,128)(2,1)}) custom-call(bf16[3072,128]{1,0:T(8,128)(2,1)} %get-tuple-element.61.refs_0_, bf16[1536,128]{1,0:T(8,128)(2,1)} %get-tuple-element.62.refs_1_, bf16[3072,128]{1,0:T(8,128)(2,1)} %get-tuple-element.63.refs_2_, bf16[1536,128]{1,0:T(8,128)(2,1)} %get-tuple-element.64.refs_3_, ...), custom_call_target="tpu_custom_call" | custom-call | tf_op jit(solution)/shard_map/pallas_call | solution.py:60
  180.5 1.9 collective-permute-start.8
  182.4 4.8 %collective-permute-start.9 = (bf16[4608,128]{1,0:T(8,128)(2,1)}, bf16[4608,128]{1,0:T(8,128)(2,1)S(1)}, u32[]{:S(2)}, u32[]{:S(2)}) collective-permute-start(bf16[4608,128]{1,0:T(8,128)(2,1)} %get-tuple-element.69), channel_id=1, source_target_pairs={{0,3},{16,28},{1,0},{17,29},{2,1},{18,30},{3,2},{19,31},{4,7},{20,... | collective-permute-start | bytes 3538952 | tf_op jit(solution)/shard_map/ppermute | solution.py:562
  187.2 3.8 %shard_map.192 = (bf16[64,256]{1,0:T(8,128)(2,1)}, f32[256,128]{1,0:T(8,128)}, f32[256,64]{1,0:T(8,128)}, f32[256,64]{1,0:T(8,128)}, f32[256,64]{1,0:T(8,128)}, ...) custom-call(f32[256,128]{1,0:T(8,128)} %get-tuple-element.81.refs_0_, ...), custom_call_target="tpu_custom_call" | custom-call | tf_op jit(solution)/shard_map/pallas_call | solution.py:60
  190.9 8.2 %collective-permute-done.8.refs_4_ = bf16[4608,128]{1,0:T(8,128)(2,1)S(1)} collective-permute-done((bf16[4608,128]{1,0:T(8,128)(2,1)}, bf16[4608,128]{1,0:T(8,128)(2,1)S(1)}, u32[]{:S(2)}, u32[]{:S(2)}) %collective-permute-start.8) | collective-permute-done | bytes 1179680 | tf_op jit(solution)/shard_map/ppermute | solution.py:562
  199.1 1.3 collective-permute-done.9.refs_5_
  200.4 3.4 %shard_map.191 = (bf16[2048,128]{1,0:T(8,128)(2,1)}, bf16[2048,128]{1,0:T(8,128)(2,1)}, bf16[128,2048]{1,0:T(8,128)(2,1)}) custom-call(f32[3072,128]{1,0:T(8,128)} %get-tuple-element.57.refs_0_, f32[3072,128]{1,0:T(8,128)} %get-tuple-element.58.refs_1_, bf16[4608,128]{1,0:T(8,128)(2,1)S(1)} %collective-permute-done.6.refs_4_.refs_2_, ...), custom_call_target="tpu_custom_call" | custom-call | tf_op jit(solution)/shard_map/pallas_call | solution.py:60
  203.8 2.6 %shard_map.193 = (f32[64,128]{1,0:T(8,128)}, bf16[64,256]{1,0:T(8,128)(2,1)}, bf16[256,128]{1,0:T(8,128)(2,1)}, f32[64,256]{1,0:T(8,128)}) custom-call(s32[3]{0:T(128)S(1)} %pad_add_fusion.refs_0_, bf16[16,96,128]{2,1,0:T(8,128)(2,1)S(1)} %all-to-all-done.5.refs_1_, f32[32,128]{1,0:T(8,128)} %get-tuple-element.79.refs_2_, ...), custom_call_target="tpu_custom_call" | custom-call | tf_op jit(solution)/shard_map/pallas_call | solution.py:60
  (15 shorter events, 0.0 us)
Async XLA Ops:
  4.2 44.5 %all-to-all-start = ((bf16[32,48,128]{2,1,0:T(8,128)(2,1)}), bf16[32,48,128]{2,1,0:T(8,128)(2,1)S(1)}, u32[]{:S(2)}, u32[]{:S(2)}) async-start(bf16[32,48,128]{2,1,0:T(8,128)(2,1)} %get-tuple-element.51), calls=%async_computation | async-start | bytes 786432 | tf_op jit(solution)/shard_map/all_to_all | solution.py:549
  23.4 40.6 %collective-permute-start = (bf16[3072,128]{1,0:T(8,128)(2,1)}, bf16[3072,128]{1,0:T(8,128)(2,1)}, u32[]{:S(2)}, u32[]{:S(2)}) collective-permute-start(bf16[3072,128]{1,0:T(8,128)(2,1)} %get-tuple-element.53.refs_1_), channel_id=1, source_target_pairs={{0,1},{16,20},{1,2},{17,21},{2,3},{18,22},{3,0},{19,23},{4,5},{20,... | collective-permute-start | bytes 2359304 | tf_op jit(solution)/shard_map/ppermute | solution.py:562
  26.6 39.5 %collective-permute-start.3 = (bf16[3072,128]{1,0:T(8,128)(2,1)}, bf16[3072,128]{1,0:T(8,128)(2,1)}, u32[]{:S(2)}, u32[]{:S(2)}) collective-permute-start(bf16[3072,128]{1,0:T(8,128)(2,1)} %get-tuple-element.54.refs_2_), channel_id=1, source_target_pairs={{0,3},{16,28},{1,0},{17,29},{2,1},{18,30},{3,2},{19,31},{4,7},{20,... | collective-permute-start | bytes 2359304 | tf_op jit(solution)/shard_map/ppermute | solution.py:562
  50.7 6.9 %copy-start.2 = (bf16[3072,128]{1,0:T(8,128)(2,1)S(1)}, bf16[3072,128]{1,0:T(8,128)(2,1)}, u32[]{:S(2)}) copy-start(bf16[3072,128]{1,0:T(8,128)(2,1)} %get-tuple-element.53.refs_1_) | copy-start | bytes 2359300
  50.7 11.4 %copy-start.3 = (bf16[3072,128]{1,0:T(8,128)(2,1)S(1)}, bf16[3072,128]{1,0:T(8,128)(2,1)}, u32[]{:S(2)}) copy-start(bf16[3072,128]{1,0:T(8,128)(2,1)} %get-tuple-element.54.refs_2_) | copy-start | bytes 2359300
  50.7 42.7 %all-to-all-start.1 = ((bf16[16,320,128]{2,1,0:T(8,128)(2,1)}), bf16[16,320,128]{2,1,0:T(8,128)(2,1)S(1)}, u32[]{:S(2)}, u32[]{:S(2)}) async-start(bf16[16,320,128]{2,1,0:T(8,128)(2,1)} %get-tuple-element.52.refs_1_), calls=%async_computation.1 | async-start | bytes 2621440 | tf_op jit(solution)/shard_map/all_to_all | solution.py:549
  57.6 25.3 %collective-permute-start.2 = (bf16[3072,128]{1,0:T(8,128)(2,1)S(1)}, bf16[3072,128]{1,0:T(8,128)(2,1)S(1)}, u32[]{:S(2)}, u32[]{:S(2)}) collective-permute-start(bf16[3072,128]{1,0:T(8,128)(2,1)S(1)} %copy-done.2), channel_id=1, source_target_pairs={{0,3},{16,28},{1,0},{17,29},{2,1},{18,30},{3,2},{19,31},{4,7},{20,... | collective-permute-start | bytes 2359304 | tf_op jit(solution)/shard_map/ppermute | solution.py:562
  62.1 22.3 %collective-permute-start.1 = (bf16[3072,128]{1,0:T(8,128)(2,1)S(1)}, bf16[3072,128]{1,0:T(8,128)(2,1)S(1)}, u32[]{:S(2)}, u32[]{:S(2)}) collective-permute-start(bf16[3072,128]{1,0:T(8,128)(2,1)S(1)} %copy-done.3), channel_id=1, source_target_pairs={{0,1},{16,20},{1,2},{17,21},{2,3},{18,22},{3,0},{19,23},{4,5},{20,... | collective-permute-start | bytes 2359304 | tf_op jit(solution)/shard_map/ppermute | solution.py:562
  64.0 28.5 %collective-permute-start.4 = (bf16[3072,128]{1,0:T(8,128)(2,1)}, bf16[3072,128]{1,0:T(8,128)(2,1)S(1)}, u32[]{:S(2)}, u32[]{:S(2)}) collective-permute-start(bf16[3072,128]{1,0:T(8,128)(2,1)} %collective-permute-done.refs_3_), channel_id=1, source_target_pairs={{0,1},{16,20},{1,2},{17,21},{2,3},{18,22},{3,0},{19,23},{4,5},{20,... | collective-permute-start | bytes 2359304 | tf_op jit(solution)/shard_map/ppermute | solution.py:562
  66.2 27.2 %collective-permute-start.5 = (bf16[3072,128]{1,0:T(8,128)(2,1)}, bf16[3072,128]{1,0:T(8,128)(2,1)}, u32[]{:S(2)}, u32[]{:S(2)}) collective-permute-start(bf16[3072,128]{1,0:T(8,128)(2,1)} %collective-permute-done.3.refs_6_), channel_id=1, source_target_pairs={{0,3},{16,28},{1,0},{17,29},{2,1},{18,30},{3,2},{19,31},{4,7},{20,... | collective-permute-start | bytes 2359304 | tf_op jit(solution)/shard_map/ppermute | solution.py:562
  82.8 9.6 %copy-start.4 = (bf16[3072,128]{1,0:T(8,128)(2,1)}, bf16[3072,128]{1,0:T(8,128)(2,1)S(1)}, u32[]{:S(2)}) copy-start(bf16[3072,128]{1,0:T(8,128)(2,1)S(1)} %collective-permute-done.2.refs_5_) | copy-start | bytes 2359300
  84.3 8.1 %copy-start.5 = (bf16[3072,128]{1,0:T(8,128)(2,1)}, bf16[3072,128]{1,0:T(8,128)(2,1)S(1)}, u32[]{:S(2)}) copy-start(bf16[3072,128]{1,0:T(8,128)(2,1)S(1)} %collective-permute-done.1.refs_4_) | copy-start | bytes 2359300
  92.5 0.9 copy-start.6
  116.4 25.2 %all-to-all-start.3 = ((bf16[32,24,128]{2,1,0:T(8,128)(2,1)}), bf16[32,24,128]{2,1,0:T(8,128)(2,1)S(1)}, u32[]{:S(2)}, u32[]{:S(2)}) async-start(bf16[32,24,128]{2,1,0:T(8,128)(2,1)} %shard_map.184), calls=%async_computation.3 | async-start | bytes 393216 | tf_op jit(solution)/shard_map/all_to_all | solution.py:549
  141.6 2.3 %copy-start = (bf16[32,24,128]{2,1,0:T(8,128)(2,1)}, bf16[32,24,128]{2,1,0:T(8,128)(2,1)S(1)}, u32[]{:S(2)}) copy-start(bf16[32,24,128]{2,1,0:T(8,128)(2,1)S(1)} %all-to-all-done.3.refs_0_) | copy-start | bytes 589828
  143.9 19.3 %all-to-all-start.4 = ((bf16[16,256,128]{2,1,0:T(8,128)(2,1)}), bf16[16,256,128]{2,1,0:T(8,128)(2,1)S(1)}, u32[]{:S(2)}, u32[]{:S(2)}) async-start(bf16[16,256,128]{2,1,0:T(8,128)(2,1)} %shard_map.186.refs_6_.refs_5_), calls=%async_computation.4 | async-start | bytes 2097152 | tf_op jit(solution)/shard_map/all_to_all | solution.py:549
  147.6 11.2 %copy-start.1 = (bf16[32,24,128]{2,1,0:T(8,128)(2,1)S(1)}, bf16[32,24,128]{2,1,0:T(8,128)(2,1)}, u32[]{:S(2)}) copy-start(bf16[32,24,128]{2,1,0:T(8,128)(2,1)} %copy-done) | copy-start | bytes 589828
  152.4 24.7 %collective-permute-start.6 = (bf16[4608,128]{1,0:T(8,128)(2,1)}, bf16[4608,128]{1,0:T(8,128)(2,1)S(1)}, u32[]{:S(2)}, u32[]{:S(2)}) collective-permute-start(bf16[4608,128]{1,0:T(8,128)(2,1)} %get-tuple-element.59), channel_id=1, source_target_pairs={{0,3},{16,28},{1,0},{17,29},{2,1},{18,30},{3,2},{19,31},{4,7},{20,... | collective-permute-start | bytes 3538952 | tf_op jit(solution)/shard_map/ppermute | solution.py:562
  156.9 20.3 %collective-permute-start.7 = (bf16[4608,128]{1,0:T(8,128)(2,1)}, bf16[4608,128]{1,0:T(8,128)(2,1)S(1)}, u32[]{:S(2)}, u32[]{:S(2)}) collective-permute-start(bf16[4608,128]{1,0:T(8,128)(2,1)} %get-tuple-element.60), channel_id=1, source_target_pairs={{0,1},{16,20},{1,2},{17,21},{2,3},{18,22},{3,0},{19,23},{4,5},{20,... | collective-permute-start | bytes 3538952 | tf_op jit(solution)/shard_map/ppermute | solution.py:562
  165.4 6.2 %collective-permute-start.10 = (bf16[1088,128]{1,0:T(8,128)(2,1)S(1)}, bf16[1088,128]{1,0:T(8,128)(2,1)S(1)}, u32[]{:S(2)}, u32[]{:S(2)}) collective-permute-start(bf16[1088,128]{1,0:T(8,128)(2,1)S(1)} %get-tuple-element.71), channel_id=1, source_target_pairs={{0,16},{16,0},{1,17},{17,1},{2,18},{18,2},{3,19},{19,3},{4,20},{20... | collective-permute-start | bytes 835592 | tf_op jit(solution)/shard_map/ppermute | solution.py:690
  173.1 30.7 %all-to-all-start.5 = ((bf16[16,96,128]{2,1,0:T(8,128)(2,1)}), bf16[16,96,128]{2,1,0:T(8,128)(2,1)S(1)}, u32[]{:S(2)}, u32[]{:S(2)}) async-start(bf16[16,96,128]{2,1,0:T(8,128)(2,1)} %get-tuple-element.75.refs_6_), calls=%async_computation.5 | async-start | bytes 786432 | tf_op jit(solution)/shard_map/all_to_all | solution.py:549
  180.5 18.7 %collective-permute-start.8 = (bf16[4608,128]{1,0:T(8,128)(2,1)}, bf16[4608,128]{1,0:T(8,128)(2,1)S(1)}, u32[]{:S(2)}, u32[]{:S(2)}) collective-permute-start(bf16[4608,128]{1,0:T(8,128)(2,1)} %get-tuple-element.68), channel_id=1, source_target_pairs={{0,1},{16,20},{1,2},{17,21},{2,3},{18,22},{3,0},{19,23},{4,5},{20,... | collective-permute-start | bytes 3538952 | tf_op jit(solution)/shard_map/ppermute | solution.py:562
  182.4 18.0 %collective-permute-start.9 = (bf16[4608,128]{1,0:T(8,128)(2,1)}, bf16[4608,128]{1,0:T(8,128)(2,1)S(1)}, u32[]{:S(2)}, u32[]{:S(2)}) collective-permute-start(bf16[4608,128]{1,0:T(8,128)(2,1)} %get-tuple-element.69), channel_id=1, source_target_pairs={{0,3},{16,28},{1,0},{17,29},{2,1},{18,30},{3,2},{19,31},{4,7},{20,... | collective-permute-start | bytes 3538952 | tf_op jit(solution)/shard_map/ppermute | solution.py:562

commit v9 on v8

--- a/solution.py
+++ b/solution.py
@@ -45,13 +45,14 @@
     return lax.broadcasted_iota(jnp.int32, shape, dim)
 
 
-def call(fn, outs, *args, scratch=(), smem=(), near=(), near_out=(), after=(), raw=()):
+def call(fn, outs, *args, scratch=(), smem=(), near=(), near_out=(), after=(), raw=(), near_after=False):
     spaces = [pltpu.VMEM if k in near else pltpu.HBM for k in range(len(args))]
     args = [
         a if k in smem else pltpu.with_memory_space_constraint(a, spaces[k])
         for k, a in enumerate(args)
     ]
-    after = [pltpu.with_memory_space_constraint(a, pltpu.HBM) for a in after]
+    after_space = pltpu.VMEM if near_after else pltpu.HBM
+    after = [pltpu.with_memory_space_constraint(a, after_space) for a in after]
     count = len(args)
 
     def run(*refs):
@@ -68,7 +69,7 @@
             )
             for k in range(count)
         ]
-        + [pl.BlockSpec(memory_space=pltpu.HBM) for _ in after],
+        + [pl.BlockSpec(memory_space=after_space) for _ in after],
         out_specs=tuple(pl.BlockSpec(memory_space=pltpu.VMEM) for _ in outs),
         scratch_shapes=scratch,
         compiler_params=pltpu.CompilerParams(vmem_limit_bytes=24 * 1024 * 1024),
@@ -175,7 +176,7 @@
     return jnp.where(place_ref[1] == 0, k % 4, k // 4)
 
 
-def copies_kernel(place_ref, recv_ref, out_ref, states_ref, reach_ref, packed, rounded):
+def copies_kernel(place_ref, recv_ref, out_ref, packed, rounded):
     for e in range(N_SP):
         block = recv_ref[e].astype(F32)
         at = (e // 8) * 2 * PART + (e % 8) * CAP
@@ -185,6 +186,13 @@
         rounded[q] = packed[q * 2 * PART : (q + 1) * 2 * PART, :].astype(BF)
     for k in range(N_TP):
         out_ref[k] = rounded[quarter_of(place_ref, k)]
+
+
+def mark_kernel(out_ref):
+    out_ref[...] = jnp.zeros((8, 128), F32)
+
+
+def scan_kernel(place_ref, recv_ref, states_ref, reach_ref):
     chip = place_ref[2]
     totals = [recv_ref[s, PAD + CAP : PAD + CAP + 1, :].astype(F32) for s in range(N_SP)]
     totals = jnp.concatenate(totals, axis=0)
@@ -603,9 +611,9 @@
     far_a = passed_on(left_a, 1)
     far_b = passed_on(right_b, -1)
     weights = (own_a, own_b, left_a, left_b, right_a, right_b, far_a, far_b)
-    copies, states, reach = call(
+    (copies,) = call(
         copies_kernel,
-        [((N_TP, 2 * PART, 128), BF), ((N_SP, 128), F32), ((24, 128), F32)],
+        [((N_TP, 2 * PART, 128), BF)],
         place,
         recv,
         scratch=[pltpu.VMEM((2 * ROWS, 128), F32), pltpu.VMEM((4, 2 * PART, 128), BF)],
@@ -614,7 +622,8 @@
         near_out=(0,),
     )
     rows = exchanged(copies, "tp")
-    (turned,) = call(turned_kernel, [((TOK, SLOTS), BF)], pick, after=(copies,))
+    (mark,) = call(mark_kernel, [((8, 128), F32)], after=(rows,), near_after=True)
+    (turned,) = call(turned_kernel, [((TOK, SLOTS), BF)], pick)
     partial_rows, grads, hidden = call(
         partial_kernel,
         [((N_TP, PART, 128), BF), ((PART, 1024), BF), ((PART, 512), BF)],
@@ -624,6 +633,15 @@
         near=(0,),
         near_out=(1, 2),
         raw=tuple(range(1, 9)),
+        after=(mark,),
+    )
+    states, reach = call(
+        scan_kernel,
+        [((N_SP, 128), F32), ((24, 128), F32)],
+        place,
+        recv,
+        smem=(0,),
+        after=(partial_rows,),
     )
     arrived = exchanged(partial_rows, "tp")
     own_grad_a, own_grad_b, to_left, to_right, *held_back = call(

time: 209 us -> 210 us (level)
  blocking collectives: 15.7 us -> 0 us
  waiting for transfers between devices: 69.9 us -> 79 us
  starting transfers between devices: 75 us -> 79.8 us
  Pallas kernels: 43.9 us -> 46.2 us
    all_to_all x1 -> x0, blocking collectives: 15.7 us -> none  [exchanged(): return lax.all_to_all(blocks, axis, split_axis=0, concat_axis=0, tiled=True)]
    all_to_all x5 -> x6, waiting for transfers between devices: 37.3 us -> 52.9 us  [exchanged(): return lax.all_to_all(blocks, axis, split_axis=0, concat_axis=0, tiled=True)]
    ppermute x10, waiting for transfers between devices: 31.4 us -> 24.9 us  [passed_on(): return lax.ppermute(array, ('sp_1', 'tp'), ring_step(step))]
    all_to_all x5 -> x6, starting transfers between devices: 37.5 us -> 42.2 us  [exchanged(): return lax.all_to_all(blocks, axis, split_axis=0, concat_axis=0, tiled=True)]
    pallas_call x15 -> x17, Pallas kernels: 43.9 us -> 46.2 us  [call(): pl.pallas_call(run, out_shape=tuple(((pltpu.VMEM if k in near_out else pl...]
  transfers between devices with their start and end apart: 16 -> 17, of which waited for: 9 -> 10; matrix products, arithmetic and copies ran while one was open for 0% -> 0% of each run, Pallas kernels for 14% -> 15%
where the time goes in v9:
time: 210 us; the launch traced here: 207 us
  starting transfers between devices  79.8 us (38%)
  waiting for transfers between devices  79 us (38%)
  Pallas kernels  46.2 us (22%)
    all_to_all x6, waiting for transfers between devices, exchanged(): return lax.all_to_all(blocks, axis, split_axis=0, concat_axis=0, tiled=True)  52.9 us
    pallas_call x17, Pallas kernels, call(): pl.pallas_call(run, out_shape=tuple(((pltpu.VMEM if k in near_out else pl...  46.2 us
    all_to_all x6, starting transfers between devices, exchanged(): return lax.all_to_all(blocks, axis, split_axis=0, concat_axis=0, tiled=True)  42.2 us
    ppermute x10, starting transfers between devices, passed_on(): return lax.ppermute(array, ('sp_1', 'tp'), ring_step(step))  32.6 us
    ppermute x10, waiting for transfers between devices, passed_on(): return lax.ppermute(array, ('sp_1', 'tp'), ring_step(step))  24.9 us
    ppermute x1, starting transfers between devices, body(): from_other = lax.ppermute(to_other, 'sp_1', [(0, 1), (1, 0)])  5.02 us
  transfers between devices with their start and end apart: 17, of which 10 were waited for; matrix products, arithmetic and copies ran while one was open for 0% of the time, Pallas kernels for 15%

profile of v9, /device:TPU:1, one launch (start us, length us, event | category | flops | bytes accessed | tf_op | source)
XLA Modules:
  0.0 206.6 jit_solution(15408010275599228430)
XLA Ops:
  0.6 3.5 %shard_map.179 = (bf16[32,48,128]{2,1,0:T(8,128)(2,1)}, bf16[768,256]{1,0:T(8,128)(2,1)}) custom-call(s32[2,256]{1,0:T(2,128)} %bitcast.30, f32[2,256]{1,0:T(2,128)} %bitcast.31, bf16[256,128]{1,0:T(8,128)(2,1)} %refs_2_.3, bf16[256,128]{1,0:T(8,128)(2,1)} %refs_2_.4, bf16[64,256]{1,0:T(8,128)(2,1)} %bitcast.24, bf16[256,128]{1,0:T(8,128)(2,1)} %refs_5_.3, ...), custom_call_target="tpu_custom_call" | custom-call | tf_op jit(solution)/shard_map/pallas_call | solution.py:61
  4.2 16.7 %all-to-all-start = ((bf16[32,48,128]{2,1,0:T(8,128)(2,1)}), bf16[32,48,128]{2,1,0:T(8,128)(2,1)S(1)}, u32[]{:S(2)}, u32[]{:S(2)}) async-start(bf16[32,48,128]{2,1,0:T(8,128)(2,1)} %get-tuple-element.50), calls=%async_computation | async-start | bytes 786432 | tf_op jit(solution)/shard_map/all_to_all | solution.py:557
  20.9 2.6 %shard_map.181 = (bf16[3072,128]{1,0:T(8,128)(2,1)}, bf16[3072,128]{1,0:T(8,128)(2,1)}) custom-call(bf16[2048,128]{1,0:T(8,128)(2,1)} %bitcast.21, bf16[2048,128]{1,0:T(8,128)(2,1)} %bitcast.22, bf16[128,2048]{1,0:T(8,128)(2,1)} %bitcast.23), custom_call_target="tpu_custom_call" | custom-call | tf_op jit(solution)/shard_map/pallas_call | solution.py:61
  23.5 3.2 %collective-permute-start = (bf16[3072,128]{1,0:T(8,128)(2,1)}, bf16[3072,128]{1,0:T(8,128)(2,1)}, u32[]{:S(2)}, u32[]{:S(2)}) collective-permute-start(bf16[3072,128]{1,0:T(8,128)(2,1)} %get-tuple-element.51.refs_1_), channel_id=1, source_target_pairs={{0,1},{16,20},{1,2},{17,21},{2,3},{18,22},{3,0},{19,23},{4,5},{20,... | collective-permute-start | bytes 2359304 | tf_op jit(solution)/shard_map/ppermute | solution.py:570
  26.7 3.4 %collective-permute-start.3 = (bf16[3072,128]{1,0:T(8,128)(2,1)}, bf16[3072,128]{1,0:T(8,128)(2,1)}, u32[]{:S(2)}, u32[]{:S(2)}) collective-permute-start(bf16[3072,128]{1,0:T(8,128)(2,1)} %get-tuple-element.52.refs_2_), channel_id=1, source_target_pairs={{0,3},{16,28},{1,0},{17,29},{2,1},{18,30},{3,2},{19,31},{4,7},{20,... | collective-permute-start | bytes 2359304 | tf_op jit(solution)/shard_map/ppermute | solution.py:570
  30.0 0.1 pad_add_fusion.refs_0_
  30.1 18.6 %all-to-all-done.refs_1_ = bf16[32,48,128]{2,1,0:T(8,128)(2,1)S(1)} async-done(((bf16[32,48,128]{2,1,0:T(8,128)(2,1)}), bf16[32,48,128]{2,1,0:T(8,128)(2,1)S(1)}, u32[]{:S(2)}, u32[]{:S(2)}) %all-to-all-start) | async-done | bytes 393248 | tf_op jit(solution)/shard_map/all_to_all | solution.py:557
  48.7 1.8 shard_map.180
  50.4 6.9 %all-to-all-start.1 = ((bf16[16,320,128]{2,1,0:T(8,128)(2,1)}), bf16[16,320,128]{2,1,0:T(8,128)(2,1)S(1)}, u32[]{:S(2)}, u32[]{:S(2)}) async-start(bf16[16,320,128]{2,1,0:T(8,128)(2,1)} %shard_map.180), calls=%async_computation.1 | async-start | bytes 2621440 | tf_op jit(solution)/shard_map/all_to_all | solution.py:557
  57.4 3.3 %collective-permute-start.1 = (bf16[3072,128]{1,0:T(8,128)(2,1)S(1)}, bf16[3072,128]{1,0:T(8,128)(2,1)}, u32[]{:S(2)}, u32[]{:S(2)}) collective-permute-start(bf16[3072,128]{1,0:T(8,128)(2,1)S(1)} %copy-done.6), channel_id=1, source_target_pairs={{0,1},{16,20},{1,2},{17,21},{2,3},{18,22},{3,0},{19,23},{4,5},{20,... | collective-permute-start | bytes 2359304 | tf_op jit(solution)/shard_map/ppermute | solution.py:570
  60.6 3.2 %collective-permute-start.2 = (bf16[3072,128]{1,0:T(8,128)(2,1)S(1)}, bf16[3072,128]{1,0:T(8,128)(2,1)}, u32[]{:S(2)}, u32[]{:S(2)}) collective-permute-start(bf16[3072,128]{1,0:T(8,128)(2,1)S(1)} %copy-done.5), channel_id=1, source_target_pairs={{0,3},{16,28},{1,0},{17,29},{2,1},{18,30},{3,2},{19,31},{4,7},{20,... | collective-permute-start | bytes 2359304 | tf_op jit(solution)/shard_map/ppermute | solution.py:570
  63.9 0.0 collective-permute-done.refs_3_
  63.9 2.1 collective-permute-start.4
  66.0 4.4 %collective-permute-start.5 = (bf16[3072,128]{1,0:T(8,128)(2,1)}, bf16[3072,128]{1,0:T(8,128)(2,1)}, u32[]{:S(2)}, u32[]{:S(2)}) collective-permute-start(bf16[3072,128]{1,0:T(8,128)(2,1)} %collective-permute-done.3.refs_6_), channel_id=1, source_target_pairs={{0,3},{16,28},{1,0},{17,29},{2,1},{18,30},{3,2},{19,31},{4,7},{20,... | collective-permute-start | bytes 2359304 | tf_op jit(solution)/shard_map/ppermute | solution.py:570
  70.4 5.9 %all-to-all-done.1.refs_0_ = bf16[16,320,128]{2,1,0:T(8,128)(2,1)S(1)} async-done(((bf16[16,320,128]{2,1,0:T(8,128)(2,1)}), bf16[16,320,128]{2,1,0:T(8,128)(2,1)S(1)}, u32[]{:S(2)}, u32[]{:S(2)}) %all-to-all-start.1) | async-done | bytes 1310752 | tf_op jit(solution)/shard_map/all_to_all | solution.py:557
  76.3 0.6 shard_map.182.refs_9_
  76.9 7.3 %collective-permute-done.1.refs_4_ = bf16[3072,128]{1,0:T(8,128)(2,1)} collective-permute-done((bf16[3072,128]{1,0:T(8,128)(2,1)S(1)}, bf16[3072,128]{1,0:T(8,128)(2,1)}, u32[]{:S(2)}, u32[]{:S(2)}) %collective-permute-start.1) | collective-permute-done | bytes 786464 | tf_op jit(solution)/shard_map/ppermute | solution.py:570
  84.2 8.1 %collective-permute-done.4.refs_7_ = bf16[3072,128]{1,0:T(8,128)(2,1)} collective-permute-done((bf16[3072,128]{1,0:T(8,128)(2,1)}, bf16[3072,128]{1,0:T(8,128)(2,1)}, u32[]{:S(2)}, u32[]{:S(2)}) %collective-permute-start.4) | collective-permute-done | bytes 786464 | tf_op jit(solution)/shard_map/ppermute | solution.py:570
  92.4 5.7 %shard_map.183 = (bf16[16,160,128]{2,1,0:T(8,128)(2,1)}, bf16[160,1024]{1,0:T(8,128)(2,1)S(1)}, bf16[160,512]{1,0:T(8,128)(2,1)S(1)}) custom-call(bf16[16,320,128]{2,1,0:T(8,128)(2,1)S(1)} %all-to-all-done.1.refs_0_, bf16[3072,128]{1,0:T(8,128)(2,1)} %get-tuple-element.51.refs_1_, bf16[3072,128]{1,0:T(8,128)(2,1)} %get-tuple-element.52.refs_2_, ...), custom_call_target="tpu_custom_call" | custom-call | tf_op jit(solution)/shard_map/pallas_call | solution.py:61
  98.1 0.7 copy-done.3
  98.8 5.0 %all-to-all-start.2 = ((bf16[16,160,128]{2,1,0:T(8,128)(2,1)}), bf16[16,160,128]{2,1,0:T(8,128)(2,1)S(1)}, u32[]{:S(2)}, u32[]{:S(2)}) async-start(bf16[16,160,128]{2,1,0:T(8,128)(2,1)} %get-tuple-element.63.refs_2_), calls=%async_computation.2 | async-start | bytes 1310720 | tf_op jit(solution)/shard_map/all_to_all | solution.py:557
  103.8 1.9 shard_map.185
  105.7 9.7 %all-to-all-done.2.refs_1_ = bf16[16,160,128]{2,1,0:T(8,128)(2,1)S(1)} async-done(((bf16[16,160,128]{2,1,0:T(8,128)(2,1)}), bf16[16,160,128]{2,1,0:T(8,128)(2,1)S(1)}, u32[]{:S(2)}, u32[]{:S(2)}) %all-to-all-start.2) | async-done | bytes 655392 | tf_op jit(solution)/shard_map/all_to_all | solution.py:557
  115.3 1.5 shard_map.186
  116.8 5.9 %all-to-all-start.3 = ((bf16[32,24,128]{2,1,0:T(8,128)(2,1)}), bf16[32,24,128]{2,1,0:T(8,128)(2,1)S(1)}, u32[]{:S(2)}, u32[]{:S(2)}) async-start(bf16[32,24,128]{2,1,0:T(8,128)(2,1)} %shard_map.186), calls=%async_computation.3 | async-start | bytes 393216 | tf_op jit(solution)/shard_map/all_to_all | solution.py:557
  122.7 1.9 shard_map.187.refs_1_
  124.6 17.0 %all-to-all-done.3.refs_0_ = bf16[32,24,128]{2,1,0:T(8,128)(2,1)S(1)} async-done(((bf16[32,24,128]{2,1,0:T(8,128)(2,1)}), bf16[32,24,128]{2,1,0:T(8,128)(2,1)S(1)}, u32[]{:S(2)}, u32[]{:S(2)}) %all-to-all-start.3) | async-done | bytes 196640 | tf_op jit(solution)/shard_map/all_to_all | solution.py:557
  141.7 2.4 %shard_map.188.refs_6_.refs_5_ = bf16[16,256,128]{2,1,0:T(8,128)(2,1)} custom-call(bf16[32,24,128]{2,1,0:T(8,128)(2,1)S(1)} %all-to-all-done.3.refs_0_, bf16[256,768]{1,0:T(8,128)(2,1)} %shard_map.187.refs_1_, bf16[256,128]{1,0:T(8,128)(2,1)} %refs_2_.4), custom_call_target="tpu_custom_call" | custom-call | tf_op jit(solution)/shard_map/pallas_call | solution.py:61
  144.0 3.8 %all-to-all-start.4 = ((bf16[16,256,128]{2,1,0:T(8,128)(2,1)}), bf16[16,256,128]{2,1,0:T(8,128)(2,1)S(1)}, u32[]{:S(2)}, u32[]{:S(2)}) async-start(bf16[16,256,128]{2,1,0:T(8,128)(2,1)} %shard_map.188.refs_6_.refs_5_), calls=%async_computation.4 | async-start | bytes 2097152 | tf_op jit(solution)/shard_map/all_to_all | solution.py:557
  147.8 0.0 copy-start.2
  147.8 4.8 %shard_map.184 = (f32[3072,128]{1,0:T(8,128)}, f32[3072,128]{1,0:T(8,128)}, bf16[4608,128]{1,0:T(8,128)(2,1)}, bf16[4608,128]{1,0:T(8,128)(2,1)}, bf16[3072,128]...) custom-call(bf16[16,320,128]{2,1,0:T(8,128)(2,1)S(1)} %all-to-all-done.1.refs_0_, ...), custom_call_target="tpu_custom_call" | custom-call | tf_op jit(solution)/shard_map/pallas_call | solution.py:61
  152.7 4.4 %collective-permute-start.6 = (bf16[4608,128]{1,0:T(8,128)(2,1)}, bf16[4608,128]{1,0:T(8,128)(2,1)S(1)}, u32[]{:S(2)}, u32[]{:S(2)}) collective-permute-start(bf16[4608,128]{1,0:T(8,128)(2,1)} %get-tuple-element.57), channel_id=1, source_target_pairs={{0,3},{16,28},{1,0},{17,29},{2,1},{18,30},{3,2},{19,31},{4,7},{20,... | collective-permute-start | bytes 3538952 | tf_op jit(solution)/shard_map/ppermute | solution.py:570
  157.1 1.9 collective-permute-start.7
  159.1 2.7 %shard_map.190 = (bf16[256,128]{1,0:T(8,128)(2,1)S(1)}, f32[4,128,64]{2,1,0:T(8,128)}) custom-call(bf16[32,24,128]{2,1,0:T(8,128)(2,1)S(1)} %copy-done.2, bf16[64,256]{1,0:T(8,128)(2,1)} %bitcast.27, bf16[64,256]{1,0:T(8,128)(2,1)} %bitcast.25, bf16[256,128]{1,0:T(8,128)(2,1)} %refs_5_.3, f32[64,256]{1,0:T(8,128)} %bitcast.18, ...), custom_call_target="tpu_custom_call" | custom-call | tf_op jit(solution)/shard_map/pallas_call | solution.py:61
  161.7 1.7 all-to-all-done.4.refs_1_
  163.4 2.2 %shard_map.191 = (f32[256,128]{1,0:T(8,128)}, f32[32,128]{1,0:T(8,128)S(1)}, bf16[1088,128]{1,0:T(8,128)(2,1)S(1)}, f32[1024,128]{1,0:T(8,128)S(1)}) custom-call(s32[3]{0:T(128)S(1)} %pad_add_fusion.refs_0_, bf16[16,256,128]{2,1,0:T(8,128)(2,1)S(1)} %all-to-all-done.4.refs_1_, bf16[2048,128]{1,0:T(8,128)(2,1)} %refs_2_.5, ...), custom_call_target="tpu_custom_call" | custom-call | tf_op jit(solution)/shard_map/pallas_call | solution.py:61
  165.6 5.0 %collective-permute-start.10 = (bf16[1088,128]{1,0:T(8,128)(2,1)S(1)}, bf16[1088,128]{1,0:T(8,128)(2,1)S(1)}, u32[]{:S(2)}, u32[]{:S(2)}) collective-permute-start(bf16[1088,128]{1,0:T(8,128)(2,1)S(1)} %get-tuple-element.69), channel_id=1, source_target_pairs={{0,16},{16,0},{1,17},{17,1},{2,18},{18,2},{3,19},{19,3},{4,20},{20... | collective-permute-start | bytes 835592 | tf_op jit(solution)/shard_map/ppermute | solution.py:708
  170.6 1.2 collective-permute-done.10.refs_1_
  171.8 1.6 shard_map.192
  173.4 4.0 %all-to-all-start.5 = ((bf16[16,96,128]{2,1,0:T(8,128)(2,1)}), bf16[16,96,128]{2,1,0:T(8,128)(2,1)S(1)}, u32[]{:S(2)}, u32[]{:S(2)}) async-start(bf16[16,96,128]{2,1,0:T(8,128)(2,1)} %get-tuple-element.73.refs_6_), calls=%async_computation.5 | async-start | bytes 786432 | tf_op jit(solution)/shard_map/all_to_all | solution.py:557
  177.4 3.3 %shard_map.189 = (bf16[4608,128]{1,0:T(8,128)(2,1)}, bf16[4608,128]{1,0:T(8,128)(2,1)}) custom-call(bf16[3072,128]{1,0:T(8,128)(2,1)} %get-tuple-element.59.refs_0_, bf16[1536,128]{1,0:T(8,128)(2,1)} %get-tuple-element.60.refs_1_, bf16[3072,128]{1,0:T(8,128)(2,1)} %get-tuple-element.61.refs_2_, bf16[1536,128]{1,0:T(8,128)(2,1)} %get-tuple-element.62.refs_3_, ...), custom_call_target="tpu_custom_call" | custom-call | tf_op jit(solution)/shard_map/pallas_call | solution.py:61
  180.7 1.9 collective-permute-start.8
  182.6 4.8 %collective-permute-start.9 = (bf16[4608,128]{1,0:T(8,128)(2,1)}, bf16[4608,128]{1,0:T(8,128)(2,1)S(1)}, u32[]{:S(2)}, u32[]{:S(2)}) collective-permute-start(bf16[4608,128]{1,0:T(8,128)(2,1)} %get-tuple-element.67), channel_id=1, source_target_pairs={{0,3},{16,28},{1,0},{17,29},{2,1},{18,30},{3,2},{19,31},{4,7},{20,... | collective-permute-start | bytes 3538952 | tf_op jit(solution)/shard_map/ppermute | solution.py:570
  187.3 3.8 %shard_map.194 = (bf16[64,256]{1,0:T(8,128)(2,1)}, f32[256,128]{1,0:T(8,128)}, f32[256,64]{1,0:T(8,128)}, f32[256,64]{1,0:T(8,128)}, f32[256,64]{1,0:T(8,128)}, ...) custom-call(f32[256,128]{1,0:T(8,128)} %get-tuple-element.79.refs_0_, ...), custom_call_target="tpu_custom_call" | custom-call | tf_op jit(solution)/shard_map/pallas_call | solution.py:61
  191.1 8.2 %collective-permute-done.8.refs_4_ = bf16[4608,128]{1,0:T(8,128)(2,1)S(1)} collective-permute-done((bf16[4608,128]{1,0:T(8,128)(2,1)}, bf16[4608,128]{1,0:T(8,128)(2,1)S(1)}, u32[]{:S(2)}, u32[]{:S(2)}) %collective-permute-start.8) | collective-permute-done | bytes 1179680 | tf_op jit(solution)/shard_map/ppermute | solution.py:570
  199.3 1.3 collective-permute-done.9.refs_5_
  200.6 3.4 %shard_map.193 = (bf16[2048,128]{1,0:T(8,128)(2,1)}, bf16[2048,128]{1,0:T(8,128)(2,1)}, bf16[128,2048]{1,0:T(8,128)(2,1)}) custom-call(f32[3072,128]{1,0:T(8,128)} %get-tuple-element.55.refs_0_, f32[3072,128]{1,0:T(8,128)} %get-tuple-element.56.refs_1_, bf16[4608,128]{1,0:T(8,128)(2,1)S(1)} %collective-permute-done.6.refs_4_.refs_2_, ...), custom_call_target="tpu_custom_call" | custom-call | tf_op jit(solution)/shard_map/pallas_call | solution.py:61
  204.0 2.6 %shard_map.195 = (f32[64,128]{1,0:T(8,128)}, bf16[64,256]{1,0:T(8,128)(2,1)}, bf16[256,128]{1,0:T(8,128)(2,1)}, f32[64,256]{1,0:T(8,128)}) custom-call(s32[3]{0:T(128)S(1)} %pad_add_fusion.refs_0_, bf16[16,96,128]{2,1,0:T(8,128)(2,1)S(1)} %all-to-all-done.5.refs_1_, f32[32,128]{1,0:T(8,128)} %get-tuple-element.77.refs_2_, ...), custom_call_target="tpu_custom_call" | custom-call | tf_op jit(solution)/shard_map/pallas_call | solution.py:61
  (18 shorter events, 0.0 us)
Async XLA Ops:
  4.2 44.5 %all-to-all-start = ((bf16[32,48,128]{2,1,0:T(8,128)(2,1)}), bf16[32,48,128]{2,1,0:T(8,128)(2,1)S(1)}, u32[]{:S(2)}, u32[]{:S(2)}) async-start(bf16[32,48,128]{2,1,0:T(8,128)(2,1)} %get-tuple-element.50), calls=%async_computation | async-start | bytes 786432 | tf_op jit(solution)/shard_map/all_to_all | solution.py:557
  23.5 40.4 %collective-permute-start = (bf16[3072,128]{1,0:T(8,128)(2,1)}, bf16[3072,128]{1,0:T(8,128)(2,1)}, u32[]{:S(2)}, u32[]{:S(2)}) collective-permute-start(bf16[3072,128]{1,0:T(8,128)(2,1)} %get-tuple-element.51.refs_1_), channel_id=1, source_target_pairs={{0,1},{16,20},{1,2},{17,21},{2,3},{18,22},{3,0},{19,23},{4,5},{20,... | collective-permute-start | bytes 2359304 | tf_op jit(solution)/shard_map/ppermute | solution.py:570
  26.7 39.3 %collective-permute-start.3 = (bf16[3072,128]{1,0:T(8,128)(2,1)}, bf16[3072,128]{1,0:T(8,128)(2,1)}, u32[]{:S(2)}, u32[]{:S(2)}) collective-permute-start(bf16[3072,128]{1,0:T(8,128)(2,1)} %get-tuple-element.52.refs_2_), channel_id=1, source_target_pairs={{0,3},{16,28},{1,0},{17,29},{2,1},{18,30},{3,2},{19,31},{4,7},{20,... | collective-permute-start | bytes 2359304 | tf_op jit(solution)/shard_map/ppermute | solution.py:570
  48.7 1.8 copy-start
  50.4 6.9 %copy-start.6 = (bf16[3072,128]{1,0:T(8,128)(2,1)S(1)}, bf16[3072,128]{1,0:T(8,128)(2,1)}, u32[]{:S(2)}) copy-start(bf16[3072,128]{1,0:T(8,128)(2,1)} %get-tuple-element.52.refs_2_) | copy-start | bytes 2359300
  50.4 10.2 %copy-start.5 = (bf16[3072,128]{1,0:T(8,128)(2,1)S(1)}, bf16[3072,128]{1,0:T(8,128)(2,1)}, u32[]{:S(2)}) copy-start(bf16[3072,128]{1,0:T(8,128)(2,1)} %get-tuple-element.51.refs_1_) | copy-start | bytes 2359300
  50.4 25.9 %all-to-all-start.1 = ((bf16[16,320,128]{2,1,0:T(8,128)(2,1)}), bf16[16,320,128]{2,1,0:T(8,128)(2,1)S(1)}, u32[]{:S(2)}, u32[]{:S(2)}) async-start(bf16[16,320,128]{2,1,0:T(8,128)(2,1)} %shard_map.180), calls=%async_computation.1 | async-start | bytes 2621440 | tf_op jit(solution)/shard_map/all_to_all | solution.py:557
  57.4 26.9 %collective-permute-start.1 = (bf16[3072,128]{1,0:T(8,128)(2,1)S(1)}, bf16[3072,128]{1,0:T(8,128)(2,1)}, u32[]{:S(2)}, u32[]{:S(2)}) collective-permute-start(bf16[3072,128]{1,0:T(8,128)(2,1)S(1)} %copy-done.6), channel_id=1, source_target_pairs={{0,1},{16,20},{1,2},{17,21},{2,3},{18,22},{3,0},{19,23},{4,5},{20,... | collective-permute-start | bytes 2359304 | tf_op jit(solution)/shard_map/ppermute | solution.py:570
  60.6 23.6 %collective-permute-start.2 = (bf16[3072,128]{1,0:T(8,128)(2,1)S(1)}, bf16[3072,128]{1,0:T(8,128)(2,1)}, u32[]{:S(2)}, u32[]{:S(2)}) collective-permute-start(bf16[3072,128]{1,0:T(8,128)(2,1)S(1)} %copy-done.5), channel_id=1, source_target_pairs={{0,3},{16,28},{1,0},{17,29},{2,1},{18,30},{3,2},{19,31},{4,7},{20,... | collective-permute-start | bytes 2359304 | tf_op jit(solution)/shard_map/ppermute | solution.py:570
  63.9 28.5 %collective-permute-start.4 = (bf16[3072,128]{1,0:T(8,128)(2,1)}, bf16[3072,128]{1,0:T(8,128)(2,1)}, u32[]{:S(2)}, u32[]{:S(2)}) collective-permute-start(bf16[3072,128]{1,0:T(8,128)(2,1)} %collective-permute-done.refs_3_), channel_id=1, source_target_pairs={{0,1},{16,20},{1,2},{17,21},{2,3},{18,22},{3,0},{19,23},{4,5},{20,... | collective-permute-start | bytes 2359304 | tf_op jit(solution)/shard_map/ppermute | solution.py:570
  66.0 26.4 %collective-permute-start.5 = (bf16[3072,128]{1,0:T(8,128)(2,1)}, bf16[3072,128]{1,0:T(8,128)(2,1)}, u32[]{:S(2)}, u32[]{:S(2)}) collective-permute-start(bf16[3072,128]{1,0:T(8,128)(2,1)} %collective-permute-done.3.refs_6_), channel_id=1, source_target_pairs={{0,3},{16,28},{1,0},{17,29},{2,1},{18,30},{3,2},{19,31},{4,7},{20,... | collective-permute-start | bytes 2359304 | tf_op jit(solution)/shard_map/ppermute | solution.py:570
  98.1 0.7 copy-start.3
  98.8 16.5 %all-to-all-start.2 = ((bf16[16,160,128]{2,1,0:T(8,128)(2,1)}), bf16[16,160,128]{2,1,0:T(8,128)(2,1)S(1)}, u32[]{:S(2)}, u32[]{:S(2)}) async-start(bf16[16,160,128]{2,1,0:T(8,128)(2,1)} %get-tuple-element.63.refs_2_), calls=%async_computation.2 | async-start | bytes 1310720 | tf_op jit(solution)/shard_map/all_to_all | solution.py:557
  116.8 24.8 %all-to-all-start.3 = ((bf16[32,24,128]{2,1,0:T(8,128)(2,1)}), bf16[32,24,128]{2,1,0:T(8,128)(2,1)S(1)}, u32[]{:S(2)}, u32[]{:S(2)}) async-start(bf16[32,24,128]{2,1,0:T(8,128)(2,1)} %shard_map.186), calls=%async_computation.3 | async-start | bytes 393216 | tf_op jit(solution)/shard_map/all_to_all | solution.py:557
  141.7 2.4 %copy-start.1 = (bf16[32,24,128]{2,1,0:T(8,128)(2,1)}, bf16[32,24,128]{2,1,0:T(8,128)(2,1)S(1)}, u32[]{:S(2)}) copy-start(bf16[32,24,128]{2,1,0:T(8,128)(2,1)S(1)} %all-to-all-done.3.refs_0_) | copy-start | bytes 589828
  144.0 3.8 %copy-start.4 = (bf16[160,512]{1,0:T(8,128)(2,1)S(1)}, bf16[160,512]{1,0:T(8,128)(2,1)}, u32[]{:S(2)}) copy-start(bf16[160,512]{1,0:T(8,128)(2,1)} %copy-done.3) | copy-start | bytes 491524
  144.0 19.4 %all-to-all-start.4 = ((bf16[16,256,128]{2,1,0:T(8,128)(2,1)}), bf16[16,256,128]{2,1,0:T(8,128)(2,1)S(1)}, u32[]{:S(2)}, u32[]{:S(2)}) async-start(bf16[16,256,128]{2,1,0:T(8,128)(2,1)} %shard_map.188.refs_6_.refs_5_), calls=%async_computation.4 | async-start | bytes 2097152 | tf_op jit(solution)/shard_map/all_to_all | solution.py:557
  147.8 11.2 %copy-start.2 = (bf16[32,24,128]{2,1,0:T(8,128)(2,1)S(1)}, bf16[32,24,128]{2,1,0:T(8,128)(2,1)}, u32[]{:S(2)}) copy-start(bf16[32,24,128]{2,1,0:T(8,128)(2,1)} %copy-done.1) | copy-start | bytes 589828
  152.7 24.7 %collective-permute-start.6 = (bf16[4608,128]{1,0:T(8,128)(2,1)}, bf16[4608,128]{1,0:T(8,128)(2,1)S(1)}, u32[]{:S(2)}, u32[]{:S(2)}) collective-permute-start(bf16[4608,128]{1,0:T(8,128)(2,1)} %get-tuple-element.57), channel_id=1, source_target_pairs={{0,3},{16,28},{1,0},{17,29},{2,1},{18,30},{3,2},{19,31},{4,7},{20,... | collective-permute-start | bytes 3538952 | tf_op jit(solution)/shard_map/ppermute | solution.py:570
  157.1 20.3 %collective-permute-start.7 = (bf16[4608,128]{1,0:T(8,128)(2,1)}, bf16[4608,128]{1,0:T(8,128)(2,1)S(1)}, u32[]{:S(2)}, u32[]{:S(2)}) collective-permute-start(bf16[4608,128]{1,0:T(8,128)(2,1)} %get-tuple-element.58), channel_id=1, source_target_pairs={{0,1},{16,20},{1,2},{17,21},{2,3},{18,22},{3,0},{19,23},{4,5},{20,... | collective-permute-start | bytes 3538952 | tf_op jit(solution)/shard_map/ppermute | solution.py:570
  165.6 6.2 %collective-permute-start.10 = (bf16[1088,128]{1,0:T(8,128)(2,1)S(1)}, bf16[1088,128]{1,0:T(8,128)(2,1)S(1)}, u32[]{:S(2)}, u32[]{:S(2)}) collective-permute-start(bf16[1088,128]{1,0:T(8,128)(2,1)S(1)} %get-tuple-element.69), channel_id=1, source_target_pairs={{0,16},{16,0},{1,17},{17,1},{2,18},{18,2},{3,19},{19,3},{4,20},{20... | collective-permute-start | bytes 835592 | tf_op jit(solution)/shard_map/ppermute | solution.py:708
  173.4 30.6 %all-to-all-start.5 = ((bf16[16,96,128]{2,1,0:T(8,128)(2,1)}), bf16[16,96,128]{2,1,0:T(8,128)(2,1)S(1)}, u32[]{:S(2)}, u32[]{:S(2)}) async-start(bf16[16,96,128]{2,1,0:T(8,128)(2,1)} %get-tuple-element.73.refs_6_), calls=%async_computation.5 | async-start | bytes 786432 | tf_op jit(solution)/shard_map/all_to_all | solution.py:557
  180.7 18.7 %collective-permute-start.8 = (bf16[4608,128]{1,0:T(8,128)(2,1)}, bf16[4608,128]{1,0:T(8,128)(2,1)S(1)}, u32[]{:S(2)}, u32[]{:S(2)}) collective-permute-start(bf16[4608,128]{1,0:T(8,128)(2,1)} %get-tuple-element.66), channel_id=1, source_target_pairs={{0,1},{16,20},{1,2},{17,21},{2,3},{18,22},{3,0},{19,23},{4,5},{20,... | collective-permute-start | bytes 3538952 | tf_op jit(solution)/shard_map/ppermute | solution.py:570
  182.6 18.0 %collective-permute-start.9 = (bf16[4608,128]{1,0:T(8,128)(2,1)}, bf16[4608,128]{1,0:T(8,128)(2,1)S(1)}, u32[]{:S(2)}, u32[]{:S(2)}) collective-permute-start(bf16[4608,128]{1,0:T(8,128)(2,1)} %get-tuple-element.67), channel_id=1, source_target_pairs={{0,3},{16,28},{1,0},{17,29},{2,1},{18,30},{3,2},{19,31},{4,7},{20,... | collective-permute-start | bytes 3538952 | tf_op jit(solution)/shard_map/ppermute | solution.py:570

commit v10 on v9

--- a/solution.py
+++ b/solution.py
@@ -21,7 +21,8 @@
 SLOTS = N_SP * PAD
 PART = ROWS // 4
 LOT = 3 * 1024
-EARLY = LOT // 2
+EARLY = 2048
+LATE = LOT - EARLY
 NBLK = TOK // BLOCK
 BF = jnp.bfloat16
 F32 = jnp.float32
@@ -45,14 +46,13 @@
     return lax.broadcasted_iota(jnp.int32, shape, dim)
 
 
-def call(fn, outs, *args, scratch=(), smem=(), near=(), near_out=(), after=(), raw=(), near_after=False):
+def call(fn, outs, *args, scratch=(), smem=(), near=(), near_out=(), after=(), raw=()):
     spaces = [pltpu.VMEM if k in near else pltpu.HBM for k in range(len(args))]
     args = [
         a if k in smem else pltpu.with_memory_space_constraint(a, spaces[k])
         for k, a in enumerate(args)
     ]
-    after_space = pltpu.VMEM if near_after else pltpu.HBM
-    after = [pltpu.with_memory_space_constraint(a, after_space) for a in after]
+    after = [pltpu.with_memory_space_constraint(a, pltpu.HBM) for a in after]
     count = len(args)
 
     def run(*refs):
@@ -69,7 +69,7 @@
             )
             for k in range(count)
         ]
-        + [pl.BlockSpec(memory_space=after_space) for _ in after],
+        + [pl.BlockSpec(memory_space=pltpu.HBM) for _ in after],
         out_specs=tuple(pl.BlockSpec(memory_space=pltpu.VMEM) for _ in outs),
         scratch_shapes=scratch,
         compiler_params=pltpu.CompilerParams(vmem_limit_bytes=24 * 1024 * 1024),
@@ -154,17 +154,19 @@
     state_high, state_low = two_parts(packed_state(state))
     total_row = jnp.concatenate(two_parts(total), axis=1)
 
-    first = (mine & (row == CAP)).astype(F32)
-    second = (mine & (row == CAP + 1)).astype(F32)
-    chosen = jnp.concatenate([pick, first, second], axis=1)
-    rows = jnp.concatenate([x_ref[...].astype(F32), state_high, state_low], axis=0)
-    sent_ref[:, :PAD, :] = mm(chosen, rows).astype(BF).reshape(N_SP, PAD, 128)
+    extra = jnp.concatenate(
+        [(mine & (row == CAP)).astype(F32), (mine & (row == CAP + 1)).astype(F32)], axis=1
+    )
+    state_rows = mm(extra, jnp.concatenate([state_high, state_low], axis=0))
 
     grad = g_ref[...].astype(F32)
     weight = jnp.concatenate([weight_ref[...], jnp.zeros((6, TOK), F32)], axis=0).T
-    rows = [(weight[:, j : j + 1] * grad).astype(BF) for j in range(TOP)]
-    sent = mm(picks[0], rows[0]) + mm(picks[1], rows[1])
-    sent = jnp.where(iota((SLOTS, 128), 0) % PAD == CAP, total_row, sent)
+    sent = jnp.zeros((SLOTS, 256), F32)
+    for j in range(TOP):
+        rows = [x_ref[...], (weight[:, j : j + 1] * grad).astype(BF)]
+        sent = sent + mm(picks[j], jnp.concatenate(rows, axis=1))
+    sent_ref[:, :PAD, :] = (sent[:, :128] + state_rows).astype(BF).reshape(N_SP, PAD, 128)
+    sent = jnp.where(iota((SLOTS, 128), 0) % PAD == CAP, total_row, sent[:, 128:])
     sent_ref[:, PAD:, :] = sent.astype(BF).reshape(N_SP, PAD, 128)
 
 
@@ -186,10 +188,6 @@
         rounded[q] = packed[q * 2 * PART : (q + 1) * 2 * PART, :].astype(BF)
     for k in range(N_TP):
         out_ref[k] = rounded[quarter_of(place_ref, k)]
-
-
-def mark_kernel(out_ref):
-    out_ref[...] = jnp.zeros((8, 128), F32)
 
 
 def scan_kernel(place_ref, recv_ref, states_ref, reach_ref):
@@ -318,8 +316,8 @@
     far_a, far_b = from_left_ref[:LOT, :].astype(F32), from_right_ref[EARLY:, :].astype(F32)
     to_right_ref[:LOT, :] = (right_a_ref[...].astype(F32) + far_a).astype(BF)
     to_right_ref[LOT:, :] = right_late_ref[...]
-    to_left_ref[:EARLY, :] = left_late_ref[...]
-    to_left_ref[EARLY:, :] = (left_b_ref[...].astype(F32) + far_b).astype(BF)
+    to_left_ref[:LATE, :] = left_late_ref[...]
+    to_left_ref[LATE:, :] = (left_b_ref[...].astype(F32) + far_b).astype(BF)
 
 
 def grad_sum_kernel(
@@ -339,7 +337,7 @@
             own, summed = (own_a_ref, row), (last_left_ref, row)
             single = (from_right_ref if row < EARLY else last_right_ref, row % EARLY)
         else:
-            own, summed = (own_b_ref, row), (last_right_ref, EARLY + row)
+            own, summed = (own_b_ref, row), (last_right_ref, LATE + row)
             single = (from_left_ref if row < EARLY else last_left_ref, LOT + row % EARLY)
         rows = [r[start : start + 128, :].astype(F32) for r, start in (own, summed, single)]
         return (rows[0] + rows[1] + rows[2]).astype(BF)
@@ -602,7 +600,12 @@
     )
     recv = exchanged(sent, SP)
     own_a, own_b = call(
-        pack_kernel, [((LOT, 128), BF), ((LOT, 128), BF)], w_gate[0], w_up[0], w_down[0]
+        pack_kernel,
+        [((LOT, 128), BF), ((LOT, 128), BF)],
+        w_gate[0],
+        w_up[0],
+        w_down[0],
+        near_out=(0, 1),
     )
     left_a = passed_on(own_a, 1)
     right_b = passed_on(own_b, -1)
@@ -619,11 +622,9 @@
         scratch=[pltpu.VMEM((2 * ROWS, 128), F32), pltpu.VMEM((4, 2 * PART, 128), BF)],
         smem=(0,),
         near=(1,),
-        near_out=(0,),
     )
     rows = exchanged(copies, "tp")
-    (mark,) = call(mark_kernel, [((8, 128), F32)], after=(rows,), near_after=True)
-    (turned,) = call(turned_kernel, [((TOK, SLOTS), BF)], pick)
+    (turned,) = call(turned_kernel, [((TOK, SLOTS), BF)], pick, after=(copies,))
     partial_rows, grads, hidden = call(
         partial_kernel,
         [((N_TP, PART, 128), BF), ((PART, 1024), BF), ((PART, 512), BF)],
@@ -633,7 +634,6 @@
         near=(0,),
         near_out=(1, 2),
         raw=tuple(range(1, 9)),
-        after=(mark,),
     )
     states, reach = call(
         scan_kernel,
@@ -648,7 +648,7 @@
         weight_grads_kernel,
         2 * [((LOT, 128), F32)]
         + 2 * [((LOT + EARLY, 128), BF)]
-        + 2 * [((LOT, 128), BF), ((EARLY, 128), BF)],
+        + 2 * [((LOT, 128), BF), ((LATE, 128), BF)],
         rows,
         grads,
         hidden,
@@ -671,7 +671,7 @@
     full_grad = exchanged(residual, "tp")
     lot_left, lot_right = call(
         relay_kernel,
-        2 * [((LOT + EARLY, 128), BF)],
+        2 * [((LOT + LATE, 128), BF)],
         *held_back,
         from_right,
         from_left,

time: 210 us -> 209 us (level)
    all_to_all x6, waiting for transfers between devices: 52.9 us -> 47.7 us  [exchanged(): return lax.all_to_all(blocks, axis, split_axis=0, concat_axis=0, tiled=True)]
    ppermute x10, waiting for transfers between devices: 24.9 us -> 30.1 us  [passed_on(): return lax.ppermute(array, ('sp_1', 'tp'), ring_step(step))]
    pallas_call x17 -> x16, Pallas kernels: 46.2 us -> 44.8 us  [call(): pl.pallas_call(run, out_shape=tuple(((pltpu.VMEM if k in near_out else pl...]
  transfers between devices with their start and end apart: 17 -> 17, of which waited for: 10 -> 10; matrix products, arithmetic and copies ran while one was open for 0% -> 0% of each run, Pallas kernels for 15% -> 14%
where the time goes in v10:
time: 209 us; the launch traced here: 205 us
  starting transfers between devices  79.9 us (38%)
  waiting for transfers between devices  78.9 us (38%)
  Pallas kernels  44.8 us (21%)
    all_to_all x6, waiting for transfers between devices, exchanged(): return lax.all_to_all(blocks, axis, split_axis=0, concat_axis=0, tiled=True)  47.7 us
    pallas_call x16, Pallas kernels, call(): pl.pallas_call(run, out_shape=tuple(((pltpu.VMEM if k in near_out else pl...  44.8 us
    all_to_all x6, starting transfers between devices, exchanged(): return lax.all_to_all(blocks, axis, split_axis=0, concat_axis=0, tiled=True)  42.5 us
    ppermute x10, starting transfers between devices, passed_on(): return lax.ppermute(array, ('sp_1', 'tp'), ring_step(step))  32.4 us
    ppermute x10, waiting for transfers between devices, passed_on(): return lax.ppermute(array, ('sp_1', 'tp'), ring_step(step))  30.1 us
    ppermute x1, starting transfers between devices, body(): from_other = lax.ppermute(to_other, 'sp_1', [(0, 1), (1, 0)])  5.02 us
  transfers between devices with their start and end apart: 17, of which 10 were waited for; matrix products, arithmetic and copies ran while one was open for 0% of the time, Pallas kernels for 14%

profile of v10, /device:TPU:1, one launch (start us, length us, event | category | flops | bytes accessed | tf_op | source)
XLA Modules:
  0.0 205.5 jit_solution(1668322833025530646)
XLA Ops:
  0.6 3.2 %shard_map.179 = (bf16[32,48,128]{2,1,0:T(8,128)(2,1)}, bf16[768,256]{1,0:T(8,128)(2,1)}) custom-call(s32[2,256]{1,0:T(2,128)} %bitcast.30, f32[2,256]{1,0:T(2,128)} %bitcast.31, bf16[256,128]{1,0:T(8,128)(2,1)} %refs_2_.3, bf16[256,128]{1,0:T(8,128)(2,1)} %refs_2_.4, bf16[64,256]{1,0:T(8,128)(2,1)} %bitcast.24, bf16[256,128]{1,0:T(8,128)(2,1)} %refs_5_.3, ...), custom_call_target="tpu_custom_call" | custom-call | tf_op jit(solution)/shard_map/pallas_call | solution.py:61
  3.8 16.7 %all-to-all-start = ((bf16[32,48,128]{2,1,0:T(8,128)(2,1)}), bf16[32,48,128]{2,1,0:T(8,128)(2,1)S(1)}, u32[]{:S(2)}, u32[]{:S(2)}) async-start(bf16[32,48,128]{2,1,0:T(8,128)(2,1)} %get-tuple-element.50), calls=%async_computation | async-start | bytes 786432 | tf_op jit(solution)/shard_map/all_to_all | solution.py:555
  20.6 1.5 shard_map.181
  22.1 3.2 %collective-permute-start = (bf16[3072,128]{1,0:T(8,128)(2,1)S(1)}, bf16[3072,128]{1,0:T(8,128)(2,1)}, u32[]{:S(2)}, u32[]{:S(2)}) collective-permute-start(bf16[3072,128]{1,0:T(8,128)(2,1)S(1)} %get-tuple-element.51.refs_1_), channel_id=1, source_target_pairs={{0,1},{16,20},{1,2},{17,21},{2,3},{18,22},{3,0},{19,23},{4,5},{20,... | collective-permute-start | bytes 2359304 | tf_op jit(solution)/shard_map/ppermute | solution.py:568
  25.3 3.4 %collective-permute-start.3 = (bf16[3072,128]{1,0:T(8,128)(2,1)S(1)}, bf16[3072,128]{1,0:T(8,128)(2,1)}, u32[]{:S(2)}, u32[]{:S(2)}) collective-permute-start(bf16[3072,128]{1,0:T(8,128)(2,1)S(1)} %get-tuple-element.52.refs_2_), channel_id=1, source_target_pairs={{0,3},{16,28},{1,0},{17,29},{2,1},{18,30},{3,2},{19,31},{4,7},{20,... | collective-permute-start | bytes 2359304 | tf_op jit(solution)/shard_map/ppermute | solution.py:568
  28.7 0.1 pad_add_fusion.refs_0_
  28.8 19.6 %all-to-all-done.refs_1_ = bf16[32,48,128]{2,1,0:T(8,128)(2,1)S(1)} async-done(((bf16[32,48,128]{2,1,0:T(8,128)(2,1)}), bf16[32,48,128]{2,1,0:T(8,128)(2,1)S(1)}, u32[]{:S(2)}, u32[]{:S(2)}) %all-to-all-start) | async-done | bytes 393248 | tf_op jit(solution)/shard_map/all_to_all | solution.py:555
  48.4 1.8 shard_map.180.refs_1_
  50.1 6.8 %all-to-all-start.1 = ((bf16[16,320,128]{2,1,0:T(8,128)(2,1)}), bf16[16,320,128]{2,1,0:T(8,128)(2,1)S(1)}, u32[]{:S(2)}, u32[]{:S(2)}) async-start(bf16[16,320,128]{2,1,0:T(8,128)(2,1)} %shard_map.180.refs_1_), calls=%async_computation.1 | async-start | bytes 2621440 | tf_op jit(solution)/shard_map/all_to_all | solution.py:555
  56.9 4.5 %collective-permute-start.2 = (bf16[3072,128]{1,0:T(8,128)(2,1)S(1)}, bf16[3072,128]{1,0:T(8,128)(2,1)S(1)}, u32[]{:S(2)}, u32[]{:S(2)}) collective-permute-start(bf16[3072,128]{1,0:T(8,128)(2,1)S(1)} %get-tuple-element.51.refs_1_), channel_id=1, source_target_pairs={{0,3},{16,28},{1,0},{17,29},{2,1},{18,30},{3,2},{19,31},{4,7},{20,... | collective-permute-start | bytes 2359304 | tf_op jit(solution)/shard_map/ppermute | solution.py:568
  61.4 1.9 collective-permute-start.1
  63.3 2.1 %collective-permute-start.4 = (bf16[3072,128]{1,0:T(8,128)(2,1)}, bf16[3072,128]{1,0:T(8,128)(2,1)S(1)}, u32[]{:S(2)}, u32[]{:S(2)}) collective-permute-start(bf16[3072,128]{1,0:T(8,128)(2,1)} %collective-permute-done.refs_3_), channel_id=1, source_target_pairs={{0,1},{16,20},{1,2},{17,21},{2,3},{18,22},{3,0},{19,23},{4,5},{20,... | collective-permute-start | bytes 2359304 | tf_op jit(solution)/shard_map/ppermute | solution.py:568
  65.5 0.0 collective-permute-done.3.refs_6_
  65.5 4.3 %collective-permute-start.5 = (bf16[3072,128]{1,0:T(8,128)(2,1)}, bf16[3072,128]{1,0:T(8,128)(2,1)}, u32[]{:S(2)}, u32[]{:S(2)}) collective-permute-start(bf16[3072,128]{1,0:T(8,128)(2,1)} %collective-permute-done.3.refs_6_), channel_id=1, source_target_pairs={{0,3},{16,28},{1,0},{17,29},{2,1},{18,30},{3,2},{19,31},{4,7},{20,... | collective-permute-start | bytes 2359304 | tf_op jit(solution)/shard_map/ppermute | solution.py:568
  69.9 12.3 %collective-permute-done.2.refs_5_ = bf16[3072,128]{1,0:T(8,128)(2,1)S(1)} collective-permute-done((bf16[3072,128]{1,0:T(8,128)(2,1)S(1)}, bf16[3072,128]{1,0:T(8,128)(2,1)S(1)}, u32[]{:S(2)}, u32[]{:S(2)}) %collective-permute-start.2) | collective-permute-done | bytes 786464 | tf_op jit(solution)/shard_map/ppermute | solution.py:568
  82.2 1.5 collective-permute-done.1.refs_4_
  83.7 8.1 %collective-permute-done.4.refs_7_ = bf16[3072,128]{1,0:T(8,128)(2,1)S(1)} collective-permute-done((bf16[3072,128]{1,0:T(8,128)(2,1)}, bf16[3072,128]{1,0:T(8,128)(2,1)S(1)}, u32[]{:S(2)}, u32[]{:S(2)}) %collective-permute-start.4) | collective-permute-done | bytes 786464 | tf_op jit(solution)/shard_map/ppermute | solution.py:568
  91.8 0.9 copy-done.5
  92.7 0.0 collective-permute-done.5.refs_8_
  92.7 5.8 %shard_map.182 = (bf16[16,160,128]{2,1,0:T(8,128)(2,1)}, bf16[160,1024]{1,0:T(8,128)(2,1)S(1)}, bf16[160,512]{1,0:T(8,128)(2,1)S(1)}) custom-call(bf16[16,320,128]{2,1,0:T(8,128)(2,1)S(1)} %all-to-all-done.1.refs_0_, bf16[3072,128]{1,0:T(8,128)(2,1)} %copy-done.1, bf16[3072,128]{1,0:T(8,128)(2,1)} %copy-done.2, ...), custom_call_target="tpu_custom_call" | custom-call | tf_op jit(solution)/shard_map/pallas_call | solution.py:61
  98.5 4.5 %all-to-all-start.2 = ((bf16[16,160,128]{2,1,0:T(8,128)(2,1)}), bf16[16,160,128]{2,1,0:T(8,128)(2,1)S(1)}, u32[]{:S(2)}, u32[]{:S(2)}) async-start(bf16[16,160,128]{2,1,0:T(8,128)(2,1)} %get-tuple-element.63.refs_2_), calls=%async_computation.2 | async-start | bytes 1310720 | tf_op jit(solution)/shard_map/all_to_all | solution.py:555
  103.0 1.9 shard_map.184
  104.9 9.3 %all-to-all-done.2.refs_1_ = bf16[16,160,128]{2,1,0:T(8,128)(2,1)S(1)} async-done(((bf16[16,160,128]{2,1,0:T(8,128)(2,1)}), bf16[16,160,128]{2,1,0:T(8,128)(2,1)S(1)}, u32[]{:S(2)}, u32[]{:S(2)}) %all-to-all-start.2) | async-done | bytes 655392 | tf_op jit(solution)/shard_map/all_to_all | solution.py:555
  114.2 1.5 shard_map.185
  115.7 6.2 %all-to-all-start.3 = ((bf16[32,24,128]{2,1,0:T(8,128)(2,1)}), bf16[32,24,128]{2,1,0:T(8,128)(2,1)S(1)}, u32[]{:S(2)}, u32[]{:S(2)}) async-start(bf16[32,24,128]{2,1,0:T(8,128)(2,1)} %shard_map.185), calls=%async_computation.3 | async-start | bytes 393216 | tf_op jit(solution)/shard_map/all_to_all | solution.py:555
  121.9 1.9 shard_map.186.refs_1_
  123.8 17.0 %all-to-all-done.3.refs_0_ = bf16[32,24,128]{2,1,0:T(8,128)(2,1)S(1)} async-done(((bf16[32,24,128]{2,1,0:T(8,128)(2,1)}), bf16[32,24,128]{2,1,0:T(8,128)(2,1)S(1)}, u32[]{:S(2)}, u32[]{:S(2)}) %all-to-all-start.3) | async-done | bytes 196640 | tf_op jit(solution)/shard_map/all_to_all | solution.py:555
  140.9 2.3 %shard_map.187.refs_6_.refs_5_ = bf16[16,256,128]{2,1,0:T(8,128)(2,1)} custom-call(bf16[32,24,128]{2,1,0:T(8,128)(2,1)S(1)} %all-to-all-done.3.refs_0_, bf16[256,768]{1,0:T(8,128)(2,1)} %shard_map.186.refs_1_, bf16[256,128]{1,0:T(8,128)(2,1)} %refs_2_.4), custom_call_target="tpu_custom_call" | custom-call | tf_op jit(solution)/shard_map/pallas_call | solution.py:61
  143.2 4.3 %all-to-all-start.4 = ((bf16[16,256,128]{2,1,0:T(8,128)(2,1)}), bf16[16,256,128]{2,1,0:T(8,128)(2,1)}, u32[]{:S(2)}, u32[]{:S(2)}) async-start(bf16[16,256,128]{2,1,0:T(8,128)(2,1)} %shard_map.187.refs_6_.refs_5_), calls=%async_computation.4 | async-start | bytes 2097152 | tf_op jit(solution)/shard_map/all_to_all | solution.py:555
  147.5 4.9 %shard_map.183 = (f32[3072,128]{1,0:T(8,128)}, f32[3072,128]{1,0:T(8,128)}, bf16[5120,128]{1,0:T(8,128)(2,1)}, bf16[5120,128]{1,0:T(8,128)(2,1)}, bf16[3072,128]...) custom-call(bf16[16,320,128]{2,1,0:T(8,128)(2,1)S(1)} %all-to-all-done.1.refs_0_, ...), custom_call_target="tpu_custom_call" | custom-call | tf_op jit(solution)/shard_map/pallas_call | solution.py:61
  152.4 4.4 %collective-permute-start.6 = (bf16[5120,128]{1,0:T(8,128)(2,1)}, bf16[5120,128]{1,0:T(8,128)(2,1)S(1)}, u32[]{:S(2)}, u32[]{:S(2)}) collective-permute-start(bf16[5120,128]{1,0:T(8,128)(2,1)} %get-tuple-element.57), channel_id=1, source_target_pairs={{0,3},{16,28},{1,0},{17,29},{2,1},{18,30},{3,2},{19,31},{4,7},{20,... | collective-permute-start | bytes 3932168 | tf_op jit(solution)/shard_map/ppermute | solution.py:568
  156.8 1.9 collective-permute-start.7
  158.7 2.6 %shard_map.189 = (bf16[256,128]{1,0:T(8,128)(2,1)S(1)}, f32[4,128,64]{2,1,0:T(8,128)}) custom-call(bf16[32,24,128]{2,1,0:T(8,128)(2,1)S(1)} %all-to-all-done.3.refs_0_, bf16[64,256]{1,0:T(8,128)(2,1)} %bitcast.27, bf16[64,256]{1,0:T(8,128)(2,1)} %bitcast.25, bf16[256,128]{1,0:T(8,128)(2,1)} %refs_5_.3, f32[64,256]{1,0:T(8,128)} %bitcast.18, ...), custom_call_target="tpu_custom_call" | custom-call | tf_op jit(solution)/shard_map/pallas_call | solution.py:61
  161.4 1.8 all-to-all-done.4.refs_1_
  163.2 2.9 %shard_map.190 = (f32[256,128]{1,0:T(8,128)}, f32[32,128]{1,0:T(8,128)S(1)}, bf16[1088,128]{1,0:T(8,128)(2,1)S(1)}, f32[1024,128]{1,0:T(8,128)S(1)}) custom-call(s32[3]{0:T(128)S(1)} %pad_add_fusion.refs_0_, bf16[16,256,128]{2,1,0:T(8,128)(2,1)} %all-to-all-done.4.refs_1_, bf16[2048,128]{1,0:T(8,128)(2,1)} %refs_2_.5, ...), custom_call_target="tpu_custom_call" | custom-call | tf_op jit(solution)/shard_map/pallas_call | solution.py:61
  166.1 5.0 %collective-permute-start.10 = (bf16[1088,128]{1,0:T(8,128)(2,1)S(1)}, bf16[1088,128]{1,0:T(8,128)(2,1)S(1)}, u32[]{:S(2)}, u32[]{:S(2)}) collective-permute-start(bf16[1088,128]{1,0:T(8,128)(2,1)S(1)} %get-tuple-element.69), channel_id=1, source_target_pairs={{0,16},{16,0},{1,17},{17,1},{2,18},{18,2},{3,19},{19,3},{4,20},{20... | collective-permute-start | bytes 835592 | tf_op jit(solution)/shard_map/ppermute | solution.py:708
  171.1 1.2 collective-permute-done.10.refs_1_
  172.3 1.5 shard_map.191
  173.8 4.0 %all-to-all-start.5 = ((bf16[16,96,128]{2,1,0:T(8,128)(2,1)}), bf16[16,96,128]{2,1,0:T(8,128)(2,1)S(1)}, u32[]{:S(2)}, u32[]{:S(2)}) async-start(bf16[16,96,128]{2,1,0:T(8,128)(2,1)} %get-tuple-element.73.refs_6_), calls=%async_computation.5 | async-start | bytes 786432 | tf_op jit(solution)/shard_map/all_to_all | solution.py:555
  177.8 0.0 collective-permute-done.7.refs_5_.refs_3_
  177.8 3.1 %shard_map.188 = (bf16[4096,128]{1,0:T(8,128)(2,1)}, bf16[4096,128]{1,0:T(8,128)(2,1)}) custom-call(bf16[3072,128]{1,0:T(8,128)(2,1)} %get-tuple-element.59.refs_0_, bf16[1024,128]{1,0:T(8,128)(2,1)} %get-tuple-element.60.refs_1_, bf16[3072,128]{1,0:T(8,128)(2,1)} %get-tuple-element.61.refs_2_, bf16[1024,128]{1,0:T(8,128)(2,1)} %get-tuple-element.62.refs_3_, ...), custom_call_target="tpu_custom_call" | custom-call | tf_op jit(solution)/shard_map/pallas_call | solution.py:61
  180.9 1.9 collective-permute-start.8
  182.9 4.8 %collective-permute-start.9 = (bf16[4096,128]{1,0:T(8,128)(2,1)}, bf16[4096,128]{1,0:T(8,128)(2,1)S(1)}, u32[]{:S(2)}, u32[]{:S(2)}) collective-permute-start(bf16[4096,128]{1,0:T(8,128)(2,1)} %get-tuple-element.67), channel_id=1, source_target_pairs={{0,3},{16,28},{1,0},{17,29},{2,1},{18,30},{3,2},{19,31},{4,7},{20,... | collective-permute-start | bytes 3145736 | tf_op jit(solution)/shard_map/ppermute | solution.py:568
  187.6 3.8 %shard_map.193 = (bf16[64,256]{1,0:T(8,128)(2,1)}, f32[256,128]{1,0:T(8,128)}, f32[256,64]{1,0:T(8,128)}, f32[256,64]{1,0:T(8,128)}, f32[256,64]{1,0:T(8,128)}, ...) custom-call(f32[256,128]{1,0:T(8,128)} %get-tuple-element.79.refs_0_, ...), custom_call_target="tpu_custom_call" | custom-call | tf_op jit(solution)/shard_map/pallas_call | solution.py:61
  191.4 6.8 %collective-permute-done.8.refs_4_ = bf16[4096,128]{1,0:T(8,128)(2,1)S(1)} collective-permute-done((bf16[4096,128]{1,0:T(8,128)(2,1)}, bf16[4096,128]{1,0:T(8,128)(2,1)S(1)}, u32[]{:S(2)}, u32[]{:S(2)}) %collective-permute-start.8) | collective-permute-done | bytes 1048608 | tf_op jit(solution)/shard_map/ppermute | solution.py:568
  198.2 1.3 collective-permute-done.9.refs_5_
  199.5 3.4 %shard_map.192 = (bf16[2048,128]{1,0:T(8,128)(2,1)}, bf16[2048,128]{1,0:T(8,128)(2,1)}, bf16[128,2048]{1,0:T(8,128)(2,1)}) custom-call(f32[3072,128]{1,0:T(8,128)} %get-tuple-element.55.refs_0_, f32[3072,128]{1,0:T(8,128)} %get-tuple-element.56.refs_1_, bf16[5120,128]{1,0:T(8,128)(2,1)S(1)} %collective-permute-done.6.refs_4_.refs_2_, ...), custom_call_target="tpu_custom_call" | custom-call | tf_op jit(solution)/shard_map/pallas_call | solution.py:61
  202.9 2.6 %shard_map.194 = (f32[64,128]{1,0:T(8,128)}, bf16[64,256]{1,0:T(8,128)(2,1)}, bf16[256,128]{1,0:T(8,128)(2,1)}, f32[64,256]{1,0:T(8,128)}) custom-call(s32[3]{0:T(128)S(1)} %pad_add_fusion.refs_0_, bf16[16,96,128]{2,1,0:T(8,128)(2,1)S(1)} %all-to-all-done.5.refs_1_, f32[32,128]{1,0:T(8,128)} %get-tuple-element.77.refs_2_, ...), custom_call_target="tpu_custom_call" | custom-call | tf_op jit(solution)/shard_map/pallas_call | solution.py:61
  (15 shorter events, 0.0 us)
Async XLA Ops:
  3.8 44.5 %all-to-all-start = ((bf16[32,48,128]{2,1,0:T(8,128)(2,1)}), bf16[32,48,128]{2,1,0:T(8,128)(2,1)S(1)}, u32[]{:S(2)}, u32[]{:S(2)}) async-start(bf16[32,48,128]{2,1,0:T(8,128)(2,1)} %get-tuple-element.50), calls=%async_computation | async-start | bytes 786432 | tf_op jit(solution)/shard_map/all_to_all | solution.py:555
  22.1 34.8 %copy-start.1 = (bf16[3072,128]{1,0:T(8,128)(2,1)}, bf16[3072,128]{1,0:T(8,128)(2,1)S(1)}, u32[]{:S(2)}) copy-start(bf16[3072,128]{1,0:T(8,128)(2,1)S(1)} %get-tuple-element.51.refs_1_) | copy-start | bytes 2359300
  22.1 39.3 %copy-start.2 = (bf16[3072,128]{1,0:T(8,128)(2,1)}, bf16[3072,128]{1,0:T(8,128)(2,1)S(1)}, u32[]{:S(2)}) copy-start(bf16[3072,128]{1,0:T(8,128)(2,1)S(1)} %get-tuple-element.52.refs_2_) | copy-start | bytes 2359300
  22.1 41.2 %collective-permute-start = (bf16[3072,128]{1,0:T(8,128)(2,1)S(1)}, bf16[3072,128]{1,0:T(8,128)(2,1)}, u32[]{:S(2)}, u32[]{:S(2)}) collective-permute-start(bf16[3072,128]{1,0:T(8,128)(2,1)S(1)} %get-tuple-element.51.refs_1_), channel_id=1, source_target_pairs={{0,1},{16,20},{1,2},{17,21},{2,3},{18,22},{3,0},{19,23},{4,5},{20,... | collective-permute-start | bytes 2359304 | tf_op jit(solution)/shard_map/ppermute | solution.py:568
  25.3 40.1 %collective-permute-start.3 = (bf16[3072,128]{1,0:T(8,128)(2,1)S(1)}, bf16[3072,128]{1,0:T(8,128)(2,1)}, u32[]{:S(2)}, u32[]{:S(2)}) collective-permute-start(bf16[3072,128]{1,0:T(8,128)(2,1)S(1)} %get-tuple-element.52.refs_2_), channel_id=1, source_target_pairs={{0,3},{16,28},{1,0},{17,29},{2,1},{18,30},{3,2},{19,31},{4,7},{20,... | collective-permute-start | bytes 2359304 | tf_op jit(solution)/shard_map/ppermute | solution.py:568
  48.3 1.8 copy-start
  50.1 42.6 %all-to-all-start.1 = ((bf16[16,320,128]{2,1,0:T(8,128)(2,1)}), bf16[16,320,128]{2,1,0:T(8,128)(2,1)S(1)}, u32[]{:S(2)}, u32[]{:S(2)}) async-start(bf16[16,320,128]{2,1,0:T(8,128)(2,1)} %shard_map.180.refs_1_), calls=%async_computation.1 | async-start | bytes 2621440 | tf_op jit(solution)/shard_map/all_to_all | solution.py:555
  56.9 25.3 %collective-permute-start.2 = (bf16[3072,128]{1,0:T(8,128)(2,1)S(1)}, bf16[3072,128]{1,0:T(8,128)(2,1)S(1)}, u32[]{:S(2)}, u32[]{:S(2)}) collective-permute-start(bf16[3072,128]{1,0:T(8,128)(2,1)S(1)} %get-tuple-element.51.refs_1_), channel_id=1, source_target_pairs={{0,3},{16,28},{1,0},{17,29},{2,1},{18,30},{3,2},{19,31},{4,7},{20,... | collective-permute-start | bytes 2359304 | tf_op jit(solution)/shard_map/ppermute | solution.py:568
  61.4 22.3 %collective-permute-start.1 = (bf16[3072,128]{1,0:T(8,128)(2,1)S(1)}, bf16[3072,128]{1,0:T(8,128)(2,1)S(1)}, u32[]{:S(2)}, u32[]{:S(2)}) collective-permute-start(bf16[3072,128]{1,0:T(8,128)(2,1)S(1)} %get-tuple-element.52.refs_2_), channel_id=1, source_target_pairs={{0,1},{16,20},{1,2},{17,21},{2,3},{18,22},{3,0},{19,23},{4,5},{20,... | collective-permute-start | bytes 2359304 | tf_op jit(solution)/shard_map/ppermute | solution.py:568
  63.3 28.5 %collective-permute-start.4 = (bf16[3072,128]{1,0:T(8,128)(2,1)}, bf16[3072,128]{1,0:T(8,128)(2,1)S(1)}, u32[]{:S(2)}, u32[]{:S(2)}) collective-permute-start(bf16[3072,128]{1,0:T(8,128)(2,1)} %collective-permute-done.refs_3_), channel_id=1, source_target_pairs={{0,1},{16,20},{1,2},{17,21},{2,3},{18,22},{3,0},{19,23},{4,5},{20,... | collective-permute-start | bytes 2359304 | tf_op jit(solution)/shard_map/ppermute | solution.py:568
  65.5 27.2 %collective-permute-start.5 = (bf16[3072,128]{1,0:T(8,128)(2,1)}, bf16[3072,128]{1,0:T(8,128)(2,1)}, u32[]{:S(2)}, u32[]{:S(2)}) collective-permute-start(bf16[3072,128]{1,0:T(8,128)(2,1)} %collective-permute-done.3.refs_6_), channel_id=1, source_target_pairs={{0,3},{16,28},{1,0},{17,29},{2,1},{18,30},{3,2},{19,31},{4,7},{20,... | collective-permute-start | bytes 2359304 | tf_op jit(solution)/shard_map/ppermute | solution.py:568
  82.2 9.6 %copy-start.3 = (bf16[3072,128]{1,0:T(8,128)(2,1)}, bf16[3072,128]{1,0:T(8,128)(2,1)S(1)}, u32[]{:S(2)}) copy-start(bf16[3072,128]{1,0:T(8,128)(2,1)S(1)} %collective-permute-done.2.refs_5_) | copy-start | bytes 2359300
  83.7 8.1 %copy-start.4 = (bf16[3072,128]{1,0:T(8,128)(2,1)}, bf16[3072,128]{1,0:T(8,128)(2,1)S(1)}, u32[]{:S(2)}) copy-start(bf16[3072,128]{1,0:T(8,128)(2,1)S(1)} %collective-permute-done.1.refs_4_) | copy-start | bytes 2359300
  91.8 0.9 copy-start.5
  98.5 15.7 %all-to-all-start.2 = ((bf16[16,160,128]{2,1,0:T(8,128)(2,1)}), bf16[16,160,128]{2,1,0:T(8,128)(2,1)S(1)}, u32[]{:S(2)}, u32[]{:S(2)}) async-start(bf16[16,160,128]{2,1,0:T(8,128)(2,1)} %get-tuple-element.63.refs_2_), calls=%async_computation.2 | async-start | bytes 1310720 | tf_op jit(solution)/shard_map/all_to_all | solution.py:555
  115.7 25.2 %all-to-all-start.3 = ((bf16[32,24,128]{2,1,0:T(8,128)(2,1)}), bf16[32,24,128]{2,1,0:T(8,128)(2,1)S(1)}, u32[]{:S(2)}, u32[]{:S(2)}) async-start(bf16[32,24,128]{2,1,0:T(8,128)(2,1)} %shard_map.185), calls=%async_computation.3 | async-start | bytes 393216 | tf_op jit(solution)/shard_map/all_to_all | solution.py:555
  143.2 20.0 %all-to-all-start.4 = ((bf16[16,256,128]{2,1,0:T(8,128)(2,1)}), bf16[16,256,128]{2,1,0:T(8,128)(2,1)}, u32[]{:S(2)}, u32[]{:S(2)}) async-start(bf16[16,256,128]{2,1,0:T(8,128)(2,1)} %shard_map.187.refs_6_.refs_5_), calls=%async_computation.4 | async-start | bytes 2097152 | tf_op jit(solution)/shard_map/all_to_all | solution.py:555
  152.4 25.4 %collective-permute-start.6 = (bf16[5120,128]{1,0:T(8,128)(2,1)}, bf16[5120,128]{1,0:T(8,128)(2,1)S(1)}, u32[]{:S(2)}, u32[]{:S(2)}) collective-permute-start(bf16[5120,128]{1,0:T(8,128)(2,1)} %get-tuple-element.57), channel_id=1, source_target_pairs={{0,3},{16,28},{1,0},{17,29},{2,1},{18,30},{3,2},{19,31},{4,7},{20,... | collective-permute-start | bytes 3932168 | tf_op jit(solution)/shard_map/ppermute | solution.py:568
  156.8 21.0 %collective-permute-start.7 = (bf16[5120,128]{1,0:T(8,128)(2,1)}, bf16[5120,128]{1,0:T(8,128)(2,1)S(1)}, u32[]{:S(2)}, u32[]{:S(2)}) collective-permute-start(bf16[5120,128]{1,0:T(8,128)(2,1)} %get-tuple-element.58), channel_id=1, source_target_pairs={{0,1},{16,20},{1,2},{17,21},{2,3},{18,22},{3,0},{19,23},{4,5},{20,... | collective-permute-start | bytes 3932168 | tf_op jit(solution)/shard_map/ppermute | solution.py:568
  166.1 6.2 %collective-permute-start.10 = (bf16[1088,128]{1,0:T(8,128)(2,1)S(1)}, bf16[1088,128]{1,0:T(8,128)(2,1)S(1)}, u32[]{:S(2)}, u32[]{:S(2)}) collective-permute-start(bf16[1088,128]{1,0:T(8,128)(2,1)S(1)} %get-tuple-element.69), channel_id=1, source_target_pairs={{0,16},{16,0},{1,17},{17,1},{2,18},{18,2},{3,19},{19,3},{4,20},{20... | collective-permute-start | bytes 835592 | tf_op jit(solution)/shard_map/ppermute | solution.py:708
  173.8 29.1 %all-to-all-start.5 = ((bf16[16,96,128]{2,1,0:T(8,128)(2,1)}), bf16[16,96,128]{2,1,0:T(8,128)(2,1)S(1)}, u32[]{:S(2)}, u32[]{:S(2)}) async-start(bf16[16,96,128]{2,1,0:T(8,128)(2,1)} %get-tuple-element.73.refs_6_), calls=%async_computation.5 | async-start | bytes 786432 | tf_op jit(solution)/shard_map/all_to_all | solution.py:555
  180.9 17.2 %collective-permute-start.8 = (bf16[4096,128]{1,0:T(8,128)(2,1)}, bf16[4096,128]{1,0:T(8,128)(2,1)S(1)}, u32[]{:S(2)}, u32[]{:S(2)}) collective-permute-start(bf16[4096,128]{1,0:T(8,128)(2,1)} %get-tuple-element.66), channel_id=1, source_target_pairs={{0,1},{16,20},{1,2},{17,21},{2,3},{18,22},{3,0},{19,23},{4,5},{20,... | collective-permute-start | bytes 3145736 | tf_op jit(solution)/shard_map/ppermute | solution.py:568
  182.9 16.6 %collective-permute-start.9 = (bf16[4096,128]{1,0:T(8,128)(2,1)}, bf16[4096,128]{1,0:T(8,128)(2,1)S(1)}, u32[]{:S(2)}, u32[]{:S(2)}) collective-permute-start(bf16[4096,128]{1,0:T(8,128)(2,1)} %get-tuple-element.67), channel_id=1, source_target_pairs={{0,3},{16,28},{1,0},{17,29},{2,1},{18,30},{3,2},{19,31},{4,7},{20,... | collective-permute-start | bytes 3145736 | tf_op jit(solution)/shard_map/ppermute | solution.py:568

commit v11 on v10

--- a/solution.py
+++ b/solution.py
@@ -21,8 +21,7 @@
 SLOTS = N_SP * PAD
 PART = ROWS // 4
 LOT = 3 * 1024
-EARLY = 2048
-LATE = LOT - EARLY
+EARLY = LOT // 2
 NBLK = TOK // BLOCK
 BF = jnp.bfloat16
 F32 = jnp.float32
@@ -72,7 +71,7 @@
         + [pl.BlockSpec(memory_space=pltpu.HBM) for _ in after],
         out_specs=tuple(pl.BlockSpec(memory_space=pltpu.VMEM) for _ in outs),
         scratch_shapes=scratch,
-        compiler_params=pltpu.CompilerParams(vmem_limit_bytes=24 * 1024 * 1024),
+        compiler_params=pltpu.CompilerParams(vmem_limit_bytes=18 * 1024 * 1024),
     )(*args, *after)
 
 
@@ -316,8 +315,8 @@
     far_a, far_b = from_left_ref[:LOT, :].astype(F32), from_right_ref[EARLY:, :].astype(F32)
     to_right_ref[:LOT, :] = (right_a_ref[...].astype(F32) + far_a).astype(BF)
     to_right_ref[LOT:, :] = right_late_ref[...]
-    to_left_ref[:LATE, :] = left_late_ref[...]
-    to_left_ref[LATE:, :] = (left_b_ref[...].astype(F32) + far_b).astype(BF)
+    to_left_ref[:EARLY, :] = left_late_ref[...]
+    to_left_ref[EARLY:, :] = (left_b_ref[...].astype(F32) + far_b).astype(BF)
 
 
 def grad_sum_kernel(
@@ -337,7 +336,7 @@
             own, summed = (own_a_ref, row), (last_left_ref, row)
             single = (from_right_ref if row < EARLY else last_right_ref, row % EARLY)
         else:
-            own, summed = (own_b_ref, row), (last_right_ref, LATE + row)
+            own, summed = (own_b_ref, row), (last_right_ref, EARLY + row)
             single = (from_left_ref if row < EARLY else last_left_ref, LOT + row % EARLY)
         rows = [r[start : start + 128, :].astype(F32) for r, start in (own, summed, single)]
         return (rows[0] + rows[1] + rows[2]).astype(BF)
@@ -648,7 +647,7 @@
         weight_grads_kernel,
         2 * [((LOT, 128), F32)]
         + 2 * [((LOT + EARLY, 128), BF)]
-        + 2 * [((LOT, 128), BF), ((LATE, 128), BF)],
+        + 2 * [((LOT, 128), BF), ((EARLY, 128), BF)],
         rows,
         grads,
         hidden,
@@ -671,7 +670,7 @@
     full_grad = exchanged(residual, "tp")
     lot_left, lot_right = call(
         relay_kernel,
-        2 * [((LOT + LATE, 128), BF)],
+        2 * [((LOT + EARLY, 128), BF)],
         *held_back,
         from_right,
         from_left,

time: 209 us -> 209 us (level)
  no operation moved by 1% of the time
where the time goes in v11:
time: 209 us; the launch traced here: 207 us
  waiting for transfers between devices  80.2 us (38%)
  starting transfers between devices  79.5 us (38%)
  Pallas kernels  44.3 us (21%)
    all_to_all x6, waiting for transfers between devices, exchanged(): return lax.all_to_all(blocks, axis, split_axis=0, concat_axis=0, tiled=True)  47.6 us
    pallas_call x16, Pallas kernels, call(): pl.pallas_call(run, out_shape=tuple(((pltpu.VMEM if k in near_out else pl...  44.3 us
    all_to_all x6, starting transfers between devices, exchanged(): return lax.all_to_all(blocks, axis, split_axis=0, concat_axis=0, tiled=True)  42 us
    ppermute x10, starting transfers between devices, passed_on(): return lax.ppermute(array, ('sp_1', 'tp'), ring_step(step))  32.5 us
    ppermute x10, waiting for transfers between devices, passed_on(): return lax.ppermute(array, ('sp_1', 'tp'), ring_step(step))  31.4 us
    ppermute x1, starting transfers between devices, body(): from_other = lax.ppermute(to_other, 'sp_1', [(0, 1), (1, 0)])  5.02 us
  transfers between devices with their start and end apart: 17, of which 10 were waited for; matrix products, arithmetic and copies ran while one was open for 0% of the time, Pallas kernels for 14%

profile of v11, /device:TPU:1, one launch (start us, length us, event | category | flops | bytes accessed | tf_op | source)
XLA Modules:
  0.0 206.6 jit_solution(92859370248613695)
XLA Ops:
  0.6 3.2 %shard_map.179 = (bf16[32,48,128]{2,1,0:T(8,128)(2,1)}, bf16[768,256]{1,0:T(8,128)(2,1)}) custom-call(s32[2,256]{1,0:T(2,128)} %bitcast.30, f32[2,256]{1,0:T(2,128)} %bitcast.31, bf16[256,128]{1,0:T(8,128)(2,1)} %refs_2_.3, bf16[256,128]{1,0:T(8,128)(2,1)} %refs_2_.4, bf16[64,256]{1,0:T(8,128)(2,1)} %bitcast.24, bf16[256,128]{1,0:T(8,128)(2,1)} %refs_5_.3, ...), custom_call_target="tpu_custom_call" | custom-call | tf_op jit(solution)/shard_map/pallas_call | solution.py:60
  3.8 16.7 %all-to-all-start = ((bf16[32,48,128]{2,1,0:T(8,128)(2,1)}), bf16[32,48,128]{2,1,0:T(8,128)(2,1)S(1)}, u32[]{:S(2)}, u32[]{:S(2)}) async-start(bf16[32,48,128]{2,1,0:T(8,128)(2,1)} %get-tuple-element.50), calls=%async_computation | async-start | bytes 786432 | tf_op jit(solution)/shard_map/all_to_all | solution.py:554
  20.6 1.5 shard_map.181
  22.1 3.2 %collective-permute-start = (bf16[3072,128]{1,0:T(8,128)(2,1)S(1)}, bf16[3072,128]{1,0:T(8,128)(2,1)}, u32[]{:S(2)}, u32[]{:S(2)}) collective-permute-start(bf16[3072,128]{1,0:T(8,128)(2,1)S(1)} %get-tuple-element.51.refs_1_), channel_id=1, source_target_pairs={{0,1},{16,20},{1,2},{17,21},{2,3},{18,22},{3,0},{19,23},{4,5},{20,... | collective-permute-start | bytes 2359304 | tf_op jit(solution)/shard_map/ppermute | solution.py:567
  25.3 3.4 %collective-permute-start.3 = (bf16[3072,128]{1,0:T(8,128)(2,1)S(1)}, bf16[3072,128]{1,0:T(8,128)(2,1)}, u32[]{:S(2)}, u32[]{:S(2)}) collective-permute-start(bf16[3072,128]{1,0:T(8,128)(2,1)S(1)} %get-tuple-element.52.refs_2_), channel_id=1, source_target_pairs={{0,3},{16,28},{1,0},{17,29},{2,1},{18,30},{3,2},{19,31},{4,7},{20,... | collective-permute-start | bytes 2359304 | tf_op jit(solution)/shard_map/ppermute | solution.py:567
  28.7 0.1 pad_add_fusion.refs_0_
  28.8 19.6 %all-to-all-done.refs_1_ = bf16[32,48,128]{2,1,0:T(8,128)(2,1)S(1)} async-done(((bf16[32,48,128]{2,1,0:T(8,128)(2,1)}), bf16[32,48,128]{2,1,0:T(8,128)(2,1)S(1)}, u32[]{:S(2)}, u32[]{:S(2)}) %all-to-all-start) | async-done | bytes 393248 | tf_op jit(solution)/shard_map/all_to_all | solution.py:554
  48.4 1.8 shard_map.180.refs_1_
  50.1 6.8 %all-to-all-start.1 = ((bf16[16,320,128]{2,1,0:T(8,128)(2,1)}), bf16[16,320,128]{2,1,0:T(8,128)(2,1)S(1)}, u32[]{:S(2)}, u32[]{:S(2)}) async-start(bf16[16,320,128]{2,1,0:T(8,128)(2,1)} %shard_map.180.refs_1_), calls=%async_computation.1 | async-start | bytes 2621440 | tf_op jit(solution)/shard_map/all_to_all | solution.py:554
  56.9 4.5 %collective-permute-start.2 = (bf16[3072,128]{1,0:T(8,128)(2,1)S(1)}, bf16[3072,128]{1,0:T(8,128)(2,1)S(1)}, u32[]{:S(2)}, u32[]{:S(2)}) collective-permute-start(bf16[3072,128]{1,0:T(8,128)(2,1)S(1)} %get-tuple-element.51.refs_1_), channel_id=1, source_target_pairs={{0,3},{16,28},{1,0},{17,29},{2,1},{18,30},{3,2},{19,31},{4,7},{20,... | collective-permute-start | bytes 2359304 | tf_op jit(solution)/shard_map/ppermute | solution.py:567
  61.4 1.9 collective-permute-start.1
  63.3 0.0 collective-permute-done.refs_3_
  63.4 2.1 %collective-permute-start.4 = (bf16[3072,128]{1,0:T(8,128)(2,1)}, bf16[3072,128]{1,0:T(8,128)(2,1)S(1)}, u32[]{:S(2)}, u32[]{:S(2)}) collective-permute-start(bf16[3072,128]{1,0:T(8,128)(2,1)} %collective-permute-done.refs_3_), channel_id=1, source_target_pairs={{0,1},{16,20},{1,2},{17,21},{2,3},{18,22},{3,0},{19,23},{4,5},{20,... | collective-permute-start | bytes 2359304 | tf_op jit(solution)/shard_map/ppermute | solution.py:567
  65.5 4.3 %collective-permute-start.5 = (bf16[3072,128]{1,0:T(8,128)(2,1)}, bf16[3072,128]{1,0:T(8,128)(2,1)}, u32[]{:S(2)}, u32[]{:S(2)}) collective-permute-start(bf16[3072,128]{1,0:T(8,128)(2,1)} %collective-permute-done.3.refs_6_), channel_id=1, source_target_pairs={{0,3},{16,28},{1,0},{17,29},{2,1},{18,30},{3,2},{19,31},{4,7},{20,... | collective-permute-start | bytes 2359304 | tf_op jit(solution)/shard_map/ppermute | solution.py:567
  69.9 12.3 %collective-permute-done.2.refs_5_ = bf16[3072,128]{1,0:T(8,128)(2,1)S(1)} collective-permute-done((bf16[3072,128]{1,0:T(8,128)(2,1)S(1)}, bf16[3072,128]{1,0:T(8,128)(2,1)S(1)}, u32[]{:S(2)}, u32[]{:S(2)}) %collective-permute-start.2) | collective-permute-done | bytes 786464 | tf_op jit(solution)/shard_map/ppermute | solution.py:567
  82.2 1.5 collective-permute-done.1.refs_4_
  83.7 8.1 %collective-permute-done.4.refs_7_ = bf16[3072,128]{1,0:T(8,128)(2,1)S(1)} collective-permute-done((bf16[3072,128]{1,0:T(8,128)(2,1)}, bf16[3072,128]{1,0:T(8,128)(2,1)S(1)}, u32[]{:S(2)}, u32[]{:S(2)}) %collective-permute-start.4) | collective-permute-done | bytes 786464 | tf_op jit(solution)/shard_map/ppermute | solution.py:567
  91.8 0.9 copy-done.9
  92.7 5.8 %shard_map.182 = (bf16[16,160,128]{2,1,0:T(8,128)(2,1)}, bf16[160,1024]{1,0:T(8,128)(2,1)S(1)}, bf16[160,512]{1,0:T(8,128)(2,1)S(1)}) custom-call(bf16[16,320,128]{2,1,0:T(8,128)(2,1)S(1)} %all-to-all-done.1.refs_0_, bf16[3072,128]{1,0:T(8,128)(2,1)} %copy-done.3, bf16[3072,128]{1,0:T(8,128)(2,1)} %copy-done.4, ...), custom_call_target="tpu_custom_call" | custom-call | tf_op jit(solution)/shard_map/pallas_call | solution.py:60
  98.5 0.7 copy-done.5
  99.2 4.5 %all-to-all-start.2 = ((bf16[16,160,128]{2,1,0:T(8,128)(2,1)}), bf16[16,160,128]{2,1,0:T(8,128)(2,1)S(1)}, u32[]{:S(2)}, u32[]{:S(2)}) async-start(bf16[16,160,128]{2,1,0:T(8,128)(2,1)} %get-tuple-element.63.refs_2_), calls=%async_computation.2 | async-start | bytes 1310720 | tf_op jit(solution)/shard_map/all_to_all | solution.py:554
  103.7 1.9 shard_map.184
  105.6 9.3 %all-to-all-done.2.refs_1_ = bf16[16,160,128]{2,1,0:T(8,128)(2,1)S(1)} async-done(((bf16[16,160,128]{2,1,0:T(8,128)(2,1)}), bf16[16,160,128]{2,1,0:T(8,128)(2,1)S(1)}, u32[]{:S(2)}, u32[]{:S(2)}) %all-to-all-start.2) | async-done | bytes 655392 | tf_op jit(solution)/shard_map/all_to_all | solution.py:554
  114.9 1.5 shard_map.185
  116.4 6.2 %all-to-all-start.3 = ((bf16[32,24,128]{2,1,0:T(8,128)(2,1)}), bf16[32,24,128]{2,1,0:T(8,128)(2,1)S(1)}, u32[]{:S(2)}, u32[]{:S(2)}) async-start(bf16[32,24,128]{2,1,0:T(8,128)(2,1)} %shard_map.185), calls=%async_computation.3 | async-start | bytes 393216 | tf_op jit(solution)/shard_map/all_to_all | solution.py:554
  122.6 1.9 shard_map.186.refs_1_
  124.5 17.0 %all-to-all-done.3.refs_0_ = bf16[32,24,128]{2,1,0:T(8,128)(2,1)S(1)} async-done(((bf16[32,24,128]{2,1,0:T(8,128)(2,1)}), bf16[32,24,128]{2,1,0:T(8,128)(2,1)S(1)}, u32[]{:S(2)}, u32[]{:S(2)}) %all-to-all-start.3) | async-done | bytes 196640 | tf_op jit(solution)/shard_map/all_to_all | solution.py:554
  141.6 2.4 %shard_map.187.refs_6_.refs_5_ = bf16[16,256,128]{2,1,0:T(8,128)(2,1)} custom-call(bf16[32,24,128]{2,1,0:T(8,128)(2,1)S(1)} %all-to-all-done.3.refs_0_, bf16[256,768]{1,0:T(8,128)(2,1)} %shard_map.186.refs_1_, bf16[256,128]{1,0:T(8,128)(2,1)} %refs_2_.4), custom_call_target="tpu_custom_call" | custom-call | tf_op jit(solution)/shard_map/pallas_call | solution.py:60
  143.9 3.8 %all-to-all-start.4 = ((bf16[16,256,128]{2,1,0:T(8,128)(2,1)}), bf16[16,256,128]{2,1,0:T(8,128)(2,1)S(1)}, u32[]{:S(2)}, u32[]{:S(2)}) async-start(bf16[16,256,128]{2,1,0:T(8,128)(2,1)} %shard_map.187.refs_6_.refs_5_), calls=%async_computation.4 | async-start | bytes 2097152 | tf_op jit(solution)/shard_map/all_to_all | solution.py:554
  147.7 0.0 copy-start.2
  147.7 4.9 %shard_map.183 = (f32[3072,128]{1,0:T(8,128)}, f32[3072,128]{1,0:T(8,128)}, bf16[4608,128]{1,0:T(8,128)(2,1)}, bf16[4608,128]{1,0:T(8,128)(2,1)}, bf16[3072,128]...) custom-call(bf16[16,320,128]{2,1,0:T(8,128)(2,1)S(1)} %all-to-all-done.1.refs_0_, ...), custom_call_target="tpu_custom_call" | custom-call | tf_op jit(solution)/shard_map/pallas_call | solution.py:60
  152.6 4.4 %collective-permute-start.6 = (bf16[4608,128]{1,0:T(8,128)(2,1)}, bf16[4608,128]{1,0:T(8,128)(2,1)S(1)}, u32[]{:S(2)}, u32[]{:S(2)}) collective-permute-start(bf16[4608,128]{1,0:T(8,128)(2,1)} %get-tuple-element.57), channel_id=1, source_target_pairs={{0,3},{16,28},{1,0},{17,29},{2,1},{18,30},{3,2},{19,31},{4,7},{20,... | collective-permute-start | bytes 3538952 | tf_op jit(solution)/shard_map/ppermute | solution.py:567
  157.0 1.9 collective-permute-start.7
  159.0 2.7 %shard_map.189 = (bf16[256,128]{1,0:T(8,128)(2,1)S(1)}, f32[4,128,64]{2,1,0:T(8,128)}) custom-call(bf16[32,24,128]{2,1,0:T(8,128)(2,1)S(1)} %copy-done.2, bf16[64,256]{1,0:T(8,128)(2,1)} %bitcast.27, bf16[64,256]{1,0:T(8,128)(2,1)} %bitcast.25, bf16[256,128]{1,0:T(8,128)(2,1)} %refs_5_.3, f32[64,256]{1,0:T(8,128)} %bitcast.18, ...), custom_call_target="tpu_custom_call" | custom-call | tf_op jit(solution)/shard_map/pallas_call | solution.py:60
  161.6 1.7 all-to-all-done.4.refs_1_
  163.3 2.2 %shard_map.190 = (f32[256,128]{1,0:T(8,128)}, f32[32,128]{1,0:T(8,128)S(1)}, bf16[1088,128]{1,0:T(8,128)(2,1)S(1)}, f32[1024,128]{1,0:T(8,128)S(1)}) custom-call(s32[3]{0:T(128)S(1)} %pad_add_fusion.refs_0_, bf16[16,256,128]{2,1,0:T(8,128)(2,1)S(1)} %all-to-all-done.4.refs_1_, bf16[2048,128]{1,0:T(8,128)(2,1)} %refs_2_.5, ...), custom_call_target="tpu_custom_call" | custom-call | tf_op jit(solution)/shard_map/pallas_call | solution.py:60
  165.5 5.0 %collective-permute-start.10 = (bf16[1088,128]{1,0:T(8,128)(2,1)S(1)}, bf16[1088,128]{1,0:T(8,128)(2,1)S(1)}, u32[]{:S(2)}, u32[]{:S(2)}) collective-permute-start(bf16[1088,128]{1,0:T(8,128)(2,1)S(1)} %get-tuple-element.69), channel_id=1, source_target_pairs={{0,16},{16,0},{1,17},{17,1},{2,18},{18,2},{3,19},{19,3},{4,20},{20... | collective-permute-start | bytes 835592 | tf_op jit(solution)/shard_map/ppermute | solution.py:707
  170.5 1.2 collective-permute-done.10.refs_1_
  171.7 1.6 shard_map.191
  173.3 4.0 %all-to-all-start.5 = ((bf16[16,96,128]{2,1,0:T(8,128)(2,1)}), bf16[16,96,128]{2,1,0:T(8,128)(2,1)S(1)}, u32[]{:S(2)}, u32[]{:S(2)}) async-start(bf16[16,96,128]{2,1,0:T(8,128)(2,1)} %get-tuple-element.73.refs_6_), calls=%async_computation.5 | async-start | bytes 786432 | tf_op jit(solution)/shard_map/all_to_all | solution.py:554
  177.4 3.3 %shard_map.188 = (bf16[4608,128]{1,0:T(8,128)(2,1)}, bf16[4608,128]{1,0:T(8,128)(2,1)}) custom-call(bf16[3072,128]{1,0:T(8,128)(2,1)} %get-tuple-element.59.refs_0_, bf16[1536,128]{1,0:T(8,128)(2,1)} %get-tuple-element.60.refs_1_, bf16[3072,128]{1,0:T(8,128)(2,1)} %get-tuple-element.61.refs_2_, bf16[1536,128]{1,0:T(8,128)(2,1)} %get-tuple-element.62.refs_3_, ...), custom_call_target="tpu_custom_call" | custom-call | tf_op jit(solution)/shard_map/pallas_call | solution.py:60
  180.6 1.9 collective-permute-start.8
  182.5 4.8 %collective-permute-start.9 = (bf16[4608,128]{1,0:T(8,128)(2,1)}, bf16[4608,128]{1,0:T(8,128)(2,1)S(1)}, u32[]{:S(2)}, u32[]{:S(2)}) collective-permute-start(bf16[4608,128]{1,0:T(8,128)(2,1)} %get-tuple-element.67), channel_id=1, source_target_pairs={{0,3},{16,28},{1,0},{17,29},{2,1},{18,30},{3,2},{19,31},{4,7},{20,... | collective-permute-start | bytes 3538952 | tf_op jit(solution)/shard_map/ppermute | solution.py:567
  187.3 3.8 %shard_map.193 = (bf16[64,256]{1,0:T(8,128)(2,1)}, f32[256,128]{1,0:T(8,128)}, f32[256,64]{1,0:T(8,128)}, f32[256,64]{1,0:T(8,128)}, f32[256,64]{1,0:T(8,128)}, ...) custom-call(f32[256,128]{1,0:T(8,128)} %get-tuple-element.79.refs_0_, ...), custom_call_target="tpu_custom_call" | custom-call | tf_op jit(solution)/shard_map/pallas_call | solution.py:60
  191.1 8.2 %collective-permute-done.8.refs_4_ = bf16[4608,128]{1,0:T(8,128)(2,1)S(1)} collective-permute-done((bf16[4608,128]{1,0:T(8,128)(2,1)}, bf16[4608,128]{1,0:T(8,128)(2,1)S(1)}, u32[]{:S(2)}, u32[]{:S(2)}) %collective-permute-start.8) | collective-permute-done | bytes 1179680 | tf_op jit(solution)/shard_map/ppermute | solution.py:567
  199.3 1.3 collective-permute-done.9.refs_5_
  200.6 3.4 %shard_map.192 = (bf16[2048,128]{1,0:T(8,128)(2,1)}, bf16[2048,128]{1,0:T(8,128)(2,1)}, bf16[128,2048]{1,0:T(8,128)(2,1)}) custom-call(f32[3072,128]{1,0:T(8,128)} %get-tuple-element.55.refs_0_, f32[3072,128]{1,0:T(8,128)} %get-tuple-element.56.refs_1_, bf16[4608,128]{1,0:T(8,128)(2,1)S(1)} %collective-permute-done.6.refs_4_.refs_2_, ...), custom_call_target="tpu_custom_call" | custom-call | tf_op jit(solution)/shard_map/pallas_call | solution.py:60
  203.9 2.6 %shard_map.194 = (f32[64,128]{1,0:T(8,128)}, bf16[64,256]{1,0:T(8,128)(2,1)}, bf16[256,128]{1,0:T(8,128)(2,1)}, f32[64,256]{1,0:T(8,128)}) custom-call(s32[3]{0:T(128)S(1)} %pad_add_fusion.refs_0_, bf16[16,96,128]{2,1,0:T(8,128)(2,1)S(1)} %all-to-all-done.5.refs_1_, f32[32,128]{1,0:T(8,128)} %get-tuple-element.77.refs_2_, ...), custom_call_target="tpu_custom_call" | custom-call | tf_op jit(solution)/shard_map/pallas_call | solution.py:60
  (23 shorter events, 0.0 us)
Async XLA Ops:
  3.8 44.5 %all-to-all-start = ((bf16[32,48,128]{2,1,0:T(8,128)(2,1)}), bf16[32,48,128]{2,1,0:T(8,128)(2,1)S(1)}, u32[]{:S(2)}, u32[]{:S(2)}) async-start(bf16[32,48,128]{2,1,0:T(8,128)(2,1)} %get-tuple-element.50), calls=%async_computation | async-start | bytes 786432 | tf_op jit(solution)/shard_map/all_to_all | solution.py:554
  22.1 34.8 %copy-start.3 = (bf16[3072,128]{1,0:T(8,128)(2,1)}, bf16[3072,128]{1,0:T(8,128)(2,1)S(1)}, u32[]{:S(2)}) copy-start(bf16[3072,128]{1,0:T(8,128)(2,1)S(1)} %get-tuple-element.51.refs_1_) | copy-start | bytes 2359300
  22.1 39.3 %copy-start.4 = (bf16[3072,128]{1,0:T(8,128)(2,1)}, bf16[3072,128]{1,0:T(8,128)(2,1)S(1)}, u32[]{:S(2)}) copy-start(bf16[3072,128]{1,0:T(8,128)(2,1)S(1)} %get-tuple-element.52.refs_2_) | copy-start | bytes 2359300
  22.1 41.2 %collective-permute-start = (bf16[3072,128]{1,0:T(8,128)(2,1)S(1)}, bf16[3072,128]{1,0:T(8,128)(2,1)}, u32[]{:S(2)}, u32[]{:S(2)}) collective-permute-start(bf16[3072,128]{1,0:T(8,128)(2,1)S(1)} %get-tuple-element.51.refs_1_), channel_id=1, source_target_pairs={{0,1},{16,20},{1,2},{17,21},{2,3},{18,22},{3,0},{19,23},{4,5},{20,... | collective-permute-start | bytes 2359304 | tf_op jit(solution)/shard_map/ppermute | solution.py:567
  25.3 40.2 %collective-permute-start.3 = (bf16[3072,128]{1,0:T(8,128)(2,1)S(1)}, bf16[3072,128]{1,0:T(8,128)(2,1)}, u32[]{:S(2)}, u32[]{:S(2)}) collective-permute-start(bf16[3072,128]{1,0:T(8,128)(2,1)S(1)} %get-tuple-element.52.refs_2_), channel_id=1, source_target_pairs={{0,3},{16,28},{1,0},{17,29},{2,1},{18,30},{3,2},{19,31},{4,7},{20,... | collective-permute-start | bytes 2359304 | tf_op jit(solution)/shard_map/ppermute | solution.py:567
  48.3 1.8 copy-start
  50.1 42.6 %all-to-all-start.1 = ((bf16[16,320,128]{2,1,0:T(8,128)(2,1)}), bf16[16,320,128]{2,1,0:T(8,128)(2,1)S(1)}, u32[]{:S(2)}, u32[]{:S(2)}) async-start(bf16[16,320,128]{2,1,0:T(8,128)(2,1)} %shard_map.180.refs_1_), calls=%async_computation.1 | async-start | bytes 2621440 | tf_op jit(solution)/shard_map/all_to_all | solution.py:554
  56.9 25.3 %collective-permute-start.2 = (bf16[3072,128]{1,0:T(8,128)(2,1)S(1)}, bf16[3072,128]{1,0:T(8,128)(2,1)S(1)}, u32[]{:S(2)}, u32[]{:S(2)}) collective-permute-start(bf16[3072,128]{1,0:T(8,128)(2,1)S(1)} %get-tuple-element.51.refs_1_), channel_id=1, source_target_pairs={{0,3},{16,28},{1,0},{17,29},{2,1},{18,30},{3,2},{19,31},{4,7},{20,... | collective-permute-start | bytes 2359304 | tf_op jit(solution)/shard_map/ppermute | solution.py:567
  61.4 22.3 %collective-permute-start.1 = (bf16[3072,128]{1,0:T(8,128)(2,1)S(1)}, bf16[3072,128]{1,0:T(8,128)(2,1)S(1)}, u32[]{:S(2)}, u32[]{:S(2)}) collective-permute-start(bf16[3072,128]{1,0:T(8,128)(2,1)S(1)} %get-tuple-element.52.refs_2_), channel_id=1, source_target_pairs={{0,1},{16,20},{1,2},{17,21},{2,3},{18,22},{3,0},{19,23},{4,5},{20,... | collective-permute-start | bytes 2359304 | tf_op jit(solution)/shard_map/ppermute | solution.py:567
  63.4 28.5 %collective-permute-start.4 = (bf16[3072,128]{1,0:T(8,128)(2,1)}, bf16[3072,128]{1,0:T(8,128)(2,1)S(1)}, u32[]{:S(2)}, u32[]{:S(2)}) collective-permute-start(bf16[3072,128]{1,0:T(8,128)(2,1)} %collective-permute-done.refs_3_), channel_id=1, source_target_pairs={{0,1},{16,20},{1,2},{17,21},{2,3},{18,22},{3,0},{19,23},{4,5},{20,... | collective-permute-start | bytes 2359304 | tf_op jit(solution)/shard_map/ppermute | solution.py:567
  65.5 27.2 %collective-permute-start.5 = (bf16[3072,128]{1,0:T(8,128)(2,1)}, bf16[3072,128]{1,0:T(8,128)(2,1)}, u32[]{:S(2)}, u32[]{:S(2)}) collective-permute-start(bf16[3072,128]{1,0:T(8,128)(2,1)} %collective-permute-done.3.refs_6_), channel_id=1, source_target_pairs={{0,3},{16,28},{1,0},{17,29},{2,1},{18,30},{3,2},{19,31},{4,7},{20,... | collective-permute-start | bytes 2359304 | tf_op jit(solution)/shard_map/ppermute | solution.py:567
  82.2 9.6 %copy-start.7 = (bf16[3072,128]{1,0:T(8,128)(2,1)}, bf16[3072,128]{1,0:T(8,128)(2,1)S(1)}, u32[]{:S(2)}) copy-start(bf16[3072,128]{1,0:T(8,128)(2,1)S(1)} %collective-permute-done.2.refs_5_) | copy-start | bytes 2359300
  83.7 8.1 %copy-start.8 = (bf16[3072,128]{1,0:T(8,128)(2,1)}, bf16[3072,128]{1,0:T(8,128)(2,1)S(1)}, u32[]{:S(2)}) copy-start(bf16[3072,128]{1,0:T(8,128)(2,1)S(1)} %collective-permute-done.1.refs_4_) | copy-start | bytes 2359300
  91.8 0.9 copy-start.9
  98.5 0.7 copy-start.5
  99.2 15.7 %all-to-all-start.2 = ((bf16[16,160,128]{2,1,0:T(8,128)(2,1)}), bf16[16,160,128]{2,1,0:T(8,128)(2,1)S(1)}, u32[]{:S(2)}, u32[]{:S(2)}) async-start(bf16[16,160,128]{2,1,0:T(8,128)(2,1)} %get-tuple-element.63.refs_2_), calls=%async_computation.2 | async-start | bytes 1310720 | tf_op jit(solution)/shard_map/all_to_all | solution.py:554
  116.4 25.2 %all-to-all-start.3 = ((bf16[32,24,128]{2,1,0:T(8,128)(2,1)}), bf16[32,24,128]{2,1,0:T(8,128)(2,1)S(1)}, u32[]{:S(2)}, u32[]{:S(2)}) async-start(bf16[32,24,128]{2,1,0:T(8,128)(2,1)} %shard_map.185), calls=%async_computation.3 | async-start | bytes 393216 | tf_op jit(solution)/shard_map/all_to_all | solution.py:554
  141.6 2.4 %copy-start.1 = (bf16[32,24,128]{2,1,0:T(8,128)(2,1)}, bf16[32,24,128]{2,1,0:T(8,128)(2,1)S(1)}, u32[]{:S(2)}) copy-start(bf16[32,24,128]{2,1,0:T(8,128)(2,1)S(1)} %all-to-all-done.3.refs_0_) | copy-start | bytes 589828
  143.9 3.8 %copy-start.6 = (bf16[160,512]{1,0:T(8,128)(2,1)S(1)}, bf16[160,512]{1,0:T(8,128)(2,1)}, u32[]{:S(2)}) copy-start(bf16[160,512]{1,0:T(8,128)(2,1)} %copy-done.5) | copy-start | bytes 491524
  143.9 19.4 %all-to-all-start.4 = ((bf16[16,256,128]{2,1,0:T(8,128)(2,1)}), bf16[16,256,128]{2,1,0:T(8,128)(2,1)S(1)}, u32[]{:S(2)}, u32[]{:S(2)}) async-start(bf16[16,256,128]{2,1,0:T(8,128)(2,1)} %shard_map.187.refs_6_.refs_5_), calls=%async_computation.4 | async-start | bytes 2097152 | tf_op jit(solution)/shard_map/all_to_all | solution.py:554
  147.7 11.2 %copy-start.2 = (bf16[32,24,128]{2,1,0:T(8,128)(2,1)S(1)}, bf16[32,24,128]{2,1,0:T(8,128)(2,1)}, u32[]{:S(2)}) copy-start(bf16[32,24,128]{2,1,0:T(8,128)(2,1)} %copy-done.1) | copy-start | bytes 589828
  152.6 24.7 %collective-permute-start.6 = (bf16[4608,128]{1,0:T(8,128)(2,1)}, bf16[4608,128]{1,0:T(8,128)(2,1)S(1)}, u32[]{:S(2)}, u32[]{:S(2)}) collective-permute-start(bf16[4608,128]{1,0:T(8,128)(2,1)} %get-tuple-element.57), channel_id=1, source_target_pairs={{0,3},{16,28},{1,0},{17,29},{2,1},{18,30},{3,2},{19,31},{4,7},{20,... | collective-permute-start | bytes 3538952 | tf_op jit(solution)/shard_map/ppermute | solution.py:567
  157.0 20.3 %collective-permute-start.7 = (bf16[4608,128]{1,0:T(8,128)(2,1)}, bf16[4608,128]{1,0:T(8,128)(2,1)S(1)}, u32[]{:S(2)}, u32[]{:S(2)}) collective-permute-start(bf16[4608,128]{1,0:T(8,128)(2,1)} %get-tuple-element.58), channel_id=1, source_target_pairs={{0,1},{16,20},{1,2},{17,21},{2,3},{18,22},{3,0},{19,23},{4,5},{20,... | collective-permute-start | bytes 3538952 | tf_op jit(solution)/shard_map/ppermute | solution.py:567
  165.5 6.2 %collective-permute-start.10 = (bf16[1088,128]{1,0:T(8,128)(2,1)S(1)}, bf16[1088,128]{1,0:T(8,128)(2,1)S(1)}, u32[]{:S(2)}, u32[]{:S(2)}) collective-permute-start(bf16[1088,128]{1,0:T(8,128)(2,1)S(1)} %get-tuple-element.69), channel_id=1, source_target_pairs={{0,16},{16,0},{1,17},{17,1},{2,18},{18,2},{3,19},{19,3},{4,20},{20... | collective-permute-start | bytes 835592 | tf_op jit(solution)/shard_map/ppermute | solution.py:707
  173.3 30.7 %all-to-all-start.5 = ((bf16[16,96,128]{2,1,0:T(8,128)(2,1)}), bf16[16,96,128]{2,1,0:T(8,128)(2,1)S(1)}, u32[]{:S(2)}, u32[]{:S(2)}) async-start(bf16[16,96,128]{2,1,0:T(8,128)(2,1)} %get-tuple-element.73.refs_6_), calls=%async_computation.5 | async-start | bytes 786432 | tf_op jit(solution)/shard_map/all_to_all | solution.py:554
  180.6 18.7 %collective-permute-start.8 = (bf16[4608,128]{1,0:T(8,128)(2,1)}, bf16[4608,128]{1,0:T(8,128)(2,1)S(1)}, u32[]{:S(2)}, u32[]{:S(2)}) collective-permute-start(bf16[4608,128]{1,0:T(8,128)(2,1)} %get-tuple-element.66), channel_id=1, source_target_pairs={{0,1},{16,20},{1,2},{17,21},{2,3},{18,22},{3,0},{19,23},{4,5},{20,... | collective-permute-start | bytes 3538952 | tf_op jit(solution)/shard_map/ppermute | solution.py:567
  182.5 18.0 %collective-permute-start.9 = (bf16[4608,128]{1,0:T(8,128)(2,1)}, bf16[4608,128]{1,0:T(8,128)(2,1)S(1)}, u32[]{:S(2)}, u32[]{:S(2)}) collective-permute-start(bf16[4608,128]{1,0:T(8,128)(2,1)} %get-tuple-element.67), channel_id=1, source_target_pairs={{0,3},{16,28},{1,0},{17,29},{2,1},{18,30},{3,2},{19,31},{4,7},{20,... | collective-permute-start | bytes 3538952 | tf_op jit(solution)/shard_map/ppermute | solution.py:567
